TPU v7x, 128 devices: a whole 4x4x4 slice. The times are simulated.
128 devices in a mesh: ep: 32 (over z, y, core), tp: 4 (over x).
Axes of the slice: x: 4, y: 4, z: 4, core: 2. Of those that a mesh axis runs over, the one named last changes fastest.
Arguments:
- tokens: bfloat16 [24576, 2048], P('ep')
- in_gain: float32 [2048], replicated, may hold values from 0.1 to 1.9
- route_ids: int32 [24576, 2], P('ep'), may hold values from 0 to 31, all different within a row; in each aligned block of 768 rows (0 to 767, 768 to 1535, ...) at most 96 rows name the same one
- route_scores: float32 [24576, 2], P('ep'), may hold values from 0.1 to 1
- gate_weight: bfloat16 [32, 2048, 1024], P('ep', None, 'tp'), may hold values from -0.125 to 0.125
- up_weight: bfloat16 [32, 2048, 1024], P('ep', None, 'tp'), may hold values from -0.125 to 0.125
- down_weight: bfloat16 [32, 1024, 2048], P('ep', 'tp')
- out_gain: float32 [2048], P('tp'), may hold values from 0.1 to 1.9
Outputs:
- mixed: bfloat16 [24576, 2048], P('ep', 'tp')
Inputs may be any that keep to these rules, and one draw needn't show every extreme that they name: `route_ids`: each row names 2 different experts. Among the rows of one index of ep (aligned blocks of 768 rows) no expert is named more than 96 times, a bound that some block reaches.
All inputs are finite; a program needn't handle non-finite values.
Results may differ from a plain program's by a relative error of at most 0.012.
Values may be sent and summed in bfloat16 or wider, within the bound.
No kernel may reach another device: no remote copies, remote signals or barrier semaphores. Data moves between devices by JAX's collectives and lax.ppermute only.
A program may use at most 128 MiB of HBM per device.

v0:
```python
import jax
import jax.numpy as jnp
from jax import lax
from jax.sharding import PartitionSpec as P

epsilon = 1e-06


def copy_for_each(value, axis):
    length = lax.axis_size(axis)
    return lax.all_to_all(
        jnp.broadcast_to(value[None], (length, *value.shape)), axis, 0, 0, tiled=True
    )


def taken_together(value, axis):
    return copy_for_each(value, axis).sum(axis=0)


def per_device(
    tokens, in_gain, route_ids, route_scores, gate_weight, up_weight, down_weight, out_gain
):
    count_ep = lax.axis_size("ep")
    count_tp = lax.axis_size("tp")
    local_experts = gate_weight.shape[0]
    experts = count_ep * local_experts
    tok_count, full_width = tokens.shape
    choose_count = route_ids.shape[1]
    capacity = 2 * tok_count * choose_count // experts
    part_width = full_width // count_tp
    as_float = tokens.astype(jnp.float32)
    normed = (
        as_float
        * lax.rsqrt(jnp.mean(as_float * as_float, axis=1, keepdims=True) + epsilon)
        * in_gain
    ).astype(jnp.bfloat16)
    flat_ids = route_ids.reshape(-1)
    one_hot = (flat_ids[:, None] == jnp.arange(experts, dtype=jnp.int32)[None, :]).astype(jnp.int32)
    slot_index = jnp.sum((jnp.cumsum(one_hot, axis=0) - 1) * one_hot, axis=1)
    row_index = jnp.arange(tok_count * choose_count, dtype=jnp.int32) // choose_count
    buffer = jnp.zeros((experts, capacity, full_width), jnp.bfloat16)
    buffer = buffer.at[flat_ids, slot_index].set(normed[row_index])
    buffer = buffer.reshape(count_ep, local_experts, capacity, full_width)
    received = lax.all_to_all(buffer, "ep", split_axis=0, concat_axis=0, tiled=True)
    gate_acts = jnp.einsum(
        "secd,edf->secf", received, gate_weight, preferred_element_type=jnp.float32
    )
    up_acts = jnp.einsum("secd,edf->secf", received, up_weight, preferred_element_type=jnp.float32)
    hidden = (jax.nn.silu(gate_acts) * up_acts).astype(jnp.bfloat16)
    partial_terms = jnp.einsum(
        "secf,efd->secd", hidden, down_weight, preferred_element_type=jnp.float32
    ).astype(jnp.bfloat16)
    summed = (
        lax.psum_scatter(partial_terms, "tp", scatter_dimension=3, tiled=True)
        .astype(jnp.float32)
        .astype(jnp.bfloat16)
    )
    returned = lax.all_to_all(summed, "ep", split_axis=0, concat_axis=0, tiled=True).reshape(
        experts, capacity, part_width
    )
    picked = (
        returned[flat_ids, slot_index]
        .astype(jnp.float32)
        .reshape(tok_count, choose_count, part_width)
    )
    mix_weight = route_scores / jnp.sum(route_scores, axis=1, keepdims=True)
    combined = jnp.sum(mix_weight[:, :, None] * picked, axis=1)
    squares_sum = taken_together(jnp.sum(combined * combined, axis=1), "tp")
    scaled = combined * lax.rsqrt(squares_sum[:, None] / full_width + epsilon) * out_gain
    return scaled.astype(jnp.bfloat16)


def solution(mesh):
    in_specs = (
        P("ep", None),
        P(),
        P("ep", None),
        P("ep", None),
        P("ep", None, "tp"),
        P("ep", None, "tp"),
        P("ep", "tp", None),
        P("tp"),
    )
    out_specs = P("ep", "tp")
    return jax.shard_map(
        per_device, mesh=mesh, in_specs=in_specs, out_specs=out_specs, check_vma=False
    )
```

profile of v0, /device:TPU:0, one launch (start us, length us, event | category | flops | bytes accessed | tf_op | source)
XLA Modules:
  0.0 443.3 jit_solution(12452868296353077085)
XLA Ops:
  6.5 0.0 copy-start
  6.5 0.0 copy-start.7
  6.5 0.0 reduce-scatter.2.cloned.1.call-start
  6.5 1.0 copy.31
  7.5 0.2 eq.29
  7.7 0.2 eq.25
  8.0 0.0 copy-start.4
  8.0 0.2 reshape.162
  8.2 0.1 fusion.28
  8.3 9.1 %reduce-window.6 = s32[32,12,128]{2,1,0:T(8,128)S(1)} reduce-window(s32[32,12,128]{2,1,0:T(8,128)S(1)} %fusion.25, s32[]{:T(128)} %constant.34.clone.1), window={size=1x1x128 pad=0_0x0_0x127_0}, to_apply=%region_1.0 | reduce-window | flops 6242304 | bytes 393220 | tf_op jit(solution)/shard_map/reduce-window
  17.4 0.1 slice.12
  17.5 0.2 copy.34
  17.7 0.1 copy.35
  17.8 0.0 copy-start.2
  17.8 0.1 add_add_fusion
  18.0 0.1 fusion.27
  18.1 0.0 copy-done.7
  18.1 0.1 multiply_reduce_fusion.2
  18.2 0.0 copy-done.6
  18.2 0.1 and_reduce_fusion
  18.3 2.8 fusion.4
  21.2 0.0 copy-done.4
  21.2 0.0 copy-done.2
  21.2 2.5 fusion.6
  23.7 34.2 %scatter_custom_fusion = bf16[3072,2048]{1,0:T(8,128)(2,1)} fusion(s32[1536]{0:T(1024)S(1)} %broadcast_select_fusion, bf16[768,2048]{1,0:T(8,128)(2,1)} %fusion.6, s32[2048]{0:T(1024)S(1)} %pad_clamp_fusion, bf16[]{:T(256)} %constant.33.clone.1), kind=kCustom, calls=%fused_computation.13 | custom fusion | bytes 12583424
  57.9 0.0 copy-start.8
  57.9 149.4 %all_to_all.16 = bf16[32,1,96,2048]{3,2,1,0:T(8,128)(2,1)S(1)} all-to-all(bf16[32,1,96,2048]{3,2,1,0:T(8,128)(2,1)} %bitcast.84), channel_id=1, replica_groups=mesh['ep'=32,'tp'=4] {'ep'}, dimensions={0} | all-to-all | bytes 25165824 | tf_op jit(solution)/shard_map/all_to_all | solution.py:44
  207.3 0.0 copy-start.1
  207.3 4.5 %copy-done.1 = bf16[32,1,96,2048]{3,2,1,0:T(8,128)(2,1)} copy-done((bf16[32,1,96,2048]{3,2,1,0:T(8,128)(2,1)}, bf16[32,1,96,2048]{3,2,1,0:T(8,128)(2,1)S(1)}, u32[]{:S(2)}) %copy-start.1) | copy-done | bytes 12582936
  211.7 0.0 copy-done.8
  211.7 0.0 copy-start.9
  211.7 5.4 %fusion.2 = f32[32,96,256]{2,1,0:T(8,128)} fusion(bf16[32,1,96,2048]{3,2,1,0:T(8,128)(2,1)S(1)} %all_to_all.16, bf16[1,2048,256]{2,1,0:T(8,128)(2,1)S(1)} %copy-done.8), kind=kOutput, calls=%fused_computation.5 | convolution fusion | flops 3221225472 | bytes 16777216 | tf_op jit(solution)/shard_map/secd,edf->secf/dot_general | solution.py:45
  217.1 0.0 copy-done
  217.1 0.0 copy-done.9
  217.1 18.7 %convert_bitcast_fusion = bf16[32,1,96,2048]{3,2,0,1:T(8,128)(2,1)} fusion(f32[32,96,256]{2,1,0:T(8,128)} %fusion.2, bf16[32,1,96,2048]{3,2,1,0:T(8,128)(2,1)} %copy-done.1, bf16[1,256,2048]{2,1,0:T(8,128)(2,1)S(1)} %copy-done, bf16[1,2048,256]{2,1,0:T(8,128)(2,1)S(1)} %copy-done.9), kind=kOutput, calls=%fused_computation.7 | convolution fusion | flops 6453460992 | bytes 30408704 | tf_op jit(solution)/shard_map/secf,efd->secd/dot_general | solution.py:50
  235.8 0.0 reduce-scatter.2.cloned.1.call-update
  235.9 112.4 %reduce-scatter.2.cloned.1.call-done = bf16[32,1,96,512]{3,2,0,1:T(8,128)(2,1)} async-done(((bf16[32,1,96,2048]{3,2,0,1:T(8,128)(2,1)}), bf16[32,1,96,512]{3,2,0,1:T(8,128)(2,1)}) %reduce-scatter.2.cloned.1.call-update) | async-done | bytes 3145744 | tf_op jit(solution)/shard_map/reduce_scatter | solution.py:54
  348.2 7.7 %all-to-all-start.1 = ((bf16[32,1,96,512]{3,2,1,0:T(8,128)(2,1)}), bf16[32,1,96,512]{3,2,1,0:T(8,128)(2,1)}, u32[]{:S(2)}, u32[]{:S(2)}) async-start(bf16[32,1,96,512]{3,2,1,0:T(8,128)(2,1)} %bitcast.85), calls=%async_computation.2 | async-start | bytes 6291456 | tf_op jit(solution)/shard_map/all_to_all | solution.py:58
  356.0 0.0 copy-done.3
  356.0 0.2 copy.30
  356.2 41.5 %all-to-all-done.1 = bf16[32,1,96,512]{3,2,1,0:T(8,128)(2,1)} async-done(((bf16[32,1,96,512]{3,2,1,0:T(8,128)(2,1)}), bf16[32,1,96,512]{3,2,1,0:T(8,128)(2,1)}, u32[]{:S(2)}, u32[]{:S(2)}) %all-to-all-start.1) | async-done | bytes 3145760 | tf_op jit(solution)/shard_map/all_to_all | solution.py:58
  397.8 20.2 %gather_fusion = bf16[1536,512]{1,0:T(8,128)(2,1)S(1)} fusion(bf16[32,96,512]{2,1,0:T(8,128)(2,1)} %bitcast.23, s32[1536]{0:T(1024)S(1)} %get-tuple-element.5), kind=kCustom, calls=%fused_computation.1 | custom fusion | bytes 3158016 | tf_op jit(solution)/shard_map/gather | solution.py:62
  417.9 3.3 reshape.176
  421.2 6.0 %multiply_reduce_fusion = f32[768,512]{1,0:T(8,128)S(1)} fusion(f32[768,2,512]{2,1,0:T(2,128)} %reshape.176, f32[768,2]{1,0:T(8,128)S(1)} %copy.30), kind=kLoop, calls=%fused_computation.23 | loop fusion | flops 1179648 | bytes 4724736 | tf_op jit(solution)/shard_map/reduce_sum | solution.py:67
  427.3 0.2 multiply_reduce_fusion.1
  427.5 7.9 %all_to_all.17 = f32[4,1,768]{2,1,0:T(1,128)S(1)} all-to-all(f32[4,1,768]{2,1,0:T(1,128)S(1)} %broadcast_in_dim.5), channel_id=1, replica_groups=mesh['ep'=32,'tp'=4] {'tp'}, dimensions={0} | all-to-all | bytes 24576 | tf_op jit(solution)/shard_map/all_to_all | solution.py:11
  435.4 0.0 copy-done.5
  435.4 1.1 multiply_convert_fusion
  (14 shorter events, 0.2 us)
Async XLA Ops:
  6.5 210.6 %copy-start = (bf16[1,256,2048]{2,1,0:T(8,128)(2,1)S(1)}, bf16[1,256,2048]{2,1,0:T(8,128)(2,1)}, u32[]{:S(2)}) copy-start(bf16[1,256,2048]{2,1,0:T(8,128)(2,1)} %param.14) | copy-start | bytes 3145732
  6.5 11.6 %copy-start.7 = (s32[2]{0:T(128)S(1)}, s32[2]{0:T(128)}, u32[]{:S(2)}) copy-start(s32[2]{0:T(128)} %constant.46) | copy-start | bytes 28
  6.5 11.7 %copy-start.6 = (s32[2]{0:T(128)S(1)}, s32[2]{0:T(128)}, u32[]{:S(2)}) copy-start(s32[2]{0:T(128)} %constant.49) | copy-start | bytes 28
  6.5 341.7 %reduce-scatter.2.cloned.1.call-start = ((), (), s32[]{:S(2)}) async-start(), calls=%async_computation.4 | async-start | bytes 15728640 | tf_op jit(solution)/shard_map/reduce_scatter | solution.py:54
  8.0 13.2 %copy-start.4 = (f32[2048]{0:T(1024)S(1)}, f32[2048]{0:T(1024)}, u32[]{:S(2)}) copy-start(f32[2048]{0:T(1024)} %param.9) | copy-start | bytes 24580
  17.8 3.4 copy-start.2
  57.9 153.8 %copy-start.8 = (bf16[1,2048,256]{2,1,0:T(8,128)(2,1)S(1)}, bf16[1,2048,256]{2,1,0:T(8,128)(2,1)}, u32[]{:S(2)}) copy-start(bf16[1,2048,256]{2,1,0:T(8,128)(2,1)} %param.12) | copy-start | bytes 3145732
  207.3 4.5 %copy-start.1 = (bf16[32,1,96,2048]{3,2,1,0:T(8,128)(2,1)}, bf16[32,1,96,2048]{3,2,1,0:T(8,128)(2,1)S(1)}, u32[]{:S(2)}) copy-start(bf16[32,1,96,2048]{3,2,1,0:T(8,128)(2,1)S(1)} %all_to_all.16) | copy-start | bytes 37748740
  211.7 5.4 %copy-start.9 = (bf16[1,2048,256]{2,1,0:T(8,128)(2,1)S(1)}, bf16[1,2048,256]{2,1,0:T(8,128)(2,1)}, u32[]{:S(2)}) copy-start(bf16[1,2048,256]{2,1,0:T(8,128)(2,1)} %param.13) | copy-start | bytes 3145732
  348.2 7.7 %copy-start.3 = (f32[768,2]{0,1:T(2,128)S(1)}, f32[768,2]{0,1:T(2,128)}, u32[]{:S(2)}) copy-start(f32[768,2]{0,1:T(2,128)} %param.11) | copy-start | bytes 18436
  348.2 49.5 %all-to-all-start.1 = ((bf16[32,1,96,512]{3,2,1,0:T(8,128)(2,1)}), bf16[32,1,96,512]{3,2,1,0:T(8,128)(2,1)}, u32[]{:S(2)}, u32[]{:S(2)}) async-start(bf16[32,1,96,512]{3,2,1,0:T(8,128)(2,1)} %bitcast.85), calls=%async_computation.2 | async-start | bytes 6291456 | tf_op jit(solution)/shard_map/all_to_all | solution.py:58
  421.2 14.1 %copy-start.5 = (f32[512]{0:T(512)S(1)}, f32[512]{0:T(512)}, u32[]{:S(2)}) copy-start(f32[512]{0:T(512)} %param.15) | copy-start | bytes 6148
Sparse Core Ops, SparseCore 0:
  236.0 112.2 reduce-scatter.1
where the time goes:
time: 444 us; the launch traced here: 443 us
  blocking collectives  157 us (35%)
  waiting for transfers between devices  154 us (35%)
  local copies, waits for them, and re-layouts  64.5 us (15%)
  matrix products  24.1 us (5%)
  other arithmetic  22.2 us (5%)
  between operations  13.6 us (3%)
  starting transfers between devices  7.74 us (2%)
    all_to_all x1, blocking collectives, per_device(): lax.all_to_all(buffer, 'ep', split_axis=0, concat_axis=0, tiled=True)  149 us
    reduce_scatter x1, waiting for transfers between devices, per_device(): lax.psum_scatter(partial_terms, 'tp', scatter_dimension=3, tiled=True)  112 us
    all_to_all x1, waiting for transfers between devices, per_device(): lax.all_to_all(summed, 'ep', split_axis=0, concat_axis=0, tiled=True)  41.5 us
    unnamed x22, local copies, waits for them, and re-layouts  39.7 us
    gather x1, local copies, waits for them, and re-layouts, per_device(): returned[flat_ids, slot_index].astype(jnp.float32)  20.2 us
    dot_general x1, matrix products, per_device(): jnp.einsum('secf,efd->secd', hidden, down_weight, preferred_element_type=...  18.7 us
    another operation x2, other arithmetic  9.11 us
  transfers between devices with their start and end apart: 2, of which 2 were waited for; matrix products, arithmetic and copies ran while one was open for 0% of the time, Pallas kernels for 0%

commit v1 on v0

v1 whole, which is shorter than its diff:
```python
import functools

import jax
import jax.numpy as jnp
from jax import lax
from jax.experimental import pallas as pl
from jax.experimental.pallas import tpu as pltpu
from jax.sharding import PartitionSpec as P

epsilon = 1e-06
AXES = ("ep", "tp")
VMEM_BYTES = 58 * 1024 * 1024


def place_of(ids, slot):
    ep = (ids // 2) * 2 + slot % 2
    tp = (ids % 2) * 2 + (slot % 4) // 2
    return ep, tp, slot // 4


def permutes(count_ep, count_tp):
    def dev(ep, x):
        return ep * count_tp + x

    first, second, swap = [], [], []
    for ep in range(count_ep):
        core = ep % 2
        for x in range(count_tp):
            own = x // 2 == core
            swap.append((dev(ep, x), dev(ep ^ 1, x)))
            if own:
                first.append((dev(ep, x), dev(ep, x ^ 1)))
                second.append((dev(ep, x), dev(ep, x)))
            else:
                first.append((dev(ep, x), dev(ep ^ 1, count_tp - 1 - x)))
                second.append((dev(ep, x), dev(ep, x ^ 1)))
    return first, second, swap


def dispatch_kernel(where_ref, ids_ref, gain_ref, tokens_ref, out_ref, raw, normed, pick, sems, *, rows, chunks):
    step = pl.program_id(0)
    count, width = raw.shape
    part = count // chunks

    @pl.when(step == 0)
    def _():
        for i in range(chunks):
            pltpu.make_async_copy(
                tokens_ref.at[pl.ds(i * part, part)], raw.at[pl.ds(i * part, part)], sems.at[i]
            ).start()
        experts = 32
        first = ids_ref[0:1, :]
        second = ids_ref[1:2, :]
        number = lax.broadcasted_iota(jnp.int32, (experts, count), 0)
        named_first = number == first
        named_second = number == second
        named = jnp.where(named_first | named_second, 1.0, 0.0).astype(jnp.bfloat16)
        before = lax.broadcasted_iota(jnp.int32, (count, count), 0) < lax.broadcasted_iota(
            jnp.int32, (count, count), 1
        )
        ranks = jnp.dot(
            named, jnp.where(before, 1.0, 0.0).astype(jnp.bfloat16), preferred_element_type=jnp.float32
        )
        slot_first = jnp.sum(jnp.where(named_first, ranks, 0.0), axis=0, keepdims=True).astype(jnp.int32)
        slot_second = jnp.sum(jnp.where(named_second, ranks, 0.0), axis=0, keepdims=True).astype(jnp.int32)
        mine = where_ref[0]

        def row_of(ids, slot):
            ep, tp, row = place_of(ids, slot)
            return jnp.where(tp == mine, ep * rows + row, -1)

        row_first = row_of(first, slot_first)
        row_second = row_of(second, slot_second)
        index = lax.broadcasted_iota(jnp.int32, (count, count), 0)
        pick[...] = jnp.where((index == row_first) | (index == row_second), 1.0, 0.0).astype(jnp.bfloat16)
        gain = gain_ref[...]
        for i in range(chunks):
            pltpu.make_async_copy(
                tokens_ref.at[pl.ds(i * part, part)], raw.at[pl.ds(i * part, part)], sems.at[i]
            ).wait()
            value = raw[pl.ds(i * part, part), :].astype(jnp.float32)
            mean = jnp.mean(value * value, axis=1, keepdims=True)
            normed[pl.ds(i * part, part), :] = (value * lax.rsqrt(mean + epsilon) * gain).astype(jnp.bfloat16)

    block = out_ref.shape[0]
    out_ref[...] = jnp.dot(
        pick[pl.ds(step * block, block), :], normed[...], preferred_element_type=jnp.float32
    ).astype(jnp.bfloat16)


def dispatch_buffer(place, ids_rows, gain, tokens, rows):
    count, width = tokens.shape
    steps, chunks = 4, 4
    return pl.pallas_call(
        functools.partial(dispatch_kernel, rows=rows, chunks=chunks),
        grid_spec=pltpu.PrefetchScalarGridSpec(
            num_scalar_prefetch=1,
            grid=(steps,),
            in_specs=[
                pl.BlockSpec((2, count), lambda i, p: (0, 0)),
                pl.BlockSpec((1, width), lambda i, p: (0, 0)),
                pl.BlockSpec(memory_space=pl.ANY),
            ],
            out_specs=pl.BlockSpec((count // steps, width), lambda i, p: (i, 0)),
            scratch_shapes=[
                pltpu.VMEM((count, width), jnp.bfloat16),
                pltpu.VMEM((count, width), jnp.bfloat16),
                pltpu.VMEM((count, count), jnp.bfloat16),
                pltpu.SemaphoreType.DMA((chunks,)),
            ],
        ),
        out_shape=jax.ShapeDtypeStruct((count, width), jnp.bfloat16),
        compiler_params=pltpu.CompilerParams(
            dimension_semantics=("arbitrary",), vmem_limit_bytes=VMEM_BYTES
        ),
        name="dispatch_buffer",
    )(place, ids_rows, gain, tokens)


def hidden_of(rows, gate, up):
    gate_acts = jnp.dot(rows, gate, preferred_element_type=jnp.float32)
    up_acts = jnp.dot(rows, up, preferred_element_type=jnp.float32)
    return (gate_acts / (1.0 + jnp.exp(-gate_acts)) * up_acts).astype(jnp.bfloat16)


def early_kernel(place_ref, rows_ref, ga, gb, g1, g2, ua, ub, u1, u2, out_ref, rows, gate, up, sems):
    flag = place_ref[1]

    def copies(a, b, dst, sem):
        @pl.when(flag == 1)
        def _():
            pltpu.make_async_copy(a, dst, sem).start()

        @pl.when(flag != 1)
        def _():
            pltpu.make_async_copy(b, dst, sem).start()

    copies(ga, gb, gate.at[0], sems.at[0])
    copies(ua, ub, up.at[0], sems.at[1])
    load = pltpu.make_async_copy(rows_ref, rows, sems.at[6])
    load.start()
    for i, (g, u) in enumerate(((g1, u1), (g2, u2))):
        pltpu.make_async_copy(g, gate.at[i + 1], sems.at[2 * i + 2]).start()
        pltpu.make_async_copy(u, up.at[i + 1], sems.at[2 * i + 3]).start()
    load.wait()
    part = gate.shape[2]
    for i in range(3):
        pltpu.make_async_copy(g1, gate.at[i], sems.at[2 * i]).wait()
        pltpu.make_async_copy(u1, up.at[i], sems.at[2 * i + 1]).wait()
        out_ref[:, i * part : (i + 1) * part] = hidden_of(rows[...], gate[i], up[i])


def early_hidden(place, rows, gates, ups):
    count, width = rows.shape
    part = gates[0].shape[1]
    any_spec = pl.BlockSpec(memory_space=pl.ANY)
    return pl.pallas_call(
        early_kernel,
        in_specs=[pl.BlockSpec(memory_space=pltpu.SMEM)] + [any_spec] * 9,
        out_specs=pl.BlockSpec((count, 3 * part), lambda: (0, 0)),
        scratch_shapes=[
            pltpu.VMEM((count, width), jnp.bfloat16),
            pltpu.VMEM((3, width, part), jnp.bfloat16),
            pltpu.VMEM((3, width, part), jnp.bfloat16),
            pltpu.SemaphoreType.DMA((7,)),
        ],
        out_shape=jax.ShapeDtypeStruct((count, 3 * part), jnp.bfloat16),
        compiler_params=pltpu.CompilerParams(vmem_limit_bytes=VMEM_BYTES),
        name="early_hidden",
    )(place, rows, *gates, *ups)


def late_kernel(
    place_ref, rows_ref, early_ref, ga, gb, ua, ub, d0a, d0b, d1, d2, d3a, d3b, out_ref, rows, gate, up, down, hidden, sems, *, slots
):
    flag = place_ref[1]

    def copies(a, b, dst, sem):
        @pl.when(flag == 1)
        def _():
            pltpu.make_async_copy(a, dst, sem).start()

        @pl.when(flag != 1)
        def _():
            pltpu.make_async_copy(b, dst, sem).start()

    load = pltpu.make_async_copy(rows_ref, rows, sems.at[0])
    load.start()
    copies(ga, gb, gate, sems.at[1])
    copies(ua, ub, up, sems.at[2])
    part = gate.shape[1]
    copies(d0a, d0b, down.at[pl.ds(0, part)], sems.at[3])
    pltpu.make_async_copy(d1, down.at[pl.ds(part, part)], sems.at[4]).start()
    pltpu.make_async_copy(d2, down.at[pl.ds(2 * part, part)], sems.at[5]).start()
    copies(d3a, d3b, down.at[pl.ds(3 * part, part)], sems.at[6])
    pre = pltpu.make_async_copy(early_ref, hidden.at[:, pl.ds(0, 3 * part)], sems.at[7])
    pre.start()
    load.wait()
    pltpu.make_async_copy(ga, gate, sems.at[1]).wait()
    pltpu.make_async_copy(ua, up, sems.at[2]).wait()
    hidden[:, 3 * part : 4 * part] = hidden_of(rows[...], gate[...], up[...])
    for i in range(4):
        pltpu.make_async_copy(d1, down.at[pl.ds(i * part, part)], sems.at[3 + i]).wait()
    pre.wait()
    senders, pieces, _, piece = out_ref.shape
    for f in range(pieces):
        value = jnp.dot(
            hidden[...], down[:, f * piece : (f + 1) * piece], preferred_element_type=jnp.float32
        )
        out_ref[:, f] = value.reshape(senders, slots, piece).astype(jnp.bfloat16)


def late_outputs(place, rows, early, gates, ups, downs, senders, pieces):
    count, width = rows.shape
    part = gates[0].shape[1]
    slots = count // senders
    any_spec = pl.BlockSpec(memory_space=pl.ANY)
    shape = (senders, pieces, slots, width // pieces)
    return pl.pallas_call(
        functools.partial(late_kernel, slots=slots),
        in_specs=[pl.BlockSpec(memory_space=pltpu.SMEM)] + [any_spec] * 12,
        out_specs=pl.BlockSpec(shape, lambda: (0, 0, 0, 0)),
        scratch_shapes=[
            pltpu.VMEM((count, width), jnp.bfloat16),
            pltpu.VMEM((width, part), jnp.bfloat16),
            pltpu.VMEM((width, part), jnp.bfloat16),
            pltpu.VMEM((4 * part, width), jnp.bfloat16),
            pltpu.VMEM((count, 4 * part), jnp.bfloat16),
            pltpu.SemaphoreType.DMA((8,)),
        ],
        out_shape=jax.ShapeDtypeStruct(shape, jnp.bfloat16),
        compiler_params=pltpu.CompilerParams(vmem_limit_bytes=VMEM_BYTES),
        name="late_outputs",
    )(place, rows, early, *gates, *ups, *downs)


def columns_kernel(ids_ref, out_ref, *, rows, count_tp):
    count = ids_ref.shape[0]
    experts = 32
    first = ids_ref[:, 0:1]
    second = ids_ref[:, 1:2]
    number = lax.broadcasted_iota(jnp.int32, (count, experts), 1)
    named_first = number == first
    named_second = number == second
    named = jnp.where(named_first | named_second, 1.0, 0.0).astype(jnp.bfloat16)
    before = lax.broadcasted_iota(jnp.int32, (count, count), 1) < lax.broadcasted_iota(
        jnp.int32, (count, count), 0
    )
    ranks = jnp.dot(
        jnp.where(before, 1.0, 0.0).astype(jnp.bfloat16), named, preferred_element_type=jnp.float32
    )

    def row_of(ids, chosen):
        slot = jnp.sum(jnp.where(chosen, ranks, 0.0), axis=1, keepdims=True).astype(jnp.int32)
        ep, tp, row = place_of(ids, slot)
        return (ep * count_tp + tp) * rows + row

    out_ref[:, 0:1] = row_of(first, named_first)
    out_ref[:, 1:2] = row_of(second, named_second)


def combine_kernel(index_ref, scores_ref, returned_ref, out_ref):
    total = returned_ref.shape[0]
    count = index_ref.shape[0]
    index = lax.broadcasted_iota(jnp.int32, (count, total), 1)
    returned = returned_ref[...]

    def picked(choice):
        hot = jnp.where(index == index_ref[:, choice : choice + 1], 1.0, 0.0).astype(jnp.bfloat16)
        return jnp.dot(hot, returned, preferred_element_type=jnp.float32)

    scores = scores_ref[...]
    mix = scores / jnp.sum(scores, axis=1, keepdims=True)
    out_ref[...] = mix[:, 0:1] * picked(0) + mix[:, 1:2] * picked(1)


def combine(index, scores, returned):
    count = index.shape[0]
    total, piece = returned.shape
    steps = 4
    return pl.pallas_call(
        combine_kernel,
        grid=(steps,),
        in_specs=[
            pl.BlockSpec((count // steps, 2), lambda i: (i, 0)),
            pl.BlockSpec((count // steps, 2), lambda i: (i, 0)),
            pl.BlockSpec((total, piece), lambda i: (0, 0)),
        ],
        out_specs=pl.BlockSpec((count // steps, piece), lambda i: (i, 0)),
        out_shape=jax.ShapeDtypeStruct((count, piece), jnp.float32),
        compiler_params=pltpu.CompilerParams(
            dimension_semantics=("arbitrary",), vmem_limit_bytes=VMEM_BYTES
        ),
        name="combine",
    )(index, scores, returned)


def per_device(
    tokens, in_gain, route_ids, route_scores, gate_weight, up_weight, down_weight, out_gain
):
    count_ep = lax.axis_size("ep")
    count_tp = lax.axis_size("tp")
    tok_count, full_width = tokens.shape
    part_width = full_width // count_tp
    capacity = 2 * tok_count * route_ids.shape[1] // count_ep
    rows = capacity // count_tp
    x = lax.axis_index("tp")
    core = lax.axis_index("ep") % 2
    place = jnp.stack([x, (x // 2 == core).astype(jnp.int32)]).astype(jnp.int32)

    first, second, swap = permutes(count_ep, count_tp)

    def spread(weight):
        moved = lax.ppermute(weight, AXES, first)
        other_own = lax.ppermute(weight, AXES, swap)
        other_moved = lax.ppermute(moved, AXES, swap)
        last = lax.ppermute(moved, AXES, second)
        other_last = lax.ppermute(last, AXES, swap)
        return (weight, other_own), moved, other_moved, (other_last, last)

    gate = spread(gate_weight[0])
    up = spread(up_weight[0])
    down = spread(down_weight[0])

    buffer = dispatch_buffer(place, route_ids.T, in_gain[None, :], tokens, rows)
    received = lax.all_to_all(
        buffer.reshape(count_ep, rows, full_width), "ep", split_axis=0, concat_axis=0, tiled=True
    ).reshape(count_ep * rows, full_width)
    early = early_hidden(
        place, received, (*gate[0], gate[1], gate[2]), (*up[0], up[1], up[2])
    )
    outputs = late_outputs(
        place, received, early, gate[3], up[3], (*down[0], down[1], down[2], *down[3]), count_ep, count_tp
    )
    returned = lax.all_to_all(
        outputs.reshape(count_ep * count_tp, rows, part_width), AXES, split_axis=0, concat_axis=0, tiled=True
    ).reshape(count_ep * count_tp * rows, part_width)
    index = pl.pallas_call(
        functools.partial(columns_kernel, rows=rows, count_tp=count_tp),
        out_shape=jax.ShapeDtypeStruct((tok_count, 2), jnp.int32),
        name="columns",
    )(route_ids)
    combined = combine(index, route_scores, returned)
    squares = jnp.sum(combined * combined, axis=1)
    total = squares
    for shift in range(1, count_tp):
        total = total + lax.ppermute(
            squares, "tp", [(i, (i + shift) % count_tp) for i in range(count_tp)]
        )
    scaled = combined * lax.rsqrt(total[:, None] / full_width + epsilon) * out_gain
    return scaled.astype(jnp.bfloat16)


def solution(mesh):
    in_specs = (
        P("ep", None),
        P(),
        P("ep", None),
        P("ep", None),
        P("ep", None, "tp"),
        P("ep", None, "tp"),
        P("ep", "tp", None),
        P("tp"),
    )
    out_specs = P("ep", "tp")
    return jax.shard_map(
        per_device, mesh=mesh, in_specs=in_specs, out_specs=out_specs, check_vma=False
    )
```

time: 444 us -> 174 us (0.39)
  blocking collectives: 157 us -> 0 us
  waiting for transfers between devices: 154 us -> 52 us
  starting transfers between devices: 7.74 us -> 69.9 us
  local copies, waits for them, and re-layouts: 64.5 us -> 5.44 us
  Pallas kernels: 0 us -> 40.5 us
  matrix products: 24.1 us -> 0 us
  other arithmetic: 22.2 us -> 3.46 us
  between operations: 13.6 us -> 0.17 us
    all_to_all x2 -> x0, blocking collectives: 157 us -> none  [the longest x1 149 us: per_device(): lax.all_to_all(buffer, 'ep', split_axis=0, concat_axis=0, tiled=True)]
    reduce_scatter x1 -> x0, waiting for transfers between devices: 112 us -> none  [per_device(): lax.psum_scatter(partial_terms, 'tp', scatter_dimension=3, tiled=True)]
    ppermute x0 -> x18, starting transfers between devices: none -> 49 us  [the longest x3 28.3 us: spread(): last = lax.ppermute(moved, AXES, second)]
    pallas_call x0 -> x5, Pallas kernels: none -> 40.5 us  [the longest x1 10.1 us: late_outputs(): pl.pallas_call(functools.partial(late_kernel, slots=slots), in_specs=[pl....]
    unnamed x22 -> x18, local copies, waits for them, and re-layouts: 39.7 us -> 5.44 us
    dot_general x2 -> x0, matrix products: 24.1 us -> none  [the longest x1 18.7 us: per_device(): jnp.einsum('secf,efd->secd', hidden, down_weight, preferred_element_type=...]
    gather x1 -> x0, local copies, waits for them, and re-layouts: 20.2 us -> none  [per_device(): returned[flat_ids, slot_index].astype(jnp.float32)]
    ppermute x0 -> x18, waiting for transfers between devices: none -> 16.6 us  [the longest x3 13.6 us: spread(): moved = lax.ppermute(weight, AXES, first)]
  transfers between devices with their start and end apart: 2 -> 20, of which waited for: 2 -> 6; matrix products, arithmetic and copies ran while one was open for 0% -> 1% of each run, Pallas kernels for 0% -> 13%
where the time goes in v1:
time: 174 us; the launch traced here: 171 us
  starting transfers between devices  69.9 us (40%)
  waiting for transfers between devices  52 us (30%)
  Pallas kernels  40.5 us (23%)
  local copies, waits for them, and re-layouts  5.44 us (3%)
  other arithmetic  3.46 us (2%)
    all_to_all x1, waiting for transfers between devices, per_device(): lax.all_to_all(outputs.reshape(count_ep * count_tp, rows, part_width), AX...  35.5 us
    ppermute x3, starting transfers between devices, spread(): last = lax.ppermute(moved, AXES, second)  28.3 us
    ppermute x3, waiting for transfers between devices, spread(): moved = lax.ppermute(weight, AXES, first)  13.6 us
    all_to_all x1, starting transfers between devices, per_device(): lax.all_to_all(outputs.reshape(count_ep * count_tp, rows, part_width), AX...  12 us
    pallas_call x1, Pallas kernels, late_outputs(): pl.pallas_call(functools.partial(late_kernel, slots=slots), in_specs=[pl....  10.1 us
    ppermute x3, starting transfers between devices, spread(): other_last = lax.ppermute(last, AXES, swap)  10 us
    pallas_call x1, Pallas kernels, early_hidden(): pl.pallas_call(early_kernel, in_specs=[pl.BlockSpec(memory_space=pltpu.SM...  9.69 us
    all_to_all x1, starting transfers between devices, per_device(): lax.all_to_all(buffer.reshape(count_ep, rows, full_width), 'ep', split_ax...  8.89 us
  transfers between devices with their start and end apart: 20, of which 6 were waited for; matrix products, arithmetic and copies ran while one was open for 1% of the time, Pallas kernels for 13%

profile of v1, /device:TPU:0, one launch (start us, length us, event | category | flops | bytes accessed | tf_op | source)
XLA Modules:
  0.0 171.5 jit_solution(16830807450650715649)
XLA Ops:
  0.0 1.6 collective-permute-start.1
  1.6 1.4 collective-permute-start
  3.0 0.2 collective-permute-start.4
  3.2 0.2 collective-permute-start.3
  3.4 1.6 collective-permute-start.11
  5.0 0.7 pad_add_fusion.where_ref.place_ref
  5.7 8.2 %dispatch_buffer.1 = bf16[768,2048]{1,0:T(8,128)(2,1)} custom-call(s32[2]{0:T(128)} %pad_add_fusion.where_ref.place_ref, s32[2,768]{1,0:T(2,128)} %bitcast.25, f32[1,2048]{1,0:T(1,128)} %bitcast.26, bf16[768,2048]{1,0:T(8,128)(2,1)} %tokens_ref.1), custom_call_target="tpu_custom_call" | custom-call | tf_op jit(solution)/shard_map/dispatch_buffer/pallas_call | solution.py:94
  13.9 8.9 %all-to-all-start = ((bf16[32,24,2048]{2,1,0:T(8,128)(2,1)}), bf16[32,24,2048]{2,1,0:T(8,128)(2,1)S(1)}, u32[]{:S(2)}, u32[]{:S(2)}) async-start(bf16[32,24,2048]{2,1,0:T(8,128)(2,1)} %bitcast.13), calls=%async_computation | async-start | bytes 6291456 | tf_op jit(solution)/shard_map/all_to_all | solution.py:326
  22.8 0.0 collective-permute-done.1.g1
  22.8 0.4 collective-permute-start.2
  23.1 3.2 %collective-permute-done.4.u1 = bf16[2048,256]{1,0:T(8,128)(2,1)} collective-permute-done((bf16[2048,256]{1,0:T(8,128)(2,1)}, bf16[2048,256]{1,0:T(8,128)(2,1)}, u32[]{:S(2)}, u32[]{:S(2)}) %collective-permute-start.4) | collective-permute-done | bytes 1048608 | tf_op jit(solution)/shard_map/ppermute | solution.py:314
  26.4 0.9 collective-permute-start.5
  27.2 10.4 %collective-permute-done.11.d1 = bf16[256,2048]{1,0:T(8,128)(2,1)} collective-permute-done((bf16[256,2048]{1,0:T(8,128)(2,1)}, bf16[256,2048]{1,0:T(8,128)(2,1)}, u32[]{:S(2)}, u32[]{:S(2)}) %collective-permute-start.11) | collective-permute-done | bytes 1048608 | tf_op jit(solution)/shard_map/ppermute | solution.py:314
  37.6 9.5 %collective-permute-start.13 = (bf16[256,2048]{1,0:T(8,128)(2,1)}, bf16[256,2048]{1,0:T(8,128)(2,1)}, u32[]{:S(2)}, u32[]{:S(2)}) collective-permute-start(bf16[256,2048]{1,0:T(8,128)(2,1)} %collective-permute-done.11.d1), channel_id=1, source_target_pairs={{0,0},{1,1},{2,3},{3,2},{4,5},{5,4},{6,6},{7,7},{8,8},{9,9},{10,11... | collective-permute-start | bytes 3145736 | tf_op jit(solution)/shard_map/ppermute | solution.py:317
  47.0 9.4 %collective-permute-start.6 = (bf16[2048,256]{1,0:T(8,128)(2,1)}, bf16[2048,256]{1,0:T(8,128)(2,1)}, u32[]{:S(2)}, u32[]{:S(2)}) collective-permute-start(bf16[2048,256]{1,0:T(8,128)(2,1)} %collective-permute-done.1.g1), channel_id=1, source_target_pairs={{0,0},{1,1},{2,3},{3,2},{4,5},{5,4},{6,6},{7,7},{8,8},{9,9},{10,11... | collective-permute-start | bytes 3145736 | tf_op jit(solution)/shard_map/ppermute | solution.py:317
  56.5 9.4 %collective-permute-start.8 = (bf16[2048,256]{1,0:T(8,128)(2,1)}, bf16[2048,256]{1,0:T(8,128)(2,1)}, u32[]{:S(2)}, u32[]{:S(2)}) collective-permute-start(bf16[2048,256]{1,0:T(8,128)(2,1)} %collective-permute-done.4.u1), channel_id=1, source_target_pairs={{0,0},{1,1},{2,3},{3,2},{4,5},{5,4},{6,6},{7,7},{8,8},{9,9},{10,11... | collective-permute-start | bytes 3145736 | tf_op jit(solution)/shard_map/ppermute | solution.py:317
  65.9 0.0 collective-permute-done.2.g2
  65.9 0.0 collective-permute-start.10
  66.0 0.5 collective-permute-start.12
  66.4 0.0 collective-permute-done.13.d3b
  66.4 0.1 collective-permute-start.14
  66.6 0.4 collective-permute-start.7
  67.0 0.0 collective-permute-done.8.ub
  67.0 0.3 copy-done.4
  67.2 9.5 %collective-permute-start.9 = (bf16[2048,256]{1,0:T(8,128)(2,1)}, bf16[2048,256]{1,0:T(8,128)(2,1)}, u32[]{:S(2)}, u32[]{:S(2)}) collective-permute-start(bf16[2048,256]{1,0:T(8,128)(2,1)} %collective-permute-done.8.ub), channel_id=1, source_target_pairs={{0,4},{1,5},{2,6},{3,7},{4,0},{5,1},{6,2},{7,3},{8,12},{9,13},{10,... | collective-permute-start | bytes 3145736 | tf_op jit(solution)/shard_map/ppermute | solution.py:318
  76.8 0.0 all-to-all-done
  76.8 1.6 copy-done
  78.4 9.7 %early_hidden.1.early_ref = bf16[768,768]{1,0:T(8,128)(2,1)} custom-call(s32[2]{0:T(128)} %pad_add_fusion.where_ref.place_ref, bf16[768,2048]{1,0:T(8,128)(2,1)} %bitcast.11, bf16[2048,256]{1,0:T(8,128)(2,1)} %bitcast.18, bf16[2048,256]{1,0:T(8,128)(2,1)} %collective-permute-done.gb, bf16[2048,256]{1,0:T(8,128)(2,1)} %collective-permute-done.1.g1, ...), custom_call_target="tpu_custom_call" | custom-call | tf_op jit(solution)/shard_map/early_hidden/pallas_call | solution.py:157
  88.1 0.0 collective-permute-done.10.d0b
  88.1 0.0 collective-permute-done.12.d2
  88.2 10.1 %late_outputs.1 = bf16[32,4,24,512]{3,2,1,0:T(8,128)(2,1)} custom-call(s32[2]{0:T(128)} %pad_add_fusion.where_ref.place_ref, bf16[768,2048]{1,0:T(8,128)(2,1)} %bitcast.12, bf16[768,768]{1,0:T(8,128)(2,1)} %early_hidden.1.early_ref, bf16[2048,256]{1,0:T(8,128)(2,1)} %collective-permute-done.7.ga, bf16[2048,256]{1,0:T(8,128)(2,1)} %collective-permute-done.6.gb, ...), custom_call_target="tpu_custom_call" | custom-call | tf_op jit(solution)/shard_map/late_outputs/pallas_call | solution.py:219
  98.3 0.0 copy-start.5
  98.3 0.0 copy-start.6
  98.3 12.0 %all-to-all-start.1 = ((bf16[128,24,512]{2,1,0:T(8,128)(2,1)}), bf16[128,24,512]{2,1,0:T(8,128)(2,1)S(1)}, u32[]{:S(2)}, u32[]{:S(2)}) async-start(bf16[128,24,512]{2,1,0:T(8,128)(2,1)} %bitcast.15), calls=%async_computation.1 | async-start | bytes 6291456 | tf_op jit(solution)/shard_map/all_to_all | solution.py:335
  110.3 0.9 copy.9.ids_ref
  111.2 3.9 %columns.1.index_ref = s32[768,2]{1,0:T(8,128)} custom-call(s32[768,2]{1,0:T(8,128)} %copy.9.ids_ref), custom_call_target="tpu_custom_call" | custom-call | tf_op jit(solution)/shard_map/columns/pallas_call | solution.py:338
  115.2 0.9 copy.10.scores_ref
  116.1 35.5 %all-to-all-done.1 = bf16[128,24,512]{2,1,0:T(8,128)(2,1)S(1)} async-done(((bf16[128,24,512]{2,1,0:T(8,128)(2,1)}), bf16[128,24,512]{2,1,0:T(8,128)(2,1)S(1)}, u32[]{:S(2)}, u32[]{:S(2)}) %all-to-all-start.1) | async-done | bytes 3145760 | tf_op jit(solution)/shard_map/all_to_all | solution.py:335
  151.6 1.6 copy-done.2
  153.2 8.6 %combine.1 = f32[768,512]{1,0:T(8,128)} custom-call(s32[768,2]{1,0:T(8,128)} %columns.1.index_ref, f32[768,2]{1,0:T(8,128)} %copy.10.scores_ref, bf16[3072,512]{1,0:T(8,128)(2,1)} %bitcast.14), custom_call_target="tpu_custom_call" | custom-call | tf_op jit(solution)/shard_map/combine/pallas_call | solution.py:281
  161.8 1.7 multiply_reduce_fusion
  163.5 0.6 collective-permute-start.15
  164.1 2.6 %collective-permute-start.16 = (f32[768]{0:T(1024)S(1)}, f32[768]{0:T(1024)S(1)}, u32[]{:S(2)}, u32[]{:S(2)}) collective-permute-start(f32[768]{0:T(1024)S(1)} %multiply_reduce_fusion), channel_id=1, source_target_pairs={{0,2},{1,3},{2,0},{3,1},{4,6},{5,7},{6,4},{7,5},{8,10},{9,11},{10,... | collective-permute-start | bytes 9224 | tf_op jit(solution)/shard_map/ppermute | solution.py:347
  166.7 0.7 collective-permute-start.17
  167.4 1.0 collective-permute-done.15
  168.4 0.9 collective-permute-done.16
  169.2 1.1 collective-permute-done.17
  170.4 1.1 multiply_convert_fusion
  (19 shorter events, 0.0 us)
Async XLA Ops:
  0.0 22.8 %collective-permute-start.1 = (bf16[2048,256]{1,0:T(8,128)(2,1)}, bf16[2048,256]{1,0:T(8,128)(2,1)}, u32[]{:S(2)}, u32[]{:S(2)}) collective-permute-start(bf16[2048,256]{1,0:T(8,128)(2,1)} %bitcast.16), channel_id=1, source_target_pairs={{0,1},{1,0},{2,5},{3,4},{4,3},{5,2},{6,7},{7,6},{8,9},{9,8},{10,13... | collective-permute-start | bytes 3145736 | tf_op jit(solution)/shard_map/ppermute | solution.py:314
  1.6 45.4 %collective-permute-start = (bf16[2048,256]{1,0:T(8,128)(2,1)}, bf16[2048,256]{1,0:T(8,128)(2,1)}, u32[]{:S(2)}, u32[]{:S(2)}) collective-permute-start(bf16[2048,256]{1,0:T(8,128)(2,1)} %bitcast.17), channel_id=1, source_target_pairs={{0,4},{1,5},{2,6},{3,7},{4,0},{5,1},{6,2},{7,3},{8,12},{9,13},{10,... | collective-permute-start | bytes 3145736 | tf_op jit(solution)/shard_map/ppermute | solution.py:315
  3.0 23.4 %collective-permute-start.4 = (bf16[2048,256]{1,0:T(8,128)(2,1)}, bf16[2048,256]{1,0:T(8,128)(2,1)}, u32[]{:S(2)}, u32[]{:S(2)}) collective-permute-start(bf16[2048,256]{1,0:T(8,128)(2,1)} %bitcast.19), channel_id=1, source_target_pairs={{0,1},{1,0},{2,5},{3,4},{4,3},{5,2},{6,7},{7,6},{8,9},{9,8},{10,13... | collective-permute-start | bytes 3145736 | tf_op jit(solution)/shard_map/ppermute | solution.py:314
  3.2 53.3 %collective-permute-start.3 = (bf16[2048,256]{1,0:T(8,128)(2,1)}, bf16[2048,256]{1,0:T(8,128)(2,1)}, u32[]{:S(2)}, u32[]{:S(2)}) collective-permute-start(bf16[2048,256]{1,0:T(8,128)(2,1)} %bitcast.20), channel_id=1, source_target_pairs={{0,4},{1,5},{2,6},{3,7},{4,0},{5,1},{6,2},{7,3},{8,12},{9,13},{10,... | collective-permute-start | bytes 3145736 | tf_op jit(solution)/shard_map/ppermute | solution.py:315
  3.4 34.2 %collective-permute-start.11 = (bf16[256,2048]{1,0:T(8,128)(2,1)}, bf16[256,2048]{1,0:T(8,128)(2,1)}, u32[]{:S(2)}, u32[]{:S(2)}) collective-permute-start(bf16[256,2048]{1,0:T(8,128)(2,1)} %bitcast.22), channel_id=1, source_target_pairs={{0,1},{1,0},{2,5},{3,4},{4,3},{5,2},{6,7},{7,6},{8,9},{9,8},{10,13... | collective-permute-start | bytes 3145736 | tf_op jit(solution)/shard_map/ppermute | solution.py:314
  13.9 62.9 %all-to-all-start = ((bf16[32,24,2048]{2,1,0:T(8,128)(2,1)}), bf16[32,24,2048]{2,1,0:T(8,128)(2,1)S(1)}, u32[]{:S(2)}, u32[]{:S(2)}) async-start(bf16[32,24,2048]{2,1,0:T(8,128)(2,1)} %bitcast.13), calls=%async_computation | async-start | bytes 6291456 | tf_op jit(solution)/shard_map/all_to_all | solution.py:326
  22.8 43.2 %collective-permute-start.2 = (bf16[2048,256]{1,0:T(8,128)(2,1)}, bf16[2048,256]{1,0:T(8,128)(2,1)S(1)}, u32[]{:S(2)}, u32[]{:S(2)}) collective-permute-start(bf16[2048,256]{1,0:T(8,128)(2,1)} %collective-permute-done.1.g1), channel_id=1, source_target_pairs={{0,4},{1,5},{2,6},{3,7},{4,0},{5,1},{6,2},{7,3},{8,12},{9,13},{10,... | collective-permute-start | bytes 3145736 | tf_op jit(solution)/shard_map/ppermute | solution.py:316
  26.4 39.6 %collective-permute-start.5 = (bf16[2048,256]{1,0:T(8,128)(2,1)}, bf16[2048,256]{1,0:T(8,128)(2,1)S(1)}, u32[]{:S(2)}, u32[]{:S(2)}) collective-permute-start(bf16[2048,256]{1,0:T(8,128)(2,1)} %collective-permute-done.4.u1), channel_id=1, source_target_pairs={{0,4},{1,5},{2,6},{3,7},{4,0},{5,1},{6,2},{7,3},{8,12},{9,13},{10,... | collective-permute-start | bytes 3145736 | tf_op jit(solution)/shard_map/ppermute | solution.py:316
  37.6 28.9 %collective-permute-start.13 = (bf16[256,2048]{1,0:T(8,128)(2,1)}, bf16[256,2048]{1,0:T(8,128)(2,1)}, u32[]{:S(2)}, u32[]{:S(2)}) collective-permute-start(bf16[256,2048]{1,0:T(8,128)(2,1)} %collective-permute-done.11.d1), channel_id=1, source_target_pairs={{0,0},{1,1},{2,3},{3,2},{4,5},{5,4},{6,6},{7,7},{8,8},{9,9},{10,11... | collective-permute-start | bytes 3145736 | tf_op jit(solution)/shard_map/ppermute | solution.py:317
  47.0 19.5 %collective-permute-start.6 = (bf16[2048,256]{1,0:T(8,128)(2,1)}, bf16[2048,256]{1,0:T(8,128)(2,1)}, u32[]{:S(2)}, u32[]{:S(2)}) collective-permute-start(bf16[2048,256]{1,0:T(8,128)(2,1)} %collective-permute-done.1.g1), channel_id=1, source_target_pairs={{0,0},{1,1},{2,3},{3,2},{4,5},{5,4},{6,6},{7,7},{8,8},{9,9},{10,11... | collective-permute-start | bytes 3145736 | tf_op jit(solution)/shard_map/ppermute | solution.py:317
  56.5 10.5 %collective-permute-start.8 = (bf16[2048,256]{1,0:T(8,128)(2,1)}, bf16[2048,256]{1,0:T(8,128)(2,1)}, u32[]{:S(2)}, u32[]{:S(2)}) collective-permute-start(bf16[2048,256]{1,0:T(8,128)(2,1)} %collective-permute-done.4.u1), channel_id=1, source_target_pairs={{0,0},{1,1},{2,3},{3,2},{4,5},{5,4},{6,6},{7,7},{8,8},{9,9},{10,11... | collective-permute-start | bytes 3145736 | tf_op jit(solution)/shard_map/ppermute | solution.py:317
  65.9 1.0 copy-start.3
  65.9 22.2 %collective-permute-start.10 = (bf16[256,2048]{1,0:T(8,128)(2,1)}, bf16[256,2048]{1,0:T(8,128)(2,1)}, u32[]{:S(2)}, u32[]{:S(2)}) collective-permute-start(bf16[256,2048]{1,0:T(8,128)(2,1)} %bitcast.23), channel_id=1, source_target_pairs={{0,4},{1,5},{2,6},{3,7},{4,0},{5,1},{6,2},{7,3},{8,12},{9,13},{10,... | collective-permute-start | bytes 3145736 | tf_op jit(solution)/shard_map/ppermute | solution.py:315
  65.9 1.3 copy-start.4
  66.0 22.2 %collective-permute-start.12 = (bf16[256,2048]{1,0:T(8,128)(2,1)}, bf16[256,2048]{1,0:T(8,128)(2,1)}, u32[]{:S(2)}, u32[]{:S(2)}) collective-permute-start(bf16[256,2048]{1,0:T(8,128)(2,1)} %collective-permute-done.11.d1), channel_id=1, source_target_pairs={{0,4},{1,5},{2,6},{3,7},{4,0},{5,1},{6,2},{7,3},{8,12},{9,13},{10,... | collective-permute-start | bytes 3145736 | tf_op jit(solution)/shard_map/ppermute | solution.py:316
  66.4 21.7 %collective-permute-start.14 = (bf16[256,2048]{1,0:T(8,128)(2,1)}, bf16[256,2048]{1,0:T(8,128)(2,1)}, u32[]{:S(2)}, u32[]{:S(2)}) collective-permute-start(bf16[256,2048]{1,0:T(8,128)(2,1)} %collective-permute-done.13.d3b), channel_id=1, source_target_pairs={{0,4},{1,5},{2,6},{3,7},{4,0},{5,1},{6,2},{7,3},{8,12},{9,13},{10,... | collective-permute-start | bytes 3145736 | tf_op jit(solution)/shard_map/ppermute | solution.py:318
  66.6 21.6 %collective-permute-start.7 = (bf16[2048,256]{1,0:T(8,128)(2,1)}, bf16[2048,256]{1,0:T(8,128)(2,1)}, u32[]{:S(2)}, u32[]{:S(2)}) collective-permute-start(bf16[2048,256]{1,0:T(8,128)(2,1)} %collective-permute-done.6.gb), channel_id=1, source_target_pairs={{0,4},{1,5},{2,6},{3,7},{4,0},{5,1},{6,2},{7,3},{8,12},{9,13},{10,... | collective-permute-start | bytes 3145736 | tf_op jit(solution)/shard_map/ppermute | solution.py:318
  67.2 20.9 %collective-permute-start.9 = (bf16[2048,256]{1,0:T(8,128)(2,1)}, bf16[2048,256]{1,0:T(8,128)(2,1)}, u32[]{:S(2)}, u32[]{:S(2)}) collective-permute-start(bf16[2048,256]{1,0:T(8,128)(2,1)} %collective-permute-done.8.ub), channel_id=1, source_target_pairs={{0,4},{1,5},{2,6},{3,7},{4,0},{5,1},{6,2},{7,3},{8,12},{9,13},{10,... | collective-permute-start | bytes 3145736 | tf_op jit(solution)/shard_map/ppermute | solution.py:318
  76.8 1.6 copy-start
  98.3 12.0 %copy-start.5 = (s32[768,2]{0,1:T(2,128)S(1)}, s32[768,2]{0,1:T(2,128)}, u32[]{:S(2)}) copy-start(s32[768,2]{0,1:T(2,128)} %param.10) | copy-start | bytes 18436
  98.3 16.9 %copy-start.6 = (f32[768,2]{0,1:T(2,128)S(1)}, f32[768,2]{0,1:T(2,128)}, u32[]{:S(2)}) copy-start(f32[768,2]{0,1:T(2,128)} %param.11) | copy-start | bytes 18436
  98.3 53.3 %all-to-all-start.1 = ((bf16[128,24,512]{2,1,0:T(8,128)(2,1)}), bf16[128,24,512]{2,1,0:T(8,128)(2,1)S(1)}, u32[]{:S(2)}, u32[]{:S(2)}) async-start(bf16[128,24,512]{2,1,0:T(8,128)(2,1)} %bitcast.15), calls=%async_computation.1 | async-start | bytes 6291456 | tf_op jit(solution)/shard_map/all_to_all | solution.py:335
  151.6 1.6 copy-start.2
  161.8 8.6 %copy-start.1 = (f32[768,512]{1,0:T(8,128)S(1)}, f32[768,512]{1,0:T(8,128)}, u32[]{:S(2)}) copy-start(f32[768,512]{1,0:T(8,128)} %combine.1) | copy-start | bytes 4718596
  161.8 8.6 %copy-start.7 = (f32[512]{0:T(512)S(1)}, f32[512]{0:T(512)}, u32[]{:S(2)}) copy-start(f32[512]{0:T(512)} %param.15) | copy-start | bytes 6148
  163.5 4.9 %collective-permute-start.15 = (f32[768]{0:T(1024)S(1)}, f32[768]{0:T(1024)S(1)}, u32[]{:S(2)}, u32[]{:S(2)}) collective-permute-start(f32[768]{0:T(1024)S(1)} %multiply_reduce_fusion), channel_id=1, source_target_pairs={{0,1},{1,2},{2,3},{3,0},{4,5},{5,6},{6,7},{7,4},{8,9},{9,10},{10,1... | collective-permute-start | bytes 9224 | tf_op jit(solution)/shard_map/ppermute | solution.py:347
  164.1 5.1 %collective-permute-start.16 = (f32[768]{0:T(1024)S(1)}, f32[768]{0:T(1024)S(1)}, u32[]{:S(2)}, u32[]{:S(2)}) collective-permute-start(f32[768]{0:T(1024)S(1)} %multiply_reduce_fusion), channel_id=1, source_target_pairs={{0,2},{1,3},{2,0},{3,1},{4,6},{5,7},{6,4},{7,5},{8,10},{9,11},{10,... | collective-permute-start | bytes 9224 | tf_op jit(solution)/shard_map/ppermute | solution.py:347
  166.7 3.6 %collective-permute-start.17 = (f32[768]{0:T(1024)S(1)}, f32[768]{0:T(1024)S(1)}, u32[]{:S(2)}, u32[]{:S(2)}) collective-permute-start(f32[768]{0:T(1024)S(1)} %multiply_reduce_fusion), channel_id=1, source_target_pairs={{0,3},{1,0},{2,1},{3,2},{4,7},{5,4},{6,5},{7,6},{8,11},{9,8},{10,9... | collective-permute-start | bytes 9224 | tf_op jit(solution)/shard_map/ppermute | solution.py:347

commit v2 on v1

v2 whole, which is shorter than its diff:
```python
import functools

import jax
import jax.numpy as jnp
from jax import lax
from jax.experimental import pallas as pl
from jax.experimental.pallas import tpu as pltpu
from jax.sharding import PartitionSpec as P


epsilon = 1e-06
AXES = ("ep", "tp")
MIB = 1024 * 1024


def place_of(ids, slot):
    ep = (ids // 2) * 2 + slot % 2
    tp = (ids % 2) * 2 + (slot % 4) // 2
    return ep, tp, slot // 4


def permutes(count_ep, count_tp):
    def dev(ep, x):
        return ep * count_tp + x

    first, second, swap = [], [], []
    for ep in range(count_ep):
        core = ep % 2
        for x in range(count_tp):
            own = x // 2 == core
            swap.append((dev(ep, x), dev(ep ^ 1, x)))
            if own:
                first.append((dev(ep, x), dev(ep, x ^ 1)))
            else:
                first.append((dev(ep, x), dev(ep ^ 1, count_tp - 1 - x)))
                second.append((dev(ep, x), dev(ep, x ^ 1)))
    return first, second, swap


def dispatch_kernel(where_ref, ids_ref, gain_ref, tokens_ref, out_ref, raw, normed, pick, sems, *, rows, chunks):
    step = pl.program_id(0)
    count, _ = raw.shape
    part = count // chunks

    @pl.when(step == 0)
    def _():
        for i in range(chunks):
            pltpu.make_async_copy(
                tokens_ref.at[pl.ds(i * part, part)], raw.at[pl.ds(i * part, part)], sems.at[i]
            ).start()
        experts = 32
        first = ids_ref[0:1, :]
        second = ids_ref[1:2, :]
        number = lax.broadcasted_iota(jnp.int32, (experts, count), 0)
        named_first = number == first
        named_second = number == second
        named = jnp.where(named_first | named_second, 1.0, 0.0).astype(jnp.bfloat16)
        before = lax.broadcasted_iota(jnp.int32, (count, count), 0) < lax.broadcasted_iota(
            jnp.int32, (count, count), 1
        )
        ranks = jnp.dot(
            named, jnp.where(before, 1.0, 0.0).astype(jnp.bfloat16), preferred_element_type=jnp.float32
        )
        slot_first = jnp.sum(jnp.where(named_first, ranks, 0.0), axis=0, keepdims=True).astype(jnp.int32)
        slot_second = jnp.sum(jnp.where(named_second, ranks, 0.0), axis=0, keepdims=True).astype(jnp.int32)
        mine = where_ref[0]

        def row_of(ids, slot):
            ep, tp, row = place_of(ids, slot)
            return jnp.where(tp == mine, ep * rows + row, -1)

        row_first = row_of(first, slot_first)
        row_second = row_of(second, slot_second)
        index = lax.broadcasted_iota(jnp.int32, (count, count), 0)
        pick[...] = jnp.where((index == row_first) | (index == row_second), 1.0, 0.0).astype(jnp.bfloat16)
        gain = gain_ref[...]
        for i in range(chunks):
            pltpu.make_async_copy(
                tokens_ref.at[pl.ds(i * part, part)], raw.at[pl.ds(i * part, part)], sems.at[i]
            ).wait()
            value = raw[pl.ds(i * part, part), :].astype(jnp.float32)
            mean = jnp.mean(value * value, axis=1, keepdims=True)
            normed[pl.ds(i * part, part), :] = (value * lax.rsqrt(mean + epsilon) * gain).astype(jnp.bfloat16)

    block = out_ref.shape[0]
    out_ref[...] = jnp.dot(
        pick[pl.ds(step * block, block), :], normed[...], preferred_element_type=jnp.float32
    ).astype(jnp.bfloat16)


def dispatch_buffer(place, ids_rows, gain, tokens, rows):
    count, width = tokens.shape
    steps, chunks = 4, 4
    return pl.pallas_call(
        functools.partial(dispatch_kernel, rows=rows, chunks=chunks),
        grid_spec=pltpu.PrefetchScalarGridSpec(
            num_scalar_prefetch=1,
            grid=(steps,),
            in_specs=[
                pl.BlockSpec((2, count), lambda i, p: (0, 0)),
                pl.BlockSpec((1, width), lambda i, p: (0, 0)),
                pl.BlockSpec(memory_space=pltpu.HBM),
            ],
            out_specs=pl.BlockSpec((count // steps, width), lambda i, p: (i, 0)),
            scratch_shapes=[
                pltpu.VMEM((count, width), jnp.bfloat16),
                pltpu.VMEM((count, width), jnp.bfloat16),
                pltpu.VMEM((count, count), jnp.bfloat16),
                pltpu.SemaphoreType.DMA((chunks,)),
            ],
        ),
        out_shape=pltpu.HBM((count, width), jnp.bfloat16),
        compiler_params=pltpu.CompilerParams(
            dimension_semantics=("arbitrary",), vmem_limit_bytes=58 * MIB
        ),
        name="dispatch_buffer",
    )(place, ids_rows, gain, tokens)


def hidden_of(rows, gate, up):
    gate_acts = jnp.dot(rows, gate, preferred_element_type=jnp.float32)
    up_acts = jnp.dot(rows, up, preferred_element_type=jnp.float32)
    return gate_acts / (1.0 + jnp.exp(-gate_acts)) * up_acts


def start_one(flag, a, b, dst, sem):
    @pl.when(flag == 1)
    def _():
        pltpu.make_async_copy(a, dst, sem).start()

    @pl.when(flag != 1)
    def _():
        pltpu.make_async_copy(b, dst, sem).start()


def early_kernel(place_ref, rows_ref, ga, gb, g1, g2, ua, ub, u1, u2, out_ref, rows, gate, up, sems):
    flag = place_ref[1]
    start_one(flag, ga, gb, gate.at[0], sems.at[0])
    start_one(flag, ua, ub, up.at[0], sems.at[1])
    load = pltpu.make_async_copy(rows_ref, rows, sems.at[6])
    load.start()
    for i, (g, u) in enumerate(((g1, u1), (g2, u2))):
        pltpu.make_async_copy(g, gate.at[i + 1], sems.at[2 * i + 2]).start()
        pltpu.make_async_copy(u, up.at[i + 1], sems.at[2 * i + 3]).start()
    load.wait()
    part = gate.shape[2]
    for i in range(3):
        pltpu.make_async_copy(g1, gate.at[i], sems.at[2 * i]).wait()
        pltpu.make_async_copy(u1, up.at[i], sems.at[2 * i + 1]).wait()
        value = hidden_of(rows[...], gate[i], up[i])
        out_ref[:, i * part : (i + 1) * part] = value.astype(jnp.bfloat16)


def middle_kernel(place_ref, rows_ref, ga, gb, ua, ub, out_ref, rows, gate, up, sems):
    flag = place_ref[1]
    load = pltpu.make_async_copy(rows_ref, rows, sems.at[0])
    load.start()
    start_one(flag, ga, gb, gate, sems.at[1])
    start_one(flag, ua, ub, up, sems.at[2])
    load.wait()
    pltpu.make_async_copy(ga, gate, sems.at[1]).wait()
    pltpu.make_async_copy(ua, up, sems.at[2]).wait()
    out_ref[...] = hidden_of(rows[...], gate[...], up[...]).astype(jnp.bfloat16)


HBM = pl.BlockSpec(memory_space=pltpu.HBM)
ANY = pl.BlockSpec(memory_space=pl.ANY)
SMEM = pl.BlockSpec(memory_space=pltpu.SMEM)


def early_hidden(place, rows, gates, ups):
    count, width = rows.shape
    part = gates[0].shape[1]
    return pl.pallas_call(
        early_kernel,
        in_specs=[SMEM, ANY] + [HBM] * 8,
        out_specs=pl.BlockSpec((count, 3 * part), lambda: (0, 0)),
        scratch_shapes=[
            pltpu.VMEM((count, width), jnp.bfloat16),
            pltpu.VMEM((3, width, part), jnp.bfloat16),
            pltpu.VMEM((3, width, part), jnp.bfloat16),
            pltpu.SemaphoreType.DMA((7,)),
        ],
        out_shape=jax.ShapeDtypeStruct((count, 3 * part), jnp.bfloat16),
        compiler_params=pltpu.CompilerParams(vmem_limit_bytes=50 * MIB),
        name="early_hidden",
    )(place, rows, *gates, *ups)


def middle_hidden(place, rows, gates, ups):
    count, width = rows.shape
    part = gates[0].shape[1]
    return pl.pallas_call(
        middle_kernel,
        in_specs=[SMEM, ANY] + [HBM] * 4,
        out_specs=pl.BlockSpec((count, part), lambda: (0, 0)),
        scratch_shapes=[
            pltpu.VMEM((count, width), jnp.bfloat16),
            pltpu.VMEM((width, part), jnp.bfloat16),
            pltpu.VMEM((width, part), jnp.bfloat16),
            pltpu.SemaphoreType.DMA((3,)),
        ],
        out_shape=jax.ShapeDtypeStruct((count, part), jnp.bfloat16),
        compiler_params=pltpu.CompilerParams(vmem_limit_bytes=50 * MIB),
        name="middle_hidden",
    )(place, rows, *gates, *ups)


def late_kernel(place_ref, early_ref, middle_ref, d0a, d0b, d1, d2, d3a, d3b, out_ref, down, hidden, out, sems, out_sems):
    flag = place_ref[1]
    senders, pieces, slots, piece = out_ref.shape
    part = d1.shape[0]
    first = pltpu.make_async_copy(early_ref, hidden.at[:, pl.ds(0, 3 * part)], sems.at[4 * pieces])
    second = pltpu.make_async_copy(middle_ref, hidden.at[:, pl.ds(3 * part, part)], sems.at[4 * pieces + 1])
    first.start()
    second.start()

    def target(i, f):
        return down.at[pl.ds(i * part, part), pl.ds(f * piece, piece)]

    def source(ref, f):
        return ref.at[:, pl.ds(f * piece, piece)]

    for f in range(pieces):
        start_one(flag, source(d0a, f), source(d0b, f), target(0, f), sems.at[4 * f])
        pltpu.make_async_copy(source(d1, f), target(1, f), sems.at[4 * f + 1]).start()
        pltpu.make_async_copy(source(d2, f), target(2, f), sems.at[4 * f + 2]).start()
        start_one(flag, source(d3a, f), source(d3b, f), target(3, f), sems.at[4 * f + 3])
    first.wait()
    second.wait()
    for f in range(pieces):
        for i in range(4):
            pltpu.make_async_copy(source(d1, f), target(i, f), sems.at[4 * f + i]).wait()
        value = jnp.dot(
            hidden[...], down[:, f * piece : (f + 1) * piece], preferred_element_type=jnp.float32
        )
        out[f] = value.reshape(senders, slots, piece).astype(jnp.bfloat16)
        pltpu.make_async_copy(out.at[f], out_ref.at[:, f], out_sems.at[f]).start()
    for f in range(pieces):
        pltpu.make_async_copy(out.at[f], out_ref.at[:, f], out_sems.at[f]).wait()


def late_outputs(place, early, middle, downs, senders, pieces):
    count = early.shape[0]
    part, width = downs[0].shape
    slots = count // senders
    piece = width // pieces
    shape = (senders, pieces, slots, piece)
    return pl.pallas_call(
        late_kernel,
        in_specs=[SMEM, ANY, ANY] + [HBM] * 6,
        out_specs=HBM,
        scratch_shapes=[
            pltpu.VMEM((4 * part, width), jnp.bfloat16),
            pltpu.VMEM((count, 4 * part), jnp.bfloat16),
            pltpu.VMEM((pieces, senders, slots, piece), jnp.bfloat16),
            pltpu.SemaphoreType.DMA((4 * pieces + 2,)),
            pltpu.SemaphoreType.DMA((pieces,)),
        ],
        out_shape=pltpu.HBM(shape, jnp.bfloat16),
        compiler_params=pltpu.CompilerParams(vmem_limit_bytes=50 * MIB),
        name="late_outputs",
    )(place, early, middle, *downs)


def columns_kernel(ids_ref, out_ref, *, cuts, count_tp):
    count = ids_ref.shape[0]
    experts = 32
    first = ids_ref[:, 0:1]
    second = ids_ref[:, 1:2]
    number = lax.broadcasted_iota(jnp.int32, (count, experts), 1)
    named_first = number == first
    named_second = number == second
    named = jnp.where(named_first | named_second, 1.0, 0.0).astype(jnp.bfloat16)
    before = lax.broadcasted_iota(jnp.int32, (count, count), 1) < lax.broadcasted_iota(
        jnp.int32, (count, count), 0
    )
    ranks = jnp.dot(
        jnp.where(before, 1.0, 0.0).astype(jnp.bfloat16), named, preferred_element_type=jnp.float32
    )
    for choice, (ids, chosen) in enumerate(((first, named_first), (second, named_second))):
        slot = jnp.sum(jnp.where(chosen, ranks, 0.0), axis=1, keepdims=True).astype(jnp.int32)
        ep, tp, row = place_of(ids, slot)
        device = ep * count_tp + tp
        for i, (lo, hi) in enumerate(cuts):
            inside = (row >= lo) & (row < hi)
            out_ref[:, 2 * i + choice : 2 * i + choice + 1] = jnp.where(
                inside, device * (hi - lo) + row - lo, -1
            )


def routing_columns(ids, cuts, count_tp):
    return pl.pallas_call(
        functools.partial(columns_kernel, cuts=cuts, count_tp=count_tp),
        out_shape=jax.ShapeDtypeStruct((ids.shape[0], 2 * len(cuts)), jnp.int32),
        compiler_params=pltpu.CompilerParams(vmem_limit_bytes=16 * MIB),
        name="columns",
    )(ids)


def combine_kernel(index_ref, scores_ref, returned_ref, out_ref, squares_ref):
    total = returned_ref.shape[0]
    count = index_ref.shape[0]
    index = lax.broadcasted_iota(jnp.int32, (count, total), 1)
    returned = returned_ref[...]

    def picked(column):
        hot = jnp.where(index == index_ref[:, column : column + 1], 1.0, 0.0).astype(jnp.bfloat16)
        return jnp.dot(hot, returned, preferred_element_type=jnp.float32)

    scores = scores_ref[...]
    mix = scores / jnp.sum(scores, axis=1, keepdims=True)
    value = mix[:, 0:1] * picked(0) + mix[:, 1:2] * picked(1)
    out_ref[...] = value
    square = value * value
    lanes = 128
    folded = square[:, 0:lanes]
    for i in range(1, square.shape[1] // lanes):
        folded = folded + square[:, i * lanes : (i + 1) * lanes]
    squares_ref[...] = jnp.sum(folded.T, axis=0, keepdims=True)


def combine(index, scores, returned):
    count = index.shape[0]
    total, piece = returned.shape
    steps = 3
    block = count // steps
    row_block = pl.BlockSpec((block, piece), lambda i: (i, 0))
    return pl.pallas_call(
        combine_kernel,
        grid=(steps,),
        in_specs=[
            pl.BlockSpec((block, 2), lambda i: (i, 0)),
            pl.BlockSpec((block, 2), lambda i: (i, 0)),
            pl.BlockSpec((total, piece), lambda i: (0, 0)),
        ],
        out_specs=[row_block, pl.BlockSpec((1, block), lambda i: (0, i))],
        out_shape=[
            jax.ShapeDtypeStruct((count, piece), jnp.float32),
            jax.ShapeDtypeStruct((1, count), jnp.float32),
        ],
        compiler_params=pltpu.CompilerParams(dimension_semantics=("arbitrary",), vmem_limit_bytes=50 * MIB),
        name="combine",
    )(index, scores, returned)


def per_device(
    tokens, in_gain, route_ids, route_scores, gate_weight, up_weight, down_weight, out_gain
):
    count_ep = lax.axis_size("ep")
    count_tp = lax.axis_size("tp")
    tok_count, full_width = tokens.shape
    part_width = full_width // count_tp
    capacity = 2 * tok_count * route_ids.shape[1] // count_ep
    rows = capacity // count_tp
    x = lax.axis_index("tp")
    core = lax.axis_index("ep") % 2
    place = jnp.stack([x, (x // 2 == core).astype(jnp.int32)]).astype(jnp.int32)

    first, second, swap = permutes(count_ep, count_tp)

    def send(weight, pairs):
        return lax.ppermute(weight, AXES, pairs)

    def spread(weight):
        moved = send(weight, first)
        other_own = send(weight, swap)
        other_moved = send(moved, swap)
        last = send(moved, second)
        other_last = send(last, swap)
        return (weight, other_own), moved, other_moved, (other_last, last)

    gate = spread(gate_weight[0])
    up = spread(up_weight[0])
    down = spread(down_weight[0])

    buffer = dispatch_buffer(place, route_ids.T, in_gain[None, :], tokens, rows)
    received = lax.all_to_all(
        buffer.reshape(count_ep, rows, full_width), "ep", split_axis=0, concat_axis=0, tiled=True
    ).reshape(count_ep * rows, full_width)
    early = early_hidden(place, received, (*gate[0], gate[1], gate[2]), (*up[0], up[1], up[2]))
    middle = middle_hidden(place, received, gate[3], up[3])
    outputs = late_outputs(
        place, early, middle, (*down[0], down[1], down[2], *down[3]), count_ep, count_tp
    )
    returned = lax.all_to_all(
        outputs.reshape(count_ep * count_tp, rows, part_width), AXES, split_axis=0, concat_axis=0, tiled=True
    ).reshape(count_ep * count_tp * rows, part_width)
    index = routing_columns(route_ids, ((0, rows),), count_tp)
    combined, squares = combine(index, route_scores, returned)
    squares = squares[0]
    total = squares
    for shift in range(1, count_tp):
        total = total + lax.ppermute(
            squares, "tp", [(i, (i + shift) % count_tp) for i in range(count_tp)]
        )
    scaled = combined * lax.rsqrt(total[:, None] / full_width + epsilon) * out_gain
    return scaled.astype(jnp.bfloat16)


def solution(mesh):
    in_specs = (
        P("ep", None),
        P(),
        P("ep", None),
        P("ep", None),
        P("ep", None, "tp"),
        P("ep", None, "tp"),
        P("ep", "tp", None),
        P("tp"),
    )
    out_specs = P("ep", "tp")
    return jax.shard_map(per_device, mesh=mesh, in_specs=in_specs, out_specs=out_specs, check_vma=False)
```

time: 174 us -> 160 us (0.920); the launches traced: 171 us -> 160 us
  starting transfers between devices: 69.9 us -> 55.9 us
  waiting for transfers between devices: 52 us -> 61.3 us
  local copies, waits for them, and re-layouts: 5.44 us -> 1.4 us
    ppermute x15, starting transfers between devices: 45.1 us -> 32 us  [send(): return lax.ppermute(weight, AXES, pairs)]
    ppermute x15, waiting for transfers between devices: 13.6 us -> 20.2 us  [send(): return lax.ppermute(weight, AXES, pairs)]
    unnamed x18 -> x16, local copies, waits for them, and re-layouts: 5.44 us -> 1.4 us
    all_to_all x1, waiting for transfers between devices: 35.5 us -> 38.2 us  [per_device(): lax.all_to_all(outputs.reshape(count_ep * count_tp, rows, part_width), AX...]
    pallas_call x4 -> x5, Pallas kernels: 32.3 us -> 31.3 us  [the longest x1 9.34 us: early_hidden(): pl.pallas_call(early_kernel, in_specs=[SMEM, ANY] + [HBM] * 8, out_specs=...]
  transfers between devices with their start and end apart: 20 -> 20, of which waited for: 6 -> 6; matrix products, arithmetic and copies ran while one was open for 1% -> 1% of each run, Pallas kernels for 13% -> 15%
where the time goes in v2:
time: 160 us
  waiting for transfers between devices  61.3 us (38%)
  starting transfers between devices  55.9 us (35%)
  Pallas kernels  39.4 us (25%)
  other arithmetic  1.75 us (1%)
    all_to_all x1, waiting for transfers between devices, per_device(): lax.all_to_all(outputs.reshape(count_ep * count_tp, rows, part_width), AX...  38.2 us
    ppermute x15, starting transfers between devices, send(): return lax.ppermute(weight, AXES, pairs)  32 us
    ppermute x15, waiting for transfers between devices, send(): return lax.ppermute(weight, AXES, pairs)  20.2 us
    all_to_all x1, starting transfers between devices, per_device(): lax.all_to_all(outputs.reshape(count_ep * count_tp, rows, part_width), AX...  10.8 us
    pallas_call x1, Pallas kernels, early_hidden(): pl.pallas_call(early_kernel, in_specs=[SMEM, ANY] + [HBM] * 8, out_specs=...  9.34 us
    all_to_all x1, starting transfers between devices, per_device(): lax.all_to_all(buffer.reshape(count_ep, rows, full_width), 'ep', split_ax...  9.13 us
    pallas_call x1, Pallas kernels, dispatch_buffer(): pl.pallas_call(functools.partial(dispatch_kernel, rows=rows, chunks=chunk...  8.13 us
    pallas_call x1, Pallas kernels, combine(): pl.pallas_call(combine_kernel, grid=(steps,), in_specs=[pl.BlockSpec((blo...  7.68 us
  transfers between devices with their start and end apart: 20, of which 6 were waited for; matrix products, arithmetic and copies ran while one was open for 1% of the time, Pallas kernels for 15%

profile of v2, /device:TPU:0, one launch (start us, length us, event | category | flops | bytes accessed | tf_op | source)
XLA Modules:
  0.0 159.9 jit_solution(4435573836927764855)
XLA Ops:
  0.0 1.6 %collective-permute-start.1 = (bf16[2048,256]{1,0:T(8,128)(2,1)}, bf16[2048,256]{1,0:T(8,128)(2,1)S(1)}, u32[]{:S(2)}, u32[]{:S(2)}) collective-permute-start(bf16[2048,256]{1,0:T(8,128)(2,1)} %bitcast.11), channel_id=1, source_target_pairs={{0,1},{1,0},{2,5},{3,4},{4,3},{5,2},{6,7},{7,6},{8,9},{9,8},{10,13... | collective-permute-start | bytes 3145736 | tf_op jit(solution)/shard_map/ppermute | solution.py:363
  1.6 1.4 collective-permute-start
  3.0 0.2 collective-permute-start.4
  3.2 0.2 collective-permute-start.3
  3.4 1.6 %collective-permute-start.11 = (bf16[256,2048]{1,0:T(8,128)(2,1)}, bf16[256,2048]{1,0:T(8,128)(2,1)}, u32[]{:S(2)}, u32[]{:S(2)}) collective-permute-start(bf16[256,2048]{1,0:T(8,128)(2,1)} %bitcast.14), channel_id=1, source_target_pairs={{0,1},{1,0},{2,5},{3,4},{4,3},{5,2},{6,7},{7,6},{8,9},{9,8},{10,13... | collective-permute-start | bytes 3145736 | tf_op jit(solution)/shard_map/ppermute | solution.py:363
  5.0 0.6 pad_add_fusion.where_ref.place_ref
  5.7 8.1 %dispatch_buffer.1 = bf16[768,2048]{1,0:T(8,128)(2,1)} custom-call(s32[2]{0:T(128)} %pad_add_fusion.where_ref.place_ref, s32[2,768]{1,0:T(2,128)} %bitcast.22, f32[1,2048]{1,0:T(1,128)} %bitcast.23, bf16[768,2048]{1,0:T(8,128)(2,1)} %tokens_ref.1), custom_call_target="tpu_custom_call" | custom-call | tf_op jit(solution)/shard_map/dispatch_buffer/pallas_call | solution.py:94
  13.8 0.0 copy-start
  13.8 9.1 %all-to-all-start = ((bf16[32,24,2048]{2,1,0:T(8,128)(2,1)}), bf16[32,24,2048]{2,1,0:T(8,128)(2,1)}, u32[]{:S(2)}, u32[]{:S(2)}) async-start(bf16[32,24,2048]{2,1,0:T(8,128)(2,1)} %bitcast.17), calls=%async_computation | async-start | bytes 6291456 | tf_op jit(solution)/shard_map/all_to_all | solution.py:378
  23.0 0.0 collective-permute-done.1.g1
  23.0 1.7 %collective-permute-start.6 = (bf16[2048,256]{1,0:T(8,128)(2,1)S(1)}, bf16[2048,256]{1,0:T(8,128)(2,1)}, u32[]{:S(2)}, u32[]{:S(2)}) collective-permute-start(bf16[2048,256]{1,0:T(8,128)(2,1)S(1)} %collective-permute-done.1.g1), channel_id=1, source_target_pairs={{2,3},{3,2},{4,5},{5,4},{10,11},{11,10},{12,13},{13,12},{18,19},{1... | collective-permute-start | bytes 3145736 | tf_op jit(solution)/shard_map/ppermute | solution.py:363
  24.6 1.7 %collective-permute-done.4.u1 = bf16[2048,256]{1,0:T(8,128)(2,1)} collective-permute-done((bf16[2048,256]{1,0:T(8,128)(2,1)}, bf16[2048,256]{1,0:T(8,128)(2,1)}, u32[]{:S(2)}, u32[]{:S(2)}) %collective-permute-start.4) | collective-permute-done | bytes 1048608 | tf_op jit(solution)/shard_map/ppermute | solution.py:363
  26.4 1.7 %collective-permute-start.8 = (bf16[2048,256]{1,0:T(8,128)(2,1)}, bf16[2048,256]{1,0:T(8,128)(2,1)}, u32[]{:S(2)}, u32[]{:S(2)}) collective-permute-start(bf16[2048,256]{1,0:T(8,128)(2,1)} %collective-permute-done.4.u1), channel_id=1, source_target_pairs={{2,3},{3,2},{4,5},{5,4},{10,11},{11,10},{12,13},{13,12},{18,19},{1... | collective-permute-start | bytes 3145736 | tf_op jit(solution)/shard_map/ppermute | solution.py:363
  28.0 1.3 collective-permute-start.2
  29.3 0.1 collective-permute-start.5
  29.4 18.4 %collective-permute-done.11.d1 = bf16[256,2048]{1,0:T(8,128)(2,1)} collective-permute-done((bf16[256,2048]{1,0:T(8,128)(2,1)}, bf16[256,2048]{1,0:T(8,128)(2,1)}, u32[]{:S(2)}, u32[]{:S(2)}) %collective-permute-start.11) | collective-permute-done | bytes 1048608 | tf_op jit(solution)/shard_map/ppermute | solution.py:363
  47.8 1.6 %collective-permute-start.13 = (bf16[256,2048]{1,0:T(8,128)(2,1)}, bf16[256,2048]{1,0:T(8,128)(2,1)}, u32[]{:S(2)}, u32[]{:S(2)}) collective-permute-start(bf16[256,2048]{1,0:T(8,128)(2,1)} %collective-permute-done.11.d1), channel_id=1, source_target_pairs={{2,3},{3,2},{4,5},{5,4},{10,11},{11,10},{12,13},{13,12},{18,19},{1... | collective-permute-start | bytes 3145736 | tf_op jit(solution)/shard_map/ppermute | solution.py:363
  49.5 0.0 collective-permute-done.8.ub
  49.5 10.4 %collective-permute-start.7 = (bf16[2048,256]{1,0:T(8,128)(2,1)}, bf16[2048,256]{1,0:T(8,128)(2,1)}, u32[]{:S(2)}, u32[]{:S(2)}) collective-permute-start(bf16[2048,256]{1,0:T(8,128)(2,1)} %collective-permute-done.6.gb), channel_id=1, source_target_pairs={{0,4},{1,5},{2,6},{3,7},{4,0},{5,1},{6,2},{7,3},{8,12},{9,13},{10,... | collective-permute-start | bytes 3145736 | tf_op jit(solution)/shard_map/ppermute | solution.py:363
  59.9 1.0 copy-done.3
  60.9 0.0 collective-permute-start.9
  60.9 0.0 collective-permute-done.5.u2
  60.9 0.5 collective-permute-start.12
  61.4 0.0 collective-permute-done.13.d3b
  61.4 9.7 %collective-permute-start.14 = (bf16[256,2048]{1,0:T(8,128)(2,1)}, bf16[256,2048]{1,0:T(8,128)(2,1)}, u32[]{:S(2)}, u32[]{:S(2)}) collective-permute-start(bf16[256,2048]{1,0:T(8,128)(2,1)} %collective-permute-done.13.d3b), channel_id=1, source_target_pairs={{0,4},{1,5},{2,6},{3,7},{4,0},{5,1},{6,2},{7,3},{8,12},{9,13},{10,... | collective-permute-start | bytes 3145736 | tf_op jit(solution)/shard_map/ppermute | solution.py:363
  71.1 0.0 all-to-all-done
  71.1 9.3 %early_hidden.1.early_ref = bf16[768,768]{1,0:T(8,128)(2,1)} custom-call(s32[2]{0:T(128)S(1)} %copy-done.2, bf16[768,2048]{1,0:T(8,128)(2,1)} %bitcast.5.rows_ref, bf16[2048,256]{1,0:T(8,128)(2,1)S(1)} %bitcast.13, bf16[2048,256]{1,0:T(8,128)(2,1)S(1)} %collective-permute-done.gb, bf16[2048,256]{1,0:T(8,128)(2,1)S(1)} %collective-permute-done.1.g1, ...), custom_call_target="tpu_custom_call" | custom-call | tf_op jit(solution)/shard_map/early_hidden/pallas_call | solution.py:174
  80.5 0.0 copy-start.1
  80.5 0.0 collective-permute-done.7.ga
  80.5 4.9 %middle_hidden.1.middle_ref = bf16[768,256]{1,0:T(8,128)(2,1)S(1)} custom-call(s32[2]{0:T(128)S(1)} %copy-done.2, bf16[768,2048]{1,0:T(8,128)(2,1)} %bitcast.5.rows_ref, bf16[2048,256]{1,0:T(8,128)(2,1)} %collective-permute-done.7.ga, bf16[2048,256]{1,0:T(8,128)(2,1)} %collective-permute-done.6.gb, bf16[2048,256]{1,0:T(8,128)(2,1)} %collective-permute-done.9.ua, ...), custom_call_target="tpu_custom_call" | custom-call | tf_op jit(solution)/shard_map/middle_hidden/pallas_call | solution.py:193
  85.4 0.0 collective-permute-done.10.d0b
  85.4 0.0 collective-permute-done.14.d3a
  85.4 7.1 %late_outputs.1 = bf16[32,4,24,512]{3,2,1,0:T(8,128)(2,1)} custom-call(s32[2]{0:T(128)S(1)} %copy-done.2, bf16[768,768]{1,0:T(8,128)(2,1)} %early_hidden.1.early_ref, bf16[768,256]{1,0:T(8,128)(2,1)S(1)} %middle_hidden.1.middle_ref, bf16[256,2048]{1,0:T(8,128)(2,1)S(1)} %bitcast.16, bf16[256,2048]{1,0:T(8,128)(2,1)} %collective-permute-done.10.d0b, ...), custom_call_target="tpu_custom_call" | custom-call | tf_op jit(solution)/shard_map/late_outputs/pallas_call | solution.py:249
  92.5 0.0 copy-start.4
  92.5 0.0 copy-start.5
  92.6 10.8 %all-to-all-start.1 = ((bf16[128,24,512]{2,1,0:T(8,128)(2,1)}), bf16[128,24,512]{2,1,0:T(8,128)(2,1)}, u32[]{:S(2)}, u32[]{:S(2)}) async-start(bf16[128,24,512]{2,1,0:T(8,128)(2,1)} %bitcast.18), calls=%async_computation.1 | async-start | bytes 6291456 | tf_op jit(solution)/shard_map/all_to_all | solution.py:386
  103.4 0.2 copy.9.ids_ref
  103.6 2.3 %columns.1.index_ref = s32[768,2]{1,0:T(8,128)S(1)} custom-call(s32[768,2]{1,0:T(8,128)S(1)} %copy.9.ids_ref), custom_call_target="tpu_custom_call" | custom-call | tf_op jit(solution)/shard_map/columns/pallas_call | solution.py:293
  105.9 0.2 copy.10.scores_ref
  106.1 38.2 %all-to-all-done.1 = bf16[128,24,512]{2,1,0:T(8,128)(2,1)} async-done(((bf16[128,24,512]{2,1,0:T(8,128)(2,1)}), bf16[128,24,512]{2,1,0:T(8,128)(2,1)}, u32[]{:S(2)}, u32[]{:S(2)}) %all-to-all-start.1) | async-done | bytes 3145760 | tf_op jit(solution)/shard_map/all_to_all | solution.py:386
  144.3 7.7 %combine.1 = (f32[768,512]{1,0:T(8,128)S(1)}, f32[1,768]{1,0:T(1,128)S(1)}) custom-call(s32[768,2]{1,0:T(8,128)S(1)} %columns.1.index_ref, f32[768,2]{1,0:T(8,128)S(1)} %copy.10.scores_ref, bf16[3072,512]{1,0:T(8,128)(2,1)} %bitcast.10.returned_ref), custom_call_target="tpu_custom_call" | custom-call | tf_op jit(solution)/shard_map/combine/pallas_call | solution.py:329
  152.0 0.7 collective-permute-start.15
  152.6 2.6 %collective-permute-start.16 = (f32[768]{0:T(1024)S(1)}, f32[768]{0:T(1024)S(1)}, u32[]{:S(2)}, u32[]{:S(2)}) collective-permute-start(f32[768]{0:T(1024)S(1)} %reduce), channel_id=1, source_target_pairs={{0,2},{1,3},{2,0},{3,1},{4,6},{5,7},{6,4},{7,5},{8,10},{9,11},{10,... | collective-permute-start | bytes 9224 | tf_op jit(solution)/shard_map/ppermute | solution.py:394
  155.2 0.7 collective-permute-start.17
  155.9 0.9 collective-permute-done.15
  156.9 0.9 collective-permute-done.16
  157.7 1.1 collective-permute-done.17
  158.9 1.1 multiply_convert_fusion
  (18 shorter events, 0.1 us)
Async XLA Ops:
  0.0 23.0 %collective-permute-start.1 = (bf16[2048,256]{1,0:T(8,128)(2,1)}, bf16[2048,256]{1,0:T(8,128)(2,1)S(1)}, u32[]{:S(2)}, u32[]{:S(2)}) collective-permute-start(bf16[2048,256]{1,0:T(8,128)(2,1)} %bitcast.11), channel_id=1, source_target_pairs={{0,1},{1,0},{2,5},{3,4},{4,3},{5,2},{6,7},{7,6},{8,9},{9,8},{10,13... | collective-permute-start | bytes 3145736 | tf_op jit(solution)/shard_map/ppermute | solution.py:363
  1.6 26.4 %collective-permute-start = (bf16[2048,256]{1,0:T(8,128)(2,1)}, bf16[2048,256]{1,0:T(8,128)(2,1)S(1)}, u32[]{:S(2)}, u32[]{:S(2)}) collective-permute-start(bf16[2048,256]{1,0:T(8,128)(2,1)} %bitcast.12), channel_id=1, source_target_pairs={{0,4},{1,5},{2,6},{3,7},{4,0},{5,1},{6,2},{7,3},{8,12},{9,13},{10,... | collective-permute-start | bytes 3145736 | tf_op jit(solution)/shard_map/ppermute | solution.py:363
  3.0 23.4 %collective-permute-start.4 = (bf16[2048,256]{1,0:T(8,128)(2,1)}, bf16[2048,256]{1,0:T(8,128)(2,1)}, u32[]{:S(2)}, u32[]{:S(2)}) collective-permute-start(bf16[2048,256]{1,0:T(8,128)(2,1)} %bitcast.19), channel_id=1, source_target_pairs={{0,1},{1,0},{2,5},{3,4},{4,3},{5,2},{6,7},{7,6},{8,9},{9,8},{10,13... | collective-permute-start | bytes 3145736 | tf_op jit(solution)/shard_map/ppermute | solution.py:363
  3.2 26.1 %collective-permute-start.3 = (bf16[2048,256]{1,0:T(8,128)(2,1)}, bf16[2048,256]{1,0:T(8,128)(2,1)}, u32[]{:S(2)}, u32[]{:S(2)}) collective-permute-start(bf16[2048,256]{1,0:T(8,128)(2,1)} %bitcast.20), channel_id=1, source_target_pairs={{0,4},{1,5},{2,6},{3,7},{4,0},{5,1},{6,2},{7,3},{8,12},{9,13},{10,... | collective-permute-start | bytes 3145736 | tf_op jit(solution)/shard_map/ppermute | solution.py:363
  3.4 44.5 %collective-permute-start.11 = (bf16[256,2048]{1,0:T(8,128)(2,1)}, bf16[256,2048]{1,0:T(8,128)(2,1)}, u32[]{:S(2)}, u32[]{:S(2)}) collective-permute-start(bf16[256,2048]{1,0:T(8,128)(2,1)} %bitcast.14), channel_id=1, source_target_pairs={{0,1},{1,0},{2,5},{3,4},{4,3},{5,2},{6,7},{7,6},{8,9},{9,8},{10,13... | collective-permute-start | bytes 3145736 | tf_op jit(solution)/shard_map/ppermute | solution.py:363
  13.8 57.3 %copy-start = (bf16[1,2048,256]{2,1,0:T(8,128)(2,1)S(1)}, bf16[1,2048,256]{2,1,0:T(8,128)(2,1)}, u32[]{:S(2)}) copy-start(bf16[1,2048,256]{2,1,0:T(8,128)(2,1)} %param.12) | copy-start | bytes 3145732
  13.8 57.3 %copy-start.2 = (s32[2]{0:T(128)S(1)}, s32[2]{0:T(128)}, u32[]{:S(2)}) copy-start(s32[2]{0:T(128)} %pad_add_fusion.where_ref.place_ref) | copy-start | bytes 28
  13.8 57.3 %all-to-all-start = ((bf16[32,24,2048]{2,1,0:T(8,128)(2,1)}), bf16[32,24,2048]{2,1,0:T(8,128)(2,1)}, u32[]{:S(2)}, u32[]{:S(2)}) async-start(bf16[32,24,2048]{2,1,0:T(8,128)(2,1)} %bitcast.17), calls=%async_computation | async-start | bytes 6291456 | tf_op jit(solution)/shard_map/all_to_all | solution.py:378
  23.0 26.5 %collective-permute-start.6 = (bf16[2048,256]{1,0:T(8,128)(2,1)S(1)}, bf16[2048,256]{1,0:T(8,128)(2,1)}, u32[]{:S(2)}, u32[]{:S(2)}) collective-permute-start(bf16[2048,256]{1,0:T(8,128)(2,1)S(1)} %collective-permute-done.1.g1), channel_id=1, source_target_pairs={{2,3},{3,2},{4,5},{5,4},{10,11},{11,10},{12,13},{13,12},{18,19},{1... | collective-permute-start | bytes 3145736 | tf_op jit(solution)/shard_map/ppermute | solution.py:363
  26.4 23.1 %collective-permute-start.8 = (bf16[2048,256]{1,0:T(8,128)(2,1)}, bf16[2048,256]{1,0:T(8,128)(2,1)}, u32[]{:S(2)}, u32[]{:S(2)}) collective-permute-start(bf16[2048,256]{1,0:T(8,128)(2,1)} %collective-permute-done.4.u1), channel_id=1, source_target_pairs={{2,3},{3,2},{4,5},{5,4},{10,11},{11,10},{12,13},{13,12},{18,19},{1... | collective-permute-start | bytes 3145736 | tf_op jit(solution)/shard_map/ppermute | solution.py:363
  28.0 31.8 %collective-permute-start.2 = (bf16[2048,256]{1,0:T(8,128)(2,1)S(1)}, bf16[2048,256]{1,0:T(8,128)(2,1)S(1)}, u32[]{:S(2)}, u32[]{:S(2)}) collective-permute-start(bf16[2048,256]{1,0:T(8,128)(2,1)S(1)} %collective-permute-done.1.g1), channel_id=1, source_target_pairs={{0,4},{1,5},{2,6},{3,7},{4,0},{5,1},{6,2},{7,3},{8,12},{9,13},{10,... | collective-permute-start | bytes 3145736 | tf_op jit(solution)/shard_map/ppermute | solution.py:363
  29.3 31.6 %collective-permute-start.5 = (bf16[2048,256]{1,0:T(8,128)(2,1)}, bf16[2048,256]{1,0:T(8,128)(2,1)}, u32[]{:S(2)}, u32[]{:S(2)}) collective-permute-start(bf16[2048,256]{1,0:T(8,128)(2,1)} %collective-permute-done.4.u1), channel_id=1, source_target_pairs={{0,4},{1,5},{2,6},{3,7},{4,0},{5,1},{6,2},{7,3},{8,12},{9,13},{10,... | collective-permute-start | bytes 3145736 | tf_op jit(solution)/shard_map/ppermute | solution.py:363
  47.8 13.6 %collective-permute-start.13 = (bf16[256,2048]{1,0:T(8,128)(2,1)}, bf16[256,2048]{1,0:T(8,128)(2,1)}, u32[]{:S(2)}, u32[]{:S(2)}) collective-permute-start(bf16[256,2048]{1,0:T(8,128)(2,1)} %collective-permute-done.11.d1), channel_id=1, source_target_pairs={{2,3},{3,2},{4,5},{5,4},{10,11},{11,10},{12,13},{13,12},{18,19},{1... | collective-permute-start | bytes 3145736 | tf_op jit(solution)/shard_map/ppermute | solution.py:363
  49.5 35.9 %collective-permute-start.10 = (bf16[256,2048]{1,0:T(8,128)(2,1)}, bf16[256,2048]{1,0:T(8,128)(2,1)}, u32[]{:S(2)}, u32[]{:S(2)}) collective-permute-start(bf16[256,2048]{1,0:T(8,128)(2,1)} %bitcast.15), channel_id=1, source_target_pairs={{0,4},{1,5},{2,6},{3,7},{4,0},{5,1},{6,2},{7,3},{8,12},{9,13},{10,... | collective-permute-start | bytes 3145736 | tf_op jit(solution)/shard_map/ppermute | solution.py:363
  49.5 31.0 %collective-permute-start.7 = (bf16[2048,256]{1,0:T(8,128)(2,1)}, bf16[2048,256]{1,0:T(8,128)(2,1)}, u32[]{:S(2)}, u32[]{:S(2)}) collective-permute-start(bf16[2048,256]{1,0:T(8,128)(2,1)} %collective-permute-done.6.gb), channel_id=1, source_target_pairs={{0,4},{1,5},{2,6},{3,7},{4,0},{5,1},{6,2},{7,3},{8,12},{9,13},{10,... | collective-permute-start | bytes 3145736 | tf_op jit(solution)/shard_map/ppermute | solution.py:363
  59.9 1.0 copy-start.3
  60.9 19.6 %collective-permute-start.9 = (bf16[2048,256]{1,0:T(8,128)(2,1)}, bf16[2048,256]{1,0:T(8,128)(2,1)}, u32[]{:S(2)}, u32[]{:S(2)}) collective-permute-start(bf16[2048,256]{1,0:T(8,128)(2,1)} %collective-permute-done.8.ub), channel_id=1, source_target_pairs={{0,4},{1,5},{2,6},{3,7},{4,0},{5,1},{6,2},{7,3},{8,12},{9,13},{10,... | collective-permute-start | bytes 3145736 | tf_op jit(solution)/shard_map/ppermute | solution.py:363
  60.9 24.5 %collective-permute-start.12 = (bf16[256,2048]{1,0:T(8,128)(2,1)}, bf16[256,2048]{1,0:T(8,128)(2,1)}, u32[]{:S(2)}, u32[]{:S(2)}) collective-permute-start(bf16[256,2048]{1,0:T(8,128)(2,1)} %collective-permute-done.11.d1), channel_id=1, source_target_pairs={{0,4},{1,5},{2,6},{3,7},{4,0},{5,1},{6,2},{7,3},{8,12},{9,13},{10,... | collective-permute-start | bytes 3145736 | tf_op jit(solution)/shard_map/ppermute | solution.py:363
  61.4 24.0 %collective-permute-start.14 = (bf16[256,2048]{1,0:T(8,128)(2,1)}, bf16[256,2048]{1,0:T(8,128)(2,1)}, u32[]{:S(2)}, u32[]{:S(2)}) collective-permute-start(bf16[256,2048]{1,0:T(8,128)(2,1)} %collective-permute-done.13.d3b), channel_id=1, source_target_pairs={{0,4},{1,5},{2,6},{3,7},{4,0},{5,1},{6,2},{7,3},{8,12},{9,13},{10,... | collective-permute-start | bytes 3145736 | tf_op jit(solution)/shard_map/ppermute | solution.py:363
  80.5 4.9 %copy-start.1 = (bf16[1,256,2048]{2,1,0:T(8,128)(2,1)S(1)}, bf16[1,256,2048]{2,1,0:T(8,128)(2,1)}, u32[]{:S(2)}) copy-start(bf16[1,256,2048]{2,1,0:T(8,128)(2,1)} %param.14) | copy-start | bytes 3145732
  92.5 10.8 %copy-start.4 = (s32[768,2]{0,1:T(2,128)S(1)}, s32[768,2]{0,1:T(2,128)}, u32[]{:S(2)}) copy-start(s32[768,2]{0,1:T(2,128)} %param.10) | copy-start | bytes 18436
  92.5 13.3 %copy-start.5 = (f32[768,2]{0,1:T(2,128)S(1)}, f32[768,2]{0,1:T(2,128)}, u32[]{:S(2)}) copy-start(f32[768,2]{0,1:T(2,128)} %param.11) | copy-start | bytes 18436
  92.6 51.7 %all-to-all-start.1 = ((bf16[128,24,512]{2,1,0:T(8,128)(2,1)}), bf16[128,24,512]{2,1,0:T(8,128)(2,1)}, u32[]{:S(2)}, u32[]{:S(2)}) async-start(bf16[128,24,512]{2,1,0:T(8,128)(2,1)} %bitcast.18), calls=%async_computation.1 | async-start | bytes 6291456 | tf_op jit(solution)/shard_map/all_to_all | solution.py:386
  144.3 14.6 %copy-start.6 = (f32[512]{0:T(512)S(1)}, f32[512]{0:T(512)}, u32[]{:S(2)}) copy-start(f32[512]{0:T(512)} %param.15) | copy-start | bytes 6148
  152.0 4.9 %collective-permute-start.15 = (f32[768]{0:T(1024)S(1)}, f32[768]{0:T(1024)S(1)}, u32[]{:S(2)}, u32[]{:S(2)}) collective-permute-start(f32[768]{0:T(1024)S(1)} %reduce), channel_id=1, source_target_pairs={{0,1},{1,2},{2,3},{3,0},{4,5},{5,6},{6,7},{7,4},{8,9},{9,10},{10,1... | collective-permute-start | bytes 9224 | tf_op jit(solution)/shard_map/ppermute | solution.py:394
  152.6 5.1 %collective-permute-start.16 = (f32[768]{0:T(1024)S(1)}, f32[768]{0:T(1024)S(1)}, u32[]{:S(2)}, u32[]{:S(2)}) collective-permute-start(f32[768]{0:T(1024)S(1)} %reduce), channel_id=1, source_target_pairs={{0,2},{1,3},{2,0},{3,1},{4,6},{5,7},{6,4},{7,5},{8,10},{9,11},{10,... | collective-permute-start | bytes 9224 | tf_op jit(solution)/shard_map/ppermute | solution.py:394
  155.2 3.6 %collective-permute-start.17 = (f32[768]{0:T(1024)S(1)}, f32[768]{0:T(1024)S(1)}, u32[]{:S(2)}, u32[]{:S(2)}) collective-permute-start(f32[768]{0:T(1024)S(1)} %reduce), channel_id=1, source_target_pairs={{0,3},{1,0},{2,1},{3,2},{4,7},{5,4},{6,5},{7,6},{8,11},{9,8},{10,9... | collective-permute-start | bytes 9224 | tf_op jit(solution)/shard_map/ppermute | solution.py:394

commit v3 on v2

--- a/solution.py
+++ b/solution.py
@@ -37,17 +37,20 @@
     return first, second, swap
 
 
-def dispatch_kernel(where_ref, ids_ref, gain_ref, tokens_ref, out_ref, raw, normed, pick, sems, *, rows, chunks):
+def dispatch_kernel(ids_ref, gain_ref, tokens_ref, out_ref, raw, pick, sems, *, rows, chunks):
     step = pl.program_id(0)
     count, _ = raw.shape
     part = count // chunks
 
+    def load(i):
+        return pltpu.make_async_copy(
+            tokens_ref.at[pl.ds(i * part, part)], raw.at[pl.ds(i * part, part)], sems.at[i]
+        )
+
     @pl.when(step == 0)
     def _():
         for i in range(chunks):
-            pltpu.make_async_copy(
-                tokens_ref.at[pl.ds(i * part, part)], raw.at[pl.ds(i * part, part)], sems.at[i]
-            ).start()
+            load(i).start()
         experts = 32
         first = ids_ref[0:1, :]
         second = ids_ref[1:2, :]
@@ -63,7 +66,7 @@
         )
         slot_first = jnp.sum(jnp.where(named_first, ranks, 0.0), axis=0, keepdims=True).astype(jnp.int32)
         slot_second = jnp.sum(jnp.where(named_second, ranks, 0.0), axis=0, keepdims=True).astype(jnp.int32)
-        mine = where_ref[0]
+        mine = lax.axis_index("tp")
 
         def row_of(ids, slot):
             ep, tp, row = place_of(ids, slot)
@@ -73,54 +76,36 @@
         row_second = row_of(second, slot_second)
         index = lax.broadcasted_iota(jnp.int32, (count, count), 0)
         pick[...] = jnp.where((index == row_first) | (index == row_second), 1.0, 0.0).astype(jnp.bfloat16)
-        gain = gain_ref[...]
         for i in range(chunks):
-            pltpu.make_async_copy(
-                tokens_ref.at[pl.ds(i * part, part)], raw.at[pl.ds(i * part, part)], sems.at[i]
-            ).wait()
-            value = raw[pl.ds(i * part, part), :].astype(jnp.float32)
-            mean = jnp.mean(value * value, axis=1, keepdims=True)
-            normed[pl.ds(i * part, part), :] = (value * lax.rsqrt(mean + epsilon) * gain).astype(jnp.bfloat16)
+            load(i).wait()
 
     block = out_ref.shape[0]
-    out_ref[...] = jnp.dot(
-        pick[pl.ds(step * block, block), :], normed[...], preferred_element_type=jnp.float32
-    ).astype(jnp.bfloat16)
-
-
-def dispatch_buffer(place, ids_rows, gain, tokens, rows):
+    value = jnp.dot(pick[pl.ds(step * block, block), :], raw[...], preferred_element_type=jnp.float32)
+    mean = jnp.mean(value * value, axis=1, keepdims=True)
+    out_ref[...] = (value * lax.rsqrt(mean + epsilon) * gain_ref[...]).astype(jnp.bfloat16)
+
+
+def dispatch_buffer(ids_rows, gain, tokens, rows):
     count, width = tokens.shape
-    steps, chunks = 4, 4
+    steps, chunks = 6, 2
     return pl.pallas_call(
         functools.partial(dispatch_kernel, rows=rows, chunks=chunks),
-        grid_spec=pltpu.PrefetchScalarGridSpec(
-            num_scalar_prefetch=1,
-            grid=(steps,),
-            in_specs=[
-                pl.BlockSpec((2, count), lambda i, p: (0, 0)),
-                pl.BlockSpec((1, width), lambda i, p: (0, 0)),
-                pl.BlockSpec(memory_space=pltpu.HBM),
-            ],
-            out_specs=pl.BlockSpec((count // steps, width), lambda i, p: (i, 0)),
-            scratch_shapes=[
-                pltpu.VMEM((count, width), jnp.bfloat16),
-                pltpu.VMEM((count, width), jnp.bfloat16),
-                pltpu.VMEM((count, count), jnp.bfloat16),
-                pltpu.SemaphoreType.DMA((chunks,)),
-            ],
-        ),
+        grid=(steps,),
+        in_specs=[
+            pl.BlockSpec((2, count), lambda i: (0, 0)),
+            pl.BlockSpec((1, width), lambda i: (0, 0)),
+            pl.BlockSpec(memory_space=pltpu.HBM),
+        ],
+        out_specs=pl.BlockSpec((count // steps, width), lambda i: (i, 0)),
+        scratch_shapes=[
+            pltpu.VMEM((count, width), jnp.bfloat16),
+            pltpu.VMEM((count, count), jnp.bfloat16),
+            pltpu.SemaphoreType.DMA((chunks,)),
+        ],
         out_shape=pltpu.HBM((count, width), jnp.bfloat16),
-        compiler_params=pltpu.CompilerParams(
-            dimension_semantics=("arbitrary",), vmem_limit_bytes=58 * MIB
-        ),
+        compiler_params=pltpu.CompilerParams(dimension_semantics=("arbitrary",), vmem_limit_bytes=58 * MIB),
         name="dispatch_buffer",
-    )(place, ids_rows, gain, tokens)
-
-
-def hidden_of(rows, gate, up):
-    gate_acts = jnp.dot(rows, gate, preferred_element_type=jnp.float32)
-    up_acts = jnp.dot(rows, up, preferred_element_type=jnp.float32)
-    return gate_acts / (1.0 + jnp.exp(-gate_acts)) * up_acts
+    )(ids_rows, gain, tokens)
 
 
 def start_one(flag, a, b, dst, sem):
@@ -133,34 +118,45 @@
         pltpu.make_async_copy(b, dst, sem).start()
 
 
-def early_kernel(place_ref, rows_ref, ga, gb, g1, g2, ua, ub, u1, u2, out_ref, rows, gate, up, sems):
+def hidden_kernel(place_ref, rows_ref, *refs, pieces):
+    gates, ups = refs[:6], refs[6:12]
+    out_ref, rows, weights, sems = refs[12:]
     flag = place_ref[1]
-    start_one(flag, ga, gb, gate.at[0], sems.at[0])
-    start_one(flag, ua, ub, up.at[0], sems.at[1])
-    load = pltpu.make_async_copy(rows_ref, rows, sems.at[6])
-    load.start()
-    for i, (g, u) in enumerate(((g1, u1), (g2, u2))):
-        pltpu.make_async_copy(g, gate.at[i + 1], sems.at[2 * i + 2]).start()
-        pltpu.make_async_copy(u, up.at[i + 1], sems.at[2 * i + 3]).start()
-    load.wait()
-    part = gate.shape[2]
-    for i in range(3):
-        pltpu.make_async_copy(g1, gate.at[i], sems.at[2 * i]).wait()
-        pltpu.make_async_copy(u1, up.at[i], sems.at[2 * i + 1]).wait()
-        value = hidden_of(rows[...], gate[i], up[i])
-        out_ref[:, i * part : (i + 1) * part] = value.astype(jnp.bfloat16)
-
-
-def middle_kernel(place_ref, rows_ref, ga, gb, ua, ub, out_ref, rows, gate, up, sems):
-    flag = place_ref[1]
-    load = pltpu.make_async_copy(rows_ref, rows, sems.at[0])
-    load.start()
-    start_one(flag, ga, gb, gate, sems.at[1])
-    start_one(flag, ua, ub, up, sems.at[2])
-    load.wait()
-    pltpu.make_async_copy(ga, gate, sems.at[1]).wait()
-    pltpu.make_async_copy(ua, up, sems.at[2]).wait()
-    out_ref[...] = hidden_of(rows[...], gate[...], up[...]).astype(jnp.bfloat16)
+    count = rows.shape[0]
+    part = gates[0].shape[1]
+    size = count // pieces
+
+    def start(refs, i, lo, sem):
+        dst = weights.at[i, :, pl.ds(lo, part)]
+        if i == 0 or i == 3:
+            at = 0 if i == 0 else 4
+            start_one(flag, refs[at], refs[at + 1], dst, sem)
+        else:
+            pltpu.make_async_copy(refs[i + 1], dst, sem).start()
+
+    def load(p):
+        return pltpu.make_async_copy(
+            rows_ref.at[pl.ds(p * size, size)], rows.at[pl.ds(p * size, size)], sems.at[8 + p]
+        )
+
+    for i in range(4):
+        start(gates, i, 0, sems.at[2 * i])
+        start(ups, i, part, sems.at[2 * i + 1])
+        if i == 0:
+            for p in range(pieces):
+                load(p).start()
+    for i in range(4):
+        pltpu.make_async_copy(gates[2], weights.at[i, :, pl.ds(0, part)], sems.at[2 * i]).wait()
+        pltpu.make_async_copy(ups[2], weights.at[i, :, pl.ds(part, part)], sems.at[2 * i + 1]).wait()
+        for p in range(pieces):
+            if i == 0:
+                load(p).wait()
+            acts = jnp.dot(
+                rows[p * size : (p + 1) * size, :], weights[i], preferred_element_type=jnp.float32
+            )
+            gate_acts = acts[:, :part]
+            value = gate_acts / (1.0 + jnp.exp(-gate_acts)) * acts[:, part:]
+            out_ref[p * size : (p + 1) * size, i * part : (i + 1) * part] = value.astype(jnp.bfloat16)
 
 
 HBM = pl.BlockSpec(memory_space=pltpu.HBM)
@@ -168,52 +164,31 @@
 SMEM = pl.BlockSpec(memory_space=pltpu.SMEM)
 
 
-def early_hidden(place, rows, gates, ups):
+def hidden_units(place, rows, gates, ups):
     count, width = rows.shape
     part = gates[0].shape[1]
-    return pl.pallas_call(
-        early_kernel,
-        in_specs=[SMEM, ANY] + [HBM] * 8,
-        out_specs=pl.BlockSpec((count, 3 * part), lambda: (0, 0)),
+    pieces = 2
+    return pl.pallas_call(
+        functools.partial(hidden_kernel, pieces=pieces),
+        in_specs=[SMEM, ANY] + [HBM] * 12,
+        out_specs=pl.BlockSpec((count, 4 * part), lambda: (0, 0)),
         scratch_shapes=[
             pltpu.VMEM((count, width), jnp.bfloat16),
-            pltpu.VMEM((3, width, part), jnp.bfloat16),
-            pltpu.VMEM((3, width, part), jnp.bfloat16),
-            pltpu.SemaphoreType.DMA((7,)),
-        ],
-        out_shape=jax.ShapeDtypeStruct((count, 3 * part), jnp.bfloat16),
+            pltpu.VMEM((4, width, 2 * part), jnp.bfloat16),
+            pltpu.SemaphoreType.DMA((8 + pieces,)),
+        ],
+        out_shape=jax.ShapeDtypeStruct((count, 4 * part), jnp.bfloat16),
         compiler_params=pltpu.CompilerParams(vmem_limit_bytes=50 * MIB),
-        name="early_hidden",
+        name="hidden_units",
     )(place, rows, *gates, *ups)
 
 
-def middle_hidden(place, rows, gates, ups):
-    count, width = rows.shape
-    part = gates[0].shape[1]
-    return pl.pallas_call(
-        middle_kernel,
-        in_specs=[SMEM, ANY] + [HBM] * 4,
-        out_specs=pl.BlockSpec((count, part), lambda: (0, 0)),
-        scratch_shapes=[
-            pltpu.VMEM((count, width), jnp.bfloat16),
-            pltpu.VMEM((width, part), jnp.bfloat16),
-            pltpu.VMEM((width, part), jnp.bfloat16),
-            pltpu.SemaphoreType.DMA((3,)),
-        ],
-        out_shape=jax.ShapeDtypeStruct((count, part), jnp.bfloat16),
-        compiler_params=pltpu.CompilerParams(vmem_limit_bytes=50 * MIB),
-        name="middle_hidden",
-    )(place, rows, *gates, *ups)
-
-
-def late_kernel(place_ref, early_ref, middle_ref, d0a, d0b, d1, d2, d3a, d3b, out_ref, down, hidden, out, sems, out_sems):
+def late_kernel(place_ref, hidden_ref, d0a, d0b, d1, d2, d3a, d3b, out_ref, down, hidden, out, sems, out_sems):
     flag = place_ref[1]
     senders, pieces, slots, piece = out_ref.shape
     part = d1.shape[0]
-    first = pltpu.make_async_copy(early_ref, hidden.at[:, pl.ds(0, 3 * part)], sems.at[4 * pieces])
-    second = pltpu.make_async_copy(middle_ref, hidden.at[:, pl.ds(3 * part, part)], sems.at[4 * pieces + 1])
-    first.start()
-    second.start()
+    load = pltpu.make_async_copy(hidden_ref, hidden, sems.at[4 * pieces])
+    load.start()
 
     def target(i, f):
         return down.at[pl.ds(i * part, part), pl.ds(f * piece, piece)]
@@ -226,8 +201,7 @@
         pltpu.make_async_copy(source(d1, f), target(1, f), sems.at[4 * f + 1]).start()
         pltpu.make_async_copy(source(d2, f), target(2, f), sems.at[4 * f + 2]).start()
         start_one(flag, source(d3a, f), source(d3b, f), target(3, f), sems.at[4 * f + 3])
-    first.wait()
-    second.wait()
+    load.wait()
     for f in range(pieces):
         for i in range(4):
             pltpu.make_async_copy(source(d1, f), target(i, f), sems.at[4 * f + i]).wait()
@@ -240,27 +214,27 @@
         pltpu.make_async_copy(out.at[f], out_ref.at[:, f], out_sems.at[f]).wait()
 
 
-def late_outputs(place, early, middle, downs, senders, pieces):
-    count = early.shape[0]
+def late_outputs(place, hidden, downs, senders, pieces):
+    count = hidden.shape[0]
     part, width = downs[0].shape
     slots = count // senders
     piece = width // pieces
     shape = (senders, pieces, slots, piece)
     return pl.pallas_call(
         late_kernel,
-        in_specs=[SMEM, ANY, ANY] + [HBM] * 6,
+        in_specs=[SMEM, ANY] + [HBM] * 6,
         out_specs=HBM,
         scratch_shapes=[
             pltpu.VMEM((4 * part, width), jnp.bfloat16),
             pltpu.VMEM((count, 4 * part), jnp.bfloat16),
             pltpu.VMEM((pieces, senders, slots, piece), jnp.bfloat16),
-            pltpu.SemaphoreType.DMA((4 * pieces + 2,)),
+            pltpu.SemaphoreType.DMA((4 * pieces + 1,)),
             pltpu.SemaphoreType.DMA((pieces,)),
         ],
         out_shape=pltpu.HBM(shape, jnp.bfloat16),
         compiler_params=pltpu.CompilerParams(vmem_limit_bytes=50 * MIB),
         name="late_outputs",
-    )(place, early, middle, *downs)
+    )(place, hidden, *downs)
 
 
 def columns_kernel(ids_ref, out_ref, *, cuts, count_tp):
@@ -374,14 +348,15 @@
     up = spread(up_weight[0])
     down = spread(down_weight[0])
 
-    buffer = dispatch_buffer(place, route_ids.T, in_gain[None, :], tokens, rows)
+    buffer = dispatch_buffer(route_ids.T, in_gain[None, :], tokens, rows)
     received = lax.all_to_all(
         buffer.reshape(count_ep, rows, full_width), "ep", split_axis=0, concat_axis=0, tiled=True
     ).reshape(count_ep * rows, full_width)
-    early = early_hidden(place, received, (*gate[0], gate[1], gate[2]), (*up[0], up[1], up[2]))
-    middle = middle_hidden(place, received, gate[3], up[3])
+    hidden = hidden_units(
+        place, received, (*gate[0], gate[1], gate[2], *gate[3]), (*up[0], up[1], up[2], *up[3])
+    )
     outputs = late_outputs(
-        place, early, middle, (*down[0], down[1], down[2], *down[3]), count_ep, count_tp
+        place, hidden, (*down[0], down[1], down[2], *down[3]), count_ep, count_tp
     )
     returned = lax.all_to_all(
         outputs.reshape(count_ep * count_tp, rows, part_width), AXES, split_axis=0, concat_axis=0, tiled=True

time: 160 us -> 158 us (0.988)
  Pallas kernels: 39.4 us -> 36.3 us
  waiting for transfers between devices: 61.3 us -> 63.7 us
    pallas_call x3 -> x2, Pallas kernels: 21.3 us -> 18.3 us  [the longest x1 11.1 us: hidden_units(): pl.pallas_call(functools.partial(hidden_kernel, pieces=pieces), in_specs=...]
    ppermute x3, waiting for transfers between devices: 2.91 us -> 4.79 us  [per_device(): lax.ppermute(squares, 'tp', [(i, (i + shift) % count_tp) for i in range(c...]
  transfers between devices with their start and end apart: 20 -> 20, of which waited for: 6 -> 6; matrix products, arithmetic and copies ran while one was open for 1% -> 0% of each run, Pallas kernels for 15% -> 14%
where the time goes in v3:
time: 158 us
  waiting for transfers between devices  63.7 us (40%)
  starting transfers between devices  54.9 us (35%)
  Pallas kernels  36.3 us (23%)
    all_to_all x1, waiting for transfers between devices, per_device(): lax.all_to_all(outputs.reshape(count_ep * count_tp, rows, part_width), AX...  38.2 us
    ppermute x15, starting transfers between devices, send(): return lax.ppermute(weight, AXES, pairs)  30.9 us
    ppermute x15, waiting for transfers between devices, send(): return lax.ppermute(weight, AXES, pairs)  20.7 us
    pallas_call x1, Pallas kernels, hidden_units(): pl.pallas_call(functools.partial(hidden_kernel, pieces=pieces), in_specs=...  11.1 us
    all_to_all x1, starting transfers between devices, per_device(): lax.all_to_all(outputs.reshape(count_ep * count_tp, rows, part_width), AX...  10.8 us
    all_to_all x1, starting transfers between devices, per_device(): lax.all_to_all(buffer.reshape(count_ep, rows, full_width), 'ep', split_ax...  10.5 us
    pallas_call x1, Pallas kernels, dispatch_buffer(): pl.pallas_call(functools.partial(dispatch_kernel, rows=rows, chunks=chunk...  8.03 us
    pallas_call x1, Pallas kernels, combine(): pl.pallas_call(combine_kernel, grid=(steps,), in_specs=[pl.BlockSpec((blo...  7.68 us
  transfers between devices with their start and end apart: 20, of which 6 were waited for; matrix products, arithmetic and copies ran while one was open for 0% of the time, Pallas kernels for 14%

profile of v3, /device:TPU:0, one launch (start us, length us, event | category | flops | bytes accessed | tf_op | source)
XLA Modules:
  0.0 157.7 jit_solution(11893490858990484177)
XLA Ops:
  0.0 1.6 %collective-permute-start.1 = (bf16[2048,256]{1,0:T(8,128)(2,1)}, bf16[2048,256]{1,0:T(8,128)(2,1)S(1)}, u32[]{:S(2)}, u32[]{:S(2)}) collective-permute-start(bf16[2048,256]{1,0:T(8,128)(2,1)} %bitcast.11), channel_id=1, source_target_pairs={{0,1},{1,0},{2,5},{3,4},{4,3},{5,2},{6,7},{7,6},{8,9},{9,8},{10,13... | collective-permute-start | bytes 3145736 | tf_op jit(solution)/shard_map/ppermute | solution.py:337
  1.6 0.4 collective-permute-start.6
  2.0 1.0 collective-permute-start
  3.0 0.0 collective-permute-start.5
  3.0 1.1 collective-permute-start.11
  4.1 8.0 %dispatch_buffer.1 = bf16[768,2048]{1,0:T(8,128)(2,1)} custom-call(s32[2,768]{1,0:T(2,128)} %bitcast.22, f32[1,2048]{1,0:T(1,128)} %bitcast.23, bf16[768,2048]{1,0:T(8,128)(2,1)} %tokens_ref.1), custom_call_target="tpu_custom_call" | custom-call | tf_op jit(solution)/shard_map/dispatch_buffer/pallas_call | solution.py:91
  12.2 0.0 copy-start
  12.2 10.5 %all-to-all-start = ((bf16[32,24,2048]{2,1,0:T(8,128)(2,1)}), bf16[32,24,2048]{2,1,0:T(8,128)(2,1)}, u32[]{:S(2)}, u32[]{:S(2)}) async-start(bf16[32,24,2048]{2,1,0:T(8,128)(2,1)} %bitcast.17), calls=%async_computation | async-start | bytes 6291456 | tf_op jit(solution)/shard_map/all_to_all | solution.py:352
  22.7 0.0 collective-permute-done.1.refs_2_
  22.7 1.6 %collective-permute-start.3 = (bf16[2048,256]{1,0:T(8,128)(2,1)S(1)}, bf16[2048,256]{1,0:T(8,128)(2,1)}, u32[]{:S(2)}, u32[]{:S(2)}) collective-permute-start(bf16[2048,256]{1,0:T(8,128)(2,1)S(1)} %collective-permute-done.1.refs_2_), channel_id=1, source_target_pairs={{2,3},{3,2},{4,5},{5,4},{10,11},{11,10},{12,13},{13,12},{18,19},{1... | collective-permute-start | bytes 3145736 | tf_op jit(solution)/shard_map/ppermute | solution.py:337
  24.4 2.0 %collective-permute-done.6.refs_8_ = bf16[2048,256]{1,0:T(8,128)(2,1)} collective-permute-done((bf16[2048,256]{1,0:T(8,128)(2,1)}, bf16[2048,256]{1,0:T(8,128)(2,1)}, u32[]{:S(2)}, u32[]{:S(2)}) %collective-permute-start.6) | collective-permute-done | bytes 1048608 | tf_op jit(solution)/shard_map/ppermute | solution.py:337
  26.4 1.6 %collective-permute-start.8 = (bf16[2048,256]{1,0:T(8,128)(2,1)}, bf16[2048,256]{1,0:T(8,128)(2,1)}, u32[]{:S(2)}, u32[]{:S(2)}) collective-permute-start(bf16[2048,256]{1,0:T(8,128)(2,1)} %collective-permute-done.6.refs_8_), channel_id=1, source_target_pairs={{2,3},{3,2},{4,5},{5,4},{10,11},{11,10},{12,13},{13,12},{18,19},{1... | collective-permute-start | bytes 3145736 | tf_op jit(solution)/shard_map/ppermute | solution.py:337
  28.0 0.0 collective-permute-done.refs_1_
  28.0 1.3 collective-permute-start.2
  29.3 0.1 collective-permute-start.7
  29.4 18.6 %collective-permute-done.11.d1 = bf16[256,2048]{1,0:T(8,128)(2,1)} collective-permute-done((bf16[256,2048]{1,0:T(8,128)(2,1)}, bf16[256,2048]{1,0:T(8,128)(2,1)}, u32[]{:S(2)}, u32[]{:S(2)}) %collective-permute-start.11) | collective-permute-done | bytes 1048608 | tf_op jit(solution)/shard_map/ppermute | solution.py:337
  48.1 1.7 %collective-permute-start.13 = (bf16[256,2048]{1,0:T(8,128)(2,1)}, bf16[256,2048]{1,0:T(8,128)(2,1)}, u32[]{:S(2)}, u32[]{:S(2)}) collective-permute-start(bf16[256,2048]{1,0:T(8,128)(2,1)} %collective-permute-done.11.d1), channel_id=1, source_target_pairs={{2,3},{3,2},{4,5},{5,4},{10,11},{11,10},{12,13},{13,12},{18,19},{1... | collective-permute-start | bytes 3145736 | tf_op jit(solution)/shard_map/ppermute | solution.py:337
  49.8 0.0 collective-permute-done.3.refs_5_
  49.8 0.0 collective-permute-start.4
  49.8 0.0 collective-permute-done.8.refs_11_
  49.8 10.1 %collective-permute-start.9 = (bf16[2048,256]{1,0:T(8,128)(2,1)}, bf16[2048,256]{1,0:T(8,128)(2,1)}, u32[]{:S(2)}, u32[]{:S(2)}) collective-permute-start(bf16[2048,256]{1,0:T(8,128)(2,1)} %collective-permute-done.8.refs_11_), channel_id=1, source_target_pairs={{0,4},{1,5},{2,6},{3,7},{4,0},{5,1},{6,2},{7,3},{8,12},{9,13},{10,... | collective-permute-start | bytes 3145736 | tf_op jit(solution)/shard_map/ppermute | solution.py:337
  59.9 1.0 copy-done.2
  60.9 0.0 collective-permute-start.10
  60.9 0.0 collective-permute-done.7.refs_9_
  60.9 0.5 collective-permute-start.12
  61.4 9.7 %collective-permute-start.14 = (bf16[256,2048]{1,0:T(8,128)(2,1)}, bf16[256,2048]{1,0:T(8,128)(2,1)}, u32[]{:S(2)}, u32[]{:S(2)}) collective-permute-start(bf16[256,2048]{1,0:T(8,128)(2,1)} %collective-permute-done.13.d3b), channel_id=1, source_target_pairs={{0,4},{1,5},{2,6},{3,7},{4,0},{5,1},{6,2},{7,3},{8,12},{9,13},{10,... | collective-permute-start | bytes 3145736 | tf_op jit(solution)/shard_map/ppermute | solution.py:337
  71.1 0.1 pad_add_fusion.place_ref
  71.2 0.0 all-to-all-done
  71.2 0.0 collective-permute-done.4.refs_4_
  71.2 0.0 copy-start.1
  71.2 11.1 %hidden_units.1.hidden_ref = bf16[768,1024]{1,0:T(8,128)(2,1)} custom-call(s32[2]{0:T(128)S(1)} %pad_add_fusion.place_ref, bf16[768,2048]{1,0:T(8,128)(2,1)} %bitcast.5.rows_ref, bf16[2048,256]{1,0:T(8,128)(2,1)S(1)} %bitcast.13, bf16[2048,256]{1,0:T(8,128)(2,1)S(1)} %collective-permute-done.refs_1_, bf16[2048,256]{1,0:T(8,128)(2,1)S(1)} %collective-permute-done.1.refs_2_, ...), custom_call_target="tpu_custom_call" | custom-call | tf_op jit(solution)/shard_map/hidden_units/pallas_call | solution.py:171
  82.3 0.0 collective-permute-done.12.d2
  82.3 7.2 %late_outputs.1 = bf16[32,4,24,512]{3,2,1,0:T(8,128)(2,1)} custom-call(s32[2]{0:T(128)S(1)} %pad_add_fusion.place_ref, bf16[768,1024]{1,0:T(8,128)(2,1)} %hidden_units.1.hidden_ref, bf16[256,2048]{1,0:T(8,128)(2,1)S(1)} %bitcast.16, bf16[256,2048]{1,0:T(8,128)(2,1)} %collective-permute-done.10.d0b, bf16[256,2048]{1,0:T(8,128)(2,1)} %collective-permute-done.11.d1, ...), custom_call_target="tpu_custom_call" | custom-call | tf_op jit(solution)/shard_map/late_outputs/pallas_call | solution.py:223
  89.6 0.0 copy-start.3
  89.6 0.0 copy-start.4
  89.6 10.8 %all-to-all-start.1 = ((bf16[128,24,512]{2,1,0:T(8,128)(2,1)}), bf16[128,24,512]{2,1,0:T(8,128)(2,1)}, u32[]{:S(2)}, u32[]{:S(2)}) async-start(bf16[128,24,512]{2,1,0:T(8,128)(2,1)} %bitcast.18), calls=%async_computation.1 | async-start | bytes 6291456 | tf_op jit(solution)/shard_map/all_to_all | solution.py:361
  100.4 0.2 copy.9.ids_ref
  100.6 2.3 %columns.1.index_ref = s32[768,2]{1,0:T(8,128)S(1)} custom-call(s32[768,2]{1,0:T(8,128)S(1)} %copy.9.ids_ref), custom_call_target="tpu_custom_call" | custom-call | tf_op jit(solution)/shard_map/columns/pallas_call | solution.py:267
  102.9 0.2 copy.10.scores_ref
  103.1 38.2 %all-to-all-done.1 = bf16[128,24,512]{2,1,0:T(8,128)(2,1)} async-done(((bf16[128,24,512]{2,1,0:T(8,128)(2,1)}), bf16[128,24,512]{2,1,0:T(8,128)(2,1)}, u32[]{:S(2)}, u32[]{:S(2)}) %all-to-all-start.1) | async-done | bytes 3145760 | tf_op jit(solution)/shard_map/all_to_all | solution.py:361
  141.3 7.7 %combine.1 = (f32[768,512]{1,0:T(8,128)S(1)}, f32[1,768]{1,0:T(1,128)S(1)}) custom-call(s32[768,2]{1,0:T(8,128)S(1)} %columns.1.index_ref, f32[768,2]{1,0:T(8,128)S(1)} %copy.10.scores_ref, bf16[3072,512]{1,0:T(8,128)(2,1)} %bitcast.10.returned_ref), custom_call_target="tpu_custom_call" | custom-call | tf_op jit(solution)/shard_map/combine/pallas_call | solution.py:303
  149.0 1.8 %collective-permute-start.17 = (f32[768]{0:T(1024)S(1)}, f32[768]{0:T(1024)S(1)}, u32[]{:S(2)}, u32[]{:S(2)}) collective-permute-start(f32[768]{0:T(1024)S(1)} %reduce), channel_id=1, source_target_pairs={{0,3},{1,0},{2,1},{3,2},{4,7},{5,4},{6,5},{7,6},{8,11},{9,8},{10,9... | collective-permute-start | bytes 9224 | tf_op jit(solution)/shard_map/ppermute | solution.py:369
  150.8 0.9 collective-permute-start.16
  151.8 0.0 collective-permute-start.15
  151.8 0.9 collective-permute-done.17
  152.7 3.2 %collective-permute-done.16 = f32[768]{0:T(1024)S(1)} collective-permute-done((f32[768]{0:T(1024)S(1)}, f32[768]{0:T(1024)S(1)}, u32[]{:S(2)}, u32[]{:S(2)}) %collective-permute-start.16) | collective-permute-done | bytes 3104 | tf_op jit(solution)/shard_map/ppermute | solution.py:369
  155.9 0.6 collective-permute-done.15
  156.6 1.1 multiply_convert_fusion
  (15 shorter events, 0.1 us)
Async XLA Ops:
  0.0 22.7 %collective-permute-start.1 = (bf16[2048,256]{1,0:T(8,128)(2,1)}, bf16[2048,256]{1,0:T(8,128)(2,1)S(1)}, u32[]{:S(2)}, u32[]{:S(2)}) collective-permute-start(bf16[2048,256]{1,0:T(8,128)(2,1)} %bitcast.11), channel_id=1, source_target_pairs={{0,1},{1,0},{2,5},{3,4},{4,3},{5,2},{6,7},{7,6},{8,9},{9,8},{10,13... | collective-permute-start | bytes 3145736 | tf_op jit(solution)/shard_map/ppermute | solution.py:337
  1.6 24.7 %collective-permute-start.6 = (bf16[2048,256]{1,0:T(8,128)(2,1)}, bf16[2048,256]{1,0:T(8,128)(2,1)}, u32[]{:S(2)}, u32[]{:S(2)}) collective-permute-start(bf16[2048,256]{1,0:T(8,128)(2,1)} %bitcast.19), channel_id=1, source_target_pairs={{0,1},{1,0},{2,5},{3,4},{4,3},{5,2},{6,7},{7,6},{8,9},{9,8},{10,13... | collective-permute-start | bytes 3145736 | tf_op jit(solution)/shard_map/ppermute | solution.py:337
  2.0 26.0 %collective-permute-start = (bf16[2048,256]{1,0:T(8,128)(2,1)}, bf16[2048,256]{1,0:T(8,128)(2,1)S(1)}, u32[]{:S(2)}, u32[]{:S(2)}) collective-permute-start(bf16[2048,256]{1,0:T(8,128)(2,1)} %bitcast.12), channel_id=1, source_target_pairs={{0,4},{1,5},{2,6},{3,7},{4,0},{5,1},{6,2},{7,3},{8,12},{9,13},{10,... | collective-permute-start | bytes 3145736 | tf_op jit(solution)/shard_map/ppermute | solution.py:337
  3.0 26.3 %collective-permute-start.5 = (bf16[2048,256]{1,0:T(8,128)(2,1)}, bf16[2048,256]{1,0:T(8,128)(2,1)}, u32[]{:S(2)}, u32[]{:S(2)}) collective-permute-start(bf16[2048,256]{1,0:T(8,128)(2,1)} %bitcast.20), channel_id=1, source_target_pairs={{0,4},{1,5},{2,6},{3,7},{4,0},{5,1},{6,2},{7,3},{8,12},{9,13},{10,... | collective-permute-start | bytes 3145736 | tf_op jit(solution)/shard_map/ppermute | solution.py:337
  3.0 45.1 %collective-permute-start.11 = (bf16[256,2048]{1,0:T(8,128)(2,1)}, bf16[256,2048]{1,0:T(8,128)(2,1)}, u32[]{:S(2)}, u32[]{:S(2)}) collective-permute-start(bf16[256,2048]{1,0:T(8,128)(2,1)} %bitcast.14), channel_id=1, source_target_pairs={{0,1},{1,0},{2,5},{3,4},{4,3},{5,2},{6,7},{7,6},{8,9},{9,8},{10,13... | collective-permute-start | bytes 3145736 | tf_op jit(solution)/shard_map/ppermute | solution.py:337
  12.2 59.0 %copy-start = (bf16[1,2048,256]{2,1,0:T(8,128)(2,1)S(1)}, bf16[1,2048,256]{2,1,0:T(8,128)(2,1)}, u32[]{:S(2)}) copy-start(bf16[1,2048,256]{2,1,0:T(8,128)(2,1)} %param.12) | copy-start | bytes 3145732
  12.2 59.0 %all-to-all-start = ((bf16[32,24,2048]{2,1,0:T(8,128)(2,1)}), bf16[32,24,2048]{2,1,0:T(8,128)(2,1)}, u32[]{:S(2)}, u32[]{:S(2)}) async-start(bf16[32,24,2048]{2,1,0:T(8,128)(2,1)} %bitcast.17), calls=%async_computation | async-start | bytes 6291456 | tf_op jit(solution)/shard_map/all_to_all | solution.py:352
  22.7 27.1 %collective-permute-start.3 = (bf16[2048,256]{1,0:T(8,128)(2,1)S(1)}, bf16[2048,256]{1,0:T(8,128)(2,1)}, u32[]{:S(2)}, u32[]{:S(2)}) collective-permute-start(bf16[2048,256]{1,0:T(8,128)(2,1)S(1)} %collective-permute-done.1.refs_2_), channel_id=1, source_target_pairs={{2,3},{3,2},{4,5},{5,4},{10,11},{11,10},{12,13},{13,12},{18,19},{1... | collective-permute-start | bytes 3145736 | tf_op jit(solution)/shard_map/ppermute | solution.py:337
  26.4 23.5 %collective-permute-start.8 = (bf16[2048,256]{1,0:T(8,128)(2,1)}, bf16[2048,256]{1,0:T(8,128)(2,1)}, u32[]{:S(2)}, u32[]{:S(2)}) collective-permute-start(bf16[2048,256]{1,0:T(8,128)(2,1)} %collective-permute-done.6.refs_8_), channel_id=1, source_target_pairs={{2,3},{3,2},{4,5},{5,4},{10,11},{11,10},{12,13},{13,12},{18,19},{1... | collective-permute-start | bytes 3145736 | tf_op jit(solution)/shard_map/ppermute | solution.py:337
  28.0 31.9 %collective-permute-start.2 = (bf16[2048,256]{1,0:T(8,128)(2,1)S(1)}, bf16[2048,256]{1,0:T(8,128)(2,1)S(1)}, u32[]{:S(2)}, u32[]{:S(2)}) collective-permute-start(bf16[2048,256]{1,0:T(8,128)(2,1)S(1)} %collective-permute-done.1.refs_2_), channel_id=1, source_target_pairs={{0,4},{1,5},{2,6},{3,7},{4,0},{5,1},{6,2},{7,3},{8,12},{9,13},{10,... | collective-permute-start | bytes 3145736 | tf_op jit(solution)/shard_map/ppermute | solution.py:337
  29.3 31.6 %collective-permute-start.7 = (bf16[2048,256]{1,0:T(8,128)(2,1)}, bf16[2048,256]{1,0:T(8,128)(2,1)}, u32[]{:S(2)}, u32[]{:S(2)}) collective-permute-start(bf16[2048,256]{1,0:T(8,128)(2,1)} %collective-permute-done.6.refs_8_), channel_id=1, source_target_pairs={{0,4},{1,5},{2,6},{3,7},{4,0},{5,1},{6,2},{7,3},{8,12},{9,13},{10,... | collective-permute-start | bytes 3145736 | tf_op jit(solution)/shard_map/ppermute | solution.py:337
  48.1 13.3 %collective-permute-start.13 = (bf16[256,2048]{1,0:T(8,128)(2,1)}, bf16[256,2048]{1,0:T(8,128)(2,1)}, u32[]{:S(2)}, u32[]{:S(2)}) collective-permute-start(bf16[256,2048]{1,0:T(8,128)(2,1)} %collective-permute-done.11.d1), channel_id=1, source_target_pairs={{2,3},{3,2},{4,5},{5,4},{10,11},{11,10},{12,13},{13,12},{18,19},{1... | collective-permute-start | bytes 3145736 | tf_op jit(solution)/shard_map/ppermute | solution.py:337
  49.8 21.4 %collective-permute-start.4 = (bf16[2048,256]{1,0:T(8,128)(2,1)}, bf16[2048,256]{1,0:T(8,128)(2,1)}, u32[]{:S(2)}, u32[]{:S(2)}) collective-permute-start(bf16[2048,256]{1,0:T(8,128)(2,1)} %collective-permute-done.3.refs_5_), channel_id=1, source_target_pairs={{0,4},{1,5},{2,6},{3,7},{4,0},{5,1},{6,2},{7,3},{8,12},{9,13},{10,... | collective-permute-start | bytes 3145736 | tf_op jit(solution)/shard_map/ppermute | solution.py:337
  49.8 21.4 %collective-permute-start.9 = (bf16[2048,256]{1,0:T(8,128)(2,1)}, bf16[2048,256]{1,0:T(8,128)(2,1)}, u32[]{:S(2)}, u32[]{:S(2)}) collective-permute-start(bf16[2048,256]{1,0:T(8,128)(2,1)} %collective-permute-done.8.refs_11_), channel_id=1, source_target_pairs={{0,4},{1,5},{2,6},{3,7},{4,0},{5,1},{6,2},{7,3},{8,12},{9,13},{10,... | collective-permute-start | bytes 3145736 | tf_op jit(solution)/shard_map/ppermute | solution.py:337
  59.9 1.0 copy-start.2
  60.9 21.4 %collective-permute-start.10 = (bf16[256,2048]{1,0:T(8,128)(2,1)}, bf16[256,2048]{1,0:T(8,128)(2,1)}, u32[]{:S(2)}, u32[]{:S(2)}) collective-permute-start(bf16[256,2048]{1,0:T(8,128)(2,1)} %bitcast.15), channel_id=1, source_target_pairs={{0,4},{1,5},{2,6},{3,7},{4,0},{5,1},{6,2},{7,3},{8,12},{9,13},{10,... | collective-permute-start | bytes 3145736 | tf_op jit(solution)/shard_map/ppermute | solution.py:337
  60.9 21.4 %collective-permute-start.12 = (bf16[256,2048]{1,0:T(8,128)(2,1)}, bf16[256,2048]{1,0:T(8,128)(2,1)}, u32[]{:S(2)}, u32[]{:S(2)}) collective-permute-start(bf16[256,2048]{1,0:T(8,128)(2,1)} %collective-permute-done.11.d1), channel_id=1, source_target_pairs={{0,4},{1,5},{2,6},{3,7},{4,0},{5,1},{6,2},{7,3},{8,12},{9,13},{10,... | collective-permute-start | bytes 3145736 | tf_op jit(solution)/shard_map/ppermute | solution.py:337
  61.4 20.9 %collective-permute-start.14 = (bf16[256,2048]{1,0:T(8,128)(2,1)}, bf16[256,2048]{1,0:T(8,128)(2,1)}, u32[]{:S(2)}, u32[]{:S(2)}) collective-permute-start(bf16[256,2048]{1,0:T(8,128)(2,1)} %collective-permute-done.13.d3b), channel_id=1, source_target_pairs={{0,4},{1,5},{2,6},{3,7},{4,0},{5,1},{6,2},{7,3},{8,12},{9,13},{10,... | collective-permute-start | bytes 3145736 | tf_op jit(solution)/shard_map/ppermute | solution.py:337
  71.2 11.1 %copy-start.1 = (bf16[1,256,2048]{2,1,0:T(8,128)(2,1)S(1)}, bf16[1,256,2048]{2,1,0:T(8,128)(2,1)}, u32[]{:S(2)}) copy-start(bf16[1,256,2048]{2,1,0:T(8,128)(2,1)} %param.14) | copy-start | bytes 3145732
  89.6 10.8 %copy-start.3 = (s32[768,2]{0,1:T(2,128)S(1)}, s32[768,2]{0,1:T(2,128)}, u32[]{:S(2)}) copy-start(s32[768,2]{0,1:T(2,128)} %param.10) | copy-start | bytes 18436
  89.6 13.3 %copy-start.4 = (f32[768,2]{0,1:T(2,128)S(1)}, f32[768,2]{0,1:T(2,128)}, u32[]{:S(2)}) copy-start(f32[768,2]{0,1:T(2,128)} %param.11) | copy-start | bytes 18436
  89.6 51.7 %all-to-all-start.1 = ((bf16[128,24,512]{2,1,0:T(8,128)(2,1)}), bf16[128,24,512]{2,1,0:T(8,128)(2,1)}, u32[]{:S(2)}, u32[]{:S(2)}) async-start(bf16[128,24,512]{2,1,0:T(8,128)(2,1)} %bitcast.18), calls=%async_computation.1 | async-start | bytes 6291456 | tf_op jit(solution)/shard_map/all_to_all | solution.py:361
  141.3 15.3 %copy-start.5 = (f32[512]{0:T(512)S(1)}, f32[512]{0:T(512)}, u32[]{:S(2)}) copy-start(f32[512]{0:T(512)} %param.15) | copy-start | bytes 6148
  149.0 3.7 %collective-permute-start.17 = (f32[768]{0:T(1024)S(1)}, f32[768]{0:T(1024)S(1)}, u32[]{:S(2)}, u32[]{:S(2)}) collective-permute-start(f32[768]{0:T(1024)S(1)} %reduce), channel_id=1, source_target_pairs={{0,3},{1,0},{2,1},{3,2},{4,7},{5,4},{6,5},{7,6},{8,11},{9,8},{10,9... | collective-permute-start | bytes 9224 | tf_op jit(solution)/shard_map/ppermute | solution.py:369
  150.8 5.1 %collective-permute-start.16 = (f32[768]{0:T(1024)S(1)}, f32[768]{0:T(1024)S(1)}, u32[]{:S(2)}, u32[]{:S(2)}) collective-permute-start(f32[768]{0:T(1024)S(1)} %reduce), channel_id=1, source_target_pairs={{0,2},{1,3},{2,0},{3,1},{4,6},{5,7},{6,4},{7,5},{8,10},{9,11},{10,... | collective-permute-start | bytes 9224 | tf_op jit(solution)/shard_map/ppermute | solution.py:369
  151.8 4.8 %collective-permute-start.15 = (f32[768]{0:T(1024)S(1)}, f32[768]{0:T(1024)S(1)}, u32[]{:S(2)}, u32[]{:S(2)}) collective-permute-start(f32[768]{0:T(1024)S(1)} %reduce), channel_id=1, source_target_pairs={{0,1},{1,2},{2,3},{3,0},{4,5},{5,6},{6,7},{7,4},{8,9},{9,10},{10,1... | collective-permute-start | bytes 9224 | tf_op jit(solution)/shard_map/ppermute | solution.py:369

commit v4 on v3

--- a/solution.py
+++ b/solution.py
@@ -17,6 +17,14 @@
     ep = (ids // 2) * 2 + slot % 2
     tp = (ids % 2) * 2 + (slot % 4) // 2
     return ep, tp, slot // 4
+
+
+def in_vmem(value):
+    return pltpu.with_memory_space_constraint(value, pltpu.VMEM)
+
+
+def in_hbm(value):
+    return pltpu.with_memory_space_constraint(value, pltpu.HBM)
 
 
 def permutes(count_ep, count_tp):
@@ -87,7 +95,7 @@
 
 def dispatch_buffer(ids_rows, gain, tokens, rows):
     count, width = tokens.shape
-    steps, chunks = 6, 2
+    steps, chunks = 2, 2
     return pl.pallas_call(
         functools.partial(dispatch_kernel, rows=rows, chunks=chunks),
         grid=(steps,),
@@ -118,77 +126,79 @@
         pltpu.make_async_copy(b, dst, sem).start()
 
 
-def hidden_kernel(place_ref, rows_ref, *refs, pieces):
-    gates, ups = refs[:6], refs[6:12]
-    out_ref, rows, weights, sems = refs[12:]
+def activation(acts, part):
+    gate_acts = acts[:, :part]
+    return (gate_acts / (1.0 + jnp.exp(-gate_acts)) * acts[:, part:]).astype(jnp.bfloat16)
+
+
+def early_kernel(place_ref, rows_ref, *refs):
+    gates, ups = refs[:4], refs[4:8]
+    out_ref, weights, sems = refs[8:]
     flag = place_ref[1]
-    count = rows.shape[0]
     part = gates[0].shape[1]
-    size = count // pieces
-
-    def start(refs, i, lo, sem):
-        dst = weights.at[i, :, pl.ds(lo, part)]
-        if i == 0 or i == 3:
-            at = 0 if i == 0 else 4
-            start_one(flag, refs[at], refs[at + 1], dst, sem)
-        else:
-            pltpu.make_async_copy(refs[i + 1], dst, sem).start()
-
-    def load(p):
-        return pltpu.make_async_copy(
-            rows_ref.at[pl.ds(p * size, size)], rows.at[pl.ds(p * size, size)], sems.at[8 + p]
-        )
-
-    for i in range(4):
-        start(gates, i, 0, sems.at[2 * i])
-        start(ups, i, part, sems.at[2 * i + 1])
-        if i == 0:
-            for p in range(pieces):
-                load(p).start()
-    for i in range(4):
+    for i in range(3):
+        for lo, r, sem in ((0, gates, sems.at[2 * i]), (part, ups, sems.at[2 * i + 1])):
+            dst = weights.at[i, :, pl.ds(lo, part)]
+            if i == 0:
+                start_one(flag, r[0], r[1], dst, sem)
+            else:
+                pltpu.make_async_copy(r[i + 1], dst, sem).start()
+    for i in range(3):
         pltpu.make_async_copy(gates[2], weights.at[i, :, pl.ds(0, part)], sems.at[2 * i]).wait()
         pltpu.make_async_copy(ups[2], weights.at[i, :, pl.ds(part, part)], sems.at[2 * i + 1]).wait()
-        for p in range(pieces):
-            if i == 0:
-                load(p).wait()
-            acts = jnp.dot(
-                rows[p * size : (p + 1) * size, :], weights[i], preferred_element_type=jnp.float32
-            )
-            gate_acts = acts[:, :part]
-            value = gate_acts / (1.0 + jnp.exp(-gate_acts)) * acts[:, part:]
-            out_ref[p * size : (p + 1) * size, i * part : (i + 1) * part] = value.astype(jnp.bfloat16)
+        acts = jnp.dot(rows_ref[...], weights[i], preferred_element_type=jnp.float32)
+        out_ref[:, i * part : (i + 1) * part] = activation(acts, part)
+
+
+def middle_kernel(place_ref, rows_ref, ga, gb, ua, ub, out_ref, weights, sems):
+    flag = place_ref[1]
+    part = ga.shape[1]
+    start_one(flag, ga, gb, weights.at[:, pl.ds(0, part)], sems.at[0])
+    start_one(flag, ua, ub, weights.at[:, pl.ds(part, part)], sems.at[1])
+    pltpu.make_async_copy(ga, weights.at[:, pl.ds(0, part)], sems.at[0]).wait()
+    pltpu.make_async_copy(ua, weights.at[:, pl.ds(part, part)], sems.at[1]).wait()
+    acts = jnp.dot(rows_ref[...], weights[...], preferred_element_type=jnp.float32)
+    out_ref[...] = activation(acts, part)
 
 
 HBM = pl.BlockSpec(memory_space=pltpu.HBM)
 ANY = pl.BlockSpec(memory_space=pl.ANY)
 SMEM = pl.BlockSpec(memory_space=pltpu.SMEM)
-
-
-def hidden_units(place, rows, gates, ups):
+VMEM = pl.BlockSpec(memory_space=pltpu.VMEM)
+
+
+def early_hidden(place, rows, gates, ups):
     count, width = rows.shape
     part = gates[0].shape[1]
-    pieces = 2
-    return pl.pallas_call(
-        functools.partial(hidden_kernel, pieces=pieces),
-        in_specs=[SMEM, ANY] + [HBM] * 12,
-        out_specs=pl.BlockSpec((count, 4 * part), lambda: (0, 0)),
-        scratch_shapes=[
-            pltpu.VMEM((count, width), jnp.bfloat16),
-            pltpu.VMEM((4, width, 2 * part), jnp.bfloat16),
-            pltpu.SemaphoreType.DMA((8 + pieces,)),
-        ],
-        out_shape=jax.ShapeDtypeStruct((count, 4 * part), jnp.bfloat16),
+    return pl.pallas_call(
+        early_kernel,
+        in_specs=[SMEM, VMEM] + [ANY] * 8,
+        out_specs=VMEM,
+        scratch_shapes=[pltpu.VMEM((3, width, 2 * part), jnp.bfloat16), pltpu.SemaphoreType.DMA((6,))],
+        out_shape=jax.ShapeDtypeStruct((count, 3 * part), jnp.bfloat16),
         compiler_params=pltpu.CompilerParams(vmem_limit_bytes=50 * MIB),
-        name="hidden_units",
+        name="early_hidden",
     )(place, rows, *gates, *ups)
 
 
-def late_kernel(place_ref, hidden_ref, d0a, d0b, d1, d2, d3a, d3b, out_ref, down, hidden, out, sems, out_sems):
+def middle_hidden(place, rows, gates, ups):
+    count, width = rows.shape
+    part = gates[0].shape[1]
+    return pl.pallas_call(
+        middle_kernel,
+        in_specs=[SMEM, VMEM] + [ANY] * 4,
+        out_specs=VMEM,
+        scratch_shapes=[pltpu.VMEM((width, 2 * part), jnp.bfloat16), pltpu.SemaphoreType.DMA((2,))],
+        out_shape=jax.ShapeDtypeStruct((count, part), jnp.bfloat16),
+        compiler_params=pltpu.CompilerParams(vmem_limit_bytes=50 * MIB),
+        name="middle_hidden",
+    )(place, rows, *gates, *ups)
+
+
+def late_kernel(place_ref, early_ref, middle_ref, d0a, d0b, d1, d2, d3a, d3b, out_ref, down, hidden, out, sems, out_sems):
     flag = place_ref[1]
     senders, pieces, slots, piece = out_ref.shape
     part = d1.shape[0]
-    load = pltpu.make_async_copy(hidden_ref, hidden, sems.at[4 * pieces])
-    load.start()
 
     def target(i, f):
         return down.at[pl.ds(i * part, part), pl.ds(f * piece, piece)]
@@ -201,7 +211,8 @@
         pltpu.make_async_copy(source(d1, f), target(1, f), sems.at[4 * f + 1]).start()
         pltpu.make_async_copy(source(d2, f), target(2, f), sems.at[4 * f + 2]).start()
         start_one(flag, source(d3a, f), source(d3b, f), target(3, f), sems.at[4 * f + 3])
-    load.wait()
+    hidden[:, 0 : 3 * part] = early_ref[...]
+    hidden[:, 3 * part : 4 * part] = middle_ref[...]
     for f in range(pieces):
         for i in range(4):
             pltpu.make_async_copy(source(d1, f), target(i, f), sems.at[4 * f + i]).wait()
@@ -214,30 +225,30 @@
         pltpu.make_async_copy(out.at[f], out_ref.at[:, f], out_sems.at[f]).wait()
 
 
-def late_outputs(place, hidden, downs, senders, pieces):
-    count = hidden.shape[0]
+def late_outputs(place, early, middle, downs, senders, pieces):
+    count = early.shape[0]
     part, width = downs[0].shape
     slots = count // senders
     piece = width // pieces
     shape = (senders, pieces, slots, piece)
     return pl.pallas_call(
         late_kernel,
-        in_specs=[SMEM, ANY] + [HBM] * 6,
+        in_specs=[SMEM, VMEM, VMEM] + [ANY] * 6,
         out_specs=HBM,
         scratch_shapes=[
             pltpu.VMEM((4 * part, width), jnp.bfloat16),
             pltpu.VMEM((count, 4 * part), jnp.bfloat16),
             pltpu.VMEM((pieces, senders, slots, piece), jnp.bfloat16),
-            pltpu.SemaphoreType.DMA((4 * pieces + 1,)),
+            pltpu.SemaphoreType.DMA((4 * pieces,)),
             pltpu.SemaphoreType.DMA((pieces,)),
         ],
         out_shape=pltpu.HBM(shape, jnp.bfloat16),
         compiler_params=pltpu.CompilerParams(vmem_limit_bytes=50 * MIB),
         name="late_outputs",
-    )(place, hidden, *downs)
-
-
-def columns_kernel(ids_ref, out_ref, *, cuts, count_tp):
+    )(place, early, middle, *downs)
+
+
+def table_kernel(ids_ref, scores_ref, out_ref, *, rows, count_tp):
     count = ids_ref.shape[0]
     experts = 32
     first = ids_ref[:, 0:1]
@@ -252,39 +263,35 @@
     ranks = jnp.dot(
         jnp.where(before, 1.0, 0.0).astype(jnp.bfloat16), named, preferred_element_type=jnp.float32
     )
+    scores = scores_ref[...]
+    out_ref[:, 2:4] = scores / jnp.sum(scores, axis=1, keepdims=True)
     for choice, (ids, chosen) in enumerate(((first, named_first), (second, named_second))):
         slot = jnp.sum(jnp.where(chosen, ranks, 0.0), axis=1, keepdims=True).astype(jnp.int32)
         ep, tp, row = place_of(ids, slot)
-        device = ep * count_tp + tp
-        for i, (lo, hi) in enumerate(cuts):
-            inside = (row >= lo) & (row < hi)
-            out_ref[:, 2 * i + choice : 2 * i + choice + 1] = jnp.where(
-                inside, device * (hi - lo) + row - lo, -1
-            )
-
-
-def routing_columns(ids, cuts, count_tp):
-    return pl.pallas_call(
-        functools.partial(columns_kernel, cuts=cuts, count_tp=count_tp),
-        out_shape=jax.ShapeDtypeStruct((ids.shape[0], 2 * len(cuts)), jnp.int32),
+        out_ref[:, choice : choice + 1] = ((ep * count_tp + tp) * rows + row).astype(jnp.float32)
+
+
+def routing_table(ids, scores, rows, count_tp):
+    return pl.pallas_call(
+        functools.partial(table_kernel, rows=rows, count_tp=count_tp),
+        out_shape=jax.ShapeDtypeStruct((ids.shape[0], 4), jnp.float32),
         compiler_params=pltpu.CompilerParams(vmem_limit_bytes=16 * MIB),
         name="columns",
-    )(ids)
-
-
-def combine_kernel(index_ref, scores_ref, returned_ref, out_ref, squares_ref):
+    )(ids, scores)
+
+
+def combine_kernel(table_ref, returned_ref, out_ref, squares_ref):
     total = returned_ref.shape[0]
-    count = index_ref.shape[0]
+    count = table_ref.shape[0]
     index = lax.broadcasted_iota(jnp.int32, (count, total), 1)
     returned = returned_ref[...]
 
-    def picked(column):
-        hot = jnp.where(index == index_ref[:, column : column + 1], 1.0, 0.0).astype(jnp.bfloat16)
+    def picked(choice):
+        row = table_ref[:, choice : choice + 1].astype(jnp.int32)
+        hot = jnp.where(index == row, 1.0, 0.0).astype(jnp.bfloat16)
         return jnp.dot(hot, returned, preferred_element_type=jnp.float32)
 
-    scores = scores_ref[...]
-    mix = scores / jnp.sum(scores, axis=1, keepdims=True)
-    value = mix[:, 0:1] * picked(0) + mix[:, 1:2] * picked(1)
+    value = table_ref[:, 2:3] * picked(0) + table_ref[:, 3:4] * picked(1)
     out_ref[...] = value
     square = value * value
     lanes = 128
@@ -294,28 +301,20 @@
     squares_ref[...] = jnp.sum(folded.T, axis=0, keepdims=True)
 
 
-def combine(index, scores, returned):
-    count = index.shape[0]
-    total, piece = returned.shape
-    steps = 3
-    block = count // steps
-    row_block = pl.BlockSpec((block, piece), lambda i: (i, 0))
+def combine(table, returned):
+    count = table.shape[0]
+    piece = returned.shape[1]
     return pl.pallas_call(
         combine_kernel,
-        grid=(steps,),
-        in_specs=[
-            pl.BlockSpec((block, 2), lambda i: (i, 0)),
-            pl.BlockSpec((block, 2), lambda i: (i, 0)),
-            pl.BlockSpec((total, piece), lambda i: (0, 0)),
-        ],
-        out_specs=[row_block, pl.BlockSpec((1, block), lambda i: (0, i))],
+        in_specs=[VMEM, VMEM],
+        out_specs=[VMEM, VMEM],
         out_shape=[
             jax.ShapeDtypeStruct((count, piece), jnp.float32),
             jax.ShapeDtypeStruct((1, count), jnp.float32),
         ],
-        compiler_params=pltpu.CompilerParams(dimension_semantics=("arbitrary",), vmem_limit_bytes=50 * MIB),
+        compiler_params=pltpu.CompilerParams(vmem_limit_bytes=50 * MIB),
         name="combine",
-    )(index, scores, returned)
+    )(table, returned)
 
 
 def per_device(
@@ -336,33 +335,34 @@
     def send(weight, pairs):
         return lax.ppermute(weight, AXES, pairs)
 
-    def spread(weight):
+    def spread(name, weight):
         moved = send(weight, first)
         other_own = send(weight, swap)
         other_moved = send(moved, swap)
         last = send(moved, second)
         other_last = send(last, swap)
-        return (weight, other_own), moved, other_moved, (other_last, last)
-
-    gate = spread(gate_weight[0])
-    up = spread(up_weight[0])
-    down = spread(down_weight[0])
+        hold = in_vmem if name == "down" else in_hbm
+        return (in_hbm(weight), in_hbm(other_own)), in_hbm(moved), in_hbm(other_moved), (hold(other_last), in_hbm(last))
+
+    gate = spread("gate", gate_weight[0])
+    up = spread("up", up_weight[0])
+    down = spread("down", down_weight[0])
 
     buffer = dispatch_buffer(route_ids.T, in_gain[None, :], tokens, rows)
     received = lax.all_to_all(
         buffer.reshape(count_ep, rows, full_width), "ep", split_axis=0, concat_axis=0, tiled=True
     ).reshape(count_ep * rows, full_width)
-    hidden = hidden_units(
-        place, received, (*gate[0], gate[1], gate[2], *gate[3]), (*up[0], up[1], up[2], *up[3])
-    )
+    received = in_vmem(received)
+    early = in_vmem(early_hidden(place, received, (*gate[0], gate[1], gate[2]), (*up[0], up[1], up[2])))
+    middle = in_vmem(middle_hidden(place, received, gate[3], up[3]))
     outputs = late_outputs(
-        place, hidden, (*down[0], down[1], down[2], *down[3]), count_ep, count_tp
+        place, early, middle, (*down[0], down[1], down[2], *down[3]), count_ep, count_tp
     )
     returned = lax.all_to_all(
         outputs.reshape(count_ep * count_tp, rows, part_width), AXES, split_axis=0, concat_axis=0, tiled=True
     ).reshape(count_ep * count_tp * rows, part_width)
-    index = routing_columns(route_ids, ((0, rows),), count_tp)
-    combined, squares = combine(index, route_scores, returned)
+    table = routing_table(route_ids, route_scores, rows, count_tp)
+    combined, squares = combine(table, in_vmem(returned))
     squares = squares[0]
     total = squares
     for shift in range(1, count_tp):

time: 158 us -> 159 us (level)
  local copies, waits for them, and re-layouts: 1.41 us -> 3.89 us
    all_to_all x1, waiting for transfers between devices: 38.2 us -> 35 us  [per_device(): lax.all_to_all(outputs.reshape(count_ep * count_tp, rows, part_width), AX...]
    ppermute x15, waiting for transfers between devices: 20.7 us -> 23.5 us  [send(): return lax.ppermute(weight, AXES, pairs)]
    unnamed x14, local copies, waits for them, and re-layouts: 1.41 us -> 3.89 us
    all_to_all x1, starting transfers between devices: 10.5 us -> 8.89 us  [per_device(): lax.all_to_all(buffer.reshape(count_ep, rows, full_width), 'ep', split_ax...]
    pallas_call x4 -> x5, Pallas kernels: 28.3 us -> 27.9 us  [the longest x1 8.61 us: early_hidden(): pl.pallas_call(early_kernel, in_specs=[SMEM, VMEM] + [ANY] * 8, out_specs...]
  transfers between devices with their start and end apart: 20 -> 20, of which waited for: 6 -> 6; matrix products, arithmetic and copies ran while one was open for 0% -> 1% of each run, Pallas kernels for 14% -> 14%
where the time goes in v4:
time: 159 us
  waiting for transfers between devices  63.3 us (40%)
  starting transfers between devices  53.7 us (34%)
  Pallas kernels  35 us (22%)
  local copies, waits for them, and re-layouts  3.89 us (2%)
  other arithmetic  2.59 us (2%)
    all_to_all x1, waiting for transfers between devices, per_device(): lax.all_to_all(outputs.reshape(count_ep * count_tp, rows, part_width), AX...  35 us
    ppermute x15, starting transfers between devices, send(): return lax.ppermute(weight, AXES, pairs)  31.5 us
    ppermute x15, waiting for transfers between devices, send(): return lax.ppermute(weight, AXES, pairs)  23.5 us
    all_to_all x1, starting transfers between devices, per_device(): lax.all_to_all(outputs.reshape(count_ep * count_tp, rows, part_width), AX...  10.6 us
    all_to_all x1, starting transfers between devices, per_device(): lax.all_to_all(buffer.reshape(count_ep, rows, full_width), 'ep', split_ax...  8.89 us
    pallas_call x1, Pallas kernels, early_hidden(): pl.pallas_call(early_kernel, in_specs=[SMEM, VMEM] + [ANY] * 8, out_specs...  8.61 us
    pallas_call x1, Pallas kernels, dispatch_buffer(): pl.pallas_call(functools.partial(dispatch_kernel, rows=rows, chunks=chunk...  7.13 us
    pallas_call x1, Pallas kernels, late_outputs(): pl.pallas_call(late_kernel, in_specs=[SMEM, VMEM, VMEM] + [ANY] * 6, out_...  6.84 us
  transfers between devices with their start and end apart: 20, of which 6 were waited for; matrix products, arithmetic and copies ran while one was open for 1% of the time, Pallas kernels for 14%

profile of v4, /device:TPU:0, one launch (start us, length us, event | category | flops | bytes accessed | tf_op | source)
XLA Modules:
  0.0 158.7 jit_solution(10344989803336652142)
XLA Ops:
  0.0 1.6 %collective-permute-start.1 = (bf16[2048,256]{1,0:T(8,128)(2,1)}, bf16[2048,256]{1,0:T(8,128)(2,1)}, u32[]{:S(2)}, u32[]{:S(2)}) collective-permute-start(bf16[2048,256]{1,0:T(8,128)(2,1)} %bitcast.16), channel_id=1, source_target_pairs={{0,1},{1,0},{2,5},{3,4},{4,3},{5,2},{6,7},{7,6},{8,9},{9,8},{10,13... | collective-permute-start | bytes 3145736 | tf_op jit(solution)/shard_map/ppermute | solution.py:336
  1.6 1.4 collective-permute-start
  3.0 0.2 collective-permute-start.4
  3.2 0.2 collective-permute-start.3
  3.4 1.6 %collective-permute-start.11 = (bf16[256,2048]{1,0:T(8,128)(2,1)}, bf16[256,2048]{1,0:T(8,128)(2,1)}, u32[]{:S(2)}, u32[]{:S(2)}) collective-permute-start(bf16[256,2048]{1,0:T(8,128)(2,1)} %bitcast.22), channel_id=1, source_target_pairs={{0,1},{1,0},{2,5},{3,4},{4,3},{5,2},{6,7},{7,6},{8,9},{9,8},{10,13... | collective-permute-start | bytes 3145736 | tf_op jit(solution)/shard_map/ppermute | solution.py:336
  5.0 7.1 %dispatch_buffer.1 = bf16[768,2048]{1,0:T(8,128)(2,1)} custom-call(s32[2,768]{1,0:T(2,128)} %bitcast.25, f32[1,2048]{1,0:T(1,128)} %bitcast.26, bf16[768,2048]{1,0:T(8,128)(2,1)} %tokens_ref.1), custom_call_target="tpu_custom_call" | custom-call | tf_op jit(solution)/shard_map/dispatch_buffer/pallas_call | solution.py:99
  12.2 8.9 %all-to-all-start = ((bf16[32,24,2048]{2,1,0:T(8,128)(2,1)}), bf16[32,24,2048]{2,1,0:T(8,128)(2,1)S(1)}, u32[]{:S(2)}, u32[]{:S(2)}) async-start(bf16[32,24,2048]{2,1,0:T(8,128)(2,1)} %bitcast.14), calls=%async_computation | async-start | bytes 6291456 | tf_op jit(solution)/shard_map/all_to_all | solution.py:352
  21.0 0.0 collective-permute-done.1.refs_2_
  21.1 0.4 collective-permute-start.2
  21.4 1.7 %collective-permute-start.6 = (bf16[2048,256]{1,0:T(8,128)(2,1)}, bf16[2048,256]{1,0:T(8,128)(2,1)}, u32[]{:S(2)}, u32[]{:S(2)}) collective-permute-start(bf16[2048,256]{1,0:T(8,128)(2,1)} %collective-permute-done.1.refs_2_), channel_id=1, source_target_pairs={{2,3},{3,2},{4,5},{5,4},{10,11},{11,10},{12,13},{13,12},{18,19},{1... | collective-permute-start | bytes 3145736 | tf_op jit(solution)/shard_map/ppermute | solution.py:336
  23.1 3.6 %collective-permute-done.4.refs_6_ = bf16[2048,256]{1,0:T(8,128)(2,1)} collective-permute-done((bf16[2048,256]{1,0:T(8,128)(2,1)}, bf16[2048,256]{1,0:T(8,128)(2,1)}, u32[]{:S(2)}, u32[]{:S(2)}) %collective-permute-start.4) | collective-permute-done | bytes 1048608 | tf_op jit(solution)/shard_map/ppermute | solution.py:336
  26.7 1.6 %collective-permute-start.8 = (bf16[2048,256]{1,0:T(8,128)(2,1)}, bf16[2048,256]{1,0:T(8,128)(2,1)}, u32[]{:S(2)}, u32[]{:S(2)}) collective-permute-start(bf16[2048,256]{1,0:T(8,128)(2,1)} %collective-permute-done.4.refs_6_), channel_id=1, source_target_pairs={{2,3},{3,2},{4,5},{5,4},{10,11},{11,10},{12,13},{13,12},{18,19},{1... | collective-permute-start | bytes 3145736 | tf_op jit(solution)/shard_map/ppermute | solution.py:336
  28.3 0.0 collective-permute-done.3.refs_5_
  28.3 0.9 collective-permute-start.5
  29.3 19.9 %collective-permute-done.11.d1 = bf16[256,2048]{1,0:T(8,128)(2,1)} collective-permute-done((bf16[256,2048]{1,0:T(8,128)(2,1)}, bf16[256,2048]{1,0:T(8,128)(2,1)}, u32[]{:S(2)}, u32[]{:S(2)}) %collective-permute-start.11) | collective-permute-done | bytes 1048608 | tf_op jit(solution)/shard_map/ppermute | solution.py:336
  49.2 1.6 %collective-permute-start.13 = (bf16[256,2048]{1,0:T(8,128)(2,1)}, bf16[256,2048]{1,0:T(8,128)(2,1)}, u32[]{:S(2)}, u32[]{:S(2)}) collective-permute-start(bf16[256,2048]{1,0:T(8,128)(2,1)} %collective-permute-done.11.d1), channel_id=1, source_target_pairs={{2,3},{3,2},{4,5},{5,4},{10,11},{11,10},{12,13},{13,12},{18,19},{1... | collective-permute-start | bytes 3145736 | tf_op jit(solution)/shard_map/ppermute | solution.py:336
  50.8 0.0 collective-permute-done.2.refs_3_
  50.8 0.0 collective-permute-start.10
  50.8 0.5 collective-permute-start.7
  51.3 0.0 collective-permute-done.8.ub
  51.3 8.6 %collective-permute-start.9 = (bf16[2048,256]{1,0:T(8,128)(2,1)}, bf16[2048,256]{1,0:T(8,128)(2,1)}, u32[]{:S(2)}, u32[]{:S(2)}) collective-permute-start(bf16[2048,256]{1,0:T(8,128)(2,1)} %collective-permute-done.8.ub), channel_id=1, source_target_pairs={{0,4},{1,5},{2,6},{3,7},{4,0},{5,1},{6,2},{7,3},{8,12},{9,13},{10,... | collective-permute-start | bytes 3145736 | tf_op jit(solution)/shard_map/ppermute | solution.py:336
  59.9 0.0 collective-permute-start.12
  59.9 11.2 %collective-permute-start.14 = (bf16[256,2048]{1,0:T(8,128)(2,1)}, bf16[256,2048]{1,0:T(8,128)(2,1)}, u32[]{:S(2)}, u32[]{:S(2)}) collective-permute-start(bf16[256,2048]{1,0:T(8,128)(2,1)} %collective-permute-done.13.d3b), channel_id=1, source_target_pairs={{0,4},{1,5},{2,6},{3,7},{4,0},{5,1},{6,2},{7,3},{8,12},{9,13},{10,... | collective-permute-start | bytes 3145736 | tf_op jit(solution)/shard_map/ppermute | solution.py:336
  71.1 0.1 pad_add_fusion.place_ref
  71.2 0.0 all-to-all-done
  71.2 8.6 %early_hidden.1.early_ref = bf16[768,768]{1,0:T(8,128)(2,1)} custom-call(s32[2]{0:T(128)S(1)} %pad_add_fusion.place_ref, bf16[768,2048]{1,0:T(8,128)(2,1)S(1)} %bitcast.11, bf16[2048,256]{1,0:T(8,128)(2,1)} %bitcast.18, bf16[2048,256]{1,0:T(8,128)(2,1)} %collective-permute-done.refs_1_, bf16[2048,256]{1,0:T(8,128)(2,1)} %collective-permute-done.1.refs_2_, ...), custom_call_target="tpu_custom_call" | custom-call | tf_op jit(solution)/shard_map/early_hidden/pallas_call | solution.py:173
  79.8 0.0 collective-permute-done.7.ga
  79.8 3.9 %middle_hidden.1.middle_ref = bf16[768,256]{1,0:T(8,128)(2,1)S(1)} custom-call(s32[2]{0:T(128)S(1)} %pad_add_fusion.place_ref, bf16[768,2048]{1,0:T(8,128)(2,1)S(1)} %bitcast.12, bf16[2048,256]{1,0:T(8,128)(2,1)} %collective-permute-done.7.ga, bf16[2048,256]{1,0:T(8,128)(2,1)} %collective-permute-done.6.gb, bf16[2048,256]{1,0:T(8,128)(2,1)} %collective-permute-done.9.ua, ...), custom_call_target="tpu_custom_call" | custom-call | tf_op jit(solution)/shard_map/middle_hidden/pallas_call | solution.py:187
  83.8 0.0 collective-permute-done.12.d2
  83.8 0.0 collective-permute-done.14.d3a
  83.8 6.8 %late_outputs.1 = bf16[32,4,24,512]{3,2,1,0:T(8,128)(2,1)} custom-call(s32[2]{0:T(128)S(1)} %pad_add_fusion.place_ref, bf16[768,768]{1,0:T(8,128)(2,1)S(1)} %copy-done, bf16[768,256]{1,0:T(8,128)(2,1)S(1)} %middle_hidden.1.middle_ref, bf16[256,2048]{1,0:T(8,128)(2,1)} %bitcast.24, bf16[256,2048]{1,0:T(8,128)(2,1)} %collective-permute-done.10.d0b, ...), custom_call_target="tpu_custom_call" | custom-call | tf_op jit(solution)/shard_map/late_outputs/pallas_call | solution.py:234
  90.6 0.0 copy-start.3
  90.7 0.0 copy-start.4
  90.7 10.6 %all-to-all-start.1 = ((bf16[128,24,512]{2,1,0:T(8,128)(2,1)}), bf16[128,24,512]{2,1,0:T(8,128)(2,1)S(1)}, u32[]{:S(2)}, u32[]{:S(2)}) async-start(bf16[128,24,512]{2,1,0:T(8,128)(2,1)} %bitcast.15), calls=%async_computation.1 | async-start | bytes 6291456 | tf_op jit(solution)/shard_map/all_to_all | solution.py:361
  101.2 0.9 copy.9.ids_ref
  102.2 0.9 copy.10.scores_ref
  103.1 1.0 copy-done.1
  104.1 1.0 copy-done.2
  105.1 2.2 %columns.1.table_ref = f32[768,4]{1,0:T(8,128)S(1)} custom-call(s32[768,2]{1,0:T(8,128)S(1)} %copy-done.1, f32[768,2]{1,0:T(8,128)S(1)} %copy-done.2), custom_call_target="tpu_custom_call" | custom-call | tf_op jit(solution)/shard_map/columns/pallas_call | solution.py:275
  107.3 35.0 %all-to-all-done.1 = bf16[128,24,512]{2,1,0:T(8,128)(2,1)S(1)} async-done(((bf16[128,24,512]{2,1,0:T(8,128)(2,1)}), bf16[128,24,512]{2,1,0:T(8,128)(2,1)S(1)}, u32[]{:S(2)}, u32[]{:S(2)}) %all-to-all-start.1) | async-done | bytes 3145760 | tf_op jit(solution)/shard_map/all_to_all | solution.py:361
  142.3 6.3 %combine.1 = (f32[768,512]{1,0:T(8,128)}, f32[1,768]{1,0:T(1,128)S(1)}) custom-call(f32[768,4]{1,0:T(8,128)S(1)} %columns.1.table_ref, bf16[3072,512]{1,0:T(8,128)(2,1)S(1)} %bitcast.13), custom_call_target="tpu_custom_call" | custom-call | tf_op jit(solution)/shard_map/combine/pallas_call | solution.py:307
  148.6 1.8 %collective-permute-start.17 = (f32[768]{0:T(1024)S(1)}, f32[768]{0:T(1024)S(1)}, u32[]{:S(2)}, u32[]{:S(2)}) collective-permute-start(f32[768]{0:T(1024)S(1)} %reduce), channel_id=1, source_target_pairs={{0,3},{1,0},{2,1},{3,2},{4,7},{5,4},{6,5},{7,6},{8,11},{9,8},{10,9... | collective-permute-start | bytes 9224 | tf_op jit(solution)/shard_map/ppermute | solution.py:369
  150.4 0.9 collective-permute-start.16
  151.4 0.0 collective-permute-start.15
  151.4 0.9 collective-permute-done.17
  152.3 3.2 %collective-permute-done.16 = f32[768]{0:T(1024)S(1)} collective-permute-done((f32[768]{0:T(1024)S(1)}, f32[768]{0:T(1024)S(1)}, u32[]{:S(2)}, u32[]{:S(2)}) %collective-permute-start.16) | collective-permute-done | bytes 3104 | tf_op jit(solution)/shard_map/ppermute | solution.py:369
  155.5 0.6 collective-permute-done.15
  156.2 2.5 %multiply_convert_fusion = bf16[768,512]{1,0:T(8,128)(2,1)} fusion(f32[768,512]{1,0:T(8,128)} %get-tuple-element.7, f32[512]{0:T(512)S(1)} %copy-done.5, f32[768]{0:T(1024)S(1)} %add_rsqrt_fusion), kind=kLoop, calls=%fused_computation | loop fusion | flops 1179648 | bytes 2364416 | tf_op jit(solution)/shard_map/convert_element_type | solution.py:373
  (16 shorter events, 0.1 us)
Async XLA Ops:
  0.0 21.0 %collective-permute-start.1 = (bf16[2048,256]{1,0:T(8,128)(2,1)}, bf16[2048,256]{1,0:T(8,128)(2,1)}, u32[]{:S(2)}, u32[]{:S(2)}) collective-permute-start(bf16[2048,256]{1,0:T(8,128)(2,1)} %bitcast.16), channel_id=1, source_target_pairs={{0,1},{1,0},{2,5},{3,4},{4,3},{5,2},{6,7},{7,6},{8,9},{9,8},{10,13... | collective-permute-start | bytes 3145736 | tf_op jit(solution)/shard_map/ppermute | solution.py:336
  1.6 19.8 %collective-permute-start = (bf16[2048,256]{1,0:T(8,128)(2,1)}, bf16[2048,256]{1,0:T(8,128)(2,1)}, u32[]{:S(2)}, u32[]{:S(2)}) collective-permute-start(bf16[2048,256]{1,0:T(8,128)(2,1)} %bitcast.17), channel_id=1, source_target_pairs={{0,4},{1,5},{2,6},{3,7},{4,0},{5,1},{6,2},{7,3},{8,12},{9,13},{10,... | collective-permute-start | bytes 3145736 | tf_op jit(solution)/shard_map/ppermute | solution.py:336
  3.0 23.7 %collective-permute-start.4 = (bf16[2048,256]{1,0:T(8,128)(2,1)}, bf16[2048,256]{1,0:T(8,128)(2,1)}, u32[]{:S(2)}, u32[]{:S(2)}) collective-permute-start(bf16[2048,256]{1,0:T(8,128)(2,1)} %bitcast.19), channel_id=1, source_target_pairs={{0,1},{1,0},{2,5},{3,4},{4,3},{5,2},{6,7},{7,6},{8,9},{9,8},{10,13... | collective-permute-start | bytes 3145736 | tf_op jit(solution)/shard_map/ppermute | solution.py:336
  3.2 25.1 %collective-permute-start.3 = (bf16[2048,256]{1,0:T(8,128)(2,1)}, bf16[2048,256]{1,0:T(8,128)(2,1)}, u32[]{:S(2)}, u32[]{:S(2)}) collective-permute-start(bf16[2048,256]{1,0:T(8,128)(2,1)} %bitcast.20), channel_id=1, source_target_pairs={{0,4},{1,5},{2,6},{3,7},{4,0},{5,1},{6,2},{7,3},{8,12},{9,13},{10,... | collective-permute-start | bytes 3145736 | tf_op jit(solution)/shard_map/ppermute | solution.py:336
  3.4 45.8 %collective-permute-start.11 = (bf16[256,2048]{1,0:T(8,128)(2,1)}, bf16[256,2048]{1,0:T(8,128)(2,1)}, u32[]{:S(2)}, u32[]{:S(2)}) collective-permute-start(bf16[256,2048]{1,0:T(8,128)(2,1)} %bitcast.22), channel_id=1, source_target_pairs={{0,1},{1,0},{2,5},{3,4},{4,3},{5,2},{6,7},{7,6},{8,9},{9,8},{10,13... | collective-permute-start | bytes 3145736 | tf_op jit(solution)/shard_map/ppermute | solution.py:336
  12.2 59.0 %all-to-all-start = ((bf16[32,24,2048]{2,1,0:T(8,128)(2,1)}), bf16[32,24,2048]{2,1,0:T(8,128)(2,1)S(1)}, u32[]{:S(2)}, u32[]{:S(2)}) async-start(bf16[32,24,2048]{2,1,0:T(8,128)(2,1)} %bitcast.14), calls=%async_computation | async-start | bytes 6291456 | tf_op jit(solution)/shard_map/all_to_all | solution.py:352
  21.1 29.7 %collective-permute-start.2 = (bf16[2048,256]{1,0:T(8,128)(2,1)}, bf16[2048,256]{1,0:T(8,128)(2,1)}, u32[]{:S(2)}, u32[]{:S(2)}) collective-permute-start(bf16[2048,256]{1,0:T(8,128)(2,1)} %collective-permute-done.1.refs_2_), channel_id=1, source_target_pairs={{0,4},{1,5},{2,6},{3,7},{4,0},{5,1},{6,2},{7,3},{8,12},{9,13},{10,... | collective-permute-start | bytes 3145736 | tf_op jit(solution)/shard_map/ppermute | solution.py:336
  21.4 29.4 %collective-permute-start.6 = (bf16[2048,256]{1,0:T(8,128)(2,1)}, bf16[2048,256]{1,0:T(8,128)(2,1)}, u32[]{:S(2)}, u32[]{:S(2)}) collective-permute-start(bf16[2048,256]{1,0:T(8,128)(2,1)} %collective-permute-done.1.refs_2_), channel_id=1, source_target_pairs={{2,3},{3,2},{4,5},{5,4},{10,11},{11,10},{12,13},{13,12},{18,19},{1... | collective-permute-start | bytes 3145736 | tf_op jit(solution)/shard_map/ppermute | solution.py:336
  26.7 24.6 %collective-permute-start.8 = (bf16[2048,256]{1,0:T(8,128)(2,1)}, bf16[2048,256]{1,0:T(8,128)(2,1)}, u32[]{:S(2)}, u32[]{:S(2)}) collective-permute-start(bf16[2048,256]{1,0:T(8,128)(2,1)} %collective-permute-done.4.refs_6_), channel_id=1, source_target_pairs={{2,3},{3,2},{4,5},{5,4},{10,11},{11,10},{12,13},{13,12},{18,19},{1... | collective-permute-start | bytes 3145736 | tf_op jit(solution)/shard_map/ppermute | solution.py:336
  28.3 31.6 %collective-permute-start.5 = (bf16[2048,256]{1,0:T(8,128)(2,1)}, bf16[2048,256]{1,0:T(8,128)(2,1)}, u32[]{:S(2)}, u32[]{:S(2)}) collective-permute-start(bf16[2048,256]{1,0:T(8,128)(2,1)} %collective-permute-done.4.refs_6_), channel_id=1, source_target_pairs={{0,4},{1,5},{2,6},{3,7},{4,0},{5,1},{6,2},{7,3},{8,12},{9,13},{10,... | collective-permute-start | bytes 3145736 | tf_op jit(solution)/shard_map/ppermute | solution.py:336
  49.2 10.7 %collective-permute-start.13 = (bf16[256,2048]{1,0:T(8,128)(2,1)}, bf16[256,2048]{1,0:T(8,128)(2,1)}, u32[]{:S(2)}, u32[]{:S(2)}) collective-permute-start(bf16[256,2048]{1,0:T(8,128)(2,1)} %collective-permute-done.11.d1), channel_id=1, source_target_pairs={{2,3},{3,2},{4,5},{5,4},{10,11},{11,10},{12,13},{13,12},{18,19},{1... | collective-permute-start | bytes 3145736 | tf_op jit(solution)/shard_map/ppermute | solution.py:336
  50.8 33.0 %collective-permute-start.10 = (bf16[256,2048]{1,0:T(8,128)(2,1)}, bf16[256,2048]{1,0:T(8,128)(2,1)}, u32[]{:S(2)}, u32[]{:S(2)}) collective-permute-start(bf16[256,2048]{1,0:T(8,128)(2,1)} %bitcast.23), channel_id=1, source_target_pairs={{0,4},{1,5},{2,6},{3,7},{4,0},{5,1},{6,2},{7,3},{8,12},{9,13},{10,... | collective-permute-start | bytes 3145736 | tf_op jit(solution)/shard_map/ppermute | solution.py:336
  50.8 29.0 %collective-permute-start.7 = (bf16[2048,256]{1,0:T(8,128)(2,1)}, bf16[2048,256]{1,0:T(8,128)(2,1)}, u32[]{:S(2)}, u32[]{:S(2)}) collective-permute-start(bf16[2048,256]{1,0:T(8,128)(2,1)} %collective-permute-done.6.gb), channel_id=1, source_target_pairs={{0,4},{1,5},{2,6},{3,7},{4,0},{5,1},{6,2},{7,3},{8,12},{9,13},{10,... | collective-permute-start | bytes 3145736 | tf_op jit(solution)/shard_map/ppermute | solution.py:336
  51.3 28.5 %collective-permute-start.9 = (bf16[2048,256]{1,0:T(8,128)(2,1)}, bf16[2048,256]{1,0:T(8,128)(2,1)}, u32[]{:S(2)}, u32[]{:S(2)}) collective-permute-start(bf16[2048,256]{1,0:T(8,128)(2,1)} %collective-permute-done.8.ub), channel_id=1, source_target_pairs={{0,4},{1,5},{2,6},{3,7},{4,0},{5,1},{6,2},{7,3},{8,12},{9,13},{10,... | collective-permute-start | bytes 3145736 | tf_op jit(solution)/shard_map/ppermute | solution.py:336
  59.9 23.9 %collective-permute-start.12 = (bf16[256,2048]{1,0:T(8,128)(2,1)}, bf16[256,2048]{1,0:T(8,128)(2,1)}, u32[]{:S(2)}, u32[]{:S(2)}) collective-permute-start(bf16[256,2048]{1,0:T(8,128)(2,1)} %collective-permute-done.11.d1), channel_id=1, source_target_pairs={{0,4},{1,5},{2,6},{3,7},{4,0},{5,1},{6,2},{7,3},{8,12},{9,13},{10,... | collective-permute-start | bytes 3145736 | tf_op jit(solution)/shard_map/ppermute | solution.py:336
  59.9 23.9 %collective-permute-start.14 = (bf16[256,2048]{1,0:T(8,128)(2,1)}, bf16[256,2048]{1,0:T(8,128)(2,1)}, u32[]{:S(2)}, u32[]{:S(2)}) collective-permute-start(bf16[256,2048]{1,0:T(8,128)(2,1)} %collective-permute-done.13.d3b), channel_id=1, source_target_pairs={{0,4},{1,5},{2,6},{3,7},{4,0},{5,1},{6,2},{7,3},{8,12},{9,13},{10,... | collective-permute-start | bytes 3145736 | tf_op jit(solution)/shard_map/ppermute | solution.py:336
  79.8 4.0 %copy-start = (bf16[768,768]{1,0:T(8,128)(2,1)S(1)}, bf16[768,768]{1,0:T(8,128)(2,1)}, u32[]{:S(2)}) copy-start(bf16[768,768]{1,0:T(8,128)(2,1)} %early_hidden.1.early_ref) | copy-start | bytes 3538948
  90.6 10.6 %copy-start.3 = (s32[768,2]{0,1:T(2,128)S(1)}, s32[768,2]{0,1:T(2,128)}, u32[]{:S(2)}) copy-start(s32[768,2]{0,1:T(2,128)} %param.10) | copy-start | bytes 18436
  90.7 11.5 %copy-start.4 = (f32[768,2]{0,1:T(2,128)S(1)}, f32[768,2]{0,1:T(2,128)}, u32[]{:S(2)}) copy-start(f32[768,2]{0,1:T(2,128)} %param.11) | copy-start | bytes 18436
  90.7 51.6 %all-to-all-start.1 = ((bf16[128,24,512]{2,1,0:T(8,128)(2,1)}), bf16[128,24,512]{2,1,0:T(8,128)(2,1)S(1)}, u32[]{:S(2)}, u32[]{:S(2)}) async-start(bf16[128,24,512]{2,1,0:T(8,128)(2,1)} %bitcast.15), calls=%async_computation.1 | async-start | bytes 6291456 | tf_op jit(solution)/shard_map/all_to_all | solution.py:361
  103.1 1.0 copy-start.1
  104.1 1.0 copy-start.2
  142.3 13.9 %copy-start.5 = (f32[512]{0:T(512)S(1)}, f32[512]{0:T(512)}, u32[]{:S(2)}) copy-start(f32[512]{0:T(512)} %param.15) | copy-start | bytes 6148
  148.6 3.7 %collective-permute-start.17 = (f32[768]{0:T(1024)S(1)}, f32[768]{0:T(1024)S(1)}, u32[]{:S(2)}, u32[]{:S(2)}) collective-permute-start(f32[768]{0:T(1024)S(1)} %reduce), channel_id=1, source_target_pairs={{0,3},{1,0},{2,1},{3,2},{4,7},{5,4},{6,5},{7,6},{8,11},{9,8},{10,9... | collective-permute-start | bytes 9224 | tf_op jit(solution)/shard_map/ppermute | solution.py:369
  150.4 5.1 %collective-permute-start.16 = (f32[768]{0:T(1024)S(1)}, f32[768]{0:T(1024)S(1)}, u32[]{:S(2)}, u32[]{:S(2)}) collective-permute-start(f32[768]{0:T(1024)S(1)} %reduce), channel_id=1, source_target_pairs={{0,2},{1,3},{2,0},{3,1},{4,6},{5,7},{6,4},{7,5},{8,10},{9,11},{10,... | collective-permute-start | bytes 9224 | tf_op jit(solution)/shard_map/ppermute | solution.py:369
  151.4 4.8 %collective-permute-start.15 = (f32[768]{0:T(1024)S(1)}, f32[768]{0:T(1024)S(1)}, u32[]{:S(2)}, u32[]{:S(2)}) collective-permute-start(f32[768]{0:T(1024)S(1)} %reduce), channel_id=1, source_target_pairs={{0,1},{1,2},{2,3},{3,0},{4,5},{5,6},{6,7},{7,4},{8,9},{9,10},{10,1... | collective-permute-start | bytes 9224 | tf_op jit(solution)/shard_map/ppermute | solution.py:369

commit v5 on v4

--- a/solution.py
+++ b/solution.py
@@ -131,34 +131,70 @@
     return (gate_acts / (1.0 + jnp.exp(-gate_acts)) * acts[:, part:]).astype(jnp.bfloat16)
 
 
-def early_kernel(place_ref, rows_ref, *refs):
-    gates, ups = refs[:4], refs[4:8]
-    out_ref, weights, sems = refs[8:]
+def halves_of(width):
+    return ((0, width // 2), (width // 2, width // 2))
+
+
+def split_block(rows_ref, weights, waits):
+    acts = None
+    for (lo, size), wait in zip(halves_of(rows_ref.shape[1]), waits):
+        wait()
+        term = jnp.dot(
+            rows_ref[:, lo : lo + size], weights[lo : lo + size, :], preferred_element_type=jnp.float32
+        )
+        acts = term if acts is None else acts + term
+    return acts
+
+
+def early_kernel(place_ref, rows_ref, ga, gb, g1, g2, ua, ub, u1, u2, out_ref, weights, sems):
     flag = place_ref[1]
-    part = gates[0].shape[1]
-    for i in range(3):
-        for lo, r, sem in ((0, gates, sems.at[2 * i]), (part, ups, sems.at[2 * i + 1])):
-            dst = weights.at[i, :, pl.ds(lo, part)]
-            if i == 0:
-                start_one(flag, r[0], r[1], dst, sem)
-            else:
-                pltpu.make_async_copy(r[i + 1], dst, sem).start()
-    for i in range(3):
-        pltpu.make_async_copy(gates[2], weights.at[i, :, pl.ds(0, part)], sems.at[2 * i]).wait()
-        pltpu.make_async_copy(ups[2], weights.at[i, :, pl.ds(part, part)], sems.at[2 * i + 1]).wait()
-        acts = jnp.dot(rows_ref[...], weights[i], preferred_element_type=jnp.float32)
-        out_ref[:, i * part : (i + 1) * part] = activation(acts, part)
+    width, part = g1.shape
+
+    def plain(at, lo, size, gate, up):
+        for n, source in enumerate((gate, up)):
+            yield (
+                source.at[pl.ds(lo, size)],
+                weights.at[at, pl.ds(lo, size), pl.ds(n * part, part)],
+            )
+
+    def wait_for(at, lo, size, sem):
+        for n, (source, target) in enumerate(plain(at, lo, size, g1, u1)):
+            pltpu.make_async_copy(source, target, sems.at[sem + n]).wait()
+
+    for half, (lo, size) in enumerate(halves_of(width)):
+        for n, (source, target) in enumerate(plain(0, lo, size, g1, u1)):
+            pltpu.make_async_copy(source, target, sems.at[2 * half + n]).start()
+    for n, (source, target) in enumerate(plain(1, 0, width, g2, u2)):
+        pltpu.make_async_copy(source, target, sems.at[4 + n]).start()
+    start_one(flag, ga, gb, weights.at[2, :, pl.ds(0, part)], sems.at[6])
+    start_one(flag, ua, ub, weights.at[2, :, pl.ds(part, part)], sems.at[7])
+    waits = [
+        functools.partial(wait_for, 0, lo, size, 2 * half) for half, (lo, size) in enumerate(halves_of(width))
+    ]
+    out_ref[:, part : 2 * part] = activation(split_block(rows_ref, weights.at[0], waits), part)
+    for at, out in ((1, 2), (2, 0)):
+        wait_for(at, 0, width, 2 + 2 * at)
+        acts = jnp.dot(rows_ref[...], weights[at], preferred_element_type=jnp.float32)
+        out_ref[:, out * part : (out + 1) * part] = activation(acts, part)
 
 
 def middle_kernel(place_ref, rows_ref, ga, gb, ua, ub, out_ref, weights, sems):
     flag = place_ref[1]
-    part = ga.shape[1]
-    start_one(flag, ga, gb, weights.at[:, pl.ds(0, part)], sems.at[0])
-    start_one(flag, ua, ub, weights.at[:, pl.ds(part, part)], sems.at[1])
-    pltpu.make_async_copy(ga, weights.at[:, pl.ds(0, part)], sems.at[0]).wait()
-    pltpu.make_async_copy(ua, weights.at[:, pl.ds(part, part)], sems.at[1]).wait()
-    acts = jnp.dot(rows_ref[...], weights[...], preferred_element_type=jnp.float32)
-    out_ref[...] = activation(acts, part)
+    width, part = ga.shape
+
+    def target(lo, size, n):
+        return weights.at[pl.ds(lo, size), pl.ds(n * part, part)]
+
+    def wait_for(half, lo, size):
+        for n in range(2):
+            pltpu.make_async_copy(ga.at[pl.ds(lo, size)], target(lo, size, n), sems.at[2 * half + n]).wait()
+
+    waits = []
+    for half, (lo, size) in enumerate(halves_of(width)):
+        for n, (a, b) in enumerate(((ga, gb), (ua, ub))):
+            start_one(flag, a.at[pl.ds(lo, size)], b.at[pl.ds(lo, size)], target(lo, size, n), sems.at[2 * half + n])
+        waits.append(functools.partial(wait_for, half, lo, size))
+    out_ref[...] = activation(split_block(rows_ref, weights, waits), part)
 
 
 HBM = pl.BlockSpec(memory_space=pltpu.HBM)
@@ -174,8 +210,8 @@
         early_kernel,
         in_specs=[SMEM, VMEM] + [ANY] * 8,
         out_specs=VMEM,
-        scratch_shapes=[pltpu.VMEM((3, width, 2 * part), jnp.bfloat16), pltpu.SemaphoreType.DMA((6,))],
-        out_shape=jax.ShapeDtypeStruct((count, 3 * part), jnp.bfloat16),
+        scratch_shapes=[pltpu.VMEM((3, width, 2 * part), jnp.bfloat16), pltpu.SemaphoreType.DMA((8,))],
+        out_shape=pltpu.VMEM((count, 3 * part), jnp.bfloat16),
         compiler_params=pltpu.CompilerParams(vmem_limit_bytes=50 * MIB),
         name="early_hidden",
     )(place, rows, *gates, *ups)
@@ -188,41 +224,49 @@
         middle_kernel,
         in_specs=[SMEM, VMEM] + [ANY] * 4,
         out_specs=VMEM,
-        scratch_shapes=[pltpu.VMEM((width, 2 * part), jnp.bfloat16), pltpu.SemaphoreType.DMA((2,))],
+        scratch_shapes=[pltpu.VMEM((width, 2 * part), jnp.bfloat16), pltpu.SemaphoreType.DMA((4,))],
         out_shape=jax.ShapeDtypeStruct((count, part), jnp.bfloat16),
         compiler_params=pltpu.CompilerParams(vmem_limit_bytes=50 * MIB),
         name="middle_hidden",
     )(place, rows, *gates, *ups)
 
 
-def late_kernel(place_ref, early_ref, middle_ref, d0a, d0b, d1, d2, d3a, d3b, out_ref, down, hidden, out, sems, out_sems):
+def late_kernel(place_ref, early_ref, middle_ref, d0a, d0b, d1, d2, d3a, d3b, out_ref, down, hidden, out, sems, out_sems, *, cuts):
     flag = place_ref[1]
     senders, pieces, slots, piece = out_ref.shape
     part = d1.shape[0]
+    size = piece // cuts
+    steps = pieces * cuts
 
     def target(i, f):
-        return down.at[pl.ds(i * part, part), pl.ds(f * piece, piece)]
+        return down.at[pl.ds(i * part, part), pl.ds(f * size, size)]
 
     def source(ref, f):
-        return ref.at[:, pl.ds(f * piece, piece)]
-
-    for f in range(pieces):
-        start_one(flag, source(d0a, f), source(d0b, f), target(0, f), sems.at[4 * f])
+        return ref.at[:, pl.ds(f * size, size)]
+
+    for f in range(steps):
         pltpu.make_async_copy(source(d1, f), target(1, f), sems.at[4 * f + 1]).start()
         pltpu.make_async_copy(source(d2, f), target(2, f), sems.at[4 * f + 2]).start()
+        start_one(flag, source(d0a, f), source(d0b, f), target(0, f), sems.at[4 * f])
         start_one(flag, source(d3a, f), source(d3b, f), target(3, f), sems.at[4 * f + 3])
     hidden[:, 0 : 3 * part] = early_ref[...]
     hidden[:, 3 * part : 4 * part] = middle_ref[...]
-    for f in range(pieces):
+
+    def store(f):
+        return pltpu.make_async_copy(
+            out.at[f], out_ref.at[:, f // cuts, :, pl.ds(f % cuts * size, size)], out_sems.at[f]
+        )
+
+    for f in range(steps):
         for i in range(4):
             pltpu.make_async_copy(source(d1, f), target(i, f), sems.at[4 * f + i]).wait()
         value = jnp.dot(
-            hidden[...], down[:, f * piece : (f + 1) * piece], preferred_element_type=jnp.float32
-        )
-        out[f] = value.reshape(senders, slots, piece).astype(jnp.bfloat16)
-        pltpu.make_async_copy(out.at[f], out_ref.at[:, f], out_sems.at[f]).start()
-    for f in range(pieces):
-        pltpu.make_async_copy(out.at[f], out_ref.at[:, f], out_sems.at[f]).wait()
+            hidden[...], down[:, f * size : (f + 1) * size], preferred_element_type=jnp.float32
+        )
+        out[f] = value.reshape(senders, slots, size).astype(jnp.bfloat16)
+        store(f).start()
+    for f in range(steps):
+        store(f).wait()
 
 
 def late_outputs(place, early, middle, downs, senders, pieces):
@@ -231,16 +275,17 @@
     slots = count // senders
     piece = width // pieces
     shape = (senders, pieces, slots, piece)
-    return pl.pallas_call(
-        late_kernel,
+    cuts = 2
+    return pl.pallas_call(
+        functools.partial(late_kernel, cuts=cuts),
         in_specs=[SMEM, VMEM, VMEM] + [ANY] * 6,
         out_specs=HBM,
         scratch_shapes=[
             pltpu.VMEM((4 * part, width), jnp.bfloat16),
             pltpu.VMEM((count, 4 * part), jnp.bfloat16),
-            pltpu.VMEM((pieces, senders, slots, piece), jnp.bfloat16),
-            pltpu.SemaphoreType.DMA((4 * pieces,)),
-            pltpu.SemaphoreType.DMA((pieces,)),
+            pltpu.VMEM((pieces * cuts, senders, slots, piece // cuts), jnp.bfloat16),
+            pltpu.SemaphoreType.DMA((4 * pieces * cuts,)),
+            pltpu.SemaphoreType.DMA((pieces * cuts,)),
         ],
         out_shape=pltpu.HBM(shape, jnp.bfloat16),
         compiler_params=pltpu.CompilerParams(vmem_limit_bytes=50 * MIB),
@@ -309,12 +354,35 @@
         in_specs=[VMEM, VMEM],
         out_specs=[VMEM, VMEM],
         out_shape=[
-            jax.ShapeDtypeStruct((count, piece), jnp.float32),
+            pltpu.VMEM((count, piece), jnp.float32),
             jax.ShapeDtypeStruct((1, count), jnp.float32),
         ],
-        compiler_params=pltpu.CompilerParams(vmem_limit_bytes=50 * MIB),
+        compiler_params=pltpu.CompilerParams(vmem_limit_bytes=32 * MIB),
         name="combine",
     )(table, returned)
+
+
+def scale_kernel(combined_ref, own_ref, a_ref, b_ref, c_ref, gain_ref, out_ref, *, width):
+    total = own_ref[...] + a_ref[...] + b_ref[...] + c_ref[...]
+    factor = lax.rsqrt(total / width + epsilon)
+    count, piece = combined_ref.shape
+    lanes = 128
+    column = jnp.broadcast_to(factor, (lanes, count)).T
+    for i in range(piece // lanes):
+        at = slice(i * lanes, (i + 1) * lanes)
+        out_ref[:, at] = (combined_ref[:, at] * column * gain_ref[:, at]).astype(jnp.bfloat16)
+
+
+def scale(combined, squares, gain, width):
+    count, piece = combined.shape
+    return pl.pallas_call(
+        functools.partial(scale_kernel, width=width),
+        in_specs=[VMEM] * 6,
+        out_specs=VMEM,
+        out_shape=jax.ShapeDtypeStruct((count, piece), jnp.bfloat16),
+        compiler_params=pltpu.CompilerParams(vmem_limit_bytes=16 * MIB),
+        name="scale",
+    )(combined, *squares, gain)
 
 
 def per_device(
@@ -353,7 +421,7 @@
         buffer.reshape(count_ep, rows, full_width), "ep", split_axis=0, concat_axis=0, tiled=True
     ).reshape(count_ep * rows, full_width)
     received = in_vmem(received)
-    early = in_vmem(early_hidden(place, received, (*gate[0], gate[1], gate[2]), (*up[0], up[1], up[2])))
+    early = early_hidden(place, received, (*gate[0], gate[1], gate[2]), (*up[0], up[1], up[2]))
     middle = in_vmem(middle_hidden(place, received, gate[3], up[3]))
     outputs = late_outputs(
         place, early, middle, (*down[0], down[1], down[2], *down[3]), count_ep, count_tp
@@ -363,14 +431,11 @@
     ).reshape(count_ep * count_tp * rows, part_width)
     table = routing_table(route_ids, route_scores, rows, count_tp)
     combined, squares = combine(table, in_vmem(returned))
-    squares = squares[0]
-    total = squares
-    for shift in range(1, count_tp):
-        total = total + lax.ppermute(
-            squares, "tp", [(i, (i + shift) % count_tp) for i in range(count_tp)]
-        )
-    scaled = combined * lax.rsqrt(total[:, None] / full_width + epsilon) * out_gain
-    return scaled.astype(jnp.bfloat16)
+    parts = [squares] + [
+        lax.ppermute(squares, "tp", [(i, (i + shift) % count_tp) for i in range(count_tp)])
+        for shift in range(1, count_tp)
+    ]
+    return scale(combined, parts, out_gain[None, :], full_width)
 
 
 def solution(mesh):

time: 159 us -> 159 us (level)
  Pallas kernels: 35 us -> 37.9 us
  other arithmetic: 2.59 us -> 0.61 us
  waiting for transfers between devices: 63.3 us -> 61.4 us
    pallas_call x1 -> x2, Pallas kernels: 6.84 us -> 11.7 us  [the longest x1 10.5 us: late_outputs(): pl.pallas_call(functools.partial(late_kernel, cuts=cuts), in_specs=[SMEM,...]
    convert_element_type x1 -> x0, other arithmetic: 2.49 us -> none  [per_device(): return scaled.astype(jnp.bfloat16)]
    ppermute x3, waiting for transfers between devices: 4.79 us -> 2.9 us  [per_device(): lax.ppermute(squares, 'tp', [(i, (i + shift) % count_tp) for i in range(c...]
  transfers between devices with their start and end apart: 20 -> 20, of which waited for: 6 -> 6; matrix products, arithmetic and copies ran while one was open for 1% -> 2% of each run, Pallas kernels for 14% -> 13%
where the time goes in v5:
time: 159 us
  waiting for transfers between devices  61.4 us (39%)
  starting transfers between devices  54.9 us (35%)
  Pallas kernels  37.9 us (24%)
  local copies, waits for them, and re-layouts  3.88 us (2%)
    all_to_all x1, waiting for transfers between devices, per_device(): lax.all_to_all(outputs.reshape(count_ep * count_tp, rows, part_width), AX...  35 us
    ppermute x15, starting transfers between devices, send(): return lax.ppermute(weight, AXES, pairs)  31.6 us
    ppermute x15, waiting for transfers between devices, send(): return lax.ppermute(weight, AXES, pairs)  23.5 us
    all_to_all x1, starting transfers between devices, per_device(): lax.all_to_all(outputs.reshape(count_ep * count_tp, rows, part_width), AX...  10.6 us
    pallas_call x1, Pallas kernels, late_outputs(): pl.pallas_call(functools.partial(late_kernel, cuts=cuts), in_specs=[SMEM,...  10.5 us
    all_to_all x1, starting transfers between devices, per_device(): lax.all_to_all(buffer.reshape(count_ep, rows, full_width), 'ep', split_ax...  8.89 us
    pallas_call x1, Pallas kernels, early_hidden(): pl.pallas_call(early_kernel, in_specs=[SMEM, VMEM] + [ANY] * 8, out_specs...  7.81 us
    pallas_call x1, Pallas kernels, dispatch_buffer(): pl.pallas_call(functools.partial(dispatch_kernel, rows=rows, chunks=chunk...  7.14 us
  transfers between devices with their start and end apart: 20, of which 6 were waited for; matrix products, arithmetic and copies ran while one was open for 2% of the time, Pallas kernels for 13%

profile of v5, /device:TPU:0, one launch (start us, length us, event | category | flops | bytes accessed | tf_op | source)
XLA Modules:
  0.0 158.9 jit_solution(16026448914379517715)
XLA Ops:
  0.0 1.6 %collective-permute-start.1 = (bf16[2048,256]{1,0:T(8,128)(2,1)}, bf16[2048,256]{1,0:T(8,128)(2,1)}, u32[]{:S(2)}, u32[]{:S(2)}) collective-permute-start(bf16[2048,256]{1,0:T(8,128)(2,1)} %bitcast.18), channel_id=1, source_target_pairs={{0,1},{1,0},{2,5},{3,4},{4,3},{5,2},{6,7},{7,6},{8,9},{9,8},{10,13... | collective-permute-start | bytes 3145736 | tf_op jit(solution)/shard_map/ppermute | solution.py:404
  1.6 1.4 collective-permute-start
  3.0 0.2 collective-permute-start.4
  3.2 0.2 collective-permute-start.3
  3.4 1.6 %collective-permute-start.11 = (bf16[256,2048]{1,0:T(8,128)(2,1)}, bf16[256,2048]{1,0:T(8,128)(2,1)}, u32[]{:S(2)}, u32[]{:S(2)}) collective-permute-start(bf16[256,2048]{1,0:T(8,128)(2,1)} %bitcast.24), channel_id=1, source_target_pairs={{0,1},{1,0},{2,5},{3,4},{4,3},{5,2},{6,7},{7,6},{8,9},{9,8},{10,13... | collective-permute-start | bytes 3145736 | tf_op jit(solution)/shard_map/ppermute | solution.py:404
  5.0 7.1 %dispatch_buffer.1 = bf16[768,2048]{1,0:T(8,128)(2,1)} custom-call(s32[2,768]{1,0:T(2,128)} %bitcast.27, f32[1,2048]{1,0:T(1,128)} %bitcast.28, bf16[768,2048]{1,0:T(8,128)(2,1)} %tokens_ref.1), custom_call_target="tpu_custom_call" | custom-call | tf_op jit(solution)/shard_map/dispatch_buffer/pallas_call | solution.py:99
  12.2 8.9 %all-to-all-start = ((bf16[32,24,2048]{2,1,0:T(8,128)(2,1)}), bf16[32,24,2048]{2,1,0:T(8,128)(2,1)S(1)}, u32[]{:S(2)}, u32[]{:S(2)}) async-start(bf16[32,24,2048]{2,1,0:T(8,128)(2,1)} %bitcast.16), calls=%async_computation | async-start | bytes 6291456 | tf_op jit(solution)/shard_map/all_to_all | solution.py:420
  21.1 0.0 collective-permute-done.1.g1
  21.1 0.4 collective-permute-start.2
  21.4 0.0 collective-permute-done.gb
  21.4 1.7 %collective-permute-start.6 = (bf16[2048,256]{1,0:T(8,128)(2,1)}, bf16[2048,256]{1,0:T(8,128)(2,1)}, u32[]{:S(2)}, u32[]{:S(2)}) collective-permute-start(bf16[2048,256]{1,0:T(8,128)(2,1)} %collective-permute-done.1.g1), channel_id=1, source_target_pairs={{2,3},{3,2},{4,5},{5,4},{10,11},{11,10},{12,13},{13,12},{18,19},{1... | collective-permute-start | bytes 3145736 | tf_op jit(solution)/shard_map/ppermute | solution.py:404
  23.1 3.6 %collective-permute-done.4.u1 = bf16[2048,256]{1,0:T(8,128)(2,1)} collective-permute-done((bf16[2048,256]{1,0:T(8,128)(2,1)}, bf16[2048,256]{1,0:T(8,128)(2,1)}, u32[]{:S(2)}, u32[]{:S(2)}) %collective-permute-start.4) | collective-permute-done | bytes 1048608 | tf_op jit(solution)/shard_map/ppermute | solution.py:404
  26.7 1.6 %collective-permute-start.8 = (bf16[2048,256]{1,0:T(8,128)(2,1)}, bf16[2048,256]{1,0:T(8,128)(2,1)}, u32[]{:S(2)}, u32[]{:S(2)}) collective-permute-start(bf16[2048,256]{1,0:T(8,128)(2,1)} %collective-permute-done.4.u1), channel_id=1, source_target_pairs={{2,3},{3,2},{4,5},{5,4},{10,11},{11,10},{12,13},{13,12},{18,19},{1... | collective-permute-start | bytes 3145736 | tf_op jit(solution)/shard_map/ppermute | solution.py:404
  28.3 0.0 collective-permute-done.3.ub
  28.3 0.9 collective-permute-start.5
  29.3 19.9 %collective-permute-done.11.d1 = bf16[256,2048]{1,0:T(8,128)(2,1)} collective-permute-done((bf16[256,2048]{1,0:T(8,128)(2,1)}, bf16[256,2048]{1,0:T(8,128)(2,1)}, u32[]{:S(2)}, u32[]{:S(2)}) %collective-permute-start.11) | collective-permute-done | bytes 1048608 | tf_op jit(solution)/shard_map/ppermute | solution.py:404
  49.2 1.6 %collective-permute-start.13 = (bf16[256,2048]{1,0:T(8,128)(2,1)}, bf16[256,2048]{1,0:T(8,128)(2,1)}, u32[]{:S(2)}, u32[]{:S(2)}) collective-permute-start(bf16[256,2048]{1,0:T(8,128)(2,1)} %collective-permute-done.11.d1), channel_id=1, source_target_pairs={{2,3},{3,2},{4,5},{5,4},{10,11},{11,10},{12,13},{13,12},{18,19},{1... | collective-permute-start | bytes 3145736 | tf_op jit(solution)/shard_map/ppermute | solution.py:404
  50.8 0.0 collective-permute-done.2.g2
  50.8 0.0 collective-permute-done.6.gb
  50.8 0.5 collective-permute-start.7
  51.3 8.6 %collective-permute-start.9 = (bf16[2048,256]{1,0:T(8,128)(2,1)}, bf16[2048,256]{1,0:T(8,128)(2,1)}, u32[]{:S(2)}, u32[]{:S(2)}) collective-permute-start(bf16[2048,256]{1,0:T(8,128)(2,1)} %collective-permute-done.8.ub), channel_id=1, source_target_pairs={{0,4},{1,5},{2,6},{3,7},{4,0},{5,1},{6,2},{7,3},{8,12},{9,13},{10,... | collective-permute-start | bytes 3145736 | tf_op jit(solution)/shard_map/ppermute | solution.py:404
  59.9 0.0 collective-permute-start.12
  59.9 11.2 %collective-permute-start.14 = (bf16[256,2048]{1,0:T(8,128)(2,1)}, bf16[256,2048]{1,0:T(8,128)(2,1)}, u32[]{:S(2)}, u32[]{:S(2)}) collective-permute-start(bf16[256,2048]{1,0:T(8,128)(2,1)} %collective-permute-done.13.d3b), channel_id=1, source_target_pairs={{0,4},{1,5},{2,6},{3,7},{4,0},{5,1},{6,2},{7,3},{8,12},{9,13},{10,... | collective-permute-start | bytes 3145736 | tf_op jit(solution)/shard_map/ppermute | solution.py:404
  71.1 0.6 pad_add_fusion.place_ref
  71.7 7.8 %early_hidden.1.early_ref = bf16[768,768]{1,0:T(8,128)(2,1)S(1)} custom-call(s32[2]{0:T(128)} %pad_add_fusion.place_ref, bf16[768,2048]{1,0:T(8,128)(2,1)S(1)} %bitcast.12, bf16[2048,256]{1,0:T(8,128)(2,1)} %bitcast.20, bf16[2048,256]{1,0:T(8,128)(2,1)} %collective-permute-done.gb, bf16[2048,256]{1,0:T(8,128)(2,1)} %collective-permute-done.1.g1, ...), custom_call_target="tpu_custom_call" | custom-call | tf_op jit(solution)/shard_map/early_hidden/pallas_call | solution.py:209
  79.6 0.0 collective-permute-done.7.ga
  79.6 0.0 collective-permute-done.9.ua
  79.6 3.9 %middle_hidden.1.middle_ref = bf16[768,256]{1,0:T(8,128)(2,1)S(1)} custom-call(s32[2]{0:T(128)S(1)} %copy-done.2, bf16[768,2048]{1,0:T(8,128)(2,1)S(1)} %bitcast.13, bf16[2048,256]{1,0:T(8,128)(2,1)} %collective-permute-done.7.ga, bf16[2048,256]{1,0:T(8,128)(2,1)} %collective-permute-done.6.gb, bf16[2048,256]{1,0:T(8,128)(2,1)} %collective-permute-done.9.ua, ...), custom_call_target="tpu_custom_call" | custom-call | tf_op jit(solution)/shard_map/middle_hidden/pallas_call | solution.py:223
  83.5 0.0 collective-permute-done.10.d0b
  83.5 10.5 %late_outputs.1 = bf16[32,4,24,512]{3,2,1,0:T(8,128)(2,1)} custom-call(s32[2]{0:T(128)S(1)} %copy-done.2, bf16[768,768]{1,0:T(8,128)(2,1)S(1)} %early_hidden.1.early_ref, bf16[768,256]{1,0:T(8,128)(2,1)S(1)} %middle_hidden.1.middle_ref, bf16[256,2048]{1,0:T(8,128)(2,1)} %bitcast.26, bf16[256,2048]{1,0:T(8,128)(2,1)} %collective-permute-done.10.d0b, ...), custom_call_target="tpu_custom_call" | custom-call | tf_op jit(solution)/shard_map/late_outputs/pallas_call | solution.py:279
  94.1 0.0 copy-start.4
  94.1 0.0 copy-start.5
  94.1 10.6 %all-to-all-start.1 = ((bf16[128,24,512]{2,1,0:T(8,128)(2,1)}), bf16[128,24,512]{2,1,0:T(8,128)(2,1)S(1)}, u32[]{:S(2)}, u32[]{:S(2)}) async-start(bf16[128,24,512]{2,1,0:T(8,128)(2,1)} %bitcast.17), calls=%async_computation.1 | async-start | bytes 6291456 | tf_op jit(solution)/shard_map/all_to_all | solution.py:429
  104.7 0.0 copy-start.3
  104.7 0.9 copy.9.ids_ref
  105.6 0.9 copy.10.scores_ref
  106.5 1.0 copy-done
  107.5 1.0 copy-done.1
  108.5 2.2 %columns.1.table_ref = f32[768,4]{1,0:T(8,128)S(1)} custom-call(s32[768,2]{1,0:T(8,128)S(1)} %copy-done, f32[768,2]{1,0:T(8,128)S(1)} %copy-done.1), custom_call_target="tpu_custom_call" | custom-call | tf_op jit(solution)/shard_map/columns/pallas_call | solution.py:320
  110.7 35.0 %all-to-all-done.1 = bf16[128,24,512]{2,1,0:T(8,128)(2,1)S(1)} async-done(((bf16[128,24,512]{2,1,0:T(8,128)(2,1)}), bf16[128,24,512]{2,1,0:T(8,128)(2,1)S(1)}, u32[]{:S(2)}, u32[]{:S(2)}) %all-to-all-start.1) | async-done | bytes 3145760 | tf_op jit(solution)/shard_map/all_to_all | solution.py:429
  145.7 5.2 %combine.1 = (f32[768,512]{1,0:T(8,128)S(1)}, f32[1,768]{1,0:T(1,128)S(1)}) custom-call(f32[768,4]{1,0:T(8,128)S(1)} %columns.1.table_ref, bf16[3072,512]{1,0:T(8,128)(2,1)S(1)} %bitcast.14), custom_call_target="tpu_custom_call" | custom-call | tf_op jit(solution)/shard_map/combine/pallas_call | solution.py:352
  150.9 0.7 collective-permute-start.15
  151.6 2.6 %collective-permute-start.16 = (f32[1,768]{1,0:T(1,128)S(1)}, f32[1,768]{1,0:T(1,128)S(1)}, u32[]{:S(2)}, u32[]{:S(2)}) collective-permute-start(f32[1,768]{1,0:T(1,128)S(1)} %get-tuple-element.8.own_ref), channel_id=1, source_target_pairs={{0,2},{1,3},{2,0},{3,1},{4,6},{5,7},{6,4},{7,5},{8,10},{9,11},{10,... | collective-permute-start | bytes 9224 | tf_op jit(solution)/shard_map/ppermute | solution.py:435
  154.2 0.7 collective-permute-start.17
  154.9 0.9 collective-permute-done.15.a_ref
  155.8 0.9 collective-permute-done.16.b_ref
  156.7 1.1 collective-permute-done.17.c_ref
  157.8 1.1 scale.1
  (14 shorter events, 0.0 us)
Async XLA Ops:
  0.0 21.1 %collective-permute-start.1 = (bf16[2048,256]{1,0:T(8,128)(2,1)}, bf16[2048,256]{1,0:T(8,128)(2,1)}, u32[]{:S(2)}, u32[]{:S(2)}) collective-permute-start(bf16[2048,256]{1,0:T(8,128)(2,1)} %bitcast.18), channel_id=1, source_target_pairs={{0,1},{1,0},{2,5},{3,4},{4,3},{5,2},{6,7},{7,6},{8,9},{9,8},{10,13... | collective-permute-start | bytes 3145736 | tf_op jit(solution)/shard_map/ppermute | solution.py:404
  1.6 19.8 %collective-permute-start = (bf16[2048,256]{1,0:T(8,128)(2,1)}, bf16[2048,256]{1,0:T(8,128)(2,1)}, u32[]{:S(2)}, u32[]{:S(2)}) collective-permute-start(bf16[2048,256]{1,0:T(8,128)(2,1)} %bitcast.19), channel_id=1, source_target_pairs={{0,4},{1,5},{2,6},{3,7},{4,0},{5,1},{6,2},{7,3},{8,12},{9,13},{10,... | collective-permute-start | bytes 3145736 | tf_op jit(solution)/shard_map/ppermute | solution.py:404
  3.0 23.7 %collective-permute-start.4 = (bf16[2048,256]{1,0:T(8,128)(2,1)}, bf16[2048,256]{1,0:T(8,128)(2,1)}, u32[]{:S(2)}, u32[]{:S(2)}) collective-permute-start(bf16[2048,256]{1,0:T(8,128)(2,1)} %bitcast.21), channel_id=1, source_target_pairs={{0,1},{1,0},{2,5},{3,4},{4,3},{5,2},{6,7},{7,6},{8,9},{9,8},{10,13... | collective-permute-start | bytes 3145736 | tf_op jit(solution)/shard_map/ppermute | solution.py:404
  3.2 25.1 %collective-permute-start.3 = (bf16[2048,256]{1,0:T(8,128)(2,1)}, bf16[2048,256]{1,0:T(8,128)(2,1)}, u32[]{:S(2)}, u32[]{:S(2)}) collective-permute-start(bf16[2048,256]{1,0:T(8,128)(2,1)} %bitcast.22), channel_id=1, source_target_pairs={{0,4},{1,5},{2,6},{3,7},{4,0},{5,1},{6,2},{7,3},{8,12},{9,13},{10,... | collective-permute-start | bytes 3145736 | tf_op jit(solution)/shard_map/ppermute | solution.py:404
  3.4 45.8 %collective-permute-start.11 = (bf16[256,2048]{1,0:T(8,128)(2,1)}, bf16[256,2048]{1,0:T(8,128)(2,1)}, u32[]{:S(2)}, u32[]{:S(2)}) collective-permute-start(bf16[256,2048]{1,0:T(8,128)(2,1)} %bitcast.24), channel_id=1, source_target_pairs={{0,1},{1,0},{2,5},{3,4},{4,3},{5,2},{6,7},{7,6},{8,9},{9,8},{10,13... | collective-permute-start | bytes 3145736 | tf_op jit(solution)/shard_map/ppermute | solution.py:404
  12.2 59.6 %all-to-all-start = ((bf16[32,24,2048]{2,1,0:T(8,128)(2,1)}), bf16[32,24,2048]{2,1,0:T(8,128)(2,1)S(1)}, u32[]{:S(2)}, u32[]{:S(2)}) async-start(bf16[32,24,2048]{2,1,0:T(8,128)(2,1)} %bitcast.16), calls=%async_computation | async-start | bytes 6291456 | tf_op jit(solution)/shard_map/all_to_all | solution.py:420
  21.1 29.7 %collective-permute-start.2 = (bf16[2048,256]{1,0:T(8,128)(2,1)}, bf16[2048,256]{1,0:T(8,128)(2,1)}, u32[]{:S(2)}, u32[]{:S(2)}) collective-permute-start(bf16[2048,256]{1,0:T(8,128)(2,1)} %collective-permute-done.1.g1), channel_id=1, source_target_pairs={{0,4},{1,5},{2,6},{3,7},{4,0},{5,1},{6,2},{7,3},{8,12},{9,13},{10,... | collective-permute-start | bytes 3145736 | tf_op jit(solution)/shard_map/ppermute | solution.py:404
  21.4 29.4 %collective-permute-start.6 = (bf16[2048,256]{1,0:T(8,128)(2,1)}, bf16[2048,256]{1,0:T(8,128)(2,1)}, u32[]{:S(2)}, u32[]{:S(2)}) collective-permute-start(bf16[2048,256]{1,0:T(8,128)(2,1)} %collective-permute-done.1.g1), channel_id=1, source_target_pairs={{2,3},{3,2},{4,5},{5,4},{10,11},{11,10},{12,13},{13,12},{18,19},{1... | collective-permute-start | bytes 3145736 | tf_op jit(solution)/shard_map/ppermute | solution.py:404
  26.7 24.6 %collective-permute-start.8 = (bf16[2048,256]{1,0:T(8,128)(2,1)}, bf16[2048,256]{1,0:T(8,128)(2,1)}, u32[]{:S(2)}, u32[]{:S(2)}) collective-permute-start(bf16[2048,256]{1,0:T(8,128)(2,1)} %collective-permute-done.4.u1), channel_id=1, source_target_pairs={{2,3},{3,2},{4,5},{5,4},{10,11},{11,10},{12,13},{13,12},{18,19},{1... | collective-permute-start | bytes 3145736 | tf_op jit(solution)/shard_map/ppermute | solution.py:404
  28.3 31.6 %collective-permute-start.5 = (bf16[2048,256]{1,0:T(8,128)(2,1)}, bf16[2048,256]{1,0:T(8,128)(2,1)}, u32[]{:S(2)}, u32[]{:S(2)}) collective-permute-start(bf16[2048,256]{1,0:T(8,128)(2,1)} %collective-permute-done.4.u1), channel_id=1, source_target_pairs={{0,4},{1,5},{2,6},{3,7},{4,0},{5,1},{6,2},{7,3},{8,12},{9,13},{10,... | collective-permute-start | bytes 3145736 | tf_op jit(solution)/shard_map/ppermute | solution.py:404
  49.2 10.7 %collective-permute-start.13 = (bf16[256,2048]{1,0:T(8,128)(2,1)}, bf16[256,2048]{1,0:T(8,128)(2,1)}, u32[]{:S(2)}, u32[]{:S(2)}) collective-permute-start(bf16[256,2048]{1,0:T(8,128)(2,1)} %collective-permute-done.11.d1), channel_id=1, source_target_pairs={{2,3},{3,2},{4,5},{5,4},{10,11},{11,10},{12,13},{13,12},{18,19},{1... | collective-permute-start | bytes 3145736 | tf_op jit(solution)/shard_map/ppermute | solution.py:404
  50.8 32.7 %collective-permute-start.10 = (bf16[256,2048]{1,0:T(8,128)(2,1)}, bf16[256,2048]{1,0:T(8,128)(2,1)}, u32[]{:S(2)}, u32[]{:S(2)}) collective-permute-start(bf16[256,2048]{1,0:T(8,128)(2,1)} %bitcast.25), channel_id=1, source_target_pairs={{0,4},{1,5},{2,6},{3,7},{4,0},{5,1},{6,2},{7,3},{8,12},{9,13},{10,... | collective-permute-start | bytes 3145736 | tf_op jit(solution)/shard_map/ppermute | solution.py:404
  50.8 28.8 %collective-permute-start.7 = (bf16[2048,256]{1,0:T(8,128)(2,1)}, bf16[2048,256]{1,0:T(8,128)(2,1)}, u32[]{:S(2)}, u32[]{:S(2)}) collective-permute-start(bf16[2048,256]{1,0:T(8,128)(2,1)} %collective-permute-done.6.gb), channel_id=1, source_target_pairs={{0,4},{1,5},{2,6},{3,7},{4,0},{5,1},{6,2},{7,3},{8,12},{9,13},{10,... | collective-permute-start | bytes 3145736 | tf_op jit(solution)/shard_map/ppermute | solution.py:404
  51.3 28.3 %collective-permute-start.9 = (bf16[2048,256]{1,0:T(8,128)(2,1)}, bf16[2048,256]{1,0:T(8,128)(2,1)}, u32[]{:S(2)}, u32[]{:S(2)}) collective-permute-start(bf16[2048,256]{1,0:T(8,128)(2,1)} %collective-permute-done.8.ub), channel_id=1, source_target_pairs={{0,4},{1,5},{2,6},{3,7},{4,0},{5,1},{6,2},{7,3},{8,12},{9,13},{10,... | collective-permute-start | bytes 3145736 | tf_op jit(solution)/shard_map/ppermute | solution.py:404
  59.9 23.6 %collective-permute-start.12 = (bf16[256,2048]{1,0:T(8,128)(2,1)}, bf16[256,2048]{1,0:T(8,128)(2,1)}, u32[]{:S(2)}, u32[]{:S(2)}) collective-permute-start(bf16[256,2048]{1,0:T(8,128)(2,1)} %collective-permute-done.11.d1), channel_id=1, source_target_pairs={{0,4},{1,5},{2,6},{3,7},{4,0},{5,1},{6,2},{7,3},{8,12},{9,13},{10,... | collective-permute-start | bytes 3145736 | tf_op jit(solution)/shard_map/ppermute | solution.py:404
  59.9 23.6 %collective-permute-start.14 = (bf16[256,2048]{1,0:T(8,128)(2,1)}, bf16[256,2048]{1,0:T(8,128)(2,1)}, u32[]{:S(2)}, u32[]{:S(2)}) collective-permute-start(bf16[256,2048]{1,0:T(8,128)(2,1)} %collective-permute-done.13.d3b), channel_id=1, source_target_pairs={{0,4},{1,5},{2,6},{3,7},{4,0},{5,1},{6,2},{7,3},{8,12},{9,13},{10,... | collective-permute-start | bytes 3145736 | tf_op jit(solution)/shard_map/ppermute | solution.py:404
  71.7 7.8 %copy-start.2 = (s32[2]{0:T(128)S(1)}, s32[2]{0:T(128)}, u32[]{:S(2)}) copy-start(s32[2]{0:T(128)} %pad_add_fusion.place_ref) | copy-start | bytes 28
  94.1 10.6 %copy-start.4 = (s32[768,2]{0,1:T(2,128)S(1)}, s32[768,2]{0,1:T(2,128)}, u32[]{:S(2)}) copy-start(s32[768,2]{0,1:T(2,128)} %param.10) | copy-start | bytes 18436
  94.1 11.5 %copy-start.5 = (f32[768,2]{0,1:T(2,128)S(1)}, f32[768,2]{0,1:T(2,128)}, u32[]{:S(2)}) copy-start(f32[768,2]{0,1:T(2,128)} %param.11) | copy-start | bytes 18436
  94.1 51.6 %all-to-all-start.1 = ((bf16[128,24,512]{2,1,0:T(8,128)(2,1)}), bf16[128,24,512]{2,1,0:T(8,128)(2,1)S(1)}, u32[]{:S(2)}, u32[]{:S(2)}) async-start(bf16[128,24,512]{2,1,0:T(8,128)(2,1)} %bitcast.17), calls=%async_computation.1 | async-start | bytes 6291456 | tf_op jit(solution)/shard_map/all_to_all | solution.py:429
  104.7 53.1 %copy-start.3 = (f32[512]{0:T(512)S(1)}, f32[512]{0:T(512)}, u32[]{:S(2)}) copy-start(f32[512]{0:T(512)} %param.15) | copy-start | bytes 6148
  106.5 1.0 copy-start
  107.5 1.0 copy-start.1
  150.9 4.9 %collective-permute-start.15 = (f32[1,768]{1,0:T(1,128)S(1)}, f32[1,768]{1,0:T(1,128)S(1)}, u32[]{:S(2)}, u32[]{:S(2)}) collective-permute-start(f32[1,768]{1,0:T(1,128)S(1)} %get-tuple-element.8.own_ref), channel_id=1, source_target_pairs={{0,1},{1,2},{2,3},{3,0},{4,5},{5,6},{6,7},{7,4},{8,9},{9,10},{10,1... | collective-permute-start | bytes 9224 | tf_op jit(solution)/shard_map/ppermute | solution.py:435
  151.6 5.1 %collective-permute-start.16 = (f32[1,768]{1,0:T(1,128)S(1)}, f32[1,768]{1,0:T(1,128)S(1)}, u32[]{:S(2)}, u32[]{:S(2)}) collective-permute-start(f32[1,768]{1,0:T(1,128)S(1)} %get-tuple-element.8.own_ref), channel_id=1, source_target_pairs={{0,2},{1,3},{2,0},{3,1},{4,6},{5,7},{6,4},{7,5},{8,10},{9,11},{10,... | collective-permute-start | bytes 9224 | tf_op jit(solution)/shard_map/ppermute | solution.py:435
  154.2 3.6 %collective-permute-start.17 = (f32[1,768]{1,0:T(1,128)S(1)}, f32[1,768]{1,0:T(1,128)S(1)}, u32[]{:S(2)}, u32[]{:S(2)}) collective-permute-start(f32[1,768]{1,0:T(1,128)S(1)} %get-tuple-element.8.own_ref), channel_id=1, source_target_pairs={{0,3},{1,0},{2,1},{3,2},{4,7},{5,4},{6,5},{7,6},{8,11},{9,8},{10,9... | collective-permute-start | bytes 9224 | tf_op jit(solution)/shard_map/ppermute | solution.py:435

commit v6 on v5

--- a/solution.py
+++ b/solution.py
@@ -275,7 +275,7 @@
     slots = count // senders
     piece = width // pieces
     shape = (senders, pieces, slots, piece)
-    cuts = 2
+    cuts = 1
     return pl.pallas_call(
         functools.partial(late_kernel, cuts=cuts),
         in_specs=[SMEM, VMEM, VMEM] + [ANY] * 6,
@@ -329,14 +329,10 @@
     total = returned_ref.shape[0]
     count = table_ref.shape[0]
     index = lax.broadcasted_iota(jnp.int32, (count, total), 1)
-    returned = returned_ref[...]
-
-    def picked(choice):
-        row = table_ref[:, choice : choice + 1].astype(jnp.int32)
-        hot = jnp.where(index == row, 1.0, 0.0).astype(jnp.bfloat16)
-        return jnp.dot(hot, returned, preferred_element_type=jnp.float32)
-
-    value = table_ref[:, 2:3] * picked(0) + table_ref[:, 3:4] * picked(1)
+    row = table_ref[:, 0:2].astype(jnp.int32)
+    mix = table_ref[:, 2:4]
+    hot = jnp.where(index == row[:, 0:1], mix[:, 0:1], jnp.where(index == row[:, 1:2], mix[:, 1:2], 0.0))
+    value = jnp.dot(hot.astype(jnp.bfloat16), returned_ref[...], preferred_element_type=jnp.float32)
     out_ref[...] = value
     square = value * value
     lanes = 128

time: 159 us -> 153 us (0.962)
  Pallas kernels: 37.9 us -> 32 us
    pallas_call x1, Pallas kernels: 10.5 us -> 6.76 us  [late_outputs(): pl.pallas_call(functools.partial(late_kernel, cuts=cuts), in_specs=[SMEM,...]
    pallas_call x1, Pallas kernels: 5.22 us -> 3.01 us  [combine(): pl.pallas_call(combine_kernel, in_specs=[VMEM, VMEM], out_specs=[VMEM, VM...]
  transfers between devices with their start and end apart: 20 -> 20, of which waited for: 6 -> 6; matrix products, arithmetic and copies ran while one was open for 2% -> 2% of each run, Pallas kernels for 13% -> 14%
where the time goes in v6:
time: 153 us
  waiting for transfers between devices  61.4 us (40%)
  starting transfers between devices  54.9 us (36%)
  Pallas kernels  32 us (21%)
  local copies, waits for them, and re-layouts  3.88 us (3%)
    all_to_all x1, waiting for transfers between devices, per_device(): lax.all_to_all(outputs.reshape(count_ep * count_tp, rows, part_width), AX...  35 us
    ppermute x15, starting transfers between devices, send(): return lax.ppermute(weight, AXES, pairs)  31.6 us
    ppermute x15, waiting for transfers between devices, send(): return lax.ppermute(weight, AXES, pairs)  23.5 us
    all_to_all x1, starting transfers between devices, per_device(): lax.all_to_all(outputs.reshape(count_ep * count_tp, rows, part_width), AX...  10.6 us
    all_to_all x1, starting transfers between devices, per_device(): lax.all_to_all(buffer.reshape(count_ep, rows, full_width), 'ep', split_ax...  8.89 us
    pallas_call x1, Pallas kernels, early_hidden(): pl.pallas_call(early_kernel, in_specs=[SMEM, VMEM] + [ANY] * 8, out_specs...  7.81 us
    pallas_call x1, Pallas kernels, dispatch_buffer(): pl.pallas_call(functools.partial(dispatch_kernel, rows=rows, chunks=chunk...  7.14 us
    pallas_call x1, Pallas kernels, late_outputs(): pl.pallas_call(functools.partial(late_kernel, cuts=cuts), in_specs=[SMEM,...  6.76 us
  transfers between devices with their start and end apart: 20, of which 6 were waited for; matrix products, arithmetic and copies ran while one was open for 2% of the time, Pallas kernels for 14%

profile of v6, /device:TPU:0, one launch (start us, length us, event | category | flops | bytes accessed | tf_op | source)
XLA Modules:
  0.0 152.9 jit_solution(10994147916236003618)
XLA Ops:
  0.0 1.6 %collective-permute-start.1 = (bf16[2048,256]{1,0:T(8,128)(2,1)}, bf16[2048,256]{1,0:T(8,128)(2,1)}, u32[]{:S(2)}, u32[]{:S(2)}) collective-permute-start(bf16[2048,256]{1,0:T(8,128)(2,1)} %bitcast.18), channel_id=1, source_target_pairs={{0,1},{1,0},{2,5},{3,4},{4,3},{5,2},{6,7},{7,6},{8,9},{9,8},{10,13... | collective-permute-start | bytes 3145736 | tf_op jit(solution)/shard_map/ppermute | solution.py:400
  1.6 1.4 collective-permute-start
  3.0 0.2 collective-permute-start.4
  3.2 0.2 collective-permute-start.3
  3.4 1.6 %collective-permute-start.11 = (bf16[256,2048]{1,0:T(8,128)(2,1)}, bf16[256,2048]{1,0:T(8,128)(2,1)}, u32[]{:S(2)}, u32[]{:S(2)}) collective-permute-start(bf16[256,2048]{1,0:T(8,128)(2,1)} %bitcast.24), channel_id=1, source_target_pairs={{0,1},{1,0},{2,5},{3,4},{4,3},{5,2},{6,7},{7,6},{8,9},{9,8},{10,13... | collective-permute-start | bytes 3145736 | tf_op jit(solution)/shard_map/ppermute | solution.py:400
  5.0 7.1 %dispatch_buffer.1 = bf16[768,2048]{1,0:T(8,128)(2,1)} custom-call(s32[2,768]{1,0:T(2,128)} %bitcast.27, f32[1,2048]{1,0:T(1,128)} %bitcast.28, bf16[768,2048]{1,0:T(8,128)(2,1)} %tokens_ref.1), custom_call_target="tpu_custom_call" | custom-call | tf_op jit(solution)/shard_map/dispatch_buffer/pallas_call | solution.py:99
  12.2 8.9 %all-to-all-start = ((bf16[32,24,2048]{2,1,0:T(8,128)(2,1)}), bf16[32,24,2048]{2,1,0:T(8,128)(2,1)S(1)}, u32[]{:S(2)}, u32[]{:S(2)}) async-start(bf16[32,24,2048]{2,1,0:T(8,128)(2,1)} %bitcast.16), calls=%async_computation | async-start | bytes 6291456 | tf_op jit(solution)/shard_map/all_to_all | solution.py:416
  21.1 0.0 collective-permute-done.1.g1
  21.1 0.4 collective-permute-start.2
  21.4 0.0 collective-permute-done.gb
  21.4 1.7 %collective-permute-start.6 = (bf16[2048,256]{1,0:T(8,128)(2,1)}, bf16[2048,256]{1,0:T(8,128)(2,1)}, u32[]{:S(2)}, u32[]{:S(2)}) collective-permute-start(bf16[2048,256]{1,0:T(8,128)(2,1)} %collective-permute-done.1.g1), channel_id=1, source_target_pairs={{2,3},{3,2},{4,5},{5,4},{10,11},{11,10},{12,13},{13,12},{18,19},{1... | collective-permute-start | bytes 3145736 | tf_op jit(solution)/shard_map/ppermute | solution.py:400
  23.1 3.6 %collective-permute-done.4.u1 = bf16[2048,256]{1,0:T(8,128)(2,1)} collective-permute-done((bf16[2048,256]{1,0:T(8,128)(2,1)}, bf16[2048,256]{1,0:T(8,128)(2,1)}, u32[]{:S(2)}, u32[]{:S(2)}) %collective-permute-start.4) | collective-permute-done | bytes 1048608 | tf_op jit(solution)/shard_map/ppermute | solution.py:400
  26.7 1.6 %collective-permute-start.8 = (bf16[2048,256]{1,0:T(8,128)(2,1)}, bf16[2048,256]{1,0:T(8,128)(2,1)}, u32[]{:S(2)}, u32[]{:S(2)}) collective-permute-start(bf16[2048,256]{1,0:T(8,128)(2,1)} %collective-permute-done.4.u1), channel_id=1, source_target_pairs={{2,3},{3,2},{4,5},{5,4},{10,11},{11,10},{12,13},{13,12},{18,19},{1... | collective-permute-start | bytes 3145736 | tf_op jit(solution)/shard_map/ppermute | solution.py:400
  28.3 0.0 collective-permute-done.3.ub
  28.3 0.9 collective-permute-start.5
  29.3 19.9 %collective-permute-done.11.d1 = bf16[256,2048]{1,0:T(8,128)(2,1)} collective-permute-done((bf16[256,2048]{1,0:T(8,128)(2,1)}, bf16[256,2048]{1,0:T(8,128)(2,1)}, u32[]{:S(2)}, u32[]{:S(2)}) %collective-permute-start.11) | collective-permute-done | bytes 1048608 | tf_op jit(solution)/shard_map/ppermute | solution.py:400
  49.2 1.6 %collective-permute-start.13 = (bf16[256,2048]{1,0:T(8,128)(2,1)}, bf16[256,2048]{1,0:T(8,128)(2,1)}, u32[]{:S(2)}, u32[]{:S(2)}) collective-permute-start(bf16[256,2048]{1,0:T(8,128)(2,1)} %collective-permute-done.11.d1), channel_id=1, source_target_pairs={{2,3},{3,2},{4,5},{5,4},{10,11},{11,10},{12,13},{13,12},{18,19},{1... | collective-permute-start | bytes 3145736 | tf_op jit(solution)/shard_map/ppermute | solution.py:400
  50.8 0.0 collective-permute-done.2.g2
  50.8 0.0 collective-permute-done.6.gb
  50.8 0.5 collective-permute-start.7
  51.3 8.6 %collective-permute-start.9 = (bf16[2048,256]{1,0:T(8,128)(2,1)}, bf16[2048,256]{1,0:T(8,128)(2,1)}, u32[]{:S(2)}, u32[]{:S(2)}) collective-permute-start(bf16[2048,256]{1,0:T(8,128)(2,1)} %collective-permute-done.8.ub), channel_id=1, source_target_pairs={{0,4},{1,5},{2,6},{3,7},{4,0},{5,1},{6,2},{7,3},{8,12},{9,13},{10,... | collective-permute-start | bytes 3145736 | tf_op jit(solution)/shard_map/ppermute | solution.py:400
  59.9 0.0 collective-permute-start.12
  59.9 11.2 %collective-permute-start.14 = (bf16[256,2048]{1,0:T(8,128)(2,1)}, bf16[256,2048]{1,0:T(8,128)(2,1)}, u32[]{:S(2)}, u32[]{:S(2)}) collective-permute-start(bf16[256,2048]{1,0:T(8,128)(2,1)} %collective-permute-done.13.d3b), channel_id=1, source_target_pairs={{0,4},{1,5},{2,6},{3,7},{4,0},{5,1},{6,2},{7,3},{8,12},{9,13},{10,... | collective-permute-start | bytes 3145736 | tf_op jit(solution)/shard_map/ppermute | solution.py:400
  71.1 0.6 pad_add_fusion.place_ref
  71.7 7.8 %early_hidden.1.early_ref = bf16[768,768]{1,0:T(8,128)(2,1)S(1)} custom-call(s32[2]{0:T(128)} %pad_add_fusion.place_ref, bf16[768,2048]{1,0:T(8,128)(2,1)S(1)} %bitcast.12, bf16[2048,256]{1,0:T(8,128)(2,1)} %bitcast.20, bf16[2048,256]{1,0:T(8,128)(2,1)} %collective-permute-done.gb, bf16[2048,256]{1,0:T(8,128)(2,1)} %collective-permute-done.1.g1, ...), custom_call_target="tpu_custom_call" | custom-call | tf_op jit(solution)/shard_map/early_hidden/pallas_call | solution.py:209
  79.6 0.0 collective-permute-done.7.ga
  79.6 0.0 collective-permute-done.9.ua
  79.6 3.9 %middle_hidden.1.middle_ref = bf16[768,256]{1,0:T(8,128)(2,1)S(1)} custom-call(s32[2]{0:T(128)S(1)} %copy-done.2, bf16[768,2048]{1,0:T(8,128)(2,1)S(1)} %bitcast.13, bf16[2048,256]{1,0:T(8,128)(2,1)} %collective-permute-done.7.ga, bf16[2048,256]{1,0:T(8,128)(2,1)} %collective-permute-done.6.gb, bf16[2048,256]{1,0:T(8,128)(2,1)} %collective-permute-done.9.ua, ...), custom_call_target="tpu_custom_call" | custom-call | tf_op jit(solution)/shard_map/middle_hidden/pallas_call | solution.py:223
  83.5 0.0 collective-permute-done.10.d0b
  83.5 6.8 %late_outputs.1 = bf16[32,4,24,512]{3,2,1,0:T(8,128)(2,1)} custom-call(s32[2]{0:T(128)S(1)} %copy-done.2, bf16[768,768]{1,0:T(8,128)(2,1)S(1)} %early_hidden.1.early_ref, bf16[768,256]{1,0:T(8,128)(2,1)S(1)} %middle_hidden.1.middle_ref, bf16[256,2048]{1,0:T(8,128)(2,1)} %bitcast.26, bf16[256,2048]{1,0:T(8,128)(2,1)} %collective-permute-done.10.d0b, ...), custom_call_target="tpu_custom_call" | custom-call | tf_op jit(solution)/shard_map/late_outputs/pallas_call | solution.py:279
  90.3 0.0 copy-start.4
  90.3 0.0 copy-start.5
  90.3 10.6 %all-to-all-start.1 = ((bf16[128,24,512]{2,1,0:T(8,128)(2,1)}), bf16[128,24,512]{2,1,0:T(8,128)(2,1)S(1)}, u32[]{:S(2)}, u32[]{:S(2)}) async-start(bf16[128,24,512]{2,1,0:T(8,128)(2,1)} %bitcast.17), calls=%async_computation.1 | async-start | bytes 6291456 | tf_op jit(solution)/shard_map/all_to_all | solution.py:425
  100.9 0.0 copy-start.3
  100.9 0.9 copy.9.ids_ref
  101.8 0.9 copy.10.scores_ref
  102.8 1.0 copy-done
  103.8 1.0 copy-done.1
  104.8 2.2 %columns.1.table_ref = f32[768,4]{1,0:T(8,128)S(1)} custom-call(s32[768,2]{1,0:T(8,128)S(1)} %copy-done, f32[768,2]{1,0:T(8,128)S(1)} %copy-done.1), custom_call_target="tpu_custom_call" | custom-call | tf_op jit(solution)/shard_map/columns/pallas_call | solution.py:320
  107.0 35.0 %all-to-all-done.1 = bf16[128,24,512]{2,1,0:T(8,128)(2,1)S(1)} async-done(((bf16[128,24,512]{2,1,0:T(8,128)(2,1)}), bf16[128,24,512]{2,1,0:T(8,128)(2,1)S(1)}, u32[]{:S(2)}, u32[]{:S(2)}) %all-to-all-start.1) | async-done | bytes 3145760 | tf_op jit(solution)/shard_map/all_to_all | solution.py:425
  141.9 3.0 %combine.1 = (f32[768,512]{1,0:T(8,128)S(1)}, f32[1,768]{1,0:T(1,128)S(1)}) custom-call(f32[768,4]{1,0:T(8,128)S(1)} %columns.1.table_ref, bf16[3072,512]{1,0:T(8,128)(2,1)S(1)} %bitcast.14), custom_call_target="tpu_custom_call" | custom-call | tf_op jit(solution)/shard_map/combine/pallas_call | solution.py:348
  144.9 0.6 collective-permute-start.15
  145.6 2.6 %collective-permute-start.16 = (f32[1,768]{1,0:T(1,128)S(1)}, f32[1,768]{1,0:T(1,128)S(1)}, u32[]{:S(2)}, u32[]{:S(2)}) collective-permute-start(f32[1,768]{1,0:T(1,128)S(1)} %get-tuple-element.8.own_ref), channel_id=1, source_target_pairs={{0,2},{1,3},{2,0},{3,1},{4,6},{5,7},{6,4},{7,5},{8,10},{9,11},{10,... | collective-permute-start | bytes 9224 | tf_op jit(solution)/shard_map/ppermute | solution.py:431
  148.2 0.7 collective-permute-start.17
  148.9 0.9 collective-permute-done.15.a_ref
  149.8 0.9 collective-permute-done.16.b_ref
  150.7 1.1 collective-permute-done.17.c_ref
  151.8 1.1 scale.1
  (14 shorter events, 0.0 us)
Async XLA Ops:
  0.0 21.1 %collective-permute-start.1 = (bf16[2048,256]{1,0:T(8,128)(2,1)}, bf16[2048,256]{1,0:T(8,128)(2,1)}, u32[]{:S(2)}, u32[]{:S(2)}) collective-permute-start(bf16[2048,256]{1,0:T(8,128)(2,1)} %bitcast.18), channel_id=1, source_target_pairs={{0,1},{1,0},{2,5},{3,4},{4,3},{5,2},{6,7},{7,6},{8,9},{9,8},{10,13... | collective-permute-start | bytes 3145736 | tf_op jit(solution)/shard_map/ppermute | solution.py:400
  1.6 19.8 %collective-permute-start = (bf16[2048,256]{1,0:T(8,128)(2,1)}, bf16[2048,256]{1,0:T(8,128)(2,1)}, u32[]{:S(2)}, u32[]{:S(2)}) collective-permute-start(bf16[2048,256]{1,0:T(8,128)(2,1)} %bitcast.19), channel_id=1, source_target_pairs={{0,4},{1,5},{2,6},{3,7},{4,0},{5,1},{6,2},{7,3},{8,12},{9,13},{10,... | collective-permute-start | bytes 3145736 | tf_op jit(solution)/shard_map/ppermute | solution.py:400
  3.0 23.7 %collective-permute-start.4 = (bf16[2048,256]{1,0:T(8,128)(2,1)}, bf16[2048,256]{1,0:T(8,128)(2,1)}, u32[]{:S(2)}, u32[]{:S(2)}) collective-permute-start(bf16[2048,256]{1,0:T(8,128)(2,1)} %bitcast.21), channel_id=1, source_target_pairs={{0,1},{1,0},{2,5},{3,4},{4,3},{5,2},{6,7},{7,6},{8,9},{9,8},{10,13... | collective-permute-start | bytes 3145736 | tf_op jit(solution)/shard_map/ppermute | solution.py:400
  3.2 25.1 %collective-permute-start.3 = (bf16[2048,256]{1,0:T(8,128)(2,1)}, bf16[2048,256]{1,0:T(8,128)(2,1)}, u32[]{:S(2)}, u32[]{:S(2)}) collective-permute-start(bf16[2048,256]{1,0:T(8,128)(2,1)} %bitcast.22), channel_id=1, source_target_pairs={{0,4},{1,5},{2,6},{3,7},{4,0},{5,1},{6,2},{7,3},{8,12},{9,13},{10,... | collective-permute-start | bytes 3145736 | tf_op jit(solution)/shard_map/ppermute | solution.py:400
  3.4 45.8 %collective-permute-start.11 = (bf16[256,2048]{1,0:T(8,128)(2,1)}, bf16[256,2048]{1,0:T(8,128)(2,1)}, u32[]{:S(2)}, u32[]{:S(2)}) collective-permute-start(bf16[256,2048]{1,0:T(8,128)(2,1)} %bitcast.24), channel_id=1, source_target_pairs={{0,1},{1,0},{2,5},{3,4},{4,3},{5,2},{6,7},{7,6},{8,9},{9,8},{10,13... | collective-permute-start | bytes 3145736 | tf_op jit(solution)/shard_map/ppermute | solution.py:400
  12.2 59.6 %all-to-all-start = ((bf16[32,24,2048]{2,1,0:T(8,128)(2,1)}), bf16[32,24,2048]{2,1,0:T(8,128)(2,1)S(1)}, u32[]{:S(2)}, u32[]{:S(2)}) async-start(bf16[32,24,2048]{2,1,0:T(8,128)(2,1)} %bitcast.16), calls=%async_computation | async-start | bytes 6291456 | tf_op jit(solution)/shard_map/all_to_all | solution.py:416
  21.1 29.7 %collective-permute-start.2 = (bf16[2048,256]{1,0:T(8,128)(2,1)}, bf16[2048,256]{1,0:T(8,128)(2,1)}, u32[]{:S(2)}, u32[]{:S(2)}) collective-permute-start(bf16[2048,256]{1,0:T(8,128)(2,1)} %collective-permute-done.1.g1), channel_id=1, source_target_pairs={{0,4},{1,5},{2,6},{3,7},{4,0},{5,1},{6,2},{7,3},{8,12},{9,13},{10,... | collective-permute-start | bytes 3145736 | tf_op jit(solution)/shard_map/ppermute | solution.py:400
  21.4 29.4 %collective-permute-start.6 = (bf16[2048,256]{1,0:T(8,128)(2,1)}, bf16[2048,256]{1,0:T(8,128)(2,1)}, u32[]{:S(2)}, u32[]{:S(2)}) collective-permute-start(bf16[2048,256]{1,0:T(8,128)(2,1)} %collective-permute-done.1.g1), channel_id=1, source_target_pairs={{2,3},{3,2},{4,5},{5,4},{10,11},{11,10},{12,13},{13,12},{18,19},{1... | collective-permute-start | bytes 3145736 | tf_op jit(solution)/shard_map/ppermute | solution.py:400
  26.7 24.6 %collective-permute-start.8 = (bf16[2048,256]{1,0:T(8,128)(2,1)}, bf16[2048,256]{1,0:T(8,128)(2,1)}, u32[]{:S(2)}, u32[]{:S(2)}) collective-permute-start(bf16[2048,256]{1,0:T(8,128)(2,1)} %collective-permute-done.4.u1), channel_id=1, source_target_pairs={{2,3},{3,2},{4,5},{5,4},{10,11},{11,10},{12,13},{13,12},{18,19},{1... | collective-permute-start | bytes 3145736 | tf_op jit(solution)/shard_map/ppermute | solution.py:400
  28.3 31.6 %collective-permute-start.5 = (bf16[2048,256]{1,0:T(8,128)(2,1)}, bf16[2048,256]{1,0:T(8,128)(2,1)}, u32[]{:S(2)}, u32[]{:S(2)}) collective-permute-start(bf16[2048,256]{1,0:T(8,128)(2,1)} %collective-permute-done.4.u1), channel_id=1, source_target_pairs={{0,4},{1,5},{2,6},{3,7},{4,0},{5,1},{6,2},{7,3},{8,12},{9,13},{10,... | collective-permute-start | bytes 3145736 | tf_op jit(solution)/shard_map/ppermute | solution.py:400
  49.2 10.7 %collective-permute-start.13 = (bf16[256,2048]{1,0:T(8,128)(2,1)}, bf16[256,2048]{1,0:T(8,128)(2,1)}, u32[]{:S(2)}, u32[]{:S(2)}) collective-permute-start(bf16[256,2048]{1,0:T(8,128)(2,1)} %collective-permute-done.11.d1), channel_id=1, source_target_pairs={{2,3},{3,2},{4,5},{5,4},{10,11},{11,10},{12,13},{13,12},{18,19},{1... | collective-permute-start | bytes 3145736 | tf_op jit(solution)/shard_map/ppermute | solution.py:400
  50.8 32.7 %collective-permute-start.10 = (bf16[256,2048]{1,0:T(8,128)(2,1)}, bf16[256,2048]{1,0:T(8,128)(2,1)}, u32[]{:S(2)}, u32[]{:S(2)}) collective-permute-start(bf16[256,2048]{1,0:T(8,128)(2,1)} %bitcast.25), channel_id=1, source_target_pairs={{0,4},{1,5},{2,6},{3,7},{4,0},{5,1},{6,2},{7,3},{8,12},{9,13},{10,... | collective-permute-start | bytes 3145736 | tf_op jit(solution)/shard_map/ppermute | solution.py:400
  50.8 28.8 %collective-permute-start.7 = (bf16[2048,256]{1,0:T(8,128)(2,1)}, bf16[2048,256]{1,0:T(8,128)(2,1)}, u32[]{:S(2)}, u32[]{:S(2)}) collective-permute-start(bf16[2048,256]{1,0:T(8,128)(2,1)} %collective-permute-done.6.gb), channel_id=1, source_target_pairs={{0,4},{1,5},{2,6},{3,7},{4,0},{5,1},{6,2},{7,3},{8,12},{9,13},{10,... | collective-permute-start | bytes 3145736 | tf_op jit(solution)/shard_map/ppermute | solution.py:400
  51.3 28.3 %collective-permute-start.9 = (bf16[2048,256]{1,0:T(8,128)(2,1)}, bf16[2048,256]{1,0:T(8,128)(2,1)}, u32[]{:S(2)}, u32[]{:S(2)}) collective-permute-start(bf16[2048,256]{1,0:T(8,128)(2,1)} %collective-permute-done.8.ub), channel_id=1, source_target_pairs={{0,4},{1,5},{2,6},{3,7},{4,0},{5,1},{6,2},{7,3},{8,12},{9,13},{10,... | collective-permute-start | bytes 3145736 | tf_op jit(solution)/shard_map/ppermute | solution.py:400
  59.9 23.6 %collective-permute-start.12 = (bf16[256,2048]{1,0:T(8,128)(2,1)}, bf16[256,2048]{1,0:T(8,128)(2,1)}, u32[]{:S(2)}, u32[]{:S(2)}) collective-permute-start(bf16[256,2048]{1,0:T(8,128)(2,1)} %collective-permute-done.11.d1), channel_id=1, source_target_pairs={{0,4},{1,5},{2,6},{3,7},{4,0},{5,1},{6,2},{7,3},{8,12},{9,13},{10,... | collective-permute-start | bytes 3145736 | tf_op jit(solution)/shard_map/ppermute | solution.py:400
  59.9 23.6 %collective-permute-start.14 = (bf16[256,2048]{1,0:T(8,128)(2,1)}, bf16[256,2048]{1,0:T(8,128)(2,1)}, u32[]{:S(2)}, u32[]{:S(2)}) collective-permute-start(bf16[256,2048]{1,0:T(8,128)(2,1)} %collective-permute-done.13.d3b), channel_id=1, source_target_pairs={{0,4},{1,5},{2,6},{3,7},{4,0},{5,1},{6,2},{7,3},{8,12},{9,13},{10,... | collective-permute-start | bytes 3145736 | tf_op jit(solution)/shard_map/ppermute | solution.py:400
  71.7 7.8 %copy-start.2 = (s32[2]{0:T(128)S(1)}, s32[2]{0:T(128)}, u32[]{:S(2)}) copy-start(s32[2]{0:T(128)} %pad_add_fusion.place_ref) | copy-start | bytes 28
  90.3 10.6 %copy-start.4 = (s32[768,2]{0,1:T(2,128)S(1)}, s32[768,2]{0,1:T(2,128)}, u32[]{:S(2)}) copy-start(s32[768,2]{0,1:T(2,128)} %param.10) | copy-start | bytes 18436
  90.3 11.5 %copy-start.5 = (f32[768,2]{0,1:T(2,128)S(1)}, f32[768,2]{0,1:T(2,128)}, u32[]{:S(2)}) copy-start(f32[768,2]{0,1:T(2,128)} %param.11) | copy-start | bytes 18436
  90.3 51.6 %all-to-all-start.1 = ((bf16[128,24,512]{2,1,0:T(8,128)(2,1)}), bf16[128,24,512]{2,1,0:T(8,128)(2,1)S(1)}, u32[]{:S(2)}, u32[]{:S(2)}) async-start(bf16[128,24,512]{2,1,0:T(8,128)(2,1)} %bitcast.17), calls=%async_computation.1 | async-start | bytes 6291456 | tf_op jit(solution)/shard_map/all_to_all | solution.py:425
  100.9 50.9 %copy-start.3 = (f32[512]{0:T(512)S(1)}, f32[512]{0:T(512)}, u32[]{:S(2)}) copy-start(f32[512]{0:T(512)} %param.15) | copy-start | bytes 6148
  102.8 1.0 copy-start
  103.8 1.0 copy-start.1
  144.9 4.9 %collective-permute-start.15 = (f32[1,768]{1,0:T(1,128)S(1)}, f32[1,768]{1,0:T(1,128)S(1)}, u32[]{:S(2)}, u32[]{:S(2)}) collective-permute-start(f32[1,768]{1,0:T(1,128)S(1)} %get-tuple-element.8.own_ref), channel_id=1, source_target_pairs={{0,1},{1,2},{2,3},{3,0},{4,5},{5,6},{6,7},{7,4},{8,9},{9,10},{10,1... | collective-permute-start | bytes 9224 | tf_op jit(solution)/shard_map/ppermute | solution.py:431
  145.6 5.1 %collective-permute-start.16 = (f32[1,768]{1,0:T(1,128)S(1)}, f32[1,768]{1,0:T(1,128)S(1)}, u32[]{:S(2)}, u32[]{:S(2)}) collective-permute-start(f32[1,768]{1,0:T(1,128)S(1)} %get-tuple-element.8.own_ref), channel_id=1, source_target_pairs={{0,2},{1,3},{2,0},{3,1},{4,6},{5,7},{6,4},{7,5},{8,10},{9,11},{10,... | collective-permute-start | bytes 9224 | tf_op jit(solution)/shard_map/ppermute | solution.py:431
  148.2 3.6 %collective-permute-start.17 = (f32[1,768]{1,0:T(1,128)S(1)}, f32[1,768]{1,0:T(1,128)S(1)}, u32[]{:S(2)}, u32[]{:S(2)}) collective-permute-start(f32[1,768]{1,0:T(1,128)S(1)} %get-tuple-element.8.own_ref), channel_id=1, source_target_pairs={{0,3},{1,0},{2,1},{3,2},{4,7},{5,4},{6,5},{7,6},{8,11},{9,8},{10,9... | collective-permute-start | bytes 9224 | tf_op jit(solution)/shard_map/ppermute | solution.py:431

commit v7 on v6

--- a/solution.py
+++ b/solution.py
@@ -358,8 +358,8 @@
     )(table, returned)
 
 
-def scale_kernel(combined_ref, own_ref, a_ref, b_ref, c_ref, gain_ref, out_ref, *, width):
-    total = own_ref[...] + a_ref[...] + b_ref[...] + c_ref[...]
+def scale_kernel(combined_ref, pair_ref, other_ref, gain_ref, out_ref, *, width):
+    total = pair_ref[...] + other_ref[...]
     factor = lax.rsqrt(total / width + epsilon)
     count, piece = combined_ref.shape
     lanes = 128
@@ -369,16 +369,16 @@
         out_ref[:, at] = (combined_ref[:, at] * column * gain_ref[:, at]).astype(jnp.bfloat16)
 
 
-def scale(combined, squares, gain, width):
+def scale(combined, pair, other, gain, width):
     count, piece = combined.shape
     return pl.pallas_call(
         functools.partial(scale_kernel, width=width),
-        in_specs=[VMEM] * 6,
+        in_specs=[VMEM] * 4,
         out_specs=VMEM,
         out_shape=jax.ShapeDtypeStruct((count, piece), jnp.bfloat16),
         compiler_params=pltpu.CompilerParams(vmem_limit_bytes=16 * MIB),
         name="scale",
-    )(combined, *squares, gain)
+    )(combined, pair, other, gain)
 
 
 def per_device(
@@ -427,11 +427,9 @@
     ).reshape(count_ep * count_tp * rows, part_width)
     table = routing_table(route_ids, route_scores, rows, count_tp)
     combined, squares = combine(table, in_vmem(returned))
-    parts = [squares] + [
-        lax.ppermute(squares, "tp", [(i, (i + shift) % count_tp) for i in range(count_tp)])
-        for shift in range(1, count_tp)
-    ]
-    return scale(combined, parts, out_gain[None, :], full_width)
+    pair = squares + lax.ppermute(squares, "tp", [(i, i ^ 1) for i in range(count_tp)])
+    other = lax.ppermute(pair, "tp", [(i, count_tp - 1 - i) for i in range(count_tp)])
+    return scale(combined, pair, other, out_gain[None, :], full_width)
 
 
 def solution(mesh):

time: 153 us -> 155 us (1.013)
  waiting for transfers between devices: 61.4 us -> 64.6 us
    ppermute x3 -> x2, waiting for transfers between devices: 2.9 us -> 6.1 us  [the longest x1 3.08 us: per_device(): lax.ppermute(pair, 'tp', [(i, count_tp - 1 - i) for i in range(count_tp)])]
    ppermute x3 -> x2, starting transfers between devices: 3.95 us -> 2.38 us  [the longest x1 1.72 us: per_device(): lax.ppermute(pair, 'tp', [(i, count_tp - 1 - i) for i in range(count_tp)])]
  transfers between devices with their start and end apart: 20 -> 19, of which waited for: 6 -> 5; matrix products, arithmetic and copies ran while one was open for 2% -> 2% of each run, Pallas kernels for 14% -> 14%
where the time goes in v7:
time: 155 us
  waiting for transfers between devices  64.6 us (42%)
  starting transfers between devices  53.4 us (34%)
  Pallas kernels  31.9 us (21%)
  local copies, waits for them, and re-layouts  3.89 us (3%)
    all_to_all x1, waiting for transfers between devices, per_device(): lax.all_to_all(outputs.reshape(count_ep * count_tp, rows, part_width), AX...  35 us
    ppermute x15, starting transfers between devices, send(): return lax.ppermute(weight, AXES, pairs)  31.6 us
    ppermute x15, waiting for transfers between devices, send(): return lax.ppermute(weight, AXES, pairs)  23.5 us
    all_to_all x1, starting transfers between devices, per_device(): lax.all_to_all(outputs.reshape(count_ep * count_tp, rows, part_width), AX...  10.6 us
    all_to_all x1, starting transfers between devices, per_device(): lax.all_to_all(buffer.reshape(count_ep, rows, full_width), 'ep', split_ax...  8.89 us
    pallas_call x1, Pallas kernels, early_hidden(): pl.pallas_call(early_kernel, in_specs=[SMEM, VMEM] + [ANY] * 8, out_specs...  7.8 us
    pallas_call x1, Pallas kernels, dispatch_buffer(): pl.pallas_call(functools.partial(dispatch_kernel, rows=rows, chunks=chunk...  7.14 us
    pallas_call x1, Pallas kernels, late_outputs(): pl.pallas_call(functools.partial(late_kernel, cuts=cuts), in_specs=[SMEM,...  6.75 us
  transfers between devices with their start and end apart: 19, of which 5 were waited for; matrix products, arithmetic and copies ran while one was open for 2% of the time, Pallas kernels for 14%

profile of v7, /device:TPU:0, one launch (start us, length us, event | category | flops | bytes accessed | tf_op | source)
XLA Modules:
  0.0 154.5 jit_solution(10384011393293969754)
XLA Ops:
  0.0 1.6 %collective-permute-start.1 = (bf16[2048,256]{1,0:T(8,128)(2,1)}, bf16[2048,256]{1,0:T(8,128)(2,1)}, u32[]{:S(2)}, u32[]{:S(2)}) collective-permute-start(bf16[2048,256]{1,0:T(8,128)(2,1)} %bitcast.18), channel_id=1, source_target_pairs={{0,1},{1,0},{2,5},{3,4},{4,3},{5,2},{6,7},{7,6},{8,9},{9,8},{10,13... | collective-permute-start | bytes 3145736 | tf_op jit(solution)/shard_map/ppermute | solution.py:400
  1.6 1.4 collective-permute-start
  3.0 0.2 collective-permute-start.4
  3.2 0.2 collective-permute-start.3
  3.4 1.6 %collective-permute-start.11 = (bf16[256,2048]{1,0:T(8,128)(2,1)}, bf16[256,2048]{1,0:T(8,128)(2,1)}, u32[]{:S(2)}, u32[]{:S(2)}) collective-permute-start(bf16[256,2048]{1,0:T(8,128)(2,1)} %bitcast.24), channel_id=1, source_target_pairs={{0,1},{1,0},{2,5},{3,4},{4,3},{5,2},{6,7},{7,6},{8,9},{9,8},{10,13... | collective-permute-start | bytes 3145736 | tf_op jit(solution)/shard_map/ppermute | solution.py:400
  5.0 7.1 %dispatch_buffer.1 = bf16[768,2048]{1,0:T(8,128)(2,1)} custom-call(s32[2,768]{1,0:T(2,128)} %bitcast.27, f32[1,2048]{1,0:T(1,128)} %bitcast.28, bf16[768,2048]{1,0:T(8,128)(2,1)} %tokens_ref.1), custom_call_target="tpu_custom_call" | custom-call | tf_op jit(solution)/shard_map/dispatch_buffer/pallas_call | solution.py:99
  12.2 8.9 %all-to-all-start = ((bf16[32,24,2048]{2,1,0:T(8,128)(2,1)}), bf16[32,24,2048]{2,1,0:T(8,128)(2,1)S(1)}, u32[]{:S(2)}, u32[]{:S(2)}) async-start(bf16[32,24,2048]{2,1,0:T(8,128)(2,1)} %bitcast.16), calls=%async_computation | async-start | bytes 6291456 | tf_op jit(solution)/shard_map/all_to_all | solution.py:416
  21.1 0.0 collective-permute-done.1.g1
  21.1 0.4 collective-permute-start.2
  21.4 0.0 collective-permute-done.gb
  21.4 1.7 %collective-permute-start.6 = (bf16[2048,256]{1,0:T(8,128)(2,1)}, bf16[2048,256]{1,0:T(8,128)(2,1)}, u32[]{:S(2)}, u32[]{:S(2)}) collective-permute-start(bf16[2048,256]{1,0:T(8,128)(2,1)} %collective-permute-done.1.g1), channel_id=1, source_target_pairs={{2,3},{3,2},{4,5},{5,4},{10,11},{11,10},{12,13},{13,12},{18,19},{1... | collective-permute-start | bytes 3145736 | tf_op jit(solution)/shard_map/ppermute | solution.py:400
  23.1 3.6 %collective-permute-done.4.u1 = bf16[2048,256]{1,0:T(8,128)(2,1)} collective-permute-done((bf16[2048,256]{1,0:T(8,128)(2,1)}, bf16[2048,256]{1,0:T(8,128)(2,1)}, u32[]{:S(2)}, u32[]{:S(2)}) %collective-permute-start.4) | collective-permute-done | bytes 1048608 | tf_op jit(solution)/shard_map/ppermute | solution.py:400
  26.7 1.6 %collective-permute-start.8 = (bf16[2048,256]{1,0:T(8,128)(2,1)}, bf16[2048,256]{1,0:T(8,128)(2,1)}, u32[]{:S(2)}, u32[]{:S(2)}) collective-permute-start(bf16[2048,256]{1,0:T(8,128)(2,1)} %collective-permute-done.4.u1), channel_id=1, source_target_pairs={{2,3},{3,2},{4,5},{5,4},{10,11},{11,10},{12,13},{13,12},{18,19},{1... | collective-permute-start | bytes 3145736 | tf_op jit(solution)/shard_map/ppermute | solution.py:400
  28.3 0.9 collective-permute-start.5
  29.3 19.9 %collective-permute-done.11.d1 = bf16[256,2048]{1,0:T(8,128)(2,1)} collective-permute-done((bf16[256,2048]{1,0:T(8,128)(2,1)}, bf16[256,2048]{1,0:T(8,128)(2,1)}, u32[]{:S(2)}, u32[]{:S(2)}) %collective-permute-start.11) | collective-permute-done | bytes 1048608 | tf_op jit(solution)/shard_map/ppermute | solution.py:400
  49.1 1.6 %collective-permute-start.13 = (bf16[256,2048]{1,0:T(8,128)(2,1)}, bf16[256,2048]{1,0:T(8,128)(2,1)}, u32[]{:S(2)}, u32[]{:S(2)}) collective-permute-start(bf16[256,2048]{1,0:T(8,128)(2,1)} %collective-permute-done.11.d1), channel_id=1, source_target_pairs={{2,3},{3,2},{4,5},{5,4},{10,11},{11,10},{12,13},{13,12},{18,19},{1... | collective-permute-start | bytes 3145736 | tf_op jit(solution)/shard_map/ppermute | solution.py:400
  50.8 0.0 collective-permute-done.2.g2
  50.8 0.0 collective-permute-start.10
  50.8 0.0 collective-permute-done.6.gb
  50.8 0.5 collective-permute-start.7
  51.3 0.0 collective-permute-done.8.ub
  51.3 8.6 %collective-permute-start.9 = (bf16[2048,256]{1,0:T(8,128)(2,1)}, bf16[2048,256]{1,0:T(8,128)(2,1)}, u32[]{:S(2)}, u32[]{:S(2)}) collective-permute-start(bf16[2048,256]{1,0:T(8,128)(2,1)} %collective-permute-done.8.ub), channel_id=1, source_target_pairs={{0,4},{1,5},{2,6},{3,7},{4,0},{5,1},{6,2},{7,3},{8,12},{9,13},{10,... | collective-permute-start | bytes 3145736 | tf_op jit(solution)/shard_map/ppermute | solution.py:400
  59.9 0.0 collective-permute-start.12
  59.9 11.2 %collective-permute-start.14 = (bf16[256,2048]{1,0:T(8,128)(2,1)}, bf16[256,2048]{1,0:T(8,128)(2,1)}, u32[]{:S(2)}, u32[]{:S(2)}) collective-permute-start(bf16[256,2048]{1,0:T(8,128)(2,1)} %collective-permute-done.13.d3b), channel_id=1, source_target_pairs={{0,4},{1,5},{2,6},{3,7},{4,0},{5,1},{6,2},{7,3},{8,12},{9,13},{10,... | collective-permute-start | bytes 3145736 | tf_op jit(solution)/shard_map/ppermute | solution.py:400
  71.1 0.6 pad_add_fusion.place_ref
  71.7 7.8 %early_hidden.1.early_ref = bf16[768,768]{1,0:T(8,128)(2,1)S(1)} custom-call(s32[2]{0:T(128)} %pad_add_fusion.place_ref, bf16[768,2048]{1,0:T(8,128)(2,1)S(1)} %bitcast.12, bf16[2048,256]{1,0:T(8,128)(2,1)} %bitcast.20, bf16[2048,256]{1,0:T(8,128)(2,1)} %collective-permute-done.gb, bf16[2048,256]{1,0:T(8,128)(2,1)} %collective-permute-done.1.g1, ...), custom_call_target="tpu_custom_call" | custom-call | tf_op jit(solution)/shard_map/early_hidden/pallas_call | solution.py:209
  79.5 0.0 collective-permute-done.7.ga
  79.5 0.0 collective-permute-done.9.ua
  79.5 3.9 %middle_hidden.1.middle_ref = bf16[768,256]{1,0:T(8,128)(2,1)S(1)} custom-call(s32[2]{0:T(128)S(1)} %copy-done.2, bf16[768,2048]{1,0:T(8,128)(2,1)S(1)} %bitcast.13, bf16[2048,256]{1,0:T(8,128)(2,1)} %collective-permute-done.7.ga, bf16[2048,256]{1,0:T(8,128)(2,1)} %collective-permute-done.6.gb, bf16[2048,256]{1,0:T(8,128)(2,1)} %collective-permute-done.9.ua, ...), custom_call_target="tpu_custom_call" | custom-call | tf_op jit(solution)/shard_map/middle_hidden/pallas_call | solution.py:223
  83.5 0.0 collective-permute-done.10.d0b
  83.5 0.0 collective-permute-done.14.d3a
  83.5 6.8 %late_outputs.1 = bf16[32,4,24,512]{3,2,1,0:T(8,128)(2,1)} custom-call(s32[2]{0:T(128)S(1)} %copy-done.2, bf16[768,768]{1,0:T(8,128)(2,1)S(1)} %early_hidden.1.early_ref, bf16[768,256]{1,0:T(8,128)(2,1)S(1)} %middle_hidden.1.middle_ref, bf16[256,2048]{1,0:T(8,128)(2,1)} %bitcast.26, bf16[256,2048]{1,0:T(8,128)(2,1)} %collective-permute-done.10.d0b, ...), custom_call_target="tpu_custom_call" | custom-call | tf_op jit(solution)/shard_map/late_outputs/pallas_call | solution.py:279
  90.2 0.0 copy-start.4
  90.3 0.0 copy-start.5
  90.3 10.6 %all-to-all-start.1 = ((bf16[128,24,512]{2,1,0:T(8,128)(2,1)}), bf16[128,24,512]{2,1,0:T(8,128)(2,1)S(1)}, u32[]{:S(2)}, u32[]{:S(2)}) async-start(bf16[128,24,512]{2,1,0:T(8,128)(2,1)} %bitcast.17), calls=%async_computation.1 | async-start | bytes 6291456 | tf_op jit(solution)/shard_map/all_to_all | solution.py:425
  100.8 0.0 copy-start.3
  100.9 0.9 copy.9.ids_ref
  101.8 0.9 copy.10.scores_ref
  102.7 1.0 copy-done
  103.7 1.0 copy-done.1
  104.7 2.2 %columns.1.table_ref = f32[768,4]{1,0:T(8,128)S(1)} custom-call(s32[768,2]{1,0:T(8,128)S(1)} %copy-done, f32[768,2]{1,0:T(8,128)S(1)} %copy-done.1), custom_call_target="tpu_custom_call" | custom-call | tf_op jit(solution)/shard_map/columns/pallas_call | solution.py:320
  106.9 35.0 %all-to-all-done.1 = bf16[128,24,512]{2,1,0:T(8,128)(2,1)S(1)} async-done(((bf16[128,24,512]{2,1,0:T(8,128)(2,1)}), bf16[128,24,512]{2,1,0:T(8,128)(2,1)S(1)}, u32[]{:S(2)}, u32[]{:S(2)}) %all-to-all-start.1) | async-done | bytes 3145760 | tf_op jit(solution)/shard_map/all_to_all | solution.py:425
  141.9 3.0 %combine.1 = (f32[768,512]{1,0:T(8,128)S(1)}, f32[1,768]{1,0:T(1,128)S(1)}) custom-call(f32[768,4]{1,0:T(8,128)S(1)} %columns.1.table_ref, bf16[3072,512]{1,0:T(8,128)(2,1)S(1)} %bitcast.14), custom_call_target="tpu_custom_call" | custom-call | tf_op jit(solution)/shard_map/combine/pallas_call | solution.py:348
  144.9 0.7 collective-permute-start.15
  145.6 3.0 %collective-permute-done.15 = f32[1,768]{1,0:T(1,128)S(1)} collective-permute-done((f32[1,768]{1,0:T(1,128)S(1)}, f32[1,768]{1,0:T(1,128)S(1)}, u32[]{:S(2)}, u32[]{:S(2)}) %collective-permute-start.15) | collective-permute-done | bytes 3104 | tf_op jit(solution)/shard_map/ppermute | solution.py:430
  148.6 1.7 %collective-permute-start.16 = (f32[1,768]{1,0:T(1,128)S(1)}, f32[1,768]{1,0:T(1,128)S(1)}, u32[]{:S(2)}, u32[]{:S(2)}) collective-permute-start(f32[1,768]{1,0:T(1,128)S(1)} %add.9.pair_ref), channel_id=1, source_target_pairs={{0,3},{1,2},{2,1},{3,0},{4,7},{5,6},{6,5},{7,4},{8,11},{9,10},{10,... | collective-permute-start | bytes 9224 | tf_op jit(solution)/shard_map/ppermute | solution.py:431
  150.3 3.1 %collective-permute-done.16.other_ref = f32[1,768]{1,0:T(1,128)S(1)} collective-permute-done((f32[1,768]{1,0:T(1,128)S(1)}, f32[1,768]{1,0:T(1,128)S(1)}, u32[]{:S(2)}, u32[]{:S(2)}) %collective-permute-start.16) | collective-permute-done | bytes 3104 | tf_op jit(solution)/shard_map/ppermute | solution.py:431
  153.4 1.1 scale.1
  (13 shorter events, 0.0 us)
Async XLA Ops:
  0.0 21.1 %collective-permute-start.1 = (bf16[2048,256]{1,0:T(8,128)(2,1)}, bf16[2048,256]{1,0:T(8,128)(2,1)}, u32[]{:S(2)}, u32[]{:S(2)}) collective-permute-start(bf16[2048,256]{1,0:T(8,128)(2,1)} %bitcast.18), channel_id=1, source_target_pairs={{0,1},{1,0},{2,5},{3,4},{4,3},{5,2},{6,7},{7,6},{8,9},{9,8},{10,13... | collective-permute-start | bytes 3145736 | tf_op jit(solution)/shard_map/ppermute | solution.py:400
  1.6 19.8 %collective-permute-start = (bf16[2048,256]{1,0:T(8,128)(2,1)}, bf16[2048,256]{1,0:T(8,128)(2,1)}, u32[]{:S(2)}, u32[]{:S(2)}) collective-permute-start(bf16[2048,256]{1,0:T(8,128)(2,1)} %bitcast.19), channel_id=1, source_target_pairs={{0,4},{1,5},{2,6},{3,7},{4,0},{5,1},{6,2},{7,3},{8,12},{9,13},{10,... | collective-permute-start | bytes 3145736 | tf_op jit(solution)/shard_map/ppermute | solution.py:400
  3.0 23.7 %collective-permute-start.4 = (bf16[2048,256]{1,0:T(8,128)(2,1)}, bf16[2048,256]{1,0:T(8,128)(2,1)}, u32[]{:S(2)}, u32[]{:S(2)}) collective-permute-start(bf16[2048,256]{1,0:T(8,128)(2,1)} %bitcast.21), channel_id=1, source_target_pairs={{0,1},{1,0},{2,5},{3,4},{4,3},{5,2},{6,7},{7,6},{8,9},{9,8},{10,13... | collective-permute-start | bytes 3145736 | tf_op jit(solution)/shard_map/ppermute | solution.py:400
  3.2 25.1 %collective-permute-start.3 = (bf16[2048,256]{1,0:T(8,128)(2,1)}, bf16[2048,256]{1,0:T(8,128)(2,1)}, u32[]{:S(2)}, u32[]{:S(2)}) collective-permute-start(bf16[2048,256]{1,0:T(8,128)(2,1)} %bitcast.22), channel_id=1, source_target_pairs={{0,4},{1,5},{2,6},{3,7},{4,0},{5,1},{6,2},{7,3},{8,12},{9,13},{10,... | collective-permute-start | bytes 3145736 | tf_op jit(solution)/shard_map/ppermute | solution.py:400
  3.4 45.8 %collective-permute-start.11 = (bf16[256,2048]{1,0:T(8,128)(2,1)}, bf16[256,2048]{1,0:T(8,128)(2,1)}, u32[]{:S(2)}, u32[]{:S(2)}) collective-permute-start(bf16[256,2048]{1,0:T(8,128)(2,1)} %bitcast.24), channel_id=1, source_target_pairs={{0,1},{1,0},{2,5},{3,4},{4,3},{5,2},{6,7},{7,6},{8,9},{9,8},{10,13... | collective-permute-start | bytes 3145736 | tf_op jit(solution)/shard_map/ppermute | solution.py:400
  12.2 59.5 %all-to-all-start = ((bf16[32,24,2048]{2,1,0:T(8,128)(2,1)}), bf16[32,24,2048]{2,1,0:T(8,128)(2,1)S(1)}, u32[]{:S(2)}, u32[]{:S(2)}) async-start(bf16[32,24,2048]{2,1,0:T(8,128)(2,1)} %bitcast.16), calls=%async_computation | async-start | bytes 6291456 | tf_op jit(solution)/shard_map/all_to_all | solution.py:416
  21.1 29.7 %collective-permute-start.2 = (bf16[2048,256]{1,0:T(8,128)(2,1)}, bf16[2048,256]{1,0:T(8,128)(2,1)}, u32[]{:S(2)}, u32[]{:S(2)}) collective-permute-start(bf16[2048,256]{1,0:T(8,128)(2,1)} %collective-permute-done.1.g1), channel_id=1, source_target_pairs={{0,4},{1,5},{2,6},{3,7},{4,0},{5,1},{6,2},{7,3},{8,12},{9,13},{10,... | collective-permute-start | bytes 3145736 | tf_op jit(solution)/shard_map/ppermute | solution.py:400
  21.4 29.4 %collective-permute-start.6 = (bf16[2048,256]{1,0:T(8,128)(2,1)}, bf16[2048,256]{1,0:T(8,128)(2,1)}, u32[]{:S(2)}, u32[]{:S(2)}) collective-permute-start(bf16[2048,256]{1,0:T(8,128)(2,1)} %collective-permute-done.1.g1), channel_id=1, source_target_pairs={{2,3},{3,2},{4,5},{5,4},{10,11},{11,10},{12,13},{13,12},{18,19},{1... | collective-permute-start | bytes 3145736 | tf_op jit(solution)/shard_map/ppermute | solution.py:400
  26.7 24.6 %collective-permute-start.8 = (bf16[2048,256]{1,0:T(8,128)(2,1)}, bf16[2048,256]{1,0:T(8,128)(2,1)}, u32[]{:S(2)}, u32[]{:S(2)}) collective-permute-start(bf16[2048,256]{1,0:T(8,128)(2,1)} %collective-permute-done.4.u1), channel_id=1, source_target_pairs={{2,3},{3,2},{4,5},{5,4},{10,11},{11,10},{12,13},{13,12},{18,19},{1... | collective-permute-start | bytes 3145736 | tf_op jit(solution)/shard_map/ppermute | solution.py:400
  28.3 31.6 %collective-permute-start.5 = (bf16[2048,256]{1,0:T(8,128)(2,1)}, bf16[2048,256]{1,0:T(8,128)(2,1)}, u32[]{:S(2)}, u32[]{:S(2)}) collective-permute-start(bf16[2048,256]{1,0:T(8,128)(2,1)} %collective-permute-done.4.u1), channel_id=1, source_target_pairs={{0,4},{1,5},{2,6},{3,7},{4,0},{5,1},{6,2},{7,3},{8,12},{9,13},{10,... | collective-permute-start | bytes 3145736 | tf_op jit(solution)/shard_map/ppermute | solution.py:400
  49.1 10.7 %collective-permute-start.13 = (bf16[256,2048]{1,0:T(8,128)(2,1)}, bf16[256,2048]{1,0:T(8,128)(2,1)}, u32[]{:S(2)}, u32[]{:S(2)}) collective-permute-start(bf16[256,2048]{1,0:T(8,128)(2,1)} %collective-permute-done.11.d1), channel_id=1, source_target_pairs={{2,3},{3,2},{4,5},{5,4},{10,11},{11,10},{12,13},{13,12},{18,19},{1... | collective-permute-start | bytes 3145736 | tf_op jit(solution)/shard_map/ppermute | solution.py:400
  50.8 32.7 %collective-permute-start.10 = (bf16[256,2048]{1,0:T(8,128)(2,1)}, bf16[256,2048]{1,0:T(8,128)(2,1)}, u32[]{:S(2)}, u32[]{:S(2)}) collective-permute-start(bf16[256,2048]{1,0:T(8,128)(2,1)} %bitcast.25), channel_id=1, source_target_pairs={{0,4},{1,5},{2,6},{3,7},{4,0},{5,1},{6,2},{7,3},{8,12},{9,13},{10,... | collective-permute-start | bytes 3145736 | tf_op jit(solution)/shard_map/ppermute | solution.py:400
  50.8 28.7 %collective-permute-start.7 = (bf16[2048,256]{1,0:T(8,128)(2,1)}, bf16[2048,256]{1,0:T(8,128)(2,1)}, u32[]{:S(2)}, u32[]{:S(2)}) collective-permute-start(bf16[2048,256]{1,0:T(8,128)(2,1)} %collective-permute-done.6.gb), channel_id=1, source_target_pairs={{0,4},{1,5},{2,6},{3,7},{4,0},{5,1},{6,2},{7,3},{8,12},{9,13},{10,... | collective-permute-start | bytes 3145736 | tf_op jit(solution)/shard_map/ppermute | solution.py:400
  51.3 28.2 %collective-permute-start.9 = (bf16[2048,256]{1,0:T(8,128)(2,1)}, bf16[2048,256]{1,0:T(8,128)(2,1)}, u32[]{:S(2)}, u32[]{:S(2)}) collective-permute-start(bf16[2048,256]{1,0:T(8,128)(2,1)} %collective-permute-done.8.ub), channel_id=1, source_target_pairs={{0,4},{1,5},{2,6},{3,7},{4,0},{5,1},{6,2},{7,3},{8,12},{9,13},{10,... | collective-permute-start | bytes 3145736 | tf_op jit(solution)/shard_map/ppermute | solution.py:400
  59.9 23.6 %collective-permute-start.12 = (bf16[256,2048]{1,0:T(8,128)(2,1)}, bf16[256,2048]{1,0:T(8,128)(2,1)}, u32[]{:S(2)}, u32[]{:S(2)}) collective-permute-start(bf16[256,2048]{1,0:T(8,128)(2,1)} %collective-permute-done.11.d1), channel_id=1, source_target_pairs={{0,4},{1,5},{2,6},{3,7},{4,0},{5,1},{6,2},{7,3},{8,12},{9,13},{10,... | collective-permute-start | bytes 3145736 | tf_op jit(solution)/shard_map/ppermute | solution.py:400
  59.9 23.6 %collective-permute-start.14 = (bf16[256,2048]{1,0:T(8,128)(2,1)}, bf16[256,2048]{1,0:T(8,128)(2,1)}, u32[]{:S(2)}, u32[]{:S(2)}) collective-permute-start(bf16[256,2048]{1,0:T(8,128)(2,1)} %collective-permute-done.13.d3b), channel_id=1, source_target_pairs={{0,4},{1,5},{2,6},{3,7},{4,0},{5,1},{6,2},{7,3},{8,12},{9,13},{10,... | collective-permute-start | bytes 3145736 | tf_op jit(solution)/shard_map/ppermute | solution.py:400
  71.7 7.8 %copy-start.2 = (s32[2]{0:T(128)S(1)}, s32[2]{0:T(128)}, u32[]{:S(2)}) copy-start(s32[2]{0:T(128)} %pad_add_fusion.place_ref) | copy-start | bytes 28
  90.2 10.6 %copy-start.4 = (s32[768,2]{0,1:T(2,128)S(1)}, s32[768,2]{0,1:T(2,128)}, u32[]{:S(2)}) copy-start(s32[768,2]{0,1:T(2,128)} %param.10) | copy-start | bytes 18436
  90.3 11.5 %copy-start.5 = (f32[768,2]{0,1:T(2,128)S(1)}, f32[768,2]{0,1:T(2,128)}, u32[]{:S(2)}) copy-start(f32[768,2]{0,1:T(2,128)} %param.11) | copy-start | bytes 18436
  90.3 51.6 %all-to-all-start.1 = ((bf16[128,24,512]{2,1,0:T(8,128)(2,1)}), bf16[128,24,512]{2,1,0:T(8,128)(2,1)S(1)}, u32[]{:S(2)}, u32[]{:S(2)}) async-start(bf16[128,24,512]{2,1,0:T(8,128)(2,1)} %bitcast.17), calls=%async_computation.1 | async-start | bytes 6291456 | tf_op jit(solution)/shard_map/all_to_all | solution.py:425
  100.8 52.5 %copy-start.3 = (f32[512]{0:T(512)S(1)}, f32[512]{0:T(512)}, u32[]{:S(2)}) copy-start(f32[512]{0:T(512)} %param.15) | copy-start | bytes 6148
  102.7 1.0 copy-start
  103.7 1.0 copy-start.1
  144.9 3.7 %collective-permute-start.15 = (f32[1,768]{1,0:T(1,128)S(1)}, f32[1,768]{1,0:T(1,128)S(1)}, u32[]{:S(2)}, u32[]{:S(2)}) collective-permute-start(f32[1,768]{1,0:T(1,128)S(1)} %get-tuple-element.8), channel_id=1, source_target_pairs={{0,1},{1,0},{2,3},{3,2},{4,5},{5,4},{6,7},{7,6},{8,9},{9,8},{10,11... | collective-permute-start | bytes 9224 | tf_op jit(solution)/shard_map/ppermute | solution.py:430
  148.6 4.8 %collective-permute-start.16 = (f32[1,768]{1,0:T(1,128)S(1)}, f32[1,768]{1,0:T(1,128)S(1)}, u32[]{:S(2)}, u32[]{:S(2)}) collective-permute-start(f32[1,768]{1,0:T(1,128)S(1)} %add.9.pair_ref), channel_id=1, source_target_pairs={{0,3},{1,2},{2,1},{3,0},{4,7},{5,6},{6,5},{7,4},{8,11},{9,10},{10,... | collective-permute-start | bytes 9224 | tf_op jit(solution)/shard_map/ppermute | solution.py:431

commit v8 on v6

--- a/solution.py
+++ b/solution.py
@@ -146,7 +146,9 @@
     return acts
 
 
-def early_kernel(place_ref, rows_ref, ga, gb, g1, g2, ua, ub, u1, u2, out_ref, weights, sems):
+def early_kernel(
+    place_ref, rows_ref, ga, gb, g1, g2, ua, ub, u1, u2, d0a, d0b, d1, d2, out_ref, down_ref, weights, sems
+):
     flag = place_ref[1]
     width, part = g1.shape
 
@@ -168,6 +170,9 @@
         pltpu.make_async_copy(source, target, sems.at[4 + n]).start()
     start_one(flag, ga, gb, weights.at[2, :, pl.ds(0, part)], sems.at[6])
     start_one(flag, ua, ub, weights.at[2, :, pl.ds(part, part)], sems.at[7])
+    start_one(flag, d0a, d0b, down_ref.at[pl.ds(0, part)], sems.at[8])
+    pltpu.make_async_copy(d1, down_ref.at[pl.ds(part, part)], sems.at[9]).start()
+    pltpu.make_async_copy(d2, down_ref.at[pl.ds(2 * part, part)], sems.at[10]).start()
     waits = [
         functools.partial(wait_for, 0, lo, size, 2 * half) for half, (lo, size) in enumerate(halves_of(width))
     ]
@@ -176,6 +181,8 @@
         wait_for(at, 0, width, 2 + 2 * at)
         acts = jnp.dot(rows_ref[...], weights[at], preferred_element_type=jnp.float32)
         out_ref[:, out * part : (out + 1) * part] = activation(acts, part)
+    for i in range(3):
+        pltpu.make_async_copy(d1, down_ref.at[pl.ds(i * part, part)], sems.at[8 + i]).wait()
 
 
 def middle_kernel(place_ref, rows_ref, ga, gb, ua, ub, out_ref, weights, sems):
@@ -203,18 +210,18 @@
 VMEM = pl.BlockSpec(memory_space=pltpu.VMEM)
 
 
-def early_hidden(place, rows, gates, ups):
+def early_hidden(place, rows, gates, ups, downs):
     count, width = rows.shape
     part = gates[0].shape[1]
     return pl.pallas_call(
         early_kernel,
-        in_specs=[SMEM, VMEM] + [ANY] * 8,
-        out_specs=VMEM,
-        scratch_shapes=[pltpu.VMEM((3, width, 2 * part), jnp.bfloat16), pltpu.SemaphoreType.DMA((8,))],
-        out_shape=pltpu.VMEM((count, 3 * part), jnp.bfloat16),
-        compiler_params=pltpu.CompilerParams(vmem_limit_bytes=50 * MIB),
+        in_specs=[SMEM, VMEM] + [ANY] * 12,
+        out_specs=[VMEM, VMEM],
+        scratch_shapes=[pltpu.VMEM((3, width, 2 * part), jnp.bfloat16), pltpu.SemaphoreType.DMA((11,))],
+        out_shape=[pltpu.VMEM((count, 3 * part), jnp.bfloat16), pltpu.VMEM((3 * part, width), jnp.bfloat16)],
+        compiler_params=pltpu.CompilerParams(vmem_limit_bytes=32 * MIB),
         name="early_hidden",
-    )(place, rows, *gates, *ups)
+    )(place, rows, *gates, *ups, *downs)
 
 
 def middle_hidden(place, rows, gates, ups):
@@ -226,71 +233,54 @@
         out_specs=VMEM,
         scratch_shapes=[pltpu.VMEM((width, 2 * part), jnp.bfloat16), pltpu.SemaphoreType.DMA((4,))],
         out_shape=jax.ShapeDtypeStruct((count, part), jnp.bfloat16),
-        compiler_params=pltpu.CompilerParams(vmem_limit_bytes=50 * MIB),
+        compiler_params=pltpu.CompilerParams(vmem_limit_bytes=32 * MIB),
         name="middle_hidden",
     )(place, rows, *gates, *ups)
 
 
-def late_kernel(place_ref, early_ref, middle_ref, d0a, d0b, d1, d2, d3a, d3b, out_ref, down, hidden, out, sems, out_sems, *, cuts):
+def late_kernel(place_ref, early_ref, middle_ref, down_ref, d3a, d3b, out_ref, last, out, sems, out_sems):
     flag = place_ref[1]
-    senders, pieces, slots, piece = out_ref.shape
-    part = d1.shape[0]
-    size = piece // cuts
-    steps = pieces * cuts
-
-    def target(i, f):
-        return down.at[pl.ds(i * part, part), pl.ds(f * size, size)]
-
-    def source(ref, f):
-        return ref.at[:, pl.ds(f * size, size)]
-
-    for f in range(steps):
-        pltpu.make_async_copy(source(d1, f), target(1, f), sems.at[4 * f + 1]).start()
-        pltpu.make_async_copy(source(d2, f), target(2, f), sems.at[4 * f + 2]).start()
-        start_one(flag, source(d0a, f), source(d0b, f), target(0, f), sems.at[4 * f])
-        start_one(flag, source(d3a, f), source(d3b, f), target(3, f), sems.at[4 * f + 3])
-    hidden[:, 0 : 3 * part] = early_ref[...]
-    hidden[:, 3 * part : 4 * part] = middle_ref[...]
+    pieces, senders, slots, piece = out.shape
+
+    def columns(ref, f):
+        return ref.at[:, pl.ds(f * piece, piece)]
 
     def store(f):
-        return pltpu.make_async_copy(
-            out.at[f], out_ref.at[:, f // cuts, :, pl.ds(f % cuts * size, size)], out_sems.at[f]
-        )
-
-    for f in range(steps):
-        for i in range(4):
-            pltpu.make_async_copy(source(d1, f), target(i, f), sems.at[4 * f + i]).wait()
-        value = jnp.dot(
-            hidden[...], down[:, f * size : (f + 1) * size], preferred_element_type=jnp.float32
-        )
-        out[f] = value.reshape(senders, slots, size).astype(jnp.bfloat16)
+        return pltpu.make_async_copy(out.at[f], out_ref.at[:, f], out_sems.at[f])
+
+    for f in range(pieces):
+        start_one(flag, columns(d3a, f), columns(d3b, f), columns(last, f), sems.at[f])
+    for f in range(pieces):
+        at = slice(f * piece, (f + 1) * piece)
+        value = jnp.dot(early_ref[...], down_ref[:, at], preferred_element_type=jnp.float32)
+        pltpu.make_async_copy(columns(d3a, f), columns(last, f), sems.at[f]).wait()
+        value = value + jnp.dot(middle_ref[...], last[:, at], preferred_element_type=jnp.float32)
+        out[f] = value.reshape(senders, slots, piece).astype(jnp.bfloat16)
         store(f).start()
-    for f in range(steps):
+    for f in range(pieces):
         store(f).wait()
 
 
-def late_outputs(place, early, middle, downs, senders, pieces):
+def late_outputs(place, early, middle, down, lasts, senders, pieces):
     count = early.shape[0]
-    part, width = downs[0].shape
+    part, width = lasts[0].shape
     slots = count // senders
     piece = width // pieces
     shape = (senders, pieces, slots, piece)
-    cuts = 1
-    return pl.pallas_call(
-        functools.partial(late_kernel, cuts=cuts),
-        in_specs=[SMEM, VMEM, VMEM] + [ANY] * 6,
+    return pl.pallas_call(
+        late_kernel,
+        in_specs=[SMEM, VMEM, VMEM, VMEM, ANY, ANY],
         out_specs=HBM,
         scratch_shapes=[
-            pltpu.VMEM((4 * part, width), jnp.bfloat16),
-            pltpu.VMEM((count, 4 * part), jnp.bfloat16),
-            pltpu.VMEM((pieces * cuts, senders, slots, piece // cuts), jnp.bfloat16),
-            pltpu.SemaphoreType.DMA((4 * pieces * cuts,)),
-            pltpu.SemaphoreType.DMA((pieces * cuts,)),
+            pltpu.VMEM((part, width), jnp.bfloat16),
+            pltpu.VMEM((pieces, senders, slots, piece), jnp.bfloat16),
+            pltpu.SemaphoreType.DMA((pieces,)),
+            pltpu.SemaphoreType.DMA((pieces,)),
         ],
         out_shape=pltpu.HBM(shape, jnp.bfloat16),
-        compiler_params=pltpu.CompilerParams(vmem_limit_bytes=50 * MIB),
+        compiler_params=pltpu.CompilerParams(vmem_limit_bytes=32 * MIB),
         name="late_outputs",
-    )(place, early, middle, *downs)
+    )(place, early, middle, down, *lasts)
 
 
 def table_kernel(ids_ref, scores_ref, out_ref, *, rows, count_tp):
@@ -417,10 +407,12 @@
         buffer.reshape(count_ep, rows, full_width), "ep", split_axis=0, concat_axis=0, tiled=True
     ).reshape(count_ep * rows, full_width)
     received = in_vmem(received)
-    early = early_hidden(place, received, (*gate[0], gate[1], gate[2]), (*up[0], up[1], up[2]))
+    early, loaded = early_hidden(
+        place, received, (*gate[0], gate[1], gate[2]), (*up[0], up[1], up[2]), (*down[0], down[1], down[2])
+    )
     middle = in_vmem(middle_hidden(place, received, gate[3], up[3]))
     outputs = late_outputs(
-        place, early, middle, (*down[0], down[1], down[2], *down[3]), count_ep, count_tp
+        place, early, middle, loaded, down[3], count_ep, count_tp
     )
     returned = lax.all_to_all(
         outputs.reshape(count_ep * count_tp, rows, part_width), AXES, split_axis=0, concat_axis=0, tiled=True
@@ -429,7 +421,7 @@
     combined, squares = combine(table, in_vmem(returned))
     parts = [squares] + [
         lax.ppermute(squares, "tp", [(i, (i + shift) % count_tp) for i in range(count_tp)])
-        for shift in range(1, count_tp)
+        for shift in (1, count_tp - 1, 2)
     ]
     return scale(combined, parts, out_gain[None, :], full_width)
 

time: 153 us -> 162 us (1.059)
  starting transfers between devices: 54.9 us -> 70.3 us
  waiting for transfers between devices: 61.4 us -> 54.9 us
    ppermute x15, starting transfers between devices: 31.6 us -> 46.3 us  [send(): return lax.ppermute(weight, AXES, pairs)]
    ppermute x15, waiting for transfers between devices: 23.5 us -> 14.8 us  [send(): return lax.ppermute(weight, AXES, pairs)]
    ppermute x3, waiting for transfers between devices: 2.9 us -> 5.06 us  [per_device(): lax.ppermute(squares, 'tp', [(i, (i + shift) % count_tp) for i in range(c...]
    unnamed x14 -> x12, local copies, waits for them, and re-layouts: 3.88 us -> 3.88 us
  transfers between devices with their start and end apart: 20 -> 20, of which waited for: 6 -> 5; matrix products, arithmetic and copies ran while one was open for 2% -> 1% of each run, Pallas kernels for 14% -> 13%
where the time goes in v8:
time: 162 us; the launch traced here: 161 us
  starting transfers between devices  70.3 us (43%)
  waiting for transfers between devices  54.9 us (34%)
  Pallas kernels  31.8 us (20%)
  local copies, waits for them, and re-layouts  3.88 us (2%)
    ppermute x15, starting transfers between devices, send(): return lax.ppermute(weight, AXES, pairs)  46.3 us
    all_to_all x1, waiting for transfers between devices, per_device(): lax.all_to_all(outputs.reshape(count_ep * count_tp, rows, part_width), AX...  35 us
    ppermute x15, waiting for transfers between devices, send(): return lax.ppermute(weight, AXES, pairs)  14.8 us
    all_to_all x1, starting transfers between devices, per_device(): lax.all_to_all(outputs.reshape(count_ep * count_tp, rows, part_width), AX...  12.2 us
    all_to_all x1, starting transfers between devices, per_device(): lax.all_to_all(buffer.reshape(count_ep, rows, full_width), 'ep', split_ax...  8.46 us
    pallas_call x1, Pallas kernels, early_hidden(): pl.pallas_call(early_kernel, in_specs=[SMEM, VMEM] + [ANY] * 12, out_spec...  7.58 us
    pallas_call x1, Pallas kernels, dispatch_buffer(): pl.pallas_call(functools.partial(dispatch_kernel, rows=rows, chunks=chunk...  7.14 us
    pallas_call x1, Pallas kernels, late_outputs(): pl.pallas_call(late_kernel, in_specs=[SMEM, VMEM, VMEM, VMEM, ANY, ANY],...  6.81 us
  transfers between devices with their start and end apart: 20, of which 5 were waited for; matrix products, arithmetic and copies ran while one was open for 1% of the time, Pallas kernels for 13%

profile of v8, /device:TPU:0, one launch (start us, length us, event | category | flops | bytes accessed | tf_op | source)
XLA Modules:
  0.0 161.0 jit_solution(9799387356529507256)
XLA Ops:
  0.0 1.6 collective-permute-start.1
  1.6 0.4 collective-permute-start.4
  2.0 1.6 collective-permute-start.7
  3.6 2.3 %collective-permute-start = (bf16[2048,256]{1,0:T(8,128)(2,1)}, bf16[2048,256]{1,0:T(8,128)(2,1)}, u32[]{:S(2)}, u32[]{:S(2)}) collective-permute-start(bf16[2048,256]{1,0:T(8,128)(2,1)} %bitcast.19), channel_id=1, source_target_pairs={{0,4},{1,5},{2,6},{3,7},{4,0},{5,1},{6,2},{7,3},{8,12},{9,13},{10,... | collective-permute-start | bytes 3145736 | tf_op jit(solution)/shard_map/ppermute | solution.py:390
  5.9 0.0 collective-permute-start.3
  5.9 7.1 %dispatch_buffer.1 = bf16[768,2048]{1,0:T(8,128)(2,1)} custom-call(s32[2,768]{1,0:T(2,128)} %bitcast.27, f32[1,2048]{1,0:T(1,128)} %bitcast.28, bf16[768,2048]{1,0:T(8,128)(2,1)} %tokens_ref.1), custom_call_target="tpu_custom_call" | custom-call | tf_op jit(solution)/shard_map/dispatch_buffer/pallas_call | solution.py:99
  13.1 8.5 %all-to-all-start = ((bf16[32,24,2048]{2,1,0:T(8,128)(2,1)}), bf16[32,24,2048]{2,1,0:T(8,128)(2,1)S(1)}, u32[]{:S(2)}, u32[]{:S(2)}) async-start(bf16[32,24,2048]{2,1,0:T(8,128)(2,1)} %bitcast.17), calls=%async_computation | async-start | bytes 6291456 | tf_op jit(solution)/shard_map/all_to_all | solution.py:406
  21.6 0.4 collective-permute-start.6
  21.9 4.4 %collective-permute-done.4.u1 = bf16[2048,256]{1,0:T(8,128)(2,1)} collective-permute-done((bf16[2048,256]{1,0:T(8,128)(2,1)}, bf16[2048,256]{1,0:T(8,128)(2,1)}, u32[]{:S(2)}, u32[]{:S(2)}) %collective-permute-start.4) | collective-permute-done | bytes 1048608 | tf_op jit(solution)/shard_map/ppermute | solution.py:390
  26.4 0.9 collective-permute-start.2
  27.2 10.4 %collective-permute-done.7.d1 = bf16[256,2048]{1,0:T(8,128)(2,1)} collective-permute-done((bf16[256,2048]{1,0:T(8,128)(2,1)}, bf16[256,2048]{1,0:T(8,128)(2,1)}, u32[]{:S(2)}, u32[]{:S(2)}) %collective-permute-start.7) | collective-permute-done | bytes 1048608 | tf_op jit(solution)/shard_map/ppermute | solution.py:390
  37.6 1.7 %collective-permute-start.9 = (bf16[2048,256]{1,0:T(8,128)(2,1)}, bf16[2048,256]{1,0:T(8,128)(2,1)}, u32[]{:S(2)}, u32[]{:S(2)}) collective-permute-start(bf16[2048,256]{1,0:T(8,128)(2,1)} %collective-permute-done.1.g1), channel_id=1, source_target_pairs={{2,3},{3,2},{4,5},{5,4},{10,11},{11,10},{12,13},{13,12},{18,19},{1... | collective-permute-start | bytes 3145736 | tf_op jit(solution)/shard_map/ppermute | solution.py:390
  39.3 0.0 collective-permute-done.gb
  39.3 1.6 %collective-permute-start.11 = (bf16[2048,256]{1,0:T(8,128)(2,1)}, bf16[2048,256]{1,0:T(8,128)(2,1)}, u32[]{:S(2)}, u32[]{:S(2)}) collective-permute-start(bf16[2048,256]{1,0:T(8,128)(2,1)} %collective-permute-done.4.u1), channel_id=1, source_target_pairs={{2,3},{3,2},{4,5},{5,4},{10,11},{11,10},{12,13},{13,12},{18,19},{1... | collective-permute-start | bytes 3145736 | tf_op jit(solution)/shard_map/ppermute | solution.py:390
  40.9 0.0 collective-permute-done.3.ub
  40.9 1.6 %collective-permute-start.13 = (bf16[256,2048]{1,0:T(8,128)(2,1)}, bf16[256,2048]{1,0:T(8,128)(2,1)}, u32[]{:S(2)}, u32[]{:S(2)}) collective-permute-start(bf16[256,2048]{1,0:T(8,128)(2,1)} %collective-permute-done.7.d1), channel_id=1, source_target_pairs={{2,3},{3,2},{4,5},{5,4},{10,11},{11,10},{12,13},{13,12},{18,19},{1... | collective-permute-start | bytes 3145736 | tf_op jit(solution)/shard_map/ppermute | solution.py:390
  42.5 3.3 %collective-permute-start.5 = (bf16[2048,256]{1,0:T(8,128)(2,1)}, bf16[2048,256]{1,0:T(8,128)(2,1)}, u32[]{:S(2)}, u32[]{:S(2)}) collective-permute-start(bf16[2048,256]{1,0:T(8,128)(2,1)} %collective-permute-done.4.u1), channel_id=1, source_target_pairs={{0,4},{1,5},{2,6},{3,7},{4,0},{5,1},{6,2},{7,3},{8,12},{9,13},{10,... | collective-permute-start | bytes 3145736 | tf_op jit(solution)/shard_map/ppermute | solution.py:390
  45.8 0.1 collective-permute-start.8
  45.9 8.6 %collective-permute-start.10 = (bf16[2048,256]{1,0:T(8,128)(2,1)}, bf16[2048,256]{1,0:T(8,128)(2,1)}, u32[]{:S(2)}, u32[]{:S(2)}) collective-permute-start(bf16[2048,256]{1,0:T(8,128)(2,1)} %collective-permute-done.9.gb), channel_id=1, source_target_pairs={{0,4},{1,5},{2,6},{3,7},{4,0},{5,1},{6,2},{7,3},{8,12},{9,13},{10,... | collective-permute-start | bytes 3145736 | tf_op jit(solution)/shard_map/ppermute | solution.py:390
  54.5 0.0 collective-permute-done.11.ub
  54.5 11.0 %collective-permute-start.12 = (bf16[2048,256]{1,0:T(8,128)(2,1)}, bf16[2048,256]{1,0:T(8,128)(2,1)}, u32[]{:S(2)}, u32[]{:S(2)}) collective-permute-start(bf16[2048,256]{1,0:T(8,128)(2,1)} %collective-permute-done.11.ub), channel_id=1, source_target_pairs={{0,4},{1,5},{2,6},{3,7},{4,0},{5,1},{6,2},{7,3},{8,12},{9,13},{10,... | collective-permute-start | bytes 3145736 | tf_op jit(solution)/shard_map/ppermute | solution.py:390
  65.5 0.0 collective-permute-done.13.d3b
  65.5 11.2 %collective-permute-start.14 = (bf16[256,2048]{1,0:T(8,128)(2,1)}, bf16[256,2048]{1,0:T(8,128)(2,1)}, u32[]{:S(2)}, u32[]{:S(2)}) collective-permute-start(bf16[256,2048]{1,0:T(8,128)(2,1)} %collective-permute-done.13.d3b), channel_id=1, source_target_pairs={{0,4},{1,5},{2,6},{3,7},{4,0},{5,1},{6,2},{7,3},{8,12},{9,13},{10,... | collective-permute-start | bytes 3145736 | tf_op jit(solution)/shard_map/ppermute | solution.py:390
  76.8 0.1 pad_add_fusion.place_ref
  76.8 0.0 collective-permute-done.5.u2
  76.8 0.0 collective-permute-done.8.d2
  76.9 7.6 %early_hidden.1 = (bf16[768,768]{1,0:T(8,128)(2,1)S(1)}, bf16[768,2048]{1,0:T(8,128)(2,1)S(1)}) custom-call(s32[2]{0:T(128)S(1)} %pad_add_fusion.place_ref, bf16[768,2048]{1,0:T(8,128)(2,1)S(1)} %bitcast.12, bf16[2048,256]{1,0:T(8,128)(2,1)} %bitcast.20, bf16[2048,256]{1,0:T(8,128)(2,1)} %collective-permute-done.gb, ...), custom_call_target="tpu_custom_call" | custom-call | tf_op jit(solution)/shard_map/early_hidden/pallas_call | solution.py:216
  84.5 0.0 collective-permute-done.12.ua
  84.5 3.9 %middle_hidden.1.middle_ref = bf16[768,256]{1,0:T(8,128)(2,1)S(1)} custom-call(s32[2]{0:T(128)S(1)} %pad_add_fusion.place_ref, bf16[768,2048]{1,0:T(8,128)(2,1)S(1)} %bitcast.13, bf16[2048,256]{1,0:T(8,128)(2,1)} %collective-permute-done.10.ga, bf16[2048,256]{1,0:T(8,128)(2,1)} %collective-permute-done.9.gb, bf16[2048,256]{1,0:T(8,128)(2,1)} %collective-permute-done.12.ua, ...), custom_call_target="tpu_custom_call" | custom-call | tf_op jit(solution)/shard_map/middle_hidden/pallas_call | solution.py:230
  88.4 0.0 collective-permute-done.14.d3a
  88.4 6.8 %late_outputs.1 = bf16[32,4,24,512]{3,2,1,0:T(8,128)(2,1)} custom-call(s32[2]{0:T(128)S(1)} %pad_add_fusion.place_ref, bf16[768,768]{1,0:T(8,128)(2,1)S(1)} %get-tuple-element.9.early_ref, bf16[768,256]{1,0:T(8,128)(2,1)S(1)} %middle_hidden.1.middle_ref, bf16[768,2048]{1,0:T(8,128)(2,1)S(1)} %get-tuple-element.10.down_ref, ...), custom_call_target="tpu_custom_call" | custom-call | tf_op jit(solution)/shard_map/late_outputs/pallas_call | solution.py:270
  95.2 0.0 copy-start.3
  95.2 0.0 copy-start.4
  95.2 12.2 %all-to-all-start.1 = ((bf16[128,24,512]{2,1,0:T(8,128)(2,1)}), bf16[128,24,512]{2,1,0:T(8,128)(2,1)S(1)}, u32[]{:S(2)}, u32[]{:S(2)}) async-start(bf16[128,24,512]{2,1,0:T(8,128)(2,1)} %bitcast.16), calls=%async_computation.1 | async-start | bytes 6291456 | tf_op jit(solution)/shard_map/all_to_all | solution.py:417
  107.4 0.0 copy-start.2
  107.4 0.9 copy.9.ids_ref
  108.4 0.9 copy.10.scores_ref
  109.3 1.0 copy-done
  110.3 1.0 copy-done.1
  111.3 2.2 %columns.1.table_ref = f32[768,4]{1,0:T(8,128)S(1)} custom-call(s32[768,2]{1,0:T(8,128)S(1)} %copy-done, f32[768,2]{1,0:T(8,128)S(1)} %copy-done.1), custom_call_target="tpu_custom_call" | custom-call | tf_op jit(solution)/shard_map/columns/pallas_call | solution.py:310
  113.5 35.0 %all-to-all-done.1 = bf16[128,24,512]{2,1,0:T(8,128)(2,1)S(1)} async-done(((bf16[128,24,512]{2,1,0:T(8,128)(2,1)}), bf16[128,24,512]{2,1,0:T(8,128)(2,1)S(1)}, u32[]{:S(2)}, u32[]{:S(2)}) %all-to-all-start.1) | async-done | bytes 3145760 | tf_op jit(solution)/shard_map/all_to_all | solution.py:417
  148.5 3.0 %combine.1 = (f32[768,512]{1,0:T(8,128)S(1)}, f32[1,768]{1,0:T(1,128)S(1)}) custom-call(f32[768,4]{1,0:T(8,128)S(1)} %columns.1.table_ref, bf16[3072,512]{1,0:T(8,128)(2,1)S(1)} %bitcast.14), custom_call_target="tpu_custom_call" | custom-call | tf_op jit(solution)/shard_map/combine/pallas_call | solution.py:338
  151.5 0.6 collective-permute-start.15
  152.1 2.7 %collective-permute-start.16 = (f32[1,768]{1,0:T(1,128)S(1)}, f32[1,768]{1,0:T(1,128)S(1)}, u32[]{:S(2)}, u32[]{:S(2)}) collective-permute-start(f32[1,768]{1,0:T(1,128)S(1)} %get-tuple-element.12.own_ref), channel_id=1, source_target_pairs={{0,3},{1,0},{2,1},{3,2},{4,7},{5,4},{6,5},{7,6},{8,11},{9,8},{10,9... | collective-permute-start | bytes 9224 | tf_op jit(solution)/shard_map/ppermute | solution.py:423
  154.8 0.0 collective-permute-start.17
  154.8 1.5 collective-permute-done.15.a_ref
  156.3 3.5 %collective-permute-done.17.c_ref = f32[1,768]{1,0:T(1,128)S(1)} collective-permute-done((f32[1,768]{1,0:T(1,128)S(1)}, f32[1,768]{1,0:T(1,128)S(1)}, u32[]{:S(2)}, u32[]{:S(2)}) %collective-permute-start.17) | collective-permute-done | bytes 3104 | tf_op jit(solution)/shard_map/ppermute | solution.py:423
  159.9 1.1 scale.1
  (12 shorter events, 0.0 us)
Async XLA Ops:
  0.0 21.6 %collective-permute-start.1 = (bf16[2048,256]{1,0:T(8,128)(2,1)}, bf16[2048,256]{1,0:T(8,128)(2,1)}, u32[]{:S(2)}, u32[]{:S(2)}) collective-permute-start(bf16[2048,256]{1,0:T(8,128)(2,1)} %bitcast.18), channel_id=1, source_target_pairs={{0,1},{1,0},{2,5},{3,4},{4,3},{5,2},{6,7},{7,6},{8,9},{9,8},{10,13... | collective-permute-start | bytes 3145736 | tf_op jit(solution)/shard_map/ppermute | solution.py:390
  1.6 24.7 %collective-permute-start.4 = (bf16[2048,256]{1,0:T(8,128)(2,1)}, bf16[2048,256]{1,0:T(8,128)(2,1)}, u32[]{:S(2)}, u32[]{:S(2)}) collective-permute-start(bf16[2048,256]{1,0:T(8,128)(2,1)} %bitcast.21), channel_id=1, source_target_pairs={{0,1},{1,0},{2,5},{3,4},{4,3},{5,2},{6,7},{7,6},{8,9},{9,8},{10,13... | collective-permute-start | bytes 3145736 | tf_op jit(solution)/shard_map/ppermute | solution.py:390
  2.0 35.6 %collective-permute-start.7 = (bf16[256,2048]{1,0:T(8,128)(2,1)}, bf16[256,2048]{1,0:T(8,128)(2,1)}, u32[]{:S(2)}, u32[]{:S(2)}) collective-permute-start(bf16[256,2048]{1,0:T(8,128)(2,1)} %bitcast.24), channel_id=1, source_target_pairs={{0,1},{1,0},{2,5},{3,4},{4,3},{5,2},{6,7},{7,6},{8,9},{9,8},{10,13... | collective-permute-start | bytes 3145736 | tf_op jit(solution)/shard_map/ppermute | solution.py:390
  3.6 35.6 %collective-permute-start = (bf16[2048,256]{1,0:T(8,128)(2,1)}, bf16[2048,256]{1,0:T(8,128)(2,1)}, u32[]{:S(2)}, u32[]{:S(2)}) collective-permute-start(bf16[2048,256]{1,0:T(8,128)(2,1)} %bitcast.19), channel_id=1, source_target_pairs={{0,4},{1,5},{2,6},{3,7},{4,0},{5,1},{6,2},{7,3},{8,12},{9,13},{10,... | collective-permute-start | bytes 3145736 | tf_op jit(solution)/shard_map/ppermute | solution.py:390
  5.9 35.0 %collective-permute-start.3 = (bf16[2048,256]{1,0:T(8,128)(2,1)}, bf16[2048,256]{1,0:T(8,128)(2,1)}, u32[]{:S(2)}, u32[]{:S(2)}) collective-permute-start(bf16[2048,256]{1,0:T(8,128)(2,1)} %bitcast.22), channel_id=1, source_target_pairs={{0,4},{1,5},{2,6},{3,7},{4,0},{5,1},{6,2},{7,3},{8,12},{9,13},{10,... | collective-permute-start | bytes 3145736 | tf_op jit(solution)/shard_map/ppermute | solution.py:390
  13.1 63.8 %all-to-all-start = ((bf16[32,24,2048]{2,1,0:T(8,128)(2,1)}), bf16[32,24,2048]{2,1,0:T(8,128)(2,1)S(1)}, u32[]{:S(2)}, u32[]{:S(2)}) async-start(bf16[32,24,2048]{2,1,0:T(8,128)(2,1)} %bitcast.17), calls=%async_computation | async-start | bytes 6291456 | tf_op jit(solution)/shard_map/all_to_all | solution.py:406
  21.6 21.0 %collective-permute-start.6 = (bf16[256,2048]{1,0:T(8,128)(2,1)}, bf16[256,2048]{1,0:T(8,128)(2,1)}, u32[]{:S(2)}, u32[]{:S(2)}) collective-permute-start(bf16[256,2048]{1,0:T(8,128)(2,1)} %bitcast.25), channel_id=1, source_target_pairs={{0,4},{1,5},{2,6},{3,7},{4,0},{5,1},{6,2},{7,3},{8,12},{9,13},{10,... | collective-permute-start | bytes 3145736 | tf_op jit(solution)/shard_map/ppermute | solution.py:390
  26.4 19.5 %collective-permute-start.2 = (bf16[2048,256]{1,0:T(8,128)(2,1)}, bf16[2048,256]{1,0:T(8,128)(2,1)}, u32[]{:S(2)}, u32[]{:S(2)}) collective-permute-start(bf16[2048,256]{1,0:T(8,128)(2,1)} %collective-permute-done.1.g1), channel_id=1, source_target_pairs={{0,4},{1,5},{2,6},{3,7},{4,0},{5,1},{6,2},{7,3},{8,12},{9,13},{10,... | collective-permute-start | bytes 3145736 | tf_op jit(solution)/shard_map/ppermute | solution.py:390
  37.6 8.3 %collective-permute-start.9 = (bf16[2048,256]{1,0:T(8,128)(2,1)}, bf16[2048,256]{1,0:T(8,128)(2,1)}, u32[]{:S(2)}, u32[]{:S(2)}) collective-permute-start(bf16[2048,256]{1,0:T(8,128)(2,1)} %collective-permute-done.1.g1), channel_id=1, source_target_pairs={{2,3},{3,2},{4,5},{5,4},{10,11},{11,10},{12,13},{13,12},{18,19},{1... | collective-permute-start | bytes 3145736 | tf_op jit(solution)/shard_map/ppermute | solution.py:390
  39.3 15.2 %collective-permute-start.11 = (bf16[2048,256]{1,0:T(8,128)(2,1)}, bf16[2048,256]{1,0:T(8,128)(2,1)}, u32[]{:S(2)}, u32[]{:S(2)}) collective-permute-start(bf16[2048,256]{1,0:T(8,128)(2,1)} %collective-permute-done.4.u1), channel_id=1, source_target_pairs={{2,3},{3,2},{4,5},{5,4},{10,11},{11,10},{12,13},{13,12},{18,19},{1... | collective-permute-start | bytes 3145736 | tf_op jit(solution)/shard_map/ppermute | solution.py:390
  40.9 24.6 %collective-permute-start.13 = (bf16[256,2048]{1,0:T(8,128)(2,1)}, bf16[256,2048]{1,0:T(8,128)(2,1)}, u32[]{:S(2)}, u32[]{:S(2)}) collective-permute-start(bf16[256,2048]{1,0:T(8,128)(2,1)} %collective-permute-done.7.d1), channel_id=1, source_target_pairs={{2,3},{3,2},{4,5},{5,4},{10,11},{11,10},{12,13},{13,12},{18,19},{1... | collective-permute-start | bytes 3145736 | tf_op jit(solution)/shard_map/ppermute | solution.py:390
  42.5 34.3 %collective-permute-start.5 = (bf16[2048,256]{1,0:T(8,128)(2,1)}, bf16[2048,256]{1,0:T(8,128)(2,1)}, u32[]{:S(2)}, u32[]{:S(2)}) collective-permute-start(bf16[2048,256]{1,0:T(8,128)(2,1)} %collective-permute-done.4.u1), channel_id=1, source_target_pairs={{0,4},{1,5},{2,6},{3,7},{4,0},{5,1},{6,2},{7,3},{8,12},{9,13},{10,... | collective-permute-start | bytes 3145736 | tf_op jit(solution)/shard_map/ppermute | solution.py:390
  45.8 31.0 %collective-permute-start.8 = (bf16[256,2048]{1,0:T(8,128)(2,1)}, bf16[256,2048]{1,0:T(8,128)(2,1)}, u32[]{:S(2)}, u32[]{:S(2)}) collective-permute-start(bf16[256,2048]{1,0:T(8,128)(2,1)} %collective-permute-done.7.d1), channel_id=1, source_target_pairs={{0,4},{1,5},{2,6},{3,7},{4,0},{5,1},{6,2},{7,3},{8,12},{9,13},{10,... | collective-permute-start | bytes 3145736 | tf_op jit(solution)/shard_map/ppermute | solution.py:390
  45.9 38.5 %collective-permute-start.10 = (bf16[2048,256]{1,0:T(8,128)(2,1)}, bf16[2048,256]{1,0:T(8,128)(2,1)}, u32[]{:S(2)}, u32[]{:S(2)}) collective-permute-start(bf16[2048,256]{1,0:T(8,128)(2,1)} %collective-permute-done.9.gb), channel_id=1, source_target_pairs={{0,4},{1,5},{2,6},{3,7},{4,0},{5,1},{6,2},{7,3},{8,12},{9,13},{10,... | collective-permute-start | bytes 3145736 | tf_op jit(solution)/shard_map/ppermute | solution.py:390
  54.5 30.0 %collective-permute-start.12 = (bf16[2048,256]{1,0:T(8,128)(2,1)}, bf16[2048,256]{1,0:T(8,128)(2,1)}, u32[]{:S(2)}, u32[]{:S(2)}) collective-permute-start(bf16[2048,256]{1,0:T(8,128)(2,1)} %collective-permute-done.11.ub), channel_id=1, source_target_pairs={{0,4},{1,5},{2,6},{3,7},{4,0},{5,1},{6,2},{7,3},{8,12},{9,13},{10,... | collective-permute-start | bytes 3145736 | tf_op jit(solution)/shard_map/ppermute | solution.py:390
  65.5 22.8 %collective-permute-start.14 = (bf16[256,2048]{1,0:T(8,128)(2,1)}, bf16[256,2048]{1,0:T(8,128)(2,1)}, u32[]{:S(2)}, u32[]{:S(2)}) collective-permute-start(bf16[256,2048]{1,0:T(8,128)(2,1)} %collective-permute-done.13.d3b), channel_id=1, source_target_pairs={{0,4},{1,5},{2,6},{3,7},{4,0},{5,1},{6,2},{7,3},{8,12},{9,13},{10,... | collective-permute-start | bytes 3145736 | tf_op jit(solution)/shard_map/ppermute | solution.py:390
  95.2 12.2 %copy-start.3 = (s32[768,2]{0,1:T(2,128)S(1)}, s32[768,2]{0,1:T(2,128)}, u32[]{:S(2)}) copy-start(s32[768,2]{0,1:T(2,128)} %param.10) | copy-start | bytes 18436
  95.2 13.2 %copy-start.4 = (f32[768,2]{0,1:T(2,128)S(1)}, f32[768,2]{0,1:T(2,128)}, u32[]{:S(2)}) copy-start(f32[768,2]{0,1:T(2,128)} %param.11) | copy-start | bytes 18436
  95.2 53.2 %all-to-all-start.1 = ((bf16[128,24,512]{2,1,0:T(8,128)(2,1)}), bf16[128,24,512]{2,1,0:T(8,128)(2,1)S(1)}, u32[]{:S(2)}, u32[]{:S(2)}) async-start(bf16[128,24,512]{2,1,0:T(8,128)(2,1)} %bitcast.16), calls=%async_computation.1 | async-start | bytes 6291456 | tf_op jit(solution)/shard_map/all_to_all | solution.py:417
  107.4 52.5 %copy-start.2 = (f32[512]{0:T(512)S(1)}, f32[512]{0:T(512)}, u32[]{:S(2)}) copy-start(f32[512]{0:T(512)} %param.15) | copy-start | bytes 6148
  109.3 1.0 copy-start
  110.3 1.0 copy-start.1
  151.5 4.9 %collective-permute-start.15 = (f32[1,768]{1,0:T(1,128)S(1)}, f32[1,768]{1,0:T(1,128)S(1)}, u32[]{:S(2)}, u32[]{:S(2)}) collective-permute-start(f32[1,768]{1,0:T(1,128)S(1)} %get-tuple-element.12.own_ref), channel_id=1, source_target_pairs={{0,1},{1,2},{2,3},{3,0},{4,5},{5,6},{6,7},{7,4},{8,9},{9,10},{10,1... | collective-permute-start | bytes 9224 | tf_op jit(solution)/shard_map/ppermute | solution.py:423
  152.1 4.2 %collective-permute-start.16 = (f32[1,768]{1,0:T(1,128)S(1)}, f32[1,768]{1,0:T(1,128)S(1)}, u32[]{:S(2)}, u32[]{:S(2)}) collective-permute-start(f32[1,768]{1,0:T(1,128)S(1)} %get-tuple-element.12.own_ref), channel_id=1, source_target_pairs={{0,3},{1,0},{2,1},{3,2},{4,7},{5,4},{6,5},{7,6},{8,11},{9,8},{10,9... | collective-permute-start | bytes 9224 | tf_op jit(solution)/shard_map/ppermute | solution.py:423
  154.8 5.1 %collective-permute-start.17 = (f32[1,768]{1,0:T(1,128)S(1)}, f32[1,768]{1,0:T(1,128)S(1)}, u32[]{:S(2)}, u32[]{:S(2)}) collective-permute-start(f32[1,768]{1,0:T(1,128)S(1)} %get-tuple-element.12.own_ref), channel_id=1, source_target_pairs={{0,2},{1,3},{2,0},{3,1},{4,6},{5,7},{6,4},{7,5},{8,10},{9,11},{10,... | collective-permute-start | bytes 9224 | tf_op jit(solution)/shard_map/ppermute | solution.py:423

commit v9 on v6

--- a/solution.py
+++ b/solution.py
@@ -146,7 +146,7 @@
     return acts
 
 
-def early_kernel(place_ref, rows_ref, ga, gb, g1, g2, ua, ub, u1, u2, out_ref, weights, sems):
+def early_kernel(place_ref, rows_ref, ga, gb, g1, g2, ua, ub, u1, u2, out_ref, own_ref, weights, sems):
     flag = place_ref[1]
     width, part = g1.shape
 
@@ -166,16 +166,24 @@
             pltpu.make_async_copy(source, target, sems.at[2 * half + n]).start()
     for n, (source, target) in enumerate(plain(1, 0, width, g2, u2)):
         pltpu.make_async_copy(source, target, sems.at[4 + n]).start()
-    start_one(flag, ga, gb, weights.at[2, :, pl.ds(0, part)], sems.at[6])
-    start_one(flag, ua, ub, weights.at[2, :, pl.ds(part, part)], sems.at[7])
+    own_gate = own_ref.at[:, pl.ds(0, part)]
+    own_up = own_ref.at[:, pl.ds(part, part)]
+    start_one(flag, ga, gb, own_gate, sems.at[6])
+    start_one(flag, ua, ub, own_up, sems.at[7])
     waits = [
         functools.partial(wait_for, 0, lo, size, 2 * half) for half, (lo, size) in enumerate(halves_of(width))
     ]
-    out_ref[:, part : 2 * part] = activation(split_block(rows_ref, weights.at[0], waits), part)
-    for at, out in ((1, 2), (2, 0)):
-        wait_for(at, 0, width, 2 + 2 * at)
-        acts = jnp.dot(rows_ref[...], weights[at], preferred_element_type=jnp.float32)
-        out_ref[:, out * part : (out + 1) * part] = activation(acts, part)
+    out_ref[:, 0:part] = activation(split_block(rows_ref, weights.at[0], waits), part)
+    wait_for(1, 0, width, 4)
+    acts = jnp.dot(rows_ref[...], weights[1], preferred_element_type=jnp.float32)
+    out_ref[:, part : 2 * part] = activation(acts, part)
+    pltpu.make_async_copy(ga, own_gate, sems.at[6]).wait()
+    pltpu.make_async_copy(ua, own_up, sems.at[7]).wait()
+
+
+def own_kernel(rows_ref, weights_ref, out_ref):
+    acts = jnp.dot(rows_ref[...], weights_ref[...], preferred_element_type=jnp.float32)
+    out_ref[...] = activation(acts, out_ref.shape[1])
 
 
 def middle_kernel(place_ref, rows_ref, ga, gb, ua, ub, out_ref, weights, sems):
@@ -209,12 +217,23 @@
     return pl.pallas_call(
         early_kernel,
         in_specs=[SMEM, VMEM] + [ANY] * 8,
-        out_specs=VMEM,
-        scratch_shapes=[pltpu.VMEM((3, width, 2 * part), jnp.bfloat16), pltpu.SemaphoreType.DMA((8,))],
-        out_shape=pltpu.VMEM((count, 3 * part), jnp.bfloat16),
-        compiler_params=pltpu.CompilerParams(vmem_limit_bytes=50 * MIB),
+        out_specs=[VMEM, VMEM],
+        scratch_shapes=[pltpu.VMEM((2, width, 2 * part), jnp.bfloat16), pltpu.SemaphoreType.DMA((8,))],
+        out_shape=[pltpu.VMEM((count, 2 * part), jnp.bfloat16), pltpu.VMEM((width, 2 * part), jnp.bfloat16)],
+        compiler_params=pltpu.CompilerParams(vmem_limit_bytes=32 * MIB),
         name="early_hidden",
     )(place, rows, *gates, *ups)
+
+
+def own_hidden(rows, weights):
+    return pl.pallas_call(
+        own_kernel,
+        in_specs=[VMEM, VMEM],
+        out_specs=VMEM,
+        out_shape=pltpu.VMEM((rows.shape[0], weights.shape[1] // 2), jnp.bfloat16),
+        compiler_params=pltpu.CompilerParams(vmem_limit_bytes=32 * MIB),
+        name="own_hidden",
+    )(rows, weights)
 
 
 def middle_hidden(place, rows, gates, ups):
@@ -225,13 +244,13 @@
         in_specs=[SMEM, VMEM] + [ANY] * 4,
         out_specs=VMEM,
         scratch_shapes=[pltpu.VMEM((width, 2 * part), jnp.bfloat16), pltpu.SemaphoreType.DMA((4,))],
-        out_shape=jax.ShapeDtypeStruct((count, part), jnp.bfloat16),
-        compiler_params=pltpu.CompilerParams(vmem_limit_bytes=50 * MIB),
+        out_shape=pltpu.VMEM((count, part), jnp.bfloat16),
+        compiler_params=pltpu.CompilerParams(vmem_limit_bytes=32 * MIB),
         name="middle_hidden",
     )(place, rows, *gates, *ups)
 
 
-def late_kernel(place_ref, early_ref, middle_ref, d0a, d0b, d1, d2, d3a, d3b, out_ref, down, hidden, out, sems, out_sems, *, cuts):
+def late_kernel(place_ref, early_ref, middle_ref, own_ref, d0a, d0b, d1, d2, d3a, d3b, out_ref, down, hidden, out, sems, out_sems, *, cuts):
     flag = place_ref[1]
     senders, pieces, slots, piece = out_ref.shape
     part = d1.shape[0]
@@ -249,7 +268,8 @@
         pltpu.make_async_copy(source(d2, f), target(2, f), sems.at[4 * f + 2]).start()
         start_one(flag, source(d0a, f), source(d0b, f), target(0, f), sems.at[4 * f])
         start_one(flag, source(d3a, f), source(d3b, f), target(3, f), sems.at[4 * f + 3])
-    hidden[:, 0 : 3 * part] = early_ref[...]
+    hidden[:, 0:part] = own_ref[...]
+    hidden[:, part : 3 * part] = early_ref[...]
     hidden[:, 3 * part : 4 * part] = middle_ref[...]
 
     def store(f):
@@ -269,7 +289,7 @@
         store(f).wait()
 
 
-def late_outputs(place, early, middle, downs, senders, pieces):
+def late_outputs(place, early, middle, own, downs, senders, pieces):
     count = early.shape[0]
     part, width = downs[0].shape
     slots = count // senders
@@ -278,7 +298,7 @@
     cuts = 1
     return pl.pallas_call(
         functools.partial(late_kernel, cuts=cuts),
-        in_specs=[SMEM, VMEM, VMEM] + [ANY] * 6,
+        in_specs=[SMEM, VMEM, VMEM, VMEM] + [ANY] * 6,
         out_specs=HBM,
         scratch_shapes=[
             pltpu.VMEM((4 * part, width), jnp.bfloat16),
@@ -290,7 +310,7 @@
         out_shape=pltpu.HBM(shape, jnp.bfloat16),
         compiler_params=pltpu.CompilerParams(vmem_limit_bytes=50 * MIB),
         name="late_outputs",
-    )(place, early, middle, *downs)
+    )(place, early, middle, own, *downs)
 
 
 def table_kernel(ids_ref, scores_ref, out_ref, *, rows, count_tp):
@@ -417,10 +437,11 @@
         buffer.reshape(count_ep, rows, full_width), "ep", split_axis=0, concat_axis=0, tiled=True
     ).reshape(count_ep * rows, full_width)
     received = in_vmem(received)
-    early = early_hidden(place, received, (*gate[0], gate[1], gate[2]), (*up[0], up[1], up[2]))
-    middle = in_vmem(middle_hidden(place, received, gate[3], up[3]))
+    early, weights = early_hidden(place, received, (*gate[0], gate[1], gate[2]), (*up[0], up[1], up[2]))
+    middle = middle_hidden(place, received, gate[3], up[3])
+    own = own_hidden(received, weights)
     outputs = late_outputs(
-        place, early, middle, (*down[0], down[1], down[2], *down[3]), count_ep, count_tp
+        place, early, middle, own, (*down[0], down[1], down[2], *down[3]), count_ep, count_tp
     )
     returned = lax.all_to_all(
         outputs.reshape(count_ep * count_tp, rows, part_width), AXES, split_axis=0, concat_axis=0, tiled=True

time: 153 us -> 153 us (level)
  starting transfers between devices: 54.9 us -> 63 us
  waiting for transfers between devices: 61.4 us -> 53.3 us
    ppermute x15, waiting for transfers between devices: 23.5 us -> 15.4 us  [send(): return lax.ppermute(weight, AXES, pairs)]
    ppermute x15, starting transfers between devices: 31.6 us -> 38.3 us  [send(): return lax.ppermute(weight, AXES, pairs)]
    pallas_call x1, Pallas kernels: 7.81 us -> 5.74 us  [early_hidden(): pl.pallas_call(early_kernel, in_specs=[SMEM, VMEM] + [ANY] * 8, out_specs...]
    pallas_call x0 -> x1, Pallas kernels: none -> 1.82 us  [own_hidden(): pl.pallas_call(own_kernel, in_specs=[VMEM, VMEM], out_specs=VMEM, out_sha...]
    unnamed x14 -> x12, local copies, waits for them, and re-layouts: 3.88 us -> 3.88 us
  transfers between devices with their start and end apart: 20 -> 20, of which waited for: 6 -> 6; matrix products, arithmetic and copies ran while one was open for 2% -> 1% of each run, Pallas kernels for 14% -> 14%
where the time goes in v9:
time: 153 us; the launch traced here: 152 us
  starting transfers between devices  63 us (41%)
  waiting for transfers between devices  53.3 us (35%)
  Pallas kernels  31.7 us (21%)
  local copies, waits for them, and re-layouts  3.88 us (3%)
    ppermute x15, starting transfers between devices, send(): return lax.ppermute(weight, AXES, pairs)  38.3 us
    all_to_all x1, waiting for transfers between devices, per_device(): lax.all_to_all(outputs.reshape(count_ep * count_tp, rows, part_width), AX...  35 us
    ppermute x15, waiting for transfers between devices, send(): return lax.ppermute(weight, AXES, pairs)  15.4 us
    all_to_all x1, starting transfers between devices, per_device(): lax.all_to_all(outputs.reshape(count_ep * count_tp, rows, part_width), AX...  10.6 us
    all_to_all x1, starting transfers between devices, per_device(): lax.all_to_all(buffer.reshape(count_ep, rows, full_width), 'ep', split_ax...  10.3 us
    pallas_call x1, Pallas kernels, dispatch_buffer(): pl.pallas_call(functools.partial(dispatch_kernel, rows=rows, chunks=chunk...  7.14 us
    pallas_call x1, Pallas kernels, late_outputs(): pl.pallas_call(functools.partial(late_kernel, cuts=cuts), in_specs=[SMEM,...  6.76 us
    pallas_call x1, Pallas kernels, early_hidden(): pl.pallas_call(early_kernel, in_specs=[SMEM, VMEM] + [ANY] * 8, out_specs...  5.74 us
  transfers between devices with their start and end apart: 20, of which 6 were waited for; matrix products, arithmetic and copies ran while one was open for 1% of the time, Pallas kernels for 14%

profile of v9, /device:TPU:0, one launch (start us, length us, event | category | flops | bytes accessed | tf_op | source)
XLA Modules:
  0.0 152.2 jit_solution(2974485208327968448)
XLA Ops:
  0.0 1.6 %collective-permute-start.1 = (bf16[2048,256]{1,0:T(8,128)(2,1)}, bf16[2048,256]{1,0:T(8,128)(2,1)}, u32[]{:S(2)}, u32[]{:S(2)}) collective-permute-start(bf16[2048,256]{1,0:T(8,128)(2,1)} %bitcast.19), channel_id=1, source_target_pairs={{0,1},{1,0},{2,5},{3,4},{4,3},{5,2},{6,7},{7,6},{8,9},{9,8},{10,13... | collective-permute-start | bytes 3145736 | tf_op jit(solution)/shard_map/ppermute | solution.py:420
  1.6 0.4 collective-permute-start.4
  2.0 1.0 collective-permute-start
  3.0 0.0 collective-permute-start.3
  3.0 1.1 collective-permute-start.11
  4.1 7.1 %dispatch_buffer.1 = bf16[768,2048]{1,0:T(8,128)(2,1)} custom-call(s32[2,768]{1,0:T(2,128)} %bitcast.28, f32[1,2048]{1,0:T(1,128)} %bitcast.29, bf16[768,2048]{1,0:T(8,128)(2,1)} %tokens_ref.1), custom_call_target="tpu_custom_call" | custom-call | tf_op jit(solution)/shard_map/dispatch_buffer/pallas_call | solution.py:99
  11.3 10.3 %all-to-all-start = ((bf16[32,24,2048]{2,1,0:T(8,128)(2,1)}), bf16[32,24,2048]{2,1,0:T(8,128)(2,1)S(1)}, u32[]{:S(2)}, u32[]{:S(2)}) async-start(bf16[32,24,2048]{2,1,0:T(8,128)(2,1)} %bitcast.17), calls=%async_computation | async-start | bytes 6291456 | tf_op jit(solution)/shard_map/all_to_all | solution.py:436
  21.6 0.0 collective-permute-done.1.g1
  21.6 0.4 collective-permute-start.2
  21.9 4.4 %collective-permute-done.4.u1 = bf16[2048,256]{1,0:T(8,128)(2,1)} collective-permute-done((bf16[2048,256]{1,0:T(8,128)(2,1)}, bf16[2048,256]{1,0:T(8,128)(2,1)}, u32[]{:S(2)}, u32[]{:S(2)}) %collective-permute-start.4) | collective-permute-done | bytes 1048608 | tf_op jit(solution)/shard_map/ppermute | solution.py:420
  26.4 1.7 %collective-permute-start.6 = (bf16[2048,256]{1,0:T(8,128)(2,1)}, bf16[2048,256]{1,0:T(8,128)(2,1)}, u32[]{:S(2)}, u32[]{:S(2)}) collective-permute-start(bf16[2048,256]{1,0:T(8,128)(2,1)} %collective-permute-done.1.g1), channel_id=1, source_target_pairs={{2,3},{3,2},{4,5},{5,4},{10,11},{11,10},{12,13},{13,12},{18,19},{1... | collective-permute-start | bytes 3145736 | tf_op jit(solution)/shard_map/ppermute | solution.py:420
  28.0 1.6 %collective-permute-start.8 = (bf16[2048,256]{1,0:T(8,128)(2,1)}, bf16[2048,256]{1,0:T(8,128)(2,1)}, u32[]{:S(2)}, u32[]{:S(2)}) collective-permute-start(bf16[2048,256]{1,0:T(8,128)(2,1)} %collective-permute-done.4.u1), channel_id=1, source_target_pairs={{2,3},{3,2},{4,5},{5,4},{10,11},{11,10},{12,13},{13,12},{18,19},{1... | collective-permute-start | bytes 3145736 | tf_op jit(solution)/shard_map/ppermute | solution.py:420
  29.7 0.0 collective-permute-done.3.ub
  29.7 2.9 %collective-permute-start.5 = (bf16[2048,256]{1,0:T(8,128)(2,1)}, bf16[2048,256]{1,0:T(8,128)(2,1)}, u32[]{:S(2)}, u32[]{:S(2)}) collective-permute-start(bf16[2048,256]{1,0:T(8,128)(2,1)} %collective-permute-done.4.u1), channel_id=1, source_target_pairs={{0,4},{1,5},{2,6},{3,7},{4,0},{5,1},{6,2},{7,3},{8,12},{9,13},{10,... | collective-permute-start | bytes 3145736 | tf_op jit(solution)/shard_map/ppermute | solution.py:420
  32.6 11.0 %collective-permute-done.11.d1 = bf16[256,2048]{1,0:T(8,128)(2,1)} collective-permute-done((bf16[256,2048]{1,0:T(8,128)(2,1)}, bf16[256,2048]{1,0:T(8,128)(2,1)}, u32[]{:S(2)}, u32[]{:S(2)}) %collective-permute-start.11) | collective-permute-done | bytes 1048608 | tf_op jit(solution)/shard_map/ppermute | solution.py:420
  43.6 1.6 %collective-permute-start.13 = (bf16[256,2048]{1,0:T(8,128)(2,1)}, bf16[256,2048]{1,0:T(8,128)(2,1)}, u32[]{:S(2)}, u32[]{:S(2)}) collective-permute-start(bf16[256,2048]{1,0:T(8,128)(2,1)} %collective-permute-done.11.d1), channel_id=1, source_target_pairs={{2,3},{3,2},{4,5},{5,4},{10,11},{11,10},{12,13},{13,12},{18,19},{1... | collective-permute-start | bytes 3145736 | tf_op jit(solution)/shard_map/ppermute | solution.py:420
  45.2 3.6 %collective-permute-start.7 = (bf16[2048,256]{1,0:T(8,128)(2,1)}, bf16[2048,256]{1,0:T(8,128)(2,1)}, u32[]{:S(2)}, u32[]{:S(2)}) collective-permute-start(bf16[2048,256]{1,0:T(8,128)(2,1)} %collective-permute-done.6.gb), channel_id=1, source_target_pairs={{0,4},{1,5},{2,6},{3,7},{4,0},{5,1},{6,2},{7,3},{8,12},{9,13},{10,... | collective-permute-start | bytes 3145736 | tf_op jit(solution)/shard_map/ppermute | solution.py:420
  48.8 0.0 collective-permute-done.8.ub
  48.8 11.0 %collective-permute-start.9 = (bf16[2048,256]{1,0:T(8,128)(2,1)}, bf16[2048,256]{1,0:T(8,128)(2,1)}, u32[]{:S(2)}, u32[]{:S(2)}) collective-permute-start(bf16[2048,256]{1,0:T(8,128)(2,1)} %collective-permute-done.8.ub), channel_id=1, source_target_pairs={{0,4},{1,5},{2,6},{3,7},{4,0},{5,1},{6,2},{7,3},{8,12},{9,13},{10,... | collective-permute-start | bytes 3145736 | tf_op jit(solution)/shard_map/ppermute | solution.py:420
  59.9 0.0 collective-permute-start.12
  59.9 11.2 %collective-permute-start.14 = (bf16[256,2048]{1,0:T(8,128)(2,1)}, bf16[256,2048]{1,0:T(8,128)(2,1)}, u32[]{:S(2)}, u32[]{:S(2)}) collective-permute-start(bf16[256,2048]{1,0:T(8,128)(2,1)} %collective-permute-done.13.d3b), channel_id=1, source_target_pairs={{0,4},{1,5},{2,6},{3,7},{4,0},{5,1},{6,2},{7,3},{8,12},{9,13},{10,... | collective-permute-start | bytes 3145736 | tf_op jit(solution)/shard_map/ppermute | solution.py:420
  71.1 0.1 pad_add_fusion.place_ref
  71.2 0.0 all-to-all-done
  71.2 5.7 %early_hidden.1 = (bf16[768,512]{1,0:T(8,128)(2,1)S(1)}, bf16[2048,512]{1,0:T(8,128)(2,1)S(1)}) custom-call(s32[2]{0:T(128)S(1)} %pad_add_fusion.place_ref, bf16[768,2048]{1,0:T(8,128)(2,1)S(1)} %bitcast.12, bf16[2048,256]{1,0:T(8,128)(2,1)} %bitcast.21, bf16[2048,256]{1,0:T(8,128)(2,1)} %collective-permute-done.gb, ...), custom_call_target="tpu_custom_call" | custom-call | tf_op jit(solution)/shard_map/early_hidden/pallas_call | solution.py:217
  76.9 1.8 %own_hidden.1.own_ref = bf16[768,256]{1,0:T(8,128)(2,1)S(1)} custom-call(bf16[768,2048]{1,0:T(8,128)(2,1)S(1)} %bitcast.13, bf16[2048,512]{1,0:T(8,128)(2,1)S(1)} %get-tuple-element.10.weights_ref), custom_call_target="tpu_custom_call" | custom-call | tf_op jit(solution)/shard_map/own_hidden/pallas_call | solution.py:229
  78.8 0.0 collective-permute-done.7.ga
  78.8 3.9 %middle_hidden.1.middle_ref = bf16[768,256]{1,0:T(8,128)(2,1)S(1)} custom-call(s32[2]{0:T(128)S(1)} %pad_add_fusion.place_ref, bf16[768,2048]{1,0:T(8,128)(2,1)S(1)} %bitcast.14, bf16[2048,256]{1,0:T(8,128)(2,1)} %collective-permute-done.7.ga, bf16[2048,256]{1,0:T(8,128)(2,1)} %collective-permute-done.6.gb, bf16[2048,256]{1,0:T(8,128)(2,1)} %collective-permute-done.9.ua, ...), custom_call_target="tpu_custom_call" | custom-call | tf_op jit(solution)/shard_map/middle_hidden/pallas_call | solution.py:242
  82.7 0.0 collective-permute-done.10.d0b
  82.7 0.0 collective-permute-done.12.d2
  82.7 6.8 %late_outputs.1 = bf16[32,4,24,512]{3,2,1,0:T(8,128)(2,1)} custom-call(s32[2]{0:T(128)S(1)} %pad_add_fusion.place_ref, bf16[768,512]{1,0:T(8,128)(2,1)S(1)} %get-tuple-element.9.early_ref, bf16[768,256]{1,0:T(8,128)(2,1)S(1)} %middle_hidden.1.middle_ref, bf16[768,256]{1,0:T(8,128)(2,1)S(1)} %own_hidden.1.own_ref, bf16[256,2048]{1,0:T(8,128)(2,1)} %bitcast.27, ...), custom_call_target="tpu_custom_call" | custom-call | tf_op jit(solution)/shard_map/late_outputs/pallas_call | solution.py:299
  89.5 0.0 copy-start.3
  89.5 0.0 copy-start.4
  89.5 10.6 %all-to-all-start.1 = ((bf16[128,24,512]{2,1,0:T(8,128)(2,1)}), bf16[128,24,512]{2,1,0:T(8,128)(2,1)S(1)}, u32[]{:S(2)}, u32[]{:S(2)}) async-start(bf16[128,24,512]{2,1,0:T(8,128)(2,1)} %bitcast.18), calls=%async_computation.1 | async-start | bytes 6291456 | tf_op jit(solution)/shard_map/all_to_all | solution.py:446
  100.1 0.0 copy-start.2
  100.1 0.9 copy.9.ids_ref
  101.1 0.9 copy.10.scores_ref
  102.0 1.0 copy-done
  103.0 1.0 copy-done.1
  104.0 2.2 %columns.1.table_ref = f32[768,4]{1,0:T(8,128)S(1)} custom-call(s32[768,2]{1,0:T(8,128)S(1)} %copy-done, f32[768,2]{1,0:T(8,128)S(1)} %copy-done.1), custom_call_target="tpu_custom_call" | custom-call | tf_op jit(solution)/shard_map/columns/pallas_call | solution.py:340
  106.2 35.0 %all-to-all-done.1 = bf16[128,24,512]{2,1,0:T(8,128)(2,1)S(1)} async-done(((bf16[128,24,512]{2,1,0:T(8,128)(2,1)}), bf16[128,24,512]{2,1,0:T(8,128)(2,1)S(1)}, u32[]{:S(2)}, u32[]{:S(2)}) %all-to-all-start.1) | async-done | bytes 3145760 | tf_op jit(solution)/shard_map/all_to_all | solution.py:446
  141.2 3.0 %combine.1 = (f32[768,512]{1,0:T(8,128)S(1)}, f32[1,768]{1,0:T(1,128)S(1)}) custom-call(f32[768,4]{1,0:T(8,128)S(1)} %columns.1.table_ref, bf16[3072,512]{1,0:T(8,128)(2,1)S(1)} %bitcast.15), custom_call_target="tpu_custom_call" | custom-call | tf_op jit(solution)/shard_map/combine/pallas_call | solution.py:368
  144.2 0.6 collective-permute-start.15
  144.8 2.6 %collective-permute-start.16 = (f32[1,768]{1,0:T(1,128)S(1)}, f32[1,768]{1,0:T(1,128)S(1)}, u32[]{:S(2)}, u32[]{:S(2)}) collective-permute-start(f32[1,768]{1,0:T(1,128)S(1)} %get-tuple-element.12.own_ref), channel_id=1, source_target_pairs={{0,2},{1,3},{2,0},{3,1},{4,6},{5,7},{6,4},{7,5},{8,10},{9,11},{10,... | collective-permute-start | bytes 9224 | tf_op jit(solution)/shard_map/ppermute | solution.py:452
  147.4 0.7 collective-permute-start.17
  148.1 0.9 collective-permute-done.15.a_ref
  149.0 0.9 collective-permute-done.16.b_ref
  149.9 1.1 collective-permute-done.17.c_ref
  151.0 1.1 scale.1
  (13 shorter events, 0.0 us)
Async XLA Ops:
  0.0 21.6 %collective-permute-start.1 = (bf16[2048,256]{1,0:T(8,128)(2,1)}, bf16[2048,256]{1,0:T(8,128)(2,1)}, u32[]{:S(2)}, u32[]{:S(2)}) collective-permute-start(bf16[2048,256]{1,0:T(8,128)(2,1)} %bitcast.19), channel_id=1, source_target_pairs={{0,1},{1,0},{2,5},{3,4},{4,3},{5,2},{6,7},{7,6},{8,9},{9,8},{10,13... | collective-permute-start | bytes 3145736 | tf_op jit(solution)/shard_map/ppermute | solution.py:420
  1.6 24.7 %collective-permute-start.4 = (bf16[2048,256]{1,0:T(8,128)(2,1)}, bf16[2048,256]{1,0:T(8,128)(2,1)}, u32[]{:S(2)}, u32[]{:S(2)}) collective-permute-start(bf16[2048,256]{1,0:T(8,128)(2,1)} %bitcast.22), channel_id=1, source_target_pairs={{0,1},{1,0},{2,5},{3,4},{4,3},{5,2},{6,7},{7,6},{8,9},{9,8},{10,13... | collective-permute-start | bytes 3145736 | tf_op jit(solution)/shard_map/ppermute | solution.py:420
  2.0 26.0 %collective-permute-start = (bf16[2048,256]{1,0:T(8,128)(2,1)}, bf16[2048,256]{1,0:T(8,128)(2,1)}, u32[]{:S(2)}, u32[]{:S(2)}) collective-permute-start(bf16[2048,256]{1,0:T(8,128)(2,1)} %bitcast.20), channel_id=1, source_target_pairs={{0,4},{1,5},{2,6},{3,7},{4,0},{5,1},{6,2},{7,3},{8,12},{9,13},{10,... | collective-permute-start | bytes 3145736 | tf_op jit(solution)/shard_map/ppermute | solution.py:420
  3.0 26.7 %collective-permute-start.3 = (bf16[2048,256]{1,0:T(8,128)(2,1)}, bf16[2048,256]{1,0:T(8,128)(2,1)}, u32[]{:S(2)}, u32[]{:S(2)}) collective-permute-start(bf16[2048,256]{1,0:T(8,128)(2,1)} %bitcast.23), channel_id=1, source_target_pairs={{0,4},{1,5},{2,6},{3,7},{4,0},{5,1},{6,2},{7,3},{8,12},{9,13},{10,... | collective-permute-start | bytes 3145736 | tf_op jit(solution)/shard_map/ppermute | solution.py:420
  3.0 40.6 %collective-permute-start.11 = (bf16[256,2048]{1,0:T(8,128)(2,1)}, bf16[256,2048]{1,0:T(8,128)(2,1)}, u32[]{:S(2)}, u32[]{:S(2)}) collective-permute-start(bf16[256,2048]{1,0:T(8,128)(2,1)} %bitcast.25), channel_id=1, source_target_pairs={{0,1},{1,0},{2,5},{3,4},{4,3},{5,2},{6,7},{7,6},{8,9},{9,8},{10,13... | collective-permute-start | bytes 3145736 | tf_op jit(solution)/shard_map/ppermute | solution.py:420
  11.3 59.9 %all-to-all-start = ((bf16[32,24,2048]{2,1,0:T(8,128)(2,1)}), bf16[32,24,2048]{2,1,0:T(8,128)(2,1)S(1)}, u32[]{:S(2)}, u32[]{:S(2)}) async-start(bf16[32,24,2048]{2,1,0:T(8,128)(2,1)} %bitcast.17), calls=%async_computation | async-start | bytes 6291456 | tf_op jit(solution)/shard_map/all_to_all | solution.py:436
  21.6 23.6 %collective-permute-start.2 = (bf16[2048,256]{1,0:T(8,128)(2,1)}, bf16[2048,256]{1,0:T(8,128)(2,1)}, u32[]{:S(2)}, u32[]{:S(2)}) collective-permute-start(bf16[2048,256]{1,0:T(8,128)(2,1)} %collective-permute-done.1.g1), channel_id=1, source_target_pairs={{0,4},{1,5},{2,6},{3,7},{4,0},{5,1},{6,2},{7,3},{8,12},{9,13},{10,... | collective-permute-start | bytes 3145736 | tf_op jit(solution)/shard_map/ppermute | solution.py:420
  26.4 18.9 %collective-permute-start.6 = (bf16[2048,256]{1,0:T(8,128)(2,1)}, bf16[2048,256]{1,0:T(8,128)(2,1)}, u32[]{:S(2)}, u32[]{:S(2)}) collective-permute-start(bf16[2048,256]{1,0:T(8,128)(2,1)} %collective-permute-done.1.g1), channel_id=1, source_target_pairs={{2,3},{3,2},{4,5},{5,4},{10,11},{11,10},{12,13},{13,12},{18,19},{1... | collective-permute-start | bytes 3145736 | tf_op jit(solution)/shard_map/ppermute | solution.py:420
  28.0 20.8 %collective-permute-start.8 = (bf16[2048,256]{1,0:T(8,128)(2,1)}, bf16[2048,256]{1,0:T(8,128)(2,1)}, u32[]{:S(2)}, u32[]{:S(2)}) collective-permute-start(bf16[2048,256]{1,0:T(8,128)(2,1)} %collective-permute-done.4.u1), channel_id=1, source_target_pairs={{2,3},{3,2},{4,5},{5,4},{10,11},{11,10},{12,13},{13,12},{18,19},{1... | collective-permute-start | bytes 3145736 | tf_op jit(solution)/shard_map/ppermute | solution.py:420
  29.7 30.2 %collective-permute-start.5 = (bf16[2048,256]{1,0:T(8,128)(2,1)}, bf16[2048,256]{1,0:T(8,128)(2,1)}, u32[]{:S(2)}, u32[]{:S(2)}) collective-permute-start(bf16[2048,256]{1,0:T(8,128)(2,1)} %collective-permute-done.4.u1), channel_id=1, source_target_pairs={{0,4},{1,5},{2,6},{3,7},{4,0},{5,1},{6,2},{7,3},{8,12},{9,13},{10,... | collective-permute-start | bytes 3145736 | tf_op jit(solution)/shard_map/ppermute | solution.py:420
  43.6 16.3 %collective-permute-start.13 = (bf16[256,2048]{1,0:T(8,128)(2,1)}, bf16[256,2048]{1,0:T(8,128)(2,1)}, u32[]{:S(2)}, u32[]{:S(2)}) collective-permute-start(bf16[256,2048]{1,0:T(8,128)(2,1)} %collective-permute-done.11.d1), channel_id=1, source_target_pairs={{2,3},{3,2},{4,5},{5,4},{10,11},{11,10},{12,13},{13,12},{18,19},{1... | collective-permute-start | bytes 3145736 | tf_op jit(solution)/shard_map/ppermute | solution.py:420
  45.2 37.5 %collective-permute-start.10 = (bf16[256,2048]{1,0:T(8,128)(2,1)}, bf16[256,2048]{1,0:T(8,128)(2,1)}, u32[]{:S(2)}, u32[]{:S(2)}) collective-permute-start(bf16[256,2048]{1,0:T(8,128)(2,1)} %bitcast.26), channel_id=1, source_target_pairs={{0,4},{1,5},{2,6},{3,7},{4,0},{5,1},{6,2},{7,3},{8,12},{9,13},{10,... | collective-permute-start | bytes 3145736 | tf_op jit(solution)/shard_map/ppermute | solution.py:420
  45.2 33.6 %collective-permute-start.7 = (bf16[2048,256]{1,0:T(8,128)(2,1)}, bf16[2048,256]{1,0:T(8,128)(2,1)}, u32[]{:S(2)}, u32[]{:S(2)}) collective-permute-start(bf16[2048,256]{1,0:T(8,128)(2,1)} %collective-permute-done.6.gb), channel_id=1, source_target_pairs={{0,4},{1,5},{2,6},{3,7},{4,0},{5,1},{6,2},{7,3},{8,12},{9,13},{10,... | collective-permute-start | bytes 3145736 | tf_op jit(solution)/shard_map/ppermute | solution.py:420
  48.8 30.0 %collective-permute-start.9 = (bf16[2048,256]{1,0:T(8,128)(2,1)}, bf16[2048,256]{1,0:T(8,128)(2,1)}, u32[]{:S(2)}, u32[]{:S(2)}) collective-permute-start(bf16[2048,256]{1,0:T(8,128)(2,1)} %collective-permute-done.8.ub), channel_id=1, source_target_pairs={{0,4},{1,5},{2,6},{3,7},{4,0},{5,1},{6,2},{7,3},{8,12},{9,13},{10,... | collective-permute-start | bytes 3145736 | tf_op jit(solution)/shard_map/ppermute | solution.py:420
  59.9 22.8 %collective-permute-start.12 = (bf16[256,2048]{1,0:T(8,128)(2,1)}, bf16[256,2048]{1,0:T(8,128)(2,1)}, u32[]{:S(2)}, u32[]{:S(2)}) collective-permute-start(bf16[256,2048]{1,0:T(8,128)(2,1)} %collective-permute-done.11.d1), channel_id=1, source_target_pairs={{0,4},{1,5},{2,6},{3,7},{4,0},{5,1},{6,2},{7,3},{8,12},{9,13},{10,... | collective-permute-start | bytes 3145736 | tf_op jit(solution)/shard_map/ppermute | solution.py:420
  59.9 22.8 %collective-permute-start.14 = (bf16[256,2048]{1,0:T(8,128)(2,1)}, bf16[256,2048]{1,0:T(8,128)(2,1)}, u32[]{:S(2)}, u32[]{:S(2)}) collective-permute-start(bf16[256,2048]{1,0:T(8,128)(2,1)} %collective-permute-done.13.d3b), channel_id=1, source_target_pairs={{0,4},{1,5},{2,6},{3,7},{4,0},{5,1},{6,2},{7,3},{8,12},{9,13},{10,... | collective-permute-start | bytes 3145736 | tf_op jit(solution)/shard_map/ppermute | solution.py:420
  89.5 10.6 %copy-start.3 = (s32[768,2]{0,1:T(2,128)S(1)}, s32[768,2]{0,1:T(2,128)}, u32[]{:S(2)}) copy-start(s32[768,2]{0,1:T(2,128)} %param.10) | copy-start | bytes 18436
  89.5 11.6 %copy-start.4 = (f32[768,2]{0,1:T(2,128)S(1)}, f32[768,2]{0,1:T(2,128)}, u32[]{:S(2)}) copy-start(f32[768,2]{0,1:T(2,128)} %param.11) | copy-start | bytes 18436
  89.5 51.6 %all-to-all-start.1 = ((bf16[128,24,512]{2,1,0:T(8,128)(2,1)}), bf16[128,24,512]{2,1,0:T(8,128)(2,1)S(1)}, u32[]{:S(2)}, u32[]{:S(2)}) async-start(bf16[128,24,512]{2,1,0:T(8,128)(2,1)} %bitcast.18), calls=%async_computation.1 | async-start | bytes 6291456 | tf_op jit(solution)/shard_map/all_to_all | solution.py:446
  100.1 50.9 %copy-start.2 = (f32[512]{0:T(512)S(1)}, f32[512]{0:T(512)}, u32[]{:S(2)}) copy-start(f32[512]{0:T(512)} %param.15) | copy-start | bytes 6148
  102.0 1.0 copy-start
  103.0 1.0 copy-start.1
  144.2 4.9 %collective-permute-start.15 = (f32[1,768]{1,0:T(1,128)S(1)}, f32[1,768]{1,0:T(1,128)S(1)}, u32[]{:S(2)}, u32[]{:S(2)}) collective-permute-start(f32[1,768]{1,0:T(1,128)S(1)} %get-tuple-element.12.own_ref), channel_id=1, source_target_pairs={{0,1},{1,2},{2,3},{3,0},{4,5},{5,6},{6,7},{7,4},{8,9},{9,10},{10,1... | collective-permute-start | bytes 9224 | tf_op jit(solution)/shard_map/ppermute | solution.py:452
  144.8 5.1 %collective-permute-start.16 = (f32[1,768]{1,0:T(1,128)S(1)}, f32[1,768]{1,0:T(1,128)S(1)}, u32[]{:S(2)}, u32[]{:S(2)}) collective-permute-start(f32[1,768]{1,0:T(1,128)S(1)} %get-tuple-element.12.own_ref), channel_id=1, source_target_pairs={{0,2},{1,3},{2,0},{3,1},{4,6},{5,7},{6,4},{7,5},{8,10},{9,11},{10,... | collective-permute-start | bytes 9224 | tf_op jit(solution)/shard_map/ppermute | solution.py:452
  147.4 3.6 %collective-permute-start.17 = (f32[1,768]{1,0:T(1,128)S(1)}, f32[1,768]{1,0:T(1,128)S(1)}, u32[]{:S(2)}, u32[]{:S(2)}) collective-permute-start(f32[1,768]{1,0:T(1,128)S(1)} %get-tuple-element.12.own_ref), channel_id=1, source_target_pairs={{0,3},{1,0},{2,1},{3,2},{4,7},{5,4},{6,5},{7,6},{8,11},{9,8},{10,9... | collective-permute-start | bytes 9224 | tf_op jit(solution)/shard_map/ppermute | solution.py:452

commit v10 on v8

--- a/solution.py
+++ b/solution.py
@@ -146,9 +146,7 @@
     return acts
 
 
-def early_kernel(
-    place_ref, rows_ref, ga, gb, g1, g2, ua, ub, u1, u2, d0a, d0b, d1, d2, out_ref, down_ref, weights, sems
-):
+def early_kernel(place_ref, rows_ref, ga, gb, g1, g2, ua, ub, u1, u2, out_ref, own_ref, weights, sems):
     flag = place_ref[1]
     width, part = g1.shape
 
@@ -168,21 +166,30 @@
             pltpu.make_async_copy(source, target, sems.at[2 * half + n]).start()
     for n, (source, target) in enumerate(plain(1, 0, width, g2, u2)):
         pltpu.make_async_copy(source, target, sems.at[4 + n]).start()
-    start_one(flag, ga, gb, weights.at[2, :, pl.ds(0, part)], sems.at[6])
-    start_one(flag, ua, ub, weights.at[2, :, pl.ds(part, part)], sems.at[7])
-    start_one(flag, d0a, d0b, down_ref.at[pl.ds(0, part)], sems.at[8])
-    pltpu.make_async_copy(d1, down_ref.at[pl.ds(part, part)], sems.at[9]).start()
-    pltpu.make_async_copy(d2, down_ref.at[pl.ds(2 * part, part)], sems.at[10]).start()
+    own_gate = own_ref.at[:, pl.ds(0, part)]
+    own_up = own_ref.at[:, pl.ds(part, part)]
+    start_one(flag, ga, gb, own_gate, sems.at[6])
+    start_one(flag, ua, ub, own_up, sems.at[7])
     waits = [
         functools.partial(wait_for, 0, lo, size, 2 * half) for half, (lo, size) in enumerate(halves_of(width))
     ]
-    out_ref[:, part : 2 * part] = activation(split_block(rows_ref, weights.at[0], waits), part)
-    for at, out in ((1, 2), (2, 0)):
-        wait_for(at, 0, width, 2 + 2 * at)
-        acts = jnp.dot(rows_ref[...], weights[at], preferred_element_type=jnp.float32)
-        out_ref[:, out * part : (out + 1) * part] = activation(acts, part)
+    out_ref[:, 0:part] = activation(split_block(rows_ref, weights.at[0], waits), part)
+    wait_for(1, 0, width, 4)
+    acts = jnp.dot(rows_ref[...], weights[1], preferred_element_type=jnp.float32)
+    out_ref[:, part : 2 * part] = activation(acts, part)
+    pltpu.make_async_copy(ga, own_gate, sems.at[6]).wait()
+    pltpu.make_async_copy(ua, own_up, sems.at[7]).wait()
+
+
+def own_kernel(place_ref, rows_ref, weights_ref, d0a, d0b, d1, d2, out_ref, down_ref, sems):
+    part = d1.shape[0]
+    start_one(place_ref[1], d0a, d0b, down_ref.at[pl.ds(0, part)], sems.at[0])
+    pltpu.make_async_copy(d1, down_ref.at[pl.ds(part, part)], sems.at[1]).start()
+    pltpu.make_async_copy(d2, down_ref.at[pl.ds(2 * part, part)], sems.at[2]).start()
+    acts = jnp.dot(rows_ref[...], weights_ref[...], preferred_element_type=jnp.float32)
+    out_ref[...] = activation(acts, out_ref.shape[1])
     for i in range(3):
-        pltpu.make_async_copy(d1, down_ref.at[pl.ds(i * part, part)], sems.at[8 + i]).wait()
+        pltpu.make_async_copy(d1, down_ref.at[pl.ds(i * part, part)], sems.at[i]).wait()
 
 
 def middle_kernel(place_ref, rows_ref, ga, gb, ua, ub, out_ref, weights, sems):
@@ -210,18 +217,34 @@
 VMEM = pl.BlockSpec(memory_space=pltpu.VMEM)
 
 
-def early_hidden(place, rows, gates, ups, downs):
+def early_hidden(place, rows, gates, ups):
     count, width = rows.shape
     part = gates[0].shape[1]
     return pl.pallas_call(
         early_kernel,
-        in_specs=[SMEM, VMEM] + [ANY] * 12,
+        in_specs=[SMEM, VMEM] + [ANY] * 8,
         out_specs=[VMEM, VMEM],
-        scratch_shapes=[pltpu.VMEM((3, width, 2 * part), jnp.bfloat16), pltpu.SemaphoreType.DMA((11,))],
-        out_shape=[pltpu.VMEM((count, 3 * part), jnp.bfloat16), pltpu.VMEM((3 * part, width), jnp.bfloat16)],
+        scratch_shapes=[pltpu.VMEM((2, width, 2 * part), jnp.bfloat16), pltpu.SemaphoreType.DMA((8,))],
+        out_shape=[pltpu.VMEM((count, 2 * part), jnp.bfloat16), pltpu.VMEM((width, 2 * part), jnp.bfloat16)],
         compiler_params=pltpu.CompilerParams(vmem_limit_bytes=32 * MIB),
         name="early_hidden",
-    )(place, rows, *gates, *ups, *downs)
+    )(place, rows, *gates, *ups)
+
+
+def own_hidden(place, rows, weights, downs):
+    part, width = downs[0].shape
+    return pl.pallas_call(
+        own_kernel,
+        in_specs=[SMEM, VMEM, VMEM] + [ANY] * 4,
+        out_specs=[VMEM, VMEM],
+        scratch_shapes=[pltpu.SemaphoreType.DMA((3,))],
+        out_shape=[
+            pltpu.VMEM((rows.shape[0], part), jnp.bfloat16),
+            pltpu.VMEM((3 * part, width), jnp.bfloat16),
+        ],
+        compiler_params=pltpu.CompilerParams(vmem_limit_bytes=32 * MIB),
+        name="own_hidden",
+    )(place, rows, weights, *downs)
 
 
 def middle_hidden(place, rows, gates, ups):
@@ -232,15 +255,16 @@
         in_specs=[SMEM, VMEM] + [ANY] * 4,
         out_specs=VMEM,
         scratch_shapes=[pltpu.VMEM((width, 2 * part), jnp.bfloat16), pltpu.SemaphoreType.DMA((4,))],
-        out_shape=jax.ShapeDtypeStruct((count, part), jnp.bfloat16),
+        out_shape=pltpu.VMEM((count, part), jnp.bfloat16),
         compiler_params=pltpu.CompilerParams(vmem_limit_bytes=32 * MIB),
         name="middle_hidden",
     )(place, rows, *gates, *ups)
 
 
-def late_kernel(place_ref, early_ref, middle_ref, down_ref, d3a, d3b, out_ref, last, out, sems, out_sems):
+def late_kernel(place_ref, early_ref, middle_ref, own_ref, down_ref, d3a, d3b, out_ref, last, hidden, out, sems, out_sems):
     flag = place_ref[1]
     pieces, senders, slots, piece = out.shape
+    part = last.shape[0]
 
     def columns(ref, f):
         return ref.at[:, pl.ds(f * piece, piece)]
@@ -250,9 +274,11 @@
 
     for f in range(pieces):
         start_one(flag, columns(d3a, f), columns(d3b, f), columns(last, f), sems.at[f])
+    hidden[:, 0:part] = own_ref[...]
+    hidden[:, part : 3 * part] = early_ref[...]
     for f in range(pieces):
         at = slice(f * piece, (f + 1) * piece)
-        value = jnp.dot(early_ref[...], down_ref[:, at], preferred_element_type=jnp.float32)
+        value = jnp.dot(hidden[...], down_ref[:, at], preferred_element_type=jnp.float32)
         pltpu.make_async_copy(columns(d3a, f), columns(last, f), sems.at[f]).wait()
         value = value + jnp.dot(middle_ref[...], last[:, at], preferred_element_type=jnp.float32)
         out[f] = value.reshape(senders, slots, piece).astype(jnp.bfloat16)
@@ -261,7 +287,7 @@
         store(f).wait()
 
 
-def late_outputs(place, early, middle, down, lasts, senders, pieces):
+def late_outputs(place, early, middle, own, down, lasts, senders, pieces):
     count = early.shape[0]
     part, width = lasts[0].shape
     slots = count // senders
@@ -269,10 +295,11 @@
     shape = (senders, pieces, slots, piece)
     return pl.pallas_call(
         late_kernel,
-        in_specs=[SMEM, VMEM, VMEM, VMEM, ANY, ANY],
+        in_specs=[SMEM, VMEM, VMEM, VMEM, VMEM, ANY, ANY],
         out_specs=HBM,
         scratch_shapes=[
             pltpu.VMEM((part, width), jnp.bfloat16),
+            pltpu.VMEM((count, 3 * part), jnp.bfloat16),
             pltpu.VMEM((pieces, senders, slots, piece), jnp.bfloat16),
             pltpu.SemaphoreType.DMA((pieces,)),
             pltpu.SemaphoreType.DMA((pieces,)),
@@ -280,7 +307,7 @@
         out_shape=pltpu.HBM(shape, jnp.bfloat16),
         compiler_params=pltpu.CompilerParams(vmem_limit_bytes=32 * MIB),
         name="late_outputs",
-    )(place, early, middle, down, *lasts)
+    )(place, early, middle, own, down, *lasts)
 
 
 def table_kernel(ids_ref, scores_ref, out_ref, *, rows, count_tp):
@@ -407,12 +434,11 @@
         buffer.reshape(count_ep, rows, full_width), "ep", split_axis=0, concat_axis=0, tiled=True
     ).reshape(count_ep * rows, full_width)
     received = in_vmem(received)
-    early, loaded = early_hidden(
-        place, received, (*gate[0], gate[1], gate[2]), (*up[0], up[1], up[2]), (*down[0], down[1], down[2])
-    )
-    middle = in_vmem(middle_hidden(place, received, gate[3], up[3]))
+    early, weights = early_hidden(place, received, (*gate[0], gate[1], gate[2]), (*up[0], up[1], up[2]))
+    middle = middle_hidden(place, received, gate[3], up[3])
+    own, loaded = own_hidden(place, received, weights, (*down[0], down[1], down[2]))
     outputs = late_outputs(
-        place, early, middle, loaded, down[3], count_ep, count_tp
+        place, early, middle, own, loaded, down[3], count_ep, count_tp
     )
     returned = lax.all_to_all(
         outputs.reshape(count_ep * count_tp, rows, part_width), AXES, split_axis=0, concat_axis=0, tiled=True
@@ -421,7 +447,7 @@
     combined, squares = combine(table, in_vmem(returned))
     parts = [squares] + [
         lax.ppermute(squares, "tp", [(i, (i + shift) % count_tp) for i in range(count_tp)])
-        for shift in (1, count_tp - 1, 2)
+        for shift in range(1, count_tp)
     ]
     return scale(combined, parts, out_gain[None, :], full_width)
 

time: 162 us -> 154 us (0.951)
  starting transfers between devices: 70.3 us -> 61.3 us
    ppermute x15, starting transfers between devices: 46.3 us -> 36.5 us  [send(): return lax.ppermute(weight, AXES, pairs)]
    ppermute x15, waiting for transfers between devices: 14.8 us -> 17.2 us  [send(): return lax.ppermute(weight, AXES, pairs)]
    ppermute x3, waiting for transfers between devices: 5.06 us -> 2.9 us  [per_device(): lax.ppermute(squares, 'tp', [(i, (i + shift) % count_tp) for i in range(c...]
    all_to_all x1, starting transfers between devices: 8.46 us -> 10.3 us  [per_device(): lax.all_to_all(buffer.reshape(count_ep, rows, full_width), 'ep', split_ax...]
    pallas_call x2 -> x3, Pallas kernels: 14.4 us -> 15.5 us  [the longest x1 6.56 us: late_outputs(): pl.pallas_call(late_kernel, in_specs=[SMEM, VMEM, VMEM, VMEM, VMEM, ANY,...]
  transfers between devices with their start and end apart: 20 -> 20, of which waited for: 5 -> 6; matrix products, arithmetic and copies ran while one was open for 1% -> 1% of each run, Pallas kernels for 13% -> 14%
where the time goes in v10:
time: 154 us; the launch traced here: 153 us
  starting transfers between devices  61.3 us (40%)
  waiting for transfers between devices  55 us (36%)
  Pallas kernels  32.8 us (21%)
  local copies, waits for them, and re-layouts  3.87 us (3%)
    ppermute x15, starting transfers between devices, send(): return lax.ppermute(weight, AXES, pairs)  36.5 us
    all_to_all x1, waiting for transfers between devices, per_device(): lax.all_to_all(outputs.reshape(count_ep * count_tp, rows, part_width), AX...  35 us
    ppermute x15, waiting for transfers between devices, send(): return lax.ppermute(weight, AXES, pairs)  17.2 us
    all_to_all x1, starting transfers between devices, per_device(): lax.all_to_all(outputs.reshape(count_ep * count_tp, rows, part_width), AX...  10.6 us
    all_to_all x1, starting transfers between devices, per_device(): lax.all_to_all(buffer.reshape(count_ep, rows, full_width), 'ep', split_ax...  10.3 us
    pallas_call x1, Pallas kernels, dispatch_buffer(): pl.pallas_call(functools.partial(dispatch_kernel, rows=rows, chunks=chunk...  7.13 us
    pallas_call x1, Pallas kernels, late_outputs(): pl.pallas_call(late_kernel, in_specs=[SMEM, VMEM, VMEM, VMEM, VMEM, ANY,...  6.56 us
    pallas_call x1, Pallas kernels, early_hidden(): pl.pallas_call(early_kernel, in_specs=[SMEM, VMEM] + [ANY] * 8, out_specs...  5.74 us
  transfers between devices with their start and end apart: 20, of which 6 were waited for; matrix products, arithmetic and copies ran while one was open for 1% of the time, Pallas kernels for 14%

profile of v10, /device:TPU:0, one launch (start us, length us, event | category | flops | bytes accessed | tf_op | source)
XLA Modules:
  0.0 153.3 jit_solution(16026882230245172507)
XLA Ops:
  0.0 1.6 %collective-permute-start.1 = (bf16[2048,256]{1,0:T(8,128)(2,1)}, bf16[2048,256]{1,0:T(8,128)(2,1)}, u32[]{:S(2)}, u32[]{:S(2)}) collective-permute-start(bf16[2048,256]{1,0:T(8,128)(2,1)} %bitcast.19), channel_id=1, source_target_pairs={{0,1},{1,0},{2,5},{3,4},{4,3},{5,2},{6,7},{7,6},{8,9},{9,8},{10,13... | collective-permute-start | bytes 3145736 | tf_op jit(solution)/shard_map/ppermute | solution.py:417
  1.6 0.4 collective-permute-start.4
  2.0 1.0 collective-permute-start
  3.0 0.0 collective-permute-start.3
  3.0 1.1 collective-permute-start.11
  4.1 7.1 %dispatch_buffer.1 = bf16[768,2048]{1,0:T(8,128)(2,1)} custom-call(s32[2,768]{1,0:T(2,128)} %bitcast.28, f32[1,2048]{1,0:T(1,128)} %bitcast.29, bf16[768,2048]{1,0:T(8,128)(2,1)} %tokens_ref.1), custom_call_target="tpu_custom_call" | custom-call | tf_op jit(solution)/shard_map/dispatch_buffer/pallas_call | solution.py:99
  11.3 10.3 %all-to-all-start = ((bf16[32,24,2048]{2,1,0:T(8,128)(2,1)}), bf16[32,24,2048]{2,1,0:T(8,128)(2,1)S(1)}, u32[]{:S(2)}, u32[]{:S(2)}) async-start(bf16[32,24,2048]{2,1,0:T(8,128)(2,1)} %bitcast.18), calls=%async_computation | async-start | bytes 6291456 | tf_op jit(solution)/shard_map/all_to_all | solution.py:433
  21.6 0.4 collective-permute-start.2
  21.9 4.4 %collective-permute-done.4.u1 = bf16[2048,256]{1,0:T(8,128)(2,1)} collective-permute-done((bf16[2048,256]{1,0:T(8,128)(2,1)}, bf16[2048,256]{1,0:T(8,128)(2,1)}, u32[]{:S(2)}, u32[]{:S(2)}) %collective-permute-start.4) | collective-permute-done | bytes 1048608 | tf_op jit(solution)/shard_map/ppermute | solution.py:417
  26.4 0.9 collective-permute-start.5
  27.2 1.6 %collective-permute-start.6 = (bf16[2048,256]{1,0:T(8,128)(2,1)}, bf16[2048,256]{1,0:T(8,128)(2,1)}, u32[]{:S(2)}, u32[]{:S(2)}) collective-permute-start(bf16[2048,256]{1,0:T(8,128)(2,1)} %collective-permute-done.1.g1), channel_id=1, source_target_pairs={{2,3},{3,2},{4,5},{5,4},{10,11},{11,10},{12,13},{13,12},{18,19},{1... | collective-permute-start | bytes 3145736 | tf_op jit(solution)/shard_map/ppermute | solution.py:417
  28.9 0.0 collective-permute-done.3.ub
  28.9 1.6 %collective-permute-start.8 = (bf16[2048,256]{1,0:T(8,128)(2,1)}, bf16[2048,256]{1,0:T(8,128)(2,1)}, u32[]{:S(2)}, u32[]{:S(2)}) collective-permute-start(bf16[2048,256]{1,0:T(8,128)(2,1)} %collective-permute-done.4.u1), channel_id=1, source_target_pairs={{2,3},{3,2},{4,5},{5,4},{10,11},{11,10},{12,13},{13,12},{18,19},{1... | collective-permute-start | bytes 3145736 | tf_op jit(solution)/shard_map/ppermute | solution.py:417
  30.5 12.7 %collective-permute-done.11.d1 = bf16[256,2048]{1,0:T(8,128)(2,1)} collective-permute-done((bf16[256,2048]{1,0:T(8,128)(2,1)}, bf16[256,2048]{1,0:T(8,128)(2,1)}, u32[]{:S(2)}, u32[]{:S(2)}) %collective-permute-start.11) | collective-permute-done | bytes 1048608 | tf_op jit(solution)/shard_map/ppermute | solution.py:417
  43.2 1.6 %collective-permute-start.13 = (bf16[256,2048]{1,0:T(8,128)(2,1)}, bf16[256,2048]{1,0:T(8,128)(2,1)}, u32[]{:S(2)}, u32[]{:S(2)}) collective-permute-start(bf16[256,2048]{1,0:T(8,128)(2,1)} %collective-permute-done.11.d1), channel_id=1, source_target_pairs={{2,3},{3,2},{4,5},{5,4},{10,11},{11,10},{12,13},{13,12},{18,19},{1... | collective-permute-start | bytes 3145736 | tf_op jit(solution)/shard_map/ppermute | solution.py:417
  44.8 0.0 collective-permute-done.2.g2
  44.8 0.0 collective-permute-start.10
  44.8 0.0 collective-permute-done.5.u2
  44.8 0.5 collective-permute-start.12
  45.3 0.0 collective-permute-done.6.gb
  45.3 3.5 %collective-permute-start.7 = (bf16[2048,256]{1,0:T(8,128)(2,1)}, bf16[2048,256]{1,0:T(8,128)(2,1)}, u32[]{:S(2)}, u32[]{:S(2)}) collective-permute-start(bf16[2048,256]{1,0:T(8,128)(2,1)} %collective-permute-done.6.gb), channel_id=1, source_target_pairs={{0,4},{1,5},{2,6},{3,7},{4,0},{5,1},{6,2},{7,3},{8,12},{9,13},{10,... | collective-permute-start | bytes 3145736 | tf_op jit(solution)/shard_map/ppermute | solution.py:417
  48.8 0.0 collective-permute-done.8.ub
  48.8 11.0 %collective-permute-start.9 = (bf16[2048,256]{1,0:T(8,128)(2,1)}, bf16[2048,256]{1,0:T(8,128)(2,1)}, u32[]{:S(2)}, u32[]{:S(2)}) collective-permute-start(bf16[2048,256]{1,0:T(8,128)(2,1)} %collective-permute-done.8.ub), channel_id=1, source_target_pairs={{0,4},{1,5},{2,6},{3,7},{4,0},{5,1},{6,2},{7,3},{8,12},{9,13},{10,... | collective-permute-start | bytes 3145736 | tf_op jit(solution)/shard_map/ppermute | solution.py:417
  59.9 11.2 %collective-permute-start.14 = (bf16[256,2048]{1,0:T(8,128)(2,1)}, bf16[256,2048]{1,0:T(8,128)(2,1)}, u32[]{:S(2)}, u32[]{:S(2)}) collective-permute-start(bf16[256,2048]{1,0:T(8,128)(2,1)} %collective-permute-done.13.d3b), channel_id=1, source_target_pairs={{0,4},{1,5},{2,6},{3,7},{4,0},{5,1},{6,2},{7,3},{8,12},{9,13},{10,... | collective-permute-start | bytes 3145736 | tf_op jit(solution)/shard_map/ppermute | solution.py:417
  71.1 0.1 pad_add_fusion.place_ref
  71.2 0.0 all-to-all-done
  71.2 5.7 %early_hidden.1 = (bf16[768,512]{1,0:T(8,128)(2,1)S(1)}, bf16[2048,512]{1,0:T(8,128)(2,1)S(1)}) custom-call(s32[2]{0:T(128)S(1)} %pad_add_fusion.place_ref, bf16[768,2048]{1,0:T(8,128)(2,1)S(1)} %bitcast.12, bf16[2048,256]{1,0:T(8,128)(2,1)} %bitcast.21, bf16[2048,256]{1,0:T(8,128)(2,1)} %collective-permute-done.gb, ...), custom_call_target="tpu_custom_call" | custom-call | tf_op jit(solution)/shard_map/early_hidden/pallas_call | solution.py:223
  77.0 3.2 %own_hidden.1 = (bf16[768,256]{1,0:T(8,128)(2,1)S(1)}, bf16[768,2048]{1,0:T(8,128)(2,1)S(1)}) custom-call(s32[2]{0:T(128)S(1)} %pad_add_fusion.place_ref, bf16[768,2048]{1,0:T(8,128)(2,1)S(1)} %bitcast.13, bf16[2048,512]{1,0:T(8,128)(2,1)S(1)} %get-tuple-element.12.weights_ref, bf16[256,2048]{1,0:T(8,128)(2,1)} %bitcast.27, ...), custom_call_target="tpu_custom_call" | custom-call | tf_op jit(solution)/shard_map/own_hidden/pallas_call | solution.py:236
  80.2 3.9 %middle_hidden.1.middle_ref = bf16[768,256]{1,0:T(8,128)(2,1)S(1)} custom-call(s32[2]{0:T(128)S(1)} %pad_add_fusion.place_ref, bf16[768,2048]{1,0:T(8,128)(2,1)S(1)} %bitcast.14, bf16[2048,256]{1,0:T(8,128)(2,1)} %collective-permute-done.7.ga, bf16[2048,256]{1,0:T(8,128)(2,1)} %collective-permute-done.6.gb, bf16[2048,256]{1,0:T(8,128)(2,1)} %collective-permute-done.9.ua, ...), custom_call_target="tpu_custom_call" | custom-call | tf_op jit(solution)/shard_map/middle_hidden/pallas_call | solution.py:253
  84.1 6.6 %late_outputs.1 = bf16[32,4,24,512]{3,2,1,0:T(8,128)(2,1)} custom-call(s32[2]{0:T(128)S(1)} %pad_add_fusion.place_ref, bf16[768,512]{1,0:T(8,128)(2,1)S(1)} %get-tuple-element.11.early_ref, bf16[768,256]{1,0:T(8,128)(2,1)S(1)} %middle_hidden.1.middle_ref, bf16[768,256]{1,0:T(8,128)(2,1)S(1)} %get-tuple-element.13.own_ref, ...), custom_call_target="tpu_custom_call" | custom-call | tf_op jit(solution)/shard_map/late_outputs/pallas_call | solution.py:296
  90.6 0.0 copy-start.3
  90.7 0.0 copy-start.4
  90.7 10.6 %all-to-all-start.1 = ((bf16[128,24,512]{2,1,0:T(8,128)(2,1)}), bf16[128,24,512]{2,1,0:T(8,128)(2,1)S(1)}, u32[]{:S(2)}, u32[]{:S(2)}) async-start(bf16[128,24,512]{2,1,0:T(8,128)(2,1)} %bitcast.17), calls=%async_computation.1 | async-start | bytes 6291456 | tf_op jit(solution)/shard_map/all_to_all | solution.py:443
  101.3 0.0 copy-start.2
  101.3 0.9 copy.9.ids_ref
  102.2 0.9 copy.10.scores_ref
  103.2 1.0 copy-done
  104.1 1.0 copy-done.1
  105.1 2.2 %columns.1.table_ref = f32[768,4]{1,0:T(8,128)S(1)} custom-call(s32[768,2]{1,0:T(8,128)S(1)} %copy-done, f32[768,2]{1,0:T(8,128)S(1)} %copy-done.1), custom_call_target="tpu_custom_call" | custom-call | tf_op jit(solution)/shard_map/columns/pallas_call | solution.py:337
  107.3 35.0 %all-to-all-done.1 = bf16[128,24,512]{2,1,0:T(8,128)(2,1)S(1)} async-done(((bf16[128,24,512]{2,1,0:T(8,128)(2,1)}), bf16[128,24,512]{2,1,0:T(8,128)(2,1)S(1)}, u32[]{:S(2)}, u32[]{:S(2)}) %all-to-all-start.1) | async-done | bytes 3145760 | tf_op jit(solution)/shard_map/all_to_all | solution.py:443
  142.3 3.0 %combine.1 = (f32[768,512]{1,0:T(8,128)S(1)}, f32[1,768]{1,0:T(1,128)S(1)}) custom-call(f32[768,4]{1,0:T(8,128)S(1)} %columns.1.table_ref, bf16[3072,512]{1,0:T(8,128)(2,1)S(1)} %bitcast.15), custom_call_target="tpu_custom_call" | custom-call | tf_op jit(solution)/shard_map/combine/pallas_call | solution.py:365
  145.3 0.6 collective-permute-start.15
  146.0 2.6 %collective-permute-start.16 = (f32[1,768]{1,0:T(1,128)S(1)}, f32[1,768]{1,0:T(1,128)S(1)}, u32[]{:S(2)}, u32[]{:S(2)}) collective-permute-start(f32[1,768]{1,0:T(1,128)S(1)} %get-tuple-element.16.own_ref), channel_id=1, source_target_pairs={{0,2},{1,3},{2,0},{3,1},{4,6},{5,7},{6,4},{7,5},{8,10},{9,11},{10,... | collective-permute-start | bytes 9224 | tf_op jit(solution)/shard_map/ppermute | solution.py:449
  148.6 0.7 collective-permute-start.17
  149.3 0.9 collective-permute-done.15.a_ref
  150.2 0.9 collective-permute-done.16.b_ref
  151.1 1.1 collective-permute-done.17.c_ref
  152.2 1.1 scale.1
  (13 shorter events, 0.0 us)
Async XLA Ops:
  0.0 21.6 %collective-permute-start.1 = (bf16[2048,256]{1,0:T(8,128)(2,1)}, bf16[2048,256]{1,0:T(8,128)(2,1)}, u32[]{:S(2)}, u32[]{:S(2)}) collective-permute-start(bf16[2048,256]{1,0:T(8,128)(2,1)} %bitcast.19), channel_id=1, source_target_pairs={{0,1},{1,0},{2,5},{3,4},{4,3},{5,2},{6,7},{7,6},{8,9},{9,8},{10,13... | collective-permute-start | bytes 3145736 | tf_op jit(solution)/shard_map/ppermute | solution.py:417
  1.6 24.7 %collective-permute-start.4 = (bf16[2048,256]{1,0:T(8,128)(2,1)}, bf16[2048,256]{1,0:T(8,128)(2,1)}, u32[]{:S(2)}, u32[]{:S(2)}) collective-permute-start(bf16[2048,256]{1,0:T(8,128)(2,1)} %bitcast.22), channel_id=1, source_target_pairs={{0,1},{1,0},{2,5},{3,4},{4,3},{5,2},{6,7},{7,6},{8,9},{9,8},{10,13... | collective-permute-start | bytes 3145736 | tf_op jit(solution)/shard_map/ppermute | solution.py:417
  2.0 25.2 %collective-permute-start = (bf16[2048,256]{1,0:T(8,128)(2,1)}, bf16[2048,256]{1,0:T(8,128)(2,1)}, u32[]{:S(2)}, u32[]{:S(2)}) collective-permute-start(bf16[2048,256]{1,0:T(8,128)(2,1)} %bitcast.20), channel_id=1, source_target_pairs={{0,4},{1,5},{2,6},{3,7},{4,0},{5,1},{6,2},{7,3},{8,12},{9,13},{10,... | collective-permute-start | bytes 3145736 | tf_op jit(solution)/shard_map/ppermute | solution.py:417
  3.0 25.8 %collective-permute-start.3 = (bf16[2048,256]{1,0:T(8,128)(2,1)}, bf16[2048,256]{1,0:T(8,128)(2,1)}, u32[]{:S(2)}, u32[]{:S(2)}) collective-permute-start(bf16[2048,256]{1,0:T(8,128)(2,1)} %bitcast.23), channel_id=1, source_target_pairs={{0,4},{1,5},{2,6},{3,7},{4,0},{5,1},{6,2},{7,3},{8,12},{9,13},{10,... | collective-permute-start | bytes 3145736 | tf_op jit(solution)/shard_map/ppermute | solution.py:417
  3.0 40.1 %collective-permute-start.11 = (bf16[256,2048]{1,0:T(8,128)(2,1)}, bf16[256,2048]{1,0:T(8,128)(2,1)}, u32[]{:S(2)}, u32[]{:S(2)}) collective-permute-start(bf16[256,2048]{1,0:T(8,128)(2,1)} %bitcast.25), channel_id=1, source_target_pairs={{0,1},{1,0},{2,5},{3,4},{4,3},{5,2},{6,7},{7,6},{8,9},{9,8},{10,13... | collective-permute-start | bytes 3145736 | tf_op jit(solution)/shard_map/ppermute | solution.py:417
  11.3 59.9 %all-to-all-start = ((bf16[32,24,2048]{2,1,0:T(8,128)(2,1)}), bf16[32,24,2048]{2,1,0:T(8,128)(2,1)S(1)}, u32[]{:S(2)}, u32[]{:S(2)}) async-start(bf16[32,24,2048]{2,1,0:T(8,128)(2,1)} %bitcast.18), calls=%async_computation | async-start | bytes 6291456 | tf_op jit(solution)/shard_map/all_to_all | solution.py:433
  21.6 23.2 %collective-permute-start.2 = (bf16[2048,256]{1,0:T(8,128)(2,1)}, bf16[2048,256]{1,0:T(8,128)(2,1)}, u32[]{:S(2)}, u32[]{:S(2)}) collective-permute-start(bf16[2048,256]{1,0:T(8,128)(2,1)} %collective-permute-done.1.g1), channel_id=1, source_target_pairs={{0,4},{1,5},{2,6},{3,7},{4,0},{5,1},{6,2},{7,3},{8,12},{9,13},{10,... | collective-permute-start | bytes 3145736 | tf_op jit(solution)/shard_map/ppermute | solution.py:417
  26.4 18.4 %collective-permute-start.5 = (bf16[2048,256]{1,0:T(8,128)(2,1)}, bf16[2048,256]{1,0:T(8,128)(2,1)}, u32[]{:S(2)}, u32[]{:S(2)}) collective-permute-start(bf16[2048,256]{1,0:T(8,128)(2,1)} %collective-permute-done.4.u1), channel_id=1, source_target_pairs={{0,4},{1,5},{2,6},{3,7},{4,0},{5,1},{6,2},{7,3},{8,12},{9,13},{10,... | collective-permute-start | bytes 3145736 | tf_op jit(solution)/shard_map/ppermute | solution.py:417
  27.2 18.1 %collective-permute-start.6 = (bf16[2048,256]{1,0:T(8,128)(2,1)}, bf16[2048,256]{1,0:T(8,128)(2,1)}, u32[]{:S(2)}, u32[]{:S(2)}) collective-permute-start(bf16[2048,256]{1,0:T(8,128)(2,1)} %collective-permute-done.1.g1), channel_id=1, source_target_pairs={{2,3},{3,2},{4,5},{5,4},{10,11},{11,10},{12,13},{13,12},{18,19},{1... | collective-permute-start | bytes 3145736 | tf_op jit(solution)/shard_map/ppermute | solution.py:417
  28.9 20.0 %collective-permute-start.8 = (bf16[2048,256]{1,0:T(8,128)(2,1)}, bf16[2048,256]{1,0:T(8,128)(2,1)}, u32[]{:S(2)}, u32[]{:S(2)}) collective-permute-start(bf16[2048,256]{1,0:T(8,128)(2,1)} %collective-permute-done.4.u1), channel_id=1, source_target_pairs={{2,3},{3,2},{4,5},{5,4},{10,11},{11,10},{12,13},{13,12},{18,19},{1... | collective-permute-start | bytes 3145736 | tf_op jit(solution)/shard_map/ppermute | solution.py:417
  43.2 16.7 %collective-permute-start.13 = (bf16[256,2048]{1,0:T(8,128)(2,1)}, bf16[256,2048]{1,0:T(8,128)(2,1)}, u32[]{:S(2)}, u32[]{:S(2)}) collective-permute-start(bf16[256,2048]{1,0:T(8,128)(2,1)} %collective-permute-done.11.d1), channel_id=1, source_target_pairs={{2,3},{3,2},{4,5},{5,4},{10,11},{11,10},{12,13},{13,12},{18,19},{1... | collective-permute-start | bytes 3145736 | tf_op jit(solution)/shard_map/ppermute | solution.py:417
  44.8 32.2 %collective-permute-start.10 = (bf16[256,2048]{1,0:T(8,128)(2,1)}, bf16[256,2048]{1,0:T(8,128)(2,1)}, u32[]{:S(2)}, u32[]{:S(2)}) collective-permute-start(bf16[256,2048]{1,0:T(8,128)(2,1)} %bitcast.26), channel_id=1, source_target_pairs={{0,4},{1,5},{2,6},{3,7},{4,0},{5,1},{6,2},{7,3},{8,12},{9,13},{10,... | collective-permute-start | bytes 3145736 | tf_op jit(solution)/shard_map/ppermute | solution.py:417
  44.8 32.2 %collective-permute-start.12 = (bf16[256,2048]{1,0:T(8,128)(2,1)}, bf16[256,2048]{1,0:T(8,128)(2,1)}, u32[]{:S(2)}, u32[]{:S(2)}) collective-permute-start(bf16[256,2048]{1,0:T(8,128)(2,1)} %collective-permute-done.11.d1), channel_id=1, source_target_pairs={{0,4},{1,5},{2,6},{3,7},{4,0},{5,1},{6,2},{7,3},{8,12},{9,13},{10,... | collective-permute-start | bytes 3145736 | tf_op jit(solution)/shard_map/ppermute | solution.py:417
  45.3 34.9 %collective-permute-start.7 = (bf16[2048,256]{1,0:T(8,128)(2,1)}, bf16[2048,256]{1,0:T(8,128)(2,1)}, u32[]{:S(2)}, u32[]{:S(2)}) collective-permute-start(bf16[2048,256]{1,0:T(8,128)(2,1)} %collective-permute-done.6.gb), channel_id=1, source_target_pairs={{0,4},{1,5},{2,6},{3,7},{4,0},{5,1},{6,2},{7,3},{8,12},{9,13},{10,... | collective-permute-start | bytes 3145736 | tf_op jit(solution)/shard_map/ppermute | solution.py:417
  48.8 31.3 %collective-permute-start.9 = (bf16[2048,256]{1,0:T(8,128)(2,1)}, bf16[2048,256]{1,0:T(8,128)(2,1)}, u32[]{:S(2)}, u32[]{:S(2)}) collective-permute-start(bf16[2048,256]{1,0:T(8,128)(2,1)} %collective-permute-done.8.ub), channel_id=1, source_target_pairs={{0,4},{1,5},{2,6},{3,7},{4,0},{5,1},{6,2},{7,3},{8,12},{9,13},{10,... | collective-permute-start | bytes 3145736 | tf_op jit(solution)/shard_map/ppermute | solution.py:417
  59.9 24.2 %collective-permute-start.14 = (bf16[256,2048]{1,0:T(8,128)(2,1)}, bf16[256,2048]{1,0:T(8,128)(2,1)}, u32[]{:S(2)}, u32[]{:S(2)}) collective-permute-start(bf16[256,2048]{1,0:T(8,128)(2,1)} %collective-permute-done.13.d3b), channel_id=1, source_target_pairs={{0,4},{1,5},{2,6},{3,7},{4,0},{5,1},{6,2},{7,3},{8,12},{9,13},{10,... | collective-permute-start | bytes 3145736 | tf_op jit(solution)/shard_map/ppermute | solution.py:417
  90.6 10.6 %copy-start.3 = (s32[768,2]{0,1:T(2,128)S(1)}, s32[768,2]{0,1:T(2,128)}, u32[]{:S(2)}) copy-start(s32[768,2]{0,1:T(2,128)} %param.10) | copy-start | bytes 18436
  90.7 11.6 %copy-start.4 = (f32[768,2]{0,1:T(2,128)S(1)}, f32[768,2]{0,1:T(2,128)}, u32[]{:S(2)}) copy-start(f32[768,2]{0,1:T(2,128)} %param.11) | copy-start | bytes 18436
  90.7 51.6 %all-to-all-start.1 = ((bf16[128,24,512]{2,1,0:T(8,128)(2,1)}), bf16[128,24,512]{2,1,0:T(8,128)(2,1)S(1)}, u32[]{:S(2)}, u32[]{:S(2)}) async-start(bf16[128,24,512]{2,1,0:T(8,128)(2,1)} %bitcast.17), calls=%async_computation.1 | async-start | bytes 6291456 | tf_op jit(solution)/shard_map/all_to_all | solution.py:443
  101.3 50.9 %copy-start.2 = (f32[512]{0:T(512)S(1)}, f32[512]{0:T(512)}, u32[]{:S(2)}) copy-start(f32[512]{0:T(512)} %param.15) | copy-start | bytes 6148
  103.2 1.0 copy-start
  104.1 1.0 copy-start.1
  145.3 4.9 %collective-permute-start.15 = (f32[1,768]{1,0:T(1,128)S(1)}, f32[1,768]{1,0:T(1,128)S(1)}, u32[]{:S(2)}, u32[]{:S(2)}) collective-permute-start(f32[1,768]{1,0:T(1,128)S(1)} %get-tuple-element.16.own_ref), channel_id=1, source_target_pairs={{0,1},{1,2},{2,3},{3,0},{4,5},{5,6},{6,7},{7,4},{8,9},{9,10},{10,1... | collective-permute-start | bytes 9224 | tf_op jit(solution)/shard_map/ppermute | solution.py:449
  146.0 5.1 %collective-permute-start.16 = (f32[1,768]{1,0:T(1,128)S(1)}, f32[1,768]{1,0:T(1,128)S(1)}, u32[]{:S(2)}, u32[]{:S(2)}) collective-permute-start(f32[1,768]{1,0:T(1,128)S(1)} %get-tuple-element.16.own_ref), channel_id=1, source_target_pairs={{0,2},{1,3},{2,0},{3,1},{4,6},{5,7},{6,4},{7,5},{8,10},{9,11},{10,... | collective-permute-start | bytes 9224 | tf_op jit(solution)/shard_map/ppermute | solution.py:449
  148.6 3.6 %collective-permute-start.17 = (f32[1,768]{1,0:T(1,128)S(1)}, f32[1,768]{1,0:T(1,128)S(1)}, u32[]{:S(2)}, u32[]{:S(2)}) collective-permute-start(f32[1,768]{1,0:T(1,128)S(1)} %get-tuple-element.16.own_ref), channel_id=1, source_target_pairs={{0,3},{1,0},{2,1},{3,2},{4,7},{5,4},{6,5},{7,6},{8,11},{9,8},{10,9... | collective-permute-start | bytes 9224 | tf_op jit(solution)/shard_map/ppermute | solution.py:449
